TPU v7x, 256 devices: a whole 4x4x8 slice. The times are simulated.
256 devices in a mesh: sp: 32 (over z, x), tp: 8 (over y, core).
Axes of the slice: x: 4, y: 4, z: 8, core: 2. Of those that a mesh axis runs over, the one named last changes fastest.
Arguments:
- tokens: bfloat16 [2, 6144, 4096], P(None, 'sp', 'tp'), may hold values from -12 to 12
- query_weight: bfloat16 [4096, 2048], P(None, 'tp'), may hold values from -0.09375 to 0.09375
- key_weight: bfloat16 [4096, 2048], P(None, 'tp'), may hold values from -0.09375 to 0.09375
- value_weight: bfloat16 [4096, 2048], P(None, 'tp'), may hold values from -0.09375 to 0.09375
- gate_weight: bfloat16 [4096, 2048], P(None, 'tp'), may hold values from -0.09375 to 0.09375
- beta_weight: bfloat16 [4096, 16], P(None, 'tp'), may hold values from -0.09375 to 0.09375
- decay_weight: bfloat16 [4096, 16], P(None, 'tp'), may hold values from -0.09375 to 0.09375
- beta_bias: float32 [16], P('tp'), may hold values from -6 to -3
- rate_log: float32 [16], P('tp'), may hold values from -12 to -2.5
- out_gain: float32 [128], replicated, may hold values from 0.1 to 1.9
- new_query: bfloat16 [2, 16, 128], P(None, 'tp'), may hold values from -6 to 6
- new_key: bfloat16 [2, 16, 128], P(None, 'tp'), may hold values from -6 to 6
- new_value: bfloat16 [2, 16, 128], P(None, 'tp'), may hold values from -6 to 6
- new_beta: float32 [2, 16], P(None, 'tp'), may hold values from 0.1 to 0.9
- new_decay: float32 [2, 16], P(None, 'tp'), may hold values from 0.3 to 1
Outputs:
- mixed_out: bfloat16 [2, 6144, 2048], P(None, 'sp', 'tp')
- cache: bfloat16 [2, 16, 128, 128], P(None, 'tp', 'sp')
- first_out: float32 [2, 2048], P(None, 'tp')
All inputs are finite; a program needn't handle non-finite values.
Results may differ from a plain program's by a relative error of at most 0.0073.
Values may be sent and summed in bfloat16 or wider, within the bound.
No kernel may reach another device: no remote copies, remote signals or barrier semaphores. Data moves between devices by JAX's collectives and lax.ppermute only.
A program may use at most 64 MiB of HBM per device.

v0:
```python
import jax
import jax.numpy as jnp
from jax import lax
from jax.sharding import Mesh
from jax.sharding import PartitionSpec as P

BLOCK = 64
SP = ("sp_0", "sp_1")


unit_floor = 1.0
norm_floor = 0.001
highest = lax.Precision.HIGHEST


def neutral_like(value, identity):
    return jax.tree.map(
        lambda a, e: jnp.broadcast_to(jnp.asarray(e, a.dtype), a.shape), value, identity
    )


def carried_in(value, axes, combine, identity):
    before = start = neutral_like(value, identity)
    subtotal = value
    for axis in reversed(axes):
        length, index = (lax.axis_size(axis), lax.axis_index(axis))
        pieces = jax.tree.map(lambda part: lax.all_gather(part, axis), subtotal)
        inside, subtotal = (start, start)
        for k in range(length):
            passed = k < index
            subtotal = combine(subtotal, jax.tree.map(lambda part: part[k], pieces))
            inside = jax.tree.map(lambda new, old: jnp.where(passed, new, old), subtotal, inside)
        before = combine(inside, before)
    return before


def split_up(value, dim, length):
    before, after = (value.shape[:dim], value.shape[dim + 1 :])
    return jnp.moveaxis(value.reshape(*before, length, -1, *after), dim, 0)


def summed_on_arrival(value, axis, dim):
    parts = split_up(value, dim, lax.axis_size(axis))
    arrived = lax.all_to_all(parts, axis, split_axis=0, concat_axis=0, tiled=True)
    return arrived.astype(jnp.float32).sum(axis=0)


def copy_for_each(value, axis):
    length = lax.axis_size(axis)
    return lax.all_to_all(
        jnp.broadcast_to(value[None], (length, *value.shape)), axis, 0, 0, tiled=True
    )


def over_copies(value, axis):
    everything = copy_for_each(value, axis)
    return jnp.sum(everything, axis=0)


def in_one(arrays, axis):
    ravelled, at, gathered = (jnp.concatenate([a.reshape(-1) for a in arrays]), 0, [])
    subtotal = over_copies(ravelled, axis)
    for a in arrays:
        gathered.append(subtotal[at : at + a.size].reshape(a.shape))
        at += a.size
    return tuple(gathered)


def matmul(form, left, right):
    return jnp.einsum(form, left, right, precision=highest)


def unit_rows(values):
    return values * lax.rsqrt(jnp.sum(values * values, axis=-1, keepdims=True) + unit_floor)


def head_norm(values, out_gain):
    return (
        values
        * lax.rsqrt(jnp.mean(values * values, axis=-1, keepdims=True) + norm_floor)
        * out_gain
    )


def stored(values):
    return lax.optimization_barrier(values.astype(jnp.bfloat16)).astype(jnp.float32)


def unit_lower_inverse(lower_part):
    extent = lower_part.shape[-1]
    nilpotent = -lower_part
    inverse = jnp.eye(extent, dtype=jnp.float32) + nilpotent
    for _ in range(extent.bit_length() - 2):
        nilpotent = matmul("...ij,...jk->...ik", nilpotent, nilpotent)
        inverse = inverse + matmul("...ij,...jk->...ik", nilpotent, inverse)
    return inverse


def prepare(
    query_rows,
    key_rows,
    value_rows,
    beta_in,
    decay_in,
    beta_bias,
    rate_log,
    seq_count,
    length,
    head_count,
):
    extent = query_rows.shape[-1] // head_count
    blocks = length // BLOCK

    def by_head(values):
        shaped = values.reshape(seq_count, blocks, BLOCK, head_count, extent)
        return shaped.transpose(0, 3, 1, 2, 4).reshape(
            seq_count * head_count, blocks, BLOCK, extent
        )

    def by_scalar(values):
        shaped = values.reshape(seq_count, blocks, BLOCK, head_count)
        return shaped.transpose(0, 3, 1, 2).reshape(seq_count * head_count, blocks, BLOCK)

    queries = unit_rows(by_head(query_rows))
    key_unit = unit_rows(by_head(key_rows))
    values = by_head(value_rows)
    strength = by_scalar(jax.nn.sigmoid(beta_in + beta_bias))
    decays = by_scalar(-jnp.exp(rate_log) * jax.nn.softplus(decay_in))
    return (queries, key_unit, values, strength, decays)


def block_terms(queries, key_unit, values, strength, decays):
    extent = decays.shape[-1]
    cumulative = jnp.cumsum(decays, axis=-1)
    causal = jnp.tril(jnp.ones((extent, extent), bool))
    strict = jnp.tril(jnp.ones((extent, extent), bool), -1)
    spread = cumulative[..., :, None] - cumulative[..., None, :]
    weights = jnp.where(causal, jnp.exp(jnp.where(causal, spread, 0.0)), 0.0)
    key_beta = key_unit * strength[..., None]
    lower_part = jnp.where(strict, matmul("...td,...sd->...ts", key_beta, key_unit) * weights, 0.0)
    inverse = unit_lower_inverse(lower_part)
    update = matmul("...ts,...se->...te", inverse, values * strength[..., None])
    carry_w = matmul("...ts,...sd->...td", inverse, key_beta * jnp.exp(cumulative)[..., None])
    scores = matmul("...td,...sd->...ts", queries, key_unit) * weights
    query_decay = queries * jnp.exp(cumulative)[..., None]
    last_log = cumulative[..., -1]
    key_decay = key_unit * jnp.exp(last_log[..., None] - cumulative)[..., None]
    return (update, carry_w, query_decay, scores, key_decay, last_log)


def finish_read(recall, retrieve, query_unit, key_unit, new_value, new_beta, new_decay, out_gain):
    seq_count, head_count, extent = recall.shape
    intersect = jnp.sum(key_unit * query_unit, axis=-1)
    fresh_values = new_value.astype(jnp.float32) - new_decay[..., None] * retrieve
    read_heads = new_decay[..., None] * recall + (new_beta * intersect)[..., None] * fresh_values
    return head_norm(read_heads, out_gain).reshape(seq_count, head_count * extent)


def project_rows(shard_rows, weights):
    row_count = shard_rows.shape[-1]
    flat_rows = shard_rows.reshape(-1, row_count)
    return tuple(
        (jnp.dot(flat_rows, weight, preferred_element_type=jnp.float32) for weight in weights)
    )


def shards(
    tokens,
    query_weight,
    key_weight,
    value_weight,
    gate_weight,
    beta_weight,
    decay_weight,
    beta_bias,
    rate_log,
    out_gain,
    new_query,
    new_key,
    new_value,
    new_beta,
    new_decay,
):
    seq_count, span_len, _ = tokens.shape
    head_count = rate_log.shape[0]
    weights = (query_weight, key_weight, value_weight, gate_weight, beta_weight, decay_weight)
    totals = project_rows(lax.all_gather(tokens, "tp", axis=2, tiled=True), weights)
    query_rows = stored(totals[0])
    key_rows = stored(totals[1])
    value_rows = stored(totals[2])
    gate_rows = stored(totals[3])
    prepared = prepare(
        query_rows,
        key_rows,
        value_rows,
        totals[4],
        totals[5],
        beta_bias,
        rate_log,
        seq_count,
        span_len,
        head_count,
    )
    block_data = block_terms(*prepared)
    batch_size = block_data[0].shape[0]
    extent = block_data[0].shape[-1]
    identity = jnp.broadcast_to(jnp.eye(extent, dtype=jnp.float32), (batch_size, extent, extent))

    def advance(carried, inputs):
        state_now, reach_map = carried
        u_block, w_block, qg_block, score_block, kd_block, gl_block = inputs
        fresh_values = u_block - matmul("btd,bde->bte", w_block, state_now)
        block_out = matmul("btd,bde->bte", qg_block, state_now) + matmul(
            "bts,bse->bte", score_block, fresh_values
        )
        reach_rows = qg_block - matmul("bts,bsd->btd", score_block, w_block)
        factor = jnp.exp(gl_block)[:, None, None]
        transit = factor * identity - matmul("bsd,bse->bde", kd_block, w_block)
        state_next = state_now * factor + matmul("bsd,bse->bde", kd_block, fresh_values)
        map_next = matmul("bde,bef->bdf", transit, reach_map)
        return ((state_next, map_next), (block_out, matmul("btd,bde->bte", reach_rows, reach_map)))

    inputs = tuple((jnp.moveaxis(member, 1, 0) for member in block_data))
    start_state = jnp.zeros((batch_size, extent, extent), jnp.float32)
    (local_state, local_map), (local_out, reach_all) = lax.scan(
        advance, (start_state, identity), inputs
    )

    def compose(earlier, later):
        return (
            matmul("bde,bef->bdf", later[0], earlier[0]),
            matmul("bde,bef->bdf", later[0], earlier[1]) + later[1],
        )

    prefix = carried_in(
        (local_map, local_state), SP, compose, (identity, jnp.zeros_like(local_state))
    )
    incoming = prefix[1]
    block_total = local_out + matmul("nbtd,bde->nbte", reach_all, incoming)
    blocks = span_len // BLOCK
    heads_out = block_total.reshape(blocks, seq_count, head_count, BLOCK, extent).transpose(
        1, 0, 3, 2, 4
    )
    heads_out = heads_out.reshape(seq_count, span_len, head_count, extent)
    gate_values = gate_rows.reshape(seq_count, span_len, head_count, extent)
    mixed_out = (head_norm(heads_out, out_gain) * jax.nn.silu(gate_values)).astype(jnp.bfloat16)
    mixed_out = mixed_out.reshape(seq_count, span_len, head_count * extent)
    final_state = matmul("bde,bef->bdf", local_map, incoming) + local_state
    final_cast = final_state.reshape(seq_count, head_count, extent, extent).astype(jnp.bfloat16)
    row_count = extent // lax.axis_size(SP)
    row_start = lax.axis_index(SP) * row_count
    query_unit = unit_rows(new_query.astype(jnp.float32))
    key_unit = unit_rows(new_key.astype(jnp.float32))
    is_last = lax.axis_index(SP) == lax.axis_size(SP) - 1
    own_term = jnp.where(is_last, final_cast.astype(jnp.float32), 0.0)
    cache_rows = summed_on_arrival(own_term.astype(jnp.bfloat16), SP, 2).astype(jnp.bfloat16)
    memory = lax.optimization_barrier(cache_rows).astype(jnp.float32)
    query_part = lax.dynamic_slice_in_dim(query_unit, row_start, row_count, 2)
    key_part = lax.dynamic_slice_in_dim(key_unit, row_start, row_count, 2)
    recall, retrieve = in_one(
        (matmul("shde,shd->she", memory, query_part), matmul("shde,shd->she", memory, key_part)), SP
    )
    first_out = finish_read(
        recall, retrieve, query_unit, key_unit, new_value, new_beta, new_decay, out_gain
    )
    return (mixed_out, cache_rows, first_out)


def solution(mesh):
    torus = Mesh(mesh.devices.reshape(8, 4, mesh.shape["tp"]), ("sp_0", "sp_1", "tp"))
    in_specs = (
        P(None, SP, "tp"),
        P(None, "tp"),
        P(None, "tp"),
        P(None, "tp"),
        P(None, "tp"),
        P(None, "tp"),
        P(None, "tp"),
        P("tp"),
        P("tp"),
        P(),
        P(None, "tp", None),
        P(None, "tp", None),
        P(None, "tp", None),
        P(None, "tp"),
        P(None, "tp"),
    )
    out_specs = (P(None, SP, "tp"), P(None, "tp", SP, None), P(None, "tp"))
    return jax.shard_map(
        shards, mesh=torus, in_specs=in_specs, out_specs=out_specs, check_vma=False
    )
```

profile of v0, /device:TPU:24, one launch (start us, length us, event | category | flops | bytes accessed | tf_op | source)
XLA Modules:
  0.0 295.1 jit_solution(3390538268324986770)
XLA Ops:
  9.4 32.4 %all-gather.10.cloned.1.call-done = bf16[2,192,4096]{2,1,0:T(8,128)(2,1)} async-done(((bf16[2,192,512]{2,1,0:T(8,128)(2,1)}), bf16[2,192,4096]{2,1,0:T(8,128)(2,1)}) %all-gather.10.cloned.1.call-update) | async-done | bytes 3145744 | tf_op jit(solution)/shard_map/all_gather | solution.py:187
  41.7 2.8 fusion.91
  46.6 2.9 convolution_convert_fusion.1
  51.1 2.8 fusion.50
  54.0 3.5 %convolution_convert_fusion.3 = bf16[384,256]{1,0:T(8,128)(2,1)S(1)} fusion(bf16[384,4096]{1,0:T(8,128)(2,1)} %bitcast.236, bf16[4096,256]{1,0:T(8,128)(2,1)} %param.19), kind=kOutput, calls=%fused_computation.61 | convolution fusion | flops 805404672 | bytes 5439488 | tf_op jit(solution)/shard_map/dot_general | solution.py:163
  59.2 3.6 %convolution_convert_fusion.2 = bf16[384,256]{1,0:T(8,128)(2,1)S(1)} fusion(bf16[384,4096]{1,0:T(8,128)(2,1)} %bitcast.237, bf16[4096,256]{1,0:T(8,128)(2,1)} %param.20), kind=kOutput, calls=%fused_computation.60 | convolution fusion | flops 805404672 | bytes 5439488 | tf_op jit(solution)/shard_map/dot_general | solution.py:163
  63.0 1.5 multiply_bitcast_fusion
  73.5 1.5 fusion.39
  75.1 29.5 %while.17 = (s32[]{:T(128)}, f32[4,128,128]{2,1,0:T(8,128)S(1)}, f32[4,128,128]{2,1,0:T(8,128)S(1)}, f32[3,4,64,128]{3,2,0,1:T(8,128)}, f32[3,4,64,128]{3,2,0,1:...) while((s32[]{:T(128)}, f32[4,128,128]{2,1,0:T(8,128)S(1)}, ...), condition=%wide.region_4.5_spmd.clone, body=%wide.region_3.4_spmd.clone.sunk | while | flops 403210240 | bytes 5445847 | solution.py:225
  79.2 1.5 convolution_add_fusion.23
  83.0 1.5 convolution_subtract_fusion.7
  89.1 1.5 convolution_add_fusion.23
  92.8 1.5 convolution_subtract_fusion.7
  98.9 1.5 convolution_add_fusion.23
  102.6 1.5 convolution_subtract_fusion.7
  106.1 27.0 %all-gather.12.cloned.1.call-done = f32[16,128,128]{2,1,0:T(8,128)} async-done(((f32[4,128,128]{2,1,0:T(8,128)}), f32[16,128,128]{2,1,0:T(8,128)}) %all-gather.12.cloned.1.call-update) | async-done | bytes 1048592 | tf_op jit(solution)/shard_map/all_gather | solution.py:27
  133.1 1.4 fusion.76
  139.6 22.4 %all-gather.16.cloned.1.call-done = f32[16,128,128]{2,1,0:T(8,128)} async-done(((f32[4,128,128]{2,1,0:T(8,128)}), f32[16,128,128]{2,1,0:T(8,128)}) %all-gather.16.cloned.1.call-update) | async-done | bytes 1048592 | tf_op jit(solution)/shard_map/all_gather | solution.py:27
  162.0 1.4 convolution_add_fusion.19
  163.4 1.4 convolution_add_fusion.18
  168.3 4.3 %convolution_convert_fusion = bf16[384,256]{1,0:T(8,128)(2,1)} fusion(bf16[384,4096]{1,0:T(8,128)(2,1)} %bitcast.238, bf16[4096,256]{1,0:T(8,128)(2,1)} %param.21), kind=kOutput, calls=%fused_computation.58 | convolution fusion | flops 805404672 | bytes 5439488 | tf_op jit(solution)/shard_map/dot_general | solution.py:163
  173.7 31.2 %all-gather.14.cloned.1.call-done = f32[32,128,128]{2,1,0:T(8,128)} async-done(((f32[4,128,128]{2,1,0:T(8,128)}), f32[32,128,128]{2,1,0:T(8,128)}) %all-gather.14.cloned.1.call-update) | async-done | bytes 2097168 | tf_op jit(solution)/shard_map/all_gather | solution.py:27
  204.9 41.1 %all-gather.18.cloned.1.call-done = f32[32,128,128]{2,1,0:T(8,128)} async-done(((f32[4,128,128]{2,1,0:T(8,128)}), f32[32,128,128]{2,1,0:T(8,128)}) %all-gather.18.cloned.1.call-update) | async-done | bytes 2097168 | tf_op jit(solution)/shard_map/all_gather | solution.py:27
  246.0 1.5 convolution_add_fusion.20
  247.5 1.4 convolution_add_fusion.15
  249.0 1.3 convolution_add_fusion.14
  254.6 7.1 %all-to-all-start = ((bf16[32,2,2,4,128]{4,3,2,1,0:T(4,128)(2,1)}), bf16[32,2,2,4,128]{4,3,2,1,0:T(4,128)(2,1)S(1)}, u32[]{:S(2)}, u32[]{:S(2)}) async-start(bf16[32,2,2,4,128]{4,3,2,1,0:T(4,128)(2,1)} %bitcast.193), calls=%async_computation | async-start | bytes 262144 | tf_op jit(solution)/shard_map/all_to_all | solution.py:44
  261.7 1.6 fusion.38
  265.1 7.1 %all-to-all-done = bf16[32,2,2,4,128]{4,3,2,1,0:T(4,128)(2,1)S(1)} async-done(((bf16[32,2,2,4,128]{4,3,2,1,0:T(4,128)(2,1)}), bf16[32,2,2,4,128]{4,3,2,1,0:T(4,128)(2,1)S(1)}, u32[]{:S(2)}, u32[]{:S(2)}) %all-to-all-start) | async-done | bytes 131104 | tf_op jit(solution)/shard_map/all_to_all | solution.py:44
  273.2 3.8 %all-to-all-start.1 = ((f32[32,1,1024]{2,1,0:T(1,128)}), f32[32,1,1024]{2,1,0:T(1,128)S(1)}, u32[]{:S(2)}, u32[]{:S(2)}) async-start(f32[32,1,1024]{2,1,0:T(1,128)} %broadcast_in_dim.80), calls=%async_computation.1 | async-start | bytes 262144 | tf_op jit(solution)/shard_map/all_to_all | solution.py:50
  277.1 1.7 fusion.60
  278.8 8.8 %all-to-all-done.1 = f32[32,1,1024]{2,1,0:T(1,128)S(1)} async-done(((f32[32,1,1024]{2,1,0:T(1,128)}), f32[32,1,1024]{2,1,0:T(1,128)S(1)}, u32[]{:S(2)}, u32[]{:S(2)}) %all-to-all-start.1) | async-done | bytes 131104 | tf_op jit(solution)/shard_map/all_to_all | solution.py:50
  (187 shorter events, 55.7 us)
Async XLA Ops:
  7.2 39.4 %copy-start = (bf16[4096,256]{1,0:T(8,128)(2,1)S(1)}, bf16[4096,256]{1,0:T(8,128)(2,1)}, u32[]{:S(2)}) copy-start(bf16[4096,256]{1,0:T(8,128)(2,1)} %param.18) | copy-start | bytes 6291460
  7.2 34.6 %all-gather.10.cloned.1.call-start = ((), (), s32[]{:S(2)}) async-start(), calls=%async_computation.2 | async-start | bytes 3538944 | tf_op jit(solution)/shard_map/all_gather | solution.py:187
  7.9 125.2 %all-gather.12.cloned.1.call-start = ((), (), s32[]{:S(2)}) async-start(), calls=%async_computation.3 | async-start | bytes 1310720 | tf_op jit(solution)/shard_map/all_gather | solution.py:27
  49.4 1.6 copy-start.23
  49.4 1.6 copy-start.28
  59.2 3.8 %copy-start.20 = (f32[2,2,3,64,128]{4,3,1,0,2:T(8,128)S(1)}, f32[2,2,3,64,128]{4,3,1,0,2:T(8,128)}, u32[]{:S(2)}) copy-start(f32[2,2,3,64,128]{4,3,1,0,2:T(8,128)} %copy.189) | copy-start | bytes 1179652
  63.0 2.4 copy-start.24
  105.3 56.7 %all-gather.16.cloned.1.call-start = ((), (), s32[]{:S(2)}) async-start(), calls=%async_computation.5 | async-start | bytes 1310720 | tf_op jit(solution)/shard_map/all_gather | solution.py:27
  106.0 98.9 %all-gather.14.cloned.1.call-start = ((), (), s32[]{:S(2)}) async-start(), calls=%async_computation.4 | async-start | bytes 2359296 | tf_op jit(solution)/shard_map/all_gather | solution.py:27
  133.1 4.2 %copy-start.3 = (f32[16,128,128]{2,1,0:T(8,128)S(1)}, f32[16,128,128]{2,1,0:T(8,128)}, u32[]{:S(2)}) copy-start(f32[16,128,128]{2,1,0:T(8,128)} %all-gather.12.cloned.1.call-done) | copy-start | bytes 3145732
  139.5 106.4 %all-gather.18.cloned.1.call-start = ((), (), s32[]{:S(2)}) async-start(), calls=%async_computation.6 | async-start | bytes 2359296 | tf_op jit(solution)/shard_map/all_gather | solution.py:27
  162.0 3.5 %copy-start.22 = (f32[16,128,128]{2,1,0:T(8,128)S(1)}, f32[16,128,128]{2,1,0:T(8,128)}, u32[]{:S(2)}) copy-start(f32[16,128,128]{2,1,0:T(8,128)} %all-gather.16.cloned.1.call-done) | copy-start | bytes 3145732
  163.4 4.4 %copy-start.26 = (bf16[2,2,128]{2,1,0:T(2,128)(2,1)S(1)}, bf16[2,2,128]{2,1,0:T(2,128)(2,1)}, u32[]{:S(2)}) copy-start(bf16[2,2,128]{2,1,0:T(2,128)(2,1)} %param.27) | copy-start | bytes 3076
  163.4 4.5 %copy-start.27 = (bf16[2,2,128]{2,1,0:T(2,128)(2,1)S(1)}, bf16[2,2,128]{2,1,0:T(2,128)(2,1)}, u32[]{:S(2)}) copy-start(bf16[2,2,128]{2,1,0:T(2,128)(2,1)} %param.28) | copy-start | bytes 3076
  163.4 4.7 %copy-start.29 = (f32[2,2]{1,0:T(2,128)S(1)}, f32[2,2]{1,0:T(2,128)}, u32[]{:S(2)}) copy-start(f32[2,2]{1,0:T(2,128)} %param.30) | copy-start | bytes 52
  163.4 4.8 %copy-start.32 = (f32[128]{0:T(128)S(1)}, f32[128]{0:T(128)}, u32[]{:S(2)}) copy-start(f32[128]{0:T(128)} %param.26) | copy-start | bytes 1540
  168.2 4.3 %copy-start.8 = (f32[4,128,128]{2,1,0:T(8,128)S(1)}, f32[4,128,128]{2,1,0:T(8,128)}, u32[]{:S(2)}) copy-start(f32[4,128,128]{2,1,0:T(8,128)} %copy-done.7) | copy-start | bytes 786436
  168.2 4.3 %copy-start.10 = (f32[4,128,128]{2,1,0:T(8,128)S(1)}, f32[4,128,128]{2,1,0:T(8,128)}, u32[]{:S(2)}) copy-start(f32[4,128,128]{2,1,0:T(8,128)} %copy-done.9) | copy-start | bytes 786436
  168.3 4.3 %copy-start.12 = (f32[4,128,128]{2,1,0:T(8,128)S(1)}, f32[4,128,128]{2,1,0:T(8,128)}, u32[]{:S(2)}) copy-start(f32[4,128,128]{2,1,0:T(8,128)} %fusion.109) | copy-start | bytes 786436
  168.3 4.3 %copy-start.18 = (f32[4,128,128]{2,1,0:T(8,128)S(1)}, f32[4,128,128]{2,1,0:T(8,128)}, u32[]{:S(2)}) copy-start(f32[4,128,128]{2,1,0:T(8,128)} %copy-done.17) | copy-start | bytes 786436
  246.0 3.0 %copy-start.6 = (f32[32,128,128]{2,1,0:T(8,128)S(1)}, f32[32,128,128]{2,1,0:T(8,128)}, u32[]{:S(2)}) copy-start(f32[32,128,128]{2,1,0:T(8,128)} %all-gather.14.cloned.1.call-done) | copy-start | bytes 6291460
  246.0 4.3 %copy-start.19 = (f32[32,128,128]{2,1,0:T(8,128)S(1)}, f32[32,128,128]{2,1,0:T(8,128)}, u32[]{:S(2)}) copy-start(f32[32,128,128]{2,1,0:T(8,128)} %all-gather.18.cloned.1.call-done) | copy-start | bytes 6291460
  251.9 1.0 copy-start.11
  251.9 1.0 copy-start.14
  252.0 1.1 copy-start.16
  252.0 1.5 copy-start.2
  252.0 1.5 copy-start.5
  254.6 17.6 %all-to-all-start = ((bf16[32,2,2,4,128]{4,3,2,1,0:T(4,128)(2,1)}), bf16[32,2,2,4,128]{4,3,2,1,0:T(4,128)(2,1)S(1)}, u32[]{:S(2)}, u32[]{:S(2)}) async-start(bf16[32,2,2,4,128]{4,3,2,1,0:T(4,128)(2,1)} %bitcast.193), calls=%async_computation | async-start | bytes 262144 | tf_op jit(solution)/shard_map/all_to_all | solution.py:44
  263.7 24.0 %copy-start.30 = (bf16[2,2,128]{2,1,0:T(2,128)(2,1)S(1)}, bf16[2,2,128]{2,1,0:T(2,128)(2,1)}, u32[]{:S(2)}) copy-start(bf16[2,2,128]{2,1,0:T(2,128)(2,1)} %param.29) | copy-start | bytes 3076
  263.8 24.0 %copy-start.31 = (f32[2,2]{1,0:T(2,128)S(1)}, f32[2,2]{1,0:T(2,128)}, u32[]{:S(2)}) copy-start(f32[2,2]{1,0:T(2,128)} %param.31) | copy-start | bytes 52
  272.2 16.4 %copy-start.25 = (bf16[2,2,4,128]{3,2,1,0:T(4,128)(2,1)}, bf16[2,2,4,128]{3,2,1,0:T(4,128)(2,1)S(1)}, u32[]{:S(2)}) copy-start(bf16[2,2,4,128]{3,2,1,0:T(4,128)(2,1)S(1)} %reduce_sum.87) | copy-start | bytes 12292
  273.2 14.4 %all-to-all-start.1 = ((f32[32,1,1024]{2,1,0:T(1,128)}), f32[32,1,1024]{2,1,0:T(1,128)S(1)}, u32[]{:S(2)}, u32[]{:S(2)}) async-start(f32[32,1,1024]{2,1,0:T(1,128)} %broadcast_in_dim.80), calls=%async_computation.1 | async-start | bytes 262144 | tf_op jit(solution)/shard_map/all_to_all | solution.py:50
  (8 other events, 6.0 us)
Sparse Core Ops, SparseCore 0:
  9.8 31.8 all-gather.9
  105.4 27.6 all-gather.11
  134.9 27.0 all-gather.15
  163.6 41.2 all-gather.13
  206.5 39.4 all-gather.17
where the time goes:
time: 296 us; the launch traced here: 295 us
  waiting for transfers between devices  171 us (58%)
  matrix products  75.5 us (26%)
  between operations  14.6 us (5%)
  local copies, waits for them, and re-layouts  13.8 us (5%)
  starting transfers between devices  11.1 us (4%)
  other arithmetic  8.51 us (3%)
    all_gather x4, waiting for transfers between devices, carried_in(): pieces = jax.tree.map(lambda part: lax.all_gather(part, axis), subtotal)  122 us
    dot_general x61, matrix products, matmul(): return jnp.einsum(form, left, right, precision=highest)  55.6 us
    all_gather x1, waiting for transfers between devices, shards(): lax.all_gather(tokens, 'tp', axis=2, tiled=True)  32.4 us
    dot_general x6, matrix products, project_rows(): jnp.dot(flat_rows, weight, preferred_element_type=jnp.float32)  19.9 us
    all_to_all x1, waiting for transfers between devices, copy_for_each(): lax.all_to_all(jnp.broadcast_to(value[None], (length, *value.shape)), axi...  8.81 us
    all_to_all x1, waiting for transfers between devices, summed_on_arrival(): lax.all_to_all(parts, axis, split_axis=0, concat_axis=0, tiled=True)  7.1 us
    all_to_all x1, starting transfers between devices, summed_on_arrival(): lax.all_to_all(parts, axis, split_axis=0, concat_axis=0, tiled=True)  7.08 us
  transfers between devices with their start and end apart: 7, of which 7 were waited for; matrix products, arithmetic and copies ran while one was open for 7% of the time, Pallas kernels for 0%

commit v1 on v0

v1 whole, which is shorter than its diff:
```python
import functools

import jax
import jax.numpy as jnp
from jax import lax
from jax.experimental import pallas as pl
from jax.experimental.pallas import tpu as pltpu
from jax.sharding import Mesh
from jax.sharding import PartitionSpec as P

NEAR = ("zl", "x")
AXES = ("zh", "zl", "x")
PACK = 16
unit_floor = 1.0
norm_floor = 0.001
bf16 = jnp.bfloat16
f32 = jnp.float32


def dot(left, right, dims=((1,), (0,))):
    return lax.dot_general(
        left.astype(bf16), right.astype(bf16), (dims, ((), ())), preferred_element_type=f32
    )


ROWS = ((1,), (1,))
COLS = ((0,), (0,))


def thirds(value):
    high = value.astype(bf16).astype(f32)
    rest = value - high
    mid = rest.astype(bf16).astype(f32)
    return high, mid, rest - mid


def iota(shape, dim):
    return lax.broadcasted_iota(jnp.int32, shape, dim)


def row_pack(values, width):
    rows = iota((PACK, width), 0)
    packed = jnp.zeros((PACK, width), f32)
    for at, value in enumerate(values):
        packed = jnp.where(rows == at, value, packed)
    return packed


def rms_scale(values, floor, mean):
    total = jnp.sum(values * values, axis=-1, keepdims=True)
    return lax.rsqrt((total / values.shape[-1] if mean else total) + floor)


def token_copies(pieces, buffer, sems):
    own, own_c, *rest = pieces
    copies = [
        [pltpu.make_async_copy(ref.at[seq], buffer.at[slot, seq], sems.at[slot]) for seq in range(2)]
        for slot, ref in enumerate((own, own_c))
    ]
    for pair in range(6):
        first, second = rest[2 * pair : 2 * pair + 2]
        slot = 2 + pair
        copies.append(
            [
                pltpu.make_async_copy(first, buffer.at[slot, 0], sems.at[slot]),
                pltpu.make_async_copy(second, buffer.at[slot, 1], sems.at[slot]),
            ]
        )
    return copies


def project_pieces(shard_of, pieces, weights, token_buffer, weight_buffers, sems, each):
    depth = token_buffer.shape[-1]
    copies = token_copies(pieces, token_buffer, sems)
    for slot in range(8):
        start = pl.multiple_of(shard_of[slot] * depth, depth)
        for weight, buffer in zip(weights, weight_buffers):
            copies[slot].append(
                pltpu.make_async_copy(
                    weight.at[pl.ds(start, depth), :], buffer.at[slot], sems.at[slot]
                )
            )
        for copy in copies[slot]:
            copy.start()
    totals = [None] * len(weights)
    for slot in range(8):
        for copy in copies[slot]:
            copy.wait()
        rows = token_buffer[slot].reshape(-1, depth)
        for at, buffer in enumerate(weight_buffers):
            part = dot(rows, buffer[slot])
            totals[at] = part if totals[at] is None else totals[at] + part
    return totals


def local_kernel(shard_of, *refs):
    pieces, refs = refs[:14], refs[14:]
    key_w, value_w, gate_w, bias_ref, rate_ref = refs[:5]
    send_ref, key_ref, fresh_ref, carry_ref, cols_ref, rows_ref = refs[5:11]
    token_buffer, key_buffer, value_buffer, gate_buffer, sems = refs[11:]
    span = token_buffer.shape[2]
    head = send_ref.shape[-1]
    key_total, value_total, gates = project_pieces(
        shard_of,
        pieces,
        (key_w, value_w, gate_w),
        token_buffer,
        (key_buffer, value_buffer, gate_buffer),
        sems,
        None,
    )
    key_rows = key_total.astype(bf16)
    value_rows = value_total.astype(bf16)
    key_ref[...] = key_rows
    strength = jax.nn.sigmoid(gates + bias_ref[...])
    decays = -jnp.exp(rate_ref[...]) * jax.nn.softplus(gates)
    wide = cols_ref.shape[1]
    pairs = []
    lanes = iota((wide, head), 1)
    causal_wide = (iota((wide, wide), 0) >= iota((wide, wide), 1)).astype(bf16)
    for seq in range(2):
        take = slice(seq * span, (seq + 1) * span)
        padded = jnp.concatenate([decays[take], jnp.zeros((wide - span, head), f32)], axis=0)
        cumulative = sum(dot(causal_wide, part) for part in thirds(padded))
        table = jnp.where((lanes == 2) | (lanes == 3), cumulative, 0.0)
        for h in range(2):
            keys = key_rows[take, h * head : (h + 1) * head].astype(f32)
            unit = jnp.concatenate(
                [rms_scale(keys, unit_floor, False), jnp.zeros((wide - span, 1), f32)], axis=0
            )
            beta = jnp.concatenate(
                [strength[take, h : h + 1], jnp.zeros((wide - span, 1), f32)], axis=0
            )
            table = jnp.where(lanes == h, beta, table)
            table = jnp.where(lanes == 4 + h, unit, table)
        cols_ref[seq] = table
        rows_ref[seq] = table.T
    t = iota((span, span), 0)
    s = iota((span, span), 1)
    lower, inverse = [], []
    for pair in range(4):
        seq, h = divmod(pair, 2)
        keys = key_rows[seq * span : (seq + 1) * span, h * head : (h + 1) * head]
        col = lambda at: cols_ref[seq, :span, at + h : at + h + 1]
        row = lambda at: rows_ref[seq, at + h : at + h + 1, :span]
        spread = jnp.where(t >= s, col(2) - row(2), 0.0)
        alike = dot(keys, keys, ROWS) * (col(0) * col(4)) * row(4) * jnp.exp(spread)
        lower.append(jnp.where(t > s, alike, 0.0))
        inverse.append(jnp.where(t // 2 == s // 2, lower[pair], 0.0))
    size = 2
    while size < span:
        mask = (t // (2 * size) == s // (2 * size)) & (t // size != s // size)
        steps = []
        for pair in range(4):
            block = jnp.where(mask, lower[pair], 0.0)
            steps.append(block - dot(block, inverse[pair]))
        for pair in range(4):
            inverse[pair] = inverse[pair] + steps[pair] - dot(inverse[pair], steps[pair])
        size *= 2
    for pair in range(4):
        seq, h = divmod(pair, 2)
        take = slice(seq * span, (seq + 1) * span)
        keys = key_rows[take, h * head : (h + 1) * head]
        values = value_rows[take, h * head : (h + 1) * head]
        col = lambda at: cols_ref[seq, :span, at + h : at + h + 1]
        row = lambda at: rows_ref[seq, at + h : at + h + 1, :span]
        fresh = col(0) * values.astype(f32) - dot(inverse[pair] * row(0), values)
        carry = (col(0) * col(4) * jnp.exp(col(2))) * keys.astype(f32) - dot(
            inverse[pair] * (row(0) * row(4) * jnp.exp(row(2))), keys
        )
        last = cols_ref[seq, span - 1 : span, 2 + h : 3 + h]
        late = col(4) * jnp.exp(last - col(2))
        reach = dot(carry * late, keys, COLS)
        gain = dot(fresh * late, keys, COLS)
        fresh_ref[pair] = fresh.astype(bf16)
        carry_ref[pair] = carry.astype(bf16)
        factor = row_pack(thirds(jnp.broadcast_to(jnp.exp(last), (1, head))), head)
        half = head // 2
        for side in range(2):
            to = 2 * pair + side
            send_ref[to, :head, :] = reach.astype(bf16)
            send_ref[to, head : head + half, :] = gain[side * half : (side + 1) * half].astype(bf16)
            send_ref[to, head + half :, :] = factor.astype(bf16)


def window_kernel(shard_of, *refs):
    pieces, refs = refs[:14], refs[14:]
    query_w, gate_w, gain_ref, key_ref, fresh_ref, carry_ref, cols_ref, rows_ref = refs[:8]
    out_ref, reach_ref, silu_ref = refs[8:11]
    token_buffer, query_buffer, gate_buffer, sems = refs[11:]
    span = token_buffer.shape[2]
    head = fresh_ref.shape[-1]
    query_total, gate_total = project_pieces(
        shard_of, pieces, (query_w, gate_w), token_buffer, (query_buffer, gate_buffer), sems, None
    )
    query_rows = query_total.astype(bf16)
    gate_rows = gate_total.astype(bf16).astype(f32)
    t = iota((span, span), 0)
    s = iota((span, span), 1)
    for pair in range(4):
        seq, h = divmod(pair, 2)
        take = slice(seq * span, (seq + 1) * span)
        part = slice(h * head, (h + 1) * head)
        col = lambda at: cols_ref[seq, :span, at + h : at + h + 1]
        row = lambda at: rows_ref[seq, at + h : at + h + 1, :span]
        queries = query_rows[take, part]
        unit = rms_scale(queries.astype(f32), unit_floor, False)
        spread = jnp.where(t >= s, col(2) - row(2), 0.0)
        scores = dot(queries, key_ref[take, part], ROWS) * unit * row(4) * jnp.exp(spread)
        scores = jnp.where(t >= s, scores, 0.0).astype(bf16)
        out_ref[pair] = dot(scores, fresh_ref[pair])
        reach = (unit * jnp.exp(col(2))) * queries.astype(f32) - dot(scores, carry_ref[pair])
        reach_ref[pair] = reach.astype(bf16)
        gate = gate_rows[take, part]
        silu_ref[pair] = gain_ref[...] * gate * jax.nn.sigmoid(gate)


def unpack_factor(block):
    block = block.astype(f32)
    return block[0:1] + block[1:2] + block[2:3]


def compose_kernel(in_ref, total_ref, maps_ref, adds_ref, factors_ref):
    count, rows, head = in_ref.shape
    body = rows - PACK

    def load(at):
        return in_ref[at, :body, :].astype(f32), unpack_factor(in_ref[at, body:, :])

    def join(first, second):
        both, factor = first
        later, later_factor = second
        tail = jnp.concatenate([factor * later[:head], later[head:]], axis=0)
        return later_factor * both - dot(both, later[:head]) + tail, factor * later_factor

    member = [load(at) for at in range(count)]
    upto = [None] * (count + 1)
    upto[1] = member[0]
    c23, c45, c67 = (join(member[at], member[at + 1]) for at in (2, 4, 6))
    upto[2] = join(member[0], member[1])
    c456 = join(c45, member[6])
    c4567 = join(c45, c67)
    upto[4] = join(upto[2], c23)
    upto[8] = join(upto[4], c4567)
    both, factor = upto[8]
    total_ref[:body, :] = both.astype(bf16)
    total_ref[body:, :] = row_pack(thirds(factor), head).astype(bf16)
    upto[3] = join(upto[2], member[2])
    upto[5] = join(upto[4], member[4])
    upto[6] = join(upto[4], c45)
    upto[7] = join(upto[4], c456)
    for at in range(1, count):
        both, factor = upto[at]
        maps_ref[at - 1] = both[:head].astype(bf16)
        adds_ref[at - 1] = both[head:]
        factors_ref[at - 1] = jnp.broadcast_to(factor, (8, head))


def spread_kernel(
    place, beta_ref, decay_ref, own, back1, back2, back3, maps_ref, adds_ref, factors_ref,
    query_ref, key_ref, value_ref, send_ref, groups_ref, wide_ref, turned_ref,
):
    rows, head = own.shape
    half = head // 2
    far, near = place[0], place[1]
    pair = near // 2
    side = near % 2
    for slot, ref in enumerate((own, back1, back2, back3)):
        groups_ref[slot] = ref[...]
    state = jnp.zeros((half, head), f32)
    begin = state
    for group in range(4):
        begin = jnp.where(far == group, state, begin)
        block = groups_ref[lax.rem(far - group + 4, 4)]
        added = block[head : head + half].astype(f32)
        if group:
            state = unpack_factor(block[head + half :]) * state - dot(state, block[:head]) + added
        else:
            state = added
    final = state.astype(bf16).astype(f32)
    wide_ref[...] = jnp.zeros((head, head), f32)
    wide_ref[pl.ds(pl.multiple_of(side * half, half), half), :] = final
    padded = wide_ref[...]
    turned_ref[...] = padded.T
    mine = turned_ref[pl.ds(pl.multiple_of(far * 32, 32), 32), :]
    query = query_ref[pl.ds(pair, 1), :]
    key = key_ref[pl.ds(pair, 1), :]
    query = query * rms_scale(query, unit_floor, False)
    key = key * rms_scale(key, unit_floor, False)
    hits = dot(row_pack(thirds(query) + thirds(key), head), padded, ROWS)
    recall = hits[0:1] + hits[1:2] + hits[2:3]
    retrieve = hits[3:4] + hits[4:5] + hits[5:6]
    intersect = jnp.sum(key * query, axis=-1, keepdims=True)
    fresh = value_ref[pl.ds(pair, 1), :] - decay_ref[pair] * retrieve
    read = decay_ref[pair] * recall + (beta_ref[pair] * intersect) * fresh
    read = jnp.where(iota((1, head), 1) // half == side, read, 0.0)
    zero = jnp.zeros((1, head), f32)
    extra = row_pack((zero, zero, zero, zero) + thirds(read), head)
    pick_row = iota((PACK, 32), 0)
    pick_col = iota((PACK, 32), 1)
    for member in range(8):
        if member:
            at = member - 1
            entry = factors_ref[at, 0:1, :] * begin - dot(begin, maps_ref[at]) + adds_ref[at]
        else:
            entry = begin
        send_ref[member, :half, :] = entry.astype(bf16)
        pick = ((pick_row < 4) & (pick_col == 4 * member + pick_row)).astype(bf16)
        send_ref[member, half:, :] = (dot(pick, mine) + extra).astype(bf16)


def finish_kernel(in_ref, out_ref, reach_ref, silu_ref, gain_ref, mixed_ref, cache_ref, read_ref):
    head = in_ref.shape[-1]
    half = head // 2
    for pair in range(4):
        seq, h = divmod(pair, 2)
        incoming = jnp.concatenate([in_ref[2 * pair, :half, :], in_ref[2 * pair + 1, :half, :]], 0)
        whole = out_ref[pair] + dot(reach_ref[pair], incoming, ROWS)
        mixed = whole * rms_scale(whole, norm_floor, True) * silu_ref[pair]
        mixed_ref[seq, :, h * head : (h + 1) * head] = mixed.astype(bf16)
        extra = in_ref[2 * pair, half:, :].astype(f32) + in_ref[2 * pair + 1, half:, :].astype(f32)
        cache_ref[seq, h] = extra[:4].astype(bf16)
        read = extra[4:5] + extra[5:6] + extra[6:7]
        read = read * rms_scale(read, norm_floor, True) * gain_ref[...]
        read_ref[seq : seq + 1, h * head : (h + 1) * head] = read


def vmem():
    return pl.BlockSpec(memory_space=pltpu.VMEM)


def smem():
    return pl.BlockSpec(memory_space=pltpu.SMEM)


def anywhere():
    return pl.BlockSpec(memory_space=pl.ANY)


def shape(dims, dtype):
    return jax.ShapeDtypeStruct(dims, dtype)


def shift(value, axis, by):
    length = lax.axis_size(axis)
    return lax.ppermute(value, axis, [(at, (at + by) % length) for at in range(length)])


def shards(
    tokens, query_weight, key_weight, value_weight, gate_weight, beta_weight, decay_weight,
    beta_bias, rate_log, out_gain, new_query, new_key, new_value, new_beta, new_decay,
):
    _, span, depth = tokens.shape
    head = out_gain.shape[0]
    half = head // 2
    wide = 256
    width = query_weight.shape[1]
    y, core = lax.axis_index("y"), lax.axis_index("c")
    first, second = tokens[0], tokens[1]
    up0 = shift(first, "y", 1)
    down1 = shift(second, "y", -1)
    up1 = shift(second, "y", 1)
    down0 = shift(first, "y", -1)
    far0 = shift(up0, "y", 1)
    far1 = shift(down1, "y", -1)
    swap = lambda value: shift(value, "c", 1)
    pieces = [tokens, swap(tokens), up0, up1, down0, down1, far0, far1]
    pieces += [swap(value) for value in (up0, up1, down0, down1, far0, far1)]
    ahead = [y, y, y + 3, y + 1, y + 2, y + 3, y + 1, y + 2]
    cores = [core, 1 - core, core, core, core, 1 - core, 1 - core, 1 - core]
    shard_of = jnp.stack([(a % 4) * 2 + c for a, c in zip(ahead, cores)]).astype(jnp.int32)
    scalars = jnp.concatenate([beta_weight, decay_weight], axis=1)
    scalars = jnp.pad(scalars, ((0, 0), (0, head - scalars.shape[1])))
    bias = jnp.pad(beta_bias, (0, head - 2))[None]
    rate = jnp.pad(rate_log, (2, head - 4))[None]
    gain = out_gain[None]

    buffers = lambda widths: [pltpu.VMEM((8, 2, span, depth), bf16)] + [
        pltpu.VMEM((8, depth, w), bf16) for w in widths
    ] + [pltpu.SemaphoreType.DMA((8,))]
    rows = head + half + PACK
    send, key_rows, fresh, carry, cols, turned = pl.pallas_call(
        local_kernel,
        name="local_terms",
        out_shape=(
            shape((8, rows, head), bf16),
            shape((2 * span, width), bf16),
            shape((4, span, head), bf16),
            shape((4, span, head), bf16),
            shape((2, wide, head), f32),
            shape((2, head, wide), f32),
        ),
        in_specs=[smem()] + [anywhere()] * 17 + [vmem()] * 2,
        out_specs=tuple(vmem() for _ in range(6)),
        scratch_shapes=buffers((width, width, head)),
    )(shard_of, *pieces, key_weight, value_weight, scalars, bias, rate)

    arrived = lax.all_to_all(send, NEAR, 0, 0, tiled=True)

    local_out, reach, silu = pl.pallas_call(
        window_kernel,
        name="window_terms",
        out_shape=(
            shape((4, span, head), f32),
            shape((4, span, head), bf16),
            shape((4, span, head), f32),
        ),
        in_specs=[smem()] + [anywhere()] * 16 + [vmem()] * 6,
        out_specs=tuple(vmem() for _ in range(3)),
        scratch_shapes=buffers((width, width)),
    )(shard_of, *pieces, query_weight, gate_weight, gain, key_rows, fresh, carry, cols, turned)

    total, maps, adds, factors = pl.pallas_call(
        compose_kernel,
        name="compose_near",
        out_shape=(
            shape((rows, head), bf16),
            shape((7, head, head), bf16),
            shape((7, half, head), f32),
            shape((7, 8, head), f32),
        ),
        in_specs=[vmem()],
        out_specs=tuple(vmem() for _ in range(4)),
    )(arrived)

    others = [shift(total, "zh", by) for by in (1, 2, 3)]
    place = jnp.stack([lax.axis_index("zh"), lax.axis_index(NEAR)]).astype(jnp.int32)
    flat = lambda value: value.reshape(4, -1).astype(f32)
    back = pl.pallas_call(
        spread_kernel,
        name="spread_states",
        out_shape=shape((8, half + PACK, head), bf16),
        in_specs=[smem()] * 3 + [vmem()] * 10,
        out_specs=vmem(),
        scratch_shapes=[
            pltpu.VMEM((4, rows, head), bf16),
            pltpu.VMEM((head, head), f32),
            pltpu.VMEM((head, head), f32),
        ],
    )(
        place, new_beta.reshape(4), new_decay.reshape(4), total, *others, maps, adds, factors,
        flat(new_query), flat(new_key), flat(new_value),
    )
    returned = lax.all_to_all(back, NEAR, 0, 0, tiled=True)
    return pl.pallas_call(
        finish_kernel,
        name="finish",
        out_shape=(
            shape((2, span, width), bf16),
            shape((2, 2, 4, head), bf16),
            shape((2, width), f32),
        ),
        in_specs=[vmem()] * 5,
        out_specs=tuple(vmem() for _ in range(3)),
    )(returned, local_out, reach, silu, gain)


def solution(mesh):
    torus = Mesh(mesh.devices.reshape(4, 2, 4, 4, 2), AXES + ("y", "c"))
    sp, tp = AXES, ("y", "c")
    weight = P(None, tp)
    in_specs = (
        P(None, sp, tp),
        weight, weight, weight, weight, weight, weight,
        P(tp), P(tp), P(),
        P(None, tp, None), P(None, tp, None), P(None, tp, None),
        P(None, tp), P(None, tp),
    )
    out_specs = (P(None, sp, tp), P(None, tp, sp, None), P(None, tp))
    return jax.shard_map(
        shards, mesh=torus, in_specs=in_specs, out_specs=out_specs, check_vma=False
    )
```

time: 296 us -> 84.4 us (0.29)
  waiting for transfers between devices: 171 us -> 18 us
  matrix products: 75.5 us -> 0 us
  Pallas kernels: 0 us -> 25.4 us
  starting transfers between devices: 11.1 us -> 27.6 us
  between operations: 14.6 us -> 0.94 us
  local copies, waits for them, and re-layouts: 13.8 us -> 8.09 us
  other arithmetic: 8.51 us -> 3.08 us
    all_gather x5 -> x0, waiting for transfers between devices: 154 us -> none  [the longest x4 122 us: carried_in(): pieces = jax.tree.map(lambda part: lax.all_gather(part, axis), subtotal)]
    dot_general x67 -> x0, matrix products: 75.5 us -> none  [the longest x61 55.6 us: matmul(): return jnp.einsum(form, left, right, precision=highest)]
    pallas_call x0 -> x5, Pallas kernels: none -> 25.4 us  [the longest x1 11.4 us: shards(): pl.pallas_call(local_kernel, name='local_terms', out_shape=(shape((8, row...]
    ppermute x0 -> x16, starting transfers between devices: none -> 20 us  [shift(): lax.ppermute(value, axis, [(at, (at + by) % length) for at in range(lengt...]
    ppermute x0 -> x16, waiting for transfers between devices: none -> 9.11 us  [shift(): lax.ppermute(value, axis, [(at, (at + by) % length) for at in range(lengt...]
    all_to_all x2, waiting for transfers between devices: 15.9 us -> 8.9 us  [the longest x1 8.89 us: shards(): arrived = lax.all_to_all(send, NEAR, 0, 0, tiled=True)]
    all_to_all x2, starting transfers between devices: 10.9 us -> 7.61 us  [the longest x1 4.23 us: shards(): arrived = lax.all_to_all(send, NEAR, 0, 0, tiled=True)]
    unnamed x68 -> x46, local copies, waits for them, and re-layouts: 5.89 us -> 2.86 us
  transfers between devices with their start and end apart: 7 -> 18, of which waited for: 7 -> 6; matrix products, arithmetic and copies ran while one was open for 7% -> 9% of each run, Pallas kernels for 0% -> 8%
where the time goes in v1:
time: 84.4 us; the launch traced here: 83.1 us
  starting transfers between devices  27.6 us (33%)
  Pallas kernels  25.4 us (30%)
  waiting for transfers between devices  18 us (21%)
  local copies, waits for them, and re-layouts  8.09 us (10%)
  other arithmetic  3.08 us (4%)
  between operations  0.94 us (1%)
    ppermute x16, starting transfers between devices, shift(): lax.ppermute(value, axis, [(at, (at + by) % length) for at in range(lengt...  20 us
    pallas_call x1, Pallas kernels, shards(): pl.pallas_call(local_kernel, name='local_terms', out_shape=(shape((8, row...  11.4 us
    ppermute x16, waiting for transfers between devices, shift(): lax.ppermute(value, axis, [(at, (at + by) % length) for at in range(lengt...  9.11 us
    all_to_all x1, waiting for transfers between devices, shards(): arrived = lax.all_to_all(send, NEAR, 0, 0, tiled=True)  8.89 us
    pallas_call x1, Pallas kernels, shards(): pl.pallas_call(window_kernel, name='window_terms', out_shape=(shape((4, s...  6.82 us
    all_to_all x1, starting transfers between devices, shards(): arrived = lax.all_to_all(send, NEAR, 0, 0, tiled=True)  4.23 us
    all_to_all x1, starting transfers between devices, shards(): returned = lax.all_to_all(back, NEAR, 0, 0, tiled=True)  3.38 us
    unnamed x46, local copies, waits for them, and re-layouts  2.86 us
  transfers between devices with their start and end apart: 18, of which 6 were waited for; matrix products, arithmetic and copies ran while one was open for 9% of the time, Pallas kernels for 8%

profile of v1, /device:TPU:24, one launch (start us, length us, event | category | flops | bytes accessed | tf_op | source)
XLA Modules:
  0.0 83.1 jit_solution(16991775527151195068)
XLA Ops:
  0.7 1.1 %slice_bitcast_fusion = (bf16[192,512]{1,0:T(8,128)(2,1)S(1)}, bf16[192,512]{1,0:T(8,128)(2,1)S(1)}) fusion(bf16[2,192,512]{2,1,0:T(8,128)(2,1)} %refs_0_.3), kind=kLoop, calls=%fused_computation | loop fusion | bytes 786432 | tf_op jit(solution)/shard_map/squeeze | solution.py:359
  1.7 2.0 %collective-permute-start.1 = (bf16[192,512]{1,0:T(8,128)(2,1)S(1)}, bf16[192,512]{1,0:T(8,128)(2,1)S(1)}, u32[]{:S(2)}, u32[]{:S(2)}) collective-permute-start(bf16[192,512]{1,0:T(8,128)(2,1)S(1)} %get-tuple-element.30), channel_id=1, source_target_pairs={{0,2},{2,4},{4,6},{6,0},{1,3},{3,5},{5,7},{7,1},{8,10},{10,12},{12... | collective-permute-start | bytes 589832 | tf_op jit(solution)/shard_map/ppermute | solution.py:346
  3.8 3.1 %collective-permute-start.2 = (bf16[192,512]{1,0:T(8,128)(2,1)S(1)}, bf16[192,512]{1,0:T(8,128)(2,1)S(1)}, u32[]{:S(2)}, u32[]{:S(2)}) collective-permute-start(bf16[192,512]{1,0:T(8,128)(2,1)S(1)} %get-tuple-element.29), channel_id=1, source_target_pairs={{0,2},{2,4},{4,6},{6,0},{1,3},{3,5},{5,7},{7,1},{8,10},{10,12},{12... | collective-permute-start | bytes 589832 | tf_op jit(solution)/shard_map/ppermute | solution.py:346
  7.0 2.6 %collective-permute-done.1.refs_2_ = bf16[192,512]{1,0:T(8,128)(2,1)S(1)} collective-permute-done((bf16[192,512]{1,0:T(8,128)(2,1)S(1)}, bf16[192,512]{1,0:T(8,128)(2,1)S(1)}, u32[]{:S(2)}, u32[]{:S(2)}) %collective-permute-start.1) | collective-permute-done | bytes 196640 | tf_op jit(solution)/shard_map/ppermute | solution.py:346
  9.6 3.1 %collective-permute-start.5 = (bf16[192,512]{1,0:T(8,128)(2,1)S(1)}, bf16[192,512]{1,0:T(8,128)(2,1)S(1)}, u32[]{:S(2)}, u32[]{:S(2)}) collective-permute-start(bf16[192,512]{1,0:T(8,128)(2,1)S(1)} %collective-permute-done.1.refs_2_), channel_id=1, source_target_pairs={{0,2},{2,4},{4,6},{6,0},{1,3},{3,5},{5,7},{7,1},{8,10},{10,12},{12... | collective-permute-start | bytes 589832 | tf_op jit(solution)/shard_map/ppermute | solution.py:346
  12.8 1.0 %collective-permute-done.2.refs_3_ = bf16[192,512]{1,0:T(8,128)(2,1)S(1)} collective-permute-done((bf16[192,512]{1,0:T(8,128)(2,1)S(1)}, bf16[192,512]{1,0:T(8,128)(2,1)S(1)}, u32[]{:S(2)}, u32[]{:S(2)}) %collective-permute-start.2) | collective-permute-done | bytes 196640 | tf_op jit(solution)/shard_map/ppermute | solution.py:346
  13.8 2.8 %collective-permute-done.3.refs_4_ = bf16[192,512]{1,0:T(8,128)(2,1)S(1)} collective-permute-done((bf16[192,512]{1,0:T(8,128)(2,1)S(1)}, bf16[192,512]{1,0:T(8,128)(2,1)S(1)}, u32[]{:S(2)}, u32[]{:S(2)}) %collective-permute-start.3) | collective-permute-done | bytes 196640 | tf_op jit(solution)/shard_map/ppermute | solution.py:346
  17.1 2.5 %collective-permute-done.6.refs_7_ = bf16[192,512]{1,0:T(8,128)(2,1)S(1)} collective-permute-done((bf16[192,512]{1,0:T(8,128)(2,1)S(1)}, bf16[192,512]{1,0:T(8,128)(2,1)S(1)}, u32[]{:S(2)}, u32[]{:S(2)}) %collective-permute-start.6) | collective-permute-done | bytes 196640 | tf_op jit(solution)/shard_map/ppermute | solution.py:346
  20.4 0.8 pad_maximum_fusion
  21.7 1.2 %pad.12.refs_16_ = bf16[4096,128]{1,0:T(8,128)(2,1)} pad(bf16[4096,4]{1,0:T(8,128)(2,1)S(1)} %copy.20, bf16[]{:T(256)} %constant.60.clone.1), padding=0_0x0_124 | pad | bytes 1081346 | tf_op jit(solution)/shard_map/jit(_pad)/pad | solution.py:373
  23.0 0.6 stack.47.shard_of
  23.6 0.6 pad_bitcast_fusion
  25.1 11.4 %local_terms.1 = (bf16[8,208,128]{2,1,0:T(8,128)(2,1)}, bf16[384,256]{1,0:T(8,128)(2,1)}, bf16[4,192,128]{2,1,0:T(8,128)(2,1)}, bf16[4,192,128]{2,1,0:T(8,128)(2...) custom-call(s32[8]{0:T(128)} %stack.47.shard_of, bf16[2,192,512]{2,1,0:T(8,128)(2,1)} %refs_0_.3, ...), custom_call_target="tpu_custom_call" | custom-call | tf_op jit(solution)/shard_map/local_terms/pallas_call | solution.py:382
  36.6 4.2 %all-to-all-start = ((bf16[8,208,128]{2,1,0:T(8,128)(2,1)}), bf16[8,208,128]{2,1,0:T(8,128)(2,1)S(1)}, u32[]{:S(2)}, u32[]{:S(2)}) async-start(bf16[8,208,128]{2,1,0:T(8,128)(2,1)} %get-tuple-element.16), calls=%async_computation | async-start | bytes 851968 | tf_op jit(solution)/shard_map/all_to_all | solution.py:398
  40.8 8.9 %all-to-all-done.in_ref = bf16[8,208,128]{2,1,0:T(8,128)(2,1)S(1)} async-done(((bf16[8,208,128]{2,1,0:T(8,128)(2,1)}), bf16[8,208,128]{2,1,0:T(8,128)(2,1)S(1)}, u32[]{:S(2)}, u32[]{:S(2)}) %all-to-all-start) | async-done | bytes 426016 | tf_op jit(solution)/shard_map/all_to_all | solution.py:398
  49.7 0.7 copy-done
  50.4 2.3 %compose_near.1 = (bf16[208,128]{1,0:T(8,128)(2,1)}, bf16[7,128,128]{2,1,0:T(8,128)(2,1)}, f32[7,64,128]{2,1,0:T(8,128)}, f32[7,8,128]{2,1,0:T(8,128)}) custom-call(bf16[8,208,128]{2,1,0:T(8,128)(2,1)} %copy-done), custom_call_target="tpu_custom_call" | custom-call | tf_op jit(solution)/shard_map/compose_near/pallas_call | solution.py:413
  52.7 3.3 %collective-permute-start.13 = (bf16[208,128]{1,0:T(8,128)(2,1)}, bf16[208,128]{1,0:T(8,128)(2,1)S(1)}, u32[]{:S(2)}, u32[]{:S(2)}) collective-permute-start(bf16[208,128]{1,0:T(8,128)(2,1)} %get-tuple-element.17.own), channel_id=1, source_target_pairs={{0,64},{64,128},{128,192},{192,0},{1,65},{65,129},{129,193},{193,1... | collective-permute-start | bytes 159752 | tf_op jit(solution)/shard_map/ppermute | solution.py:346
  56.0 4.5 %collective-permute-start.14 = (bf16[208,128]{1,0:T(8,128)(2,1)}, bf16[208,128]{1,0:T(8,128)(2,1)S(1)}, u32[]{:S(2)}, u32[]{:S(2)}) collective-permute-start(bf16[208,128]{1,0:T(8,128)(2,1)} %get-tuple-element.17.own), channel_id=1, source_target_pairs={{0,128},{64,192},{128,0},{192,64},{1,129},{65,193},{129,1},{193,65... | collective-permute-start | bytes 159752 | tf_op jit(solution)/shard_map/ppermute | solution.py:346
  60.5 2.7 %collective-permute-start.15 = (bf16[208,128]{1,0:T(8,128)(2,1)}, bf16[208,128]{1,0:T(8,128)(2,1)S(1)}, u32[]{:S(2)}, u32[]{:S(2)}) collective-permute-start(bf16[208,128]{1,0:T(8,128)(2,1)} %get-tuple-element.17.own), channel_id=1, source_target_pairs={{0,192},{64,0},{128,64},{192,128},{1,193},{65,1},{129,65},{193,129... | collective-permute-start | bytes 159752 | tf_op jit(solution)/shard_map/ppermute | solution.py:346
  63.2 0.6 pad_add_fusion.place
  63.7 0.6 convert.3.query_ref
  64.3 0.6 convert.4.key_ref
  64.9 0.6 convert.5.value_ref
  65.5 0.6 reshape.21.beta_ref
  66.1 0.6 reshape.22.decay_ref
  66.8 0.6 copy-done.13
  67.4 2.6 %spread_states.1 = bf16[8,80,128]{2,1,0:T(8,128)(2,1)} custom-call(s32[2]{0:T(128)} %pad_add_fusion.place, f32[4]{0:T(128)} %reshape.21.beta_ref, f32[4]{0:T(128)} %reshape.22.decay_ref, bf16[208,128]{1,0:T(8,128)(2,1)} %get-tuple-element.17.own, bf16[208,128]{1,0:T(8,128)(2,1)} %copy-done.13, bf16[208,128]{1,0:T(8,128)(2,1)} %copy-done.14, ...), custom_call_target="tpu_custom_call" | custom-call | tf_op jit(solution)/shard_map/spread_states/pallas_call | solution.py:429
  70.0 3.4 %all-to-all-start.1 = ((bf16[8,80,128]{2,1,0:T(8,128)(2,1)}), bf16[8,80,128]{2,1,0:T(8,128)(2,1)S(1)}, u32[]{:S(2)}, u32[]{:S(2)}) async-start(bf16[8,80,128]{2,1,0:T(8,128)(2,1)} %spread_states.1), calls=%async_computation.1 | async-start | bytes 327680 | tf_op jit(solution)/shard_map/all_to_all | solution.py:444
  73.4 6.8 %window_terms.1 = (f32[4,192,128]{2,1,0:T(8,128)}, bf16[4,192,128]{2,1,0:T(8,128)(2,1)}, f32[4,192,128]{2,1,0:T(8,128)}) custom-call(s32[8]{0:T(128)} %stack.47.shard_of, bf16[2,192,512]{2,1,0:T(8,128)(2,1)} %refs_0_.3, bf16[2,192,512]{2,1,0:T(8,128)(2,1)} %copy-done.1, bf16[192,512]{1,0:T(8,128)(2,1)} %copy-done.2, bf16[192,512]{1,0:T(8,128)(2,1)} %copy-done.4, ...), custom_call_target="tpu_custom_call" | custom-call | tf_op jit(solution)/shard_map/window_terms/pallas_call | solution.py:400
  80.2 0.7 copy-done.12
  80.9 2.2 %finish.1 = (bf16[2,192,256]{2,1,0:T(8,128)(2,1)}, bf16[2,2,4,128]{3,2,1,0:T(4,128)(2,1)}, f32[2,256]{1,0:T(2,128)}) custom-call(bf16[8,80,128]{2,1,0:T(8,128)(2,1)} %copy-done.12, f32[4,192,128]{2,1,0:T(8,128)} %get-tuple-element.26.out_ref, bf16[4,192,128]{2,1,0:T(8,128)(2,1)} %get-tuple-element.27.reach_ref, f32[4,192,128]{2,1,0:T(8,128)} %get-tuple-element.28.silu_ref, ...), custom_call_target="tpu_custom_call" | custom-call | tf_op jit(solution)/shard_map/finish/pallas_call | solution.py:445
  (67 shorter events, 2.9 us)
Async XLA Ops:
  0.6 22.9 %copy-start.20 = (f32[2]{0:T(128)S(1)}, f32[2]{0:T(128)}, u32[]{:S(2)}) copy-start(f32[2]{0:T(128)} %param.22) | copy-start | bytes 28
  0.6 22.9 %copy-start.19 = (f32[2]{0:T(128)S(1)}, f32[2]{0:T(128)}, u32[]{:S(2)}) copy-start(f32[2]{0:T(128)} %param.23) | copy-start | bytes 28
  1.7 7.8 %collective-permute-start.1 = (bf16[192,512]{1,0:T(8,128)(2,1)S(1)}, bf16[192,512]{1,0:T(8,128)(2,1)S(1)}, u32[]{:S(2)}, u32[]{:S(2)}) collective-permute-start(bf16[192,512]{1,0:T(8,128)(2,1)S(1)} %get-tuple-element.30), channel_id=1, source_target_pairs={{0,2},{2,4},{4,6},{6,0},{1,3},{3,5},{5,7},{7,1},{8,10},{10,12},{12... | collective-permute-start | bytes 589832 | tf_op jit(solution)/shard_map/ppermute | solution.py:346
  3.7 9.0 %collective-permute-start.4 = (bf16[192,512]{1,0:T(8,128)(2,1)S(1)}, bf16[192,512]{1,0:T(8,128)(2,1)S(1)}, u32[]{:S(2)}, u32[]{:S(2)}) collective-permute-start(bf16[192,512]{1,0:T(8,128)(2,1)S(1)} %get-tuple-element.29), channel_id=1, source_target_pairs={{0,6},{2,0},{4,2},{6,4},{1,7},{3,1},{5,3},{7,5},{8,14},{10,8},{12,... | collective-permute-start | bytes 589832 | tf_op jit(solution)/shard_map/ppermute | solution.py:346
  3.8 10.0 %collective-permute-start.2 = (bf16[192,512]{1,0:T(8,128)(2,1)S(1)}, bf16[192,512]{1,0:T(8,128)(2,1)S(1)}, u32[]{:S(2)}, u32[]{:S(2)}) collective-permute-start(bf16[192,512]{1,0:T(8,128)(2,1)S(1)} %get-tuple-element.29), channel_id=1, source_target_pairs={{0,2},{2,4},{4,6},{6,0},{1,3},{3,5},{5,7},{7,1},{8,10},{10,12},{12... | collective-permute-start | bytes 589832 | tf_op jit(solution)/shard_map/ppermute | solution.py:346
  7.0 9.7 %collective-permute-start.3 = (bf16[192,512]{1,0:T(8,128)(2,1)S(1)}, bf16[192,512]{1,0:T(8,128)(2,1)S(1)}, u32[]{:S(2)}, u32[]{:S(2)}) collective-permute-start(bf16[192,512]{1,0:T(8,128)(2,1)S(1)} %get-tuple-element.30), channel_id=1, source_target_pairs={{0,6},{2,0},{4,2},{6,4},{1,7},{3,1},{5,3},{7,5},{8,14},{10,8},{12,... | collective-permute-start | bytes 589832 | tf_op jit(solution)/shard_map/ppermute | solution.py:346
  9.6 14.7 %copy-start.2 = (bf16[192,512]{1,0:T(8,128)(2,1)}, bf16[192,512]{1,0:T(8,128)(2,1)S(1)}, u32[]{:S(2)}) copy-start(bf16[192,512]{1,0:T(8,128)(2,1)S(1)} %collective-permute-done.1.refs_2_) | copy-start | bytes 589828
  9.6 7.3 %collective-permute-start.5 = (bf16[192,512]{1,0:T(8,128)(2,1)S(1)}, bf16[192,512]{1,0:T(8,128)(2,1)S(1)}, u32[]{:S(2)}, u32[]{:S(2)}) collective-permute-start(bf16[192,512]{1,0:T(8,128)(2,1)S(1)} %collective-permute-done.1.refs_2_), channel_id=1, source_target_pairs={{0,2},{2,4},{4,6},{6,0},{1,3},{3,5},{5,7},{7,1},{8,10},{10,12},{12... | collective-permute-start | bytes 589832 | tf_op jit(solution)/shard_map/ppermute | solution.py:346
  12.7 11.5 %copy-start.3 = (bf16[192,512]{1,0:T(8,128)(2,1)}, bf16[192,512]{1,0:T(8,128)(2,1)S(1)}, u32[]{:S(2)}) copy-start(bf16[192,512]{1,0:T(8,128)(2,1)S(1)} %collective-permute-done.4.refs_5_) | copy-start | bytes 589828
  12.7 6.9 %collective-permute-start.6 = (bf16[192,512]{1,0:T(8,128)(2,1)S(1)}, bf16[192,512]{1,0:T(8,128)(2,1)S(1)}, u32[]{:S(2)}, u32[]{:S(2)}) collective-permute-start(bf16[192,512]{1,0:T(8,128)(2,1)S(1)} %collective-permute-done.4.refs_5_), channel_id=1, source_target_pairs={{0,6},{2,0},{4,2},{6,4},{1,7},{3,1},{5,3},{7,5},{8,14},{10,8},{12,... | collective-permute-start | bytes 589832 | tf_op jit(solution)/shard_map/ppermute | solution.py:346
  12.7 6.9 %collective-permute-start.10 = (bf16[192,512]{1,0:T(8,128)(2,1)S(1)}, bf16[192,512]{1,0:T(8,128)(2,1)S(1)}, u32[]{:S(2)}, u32[]{:S(2)}) collective-permute-start(bf16[192,512]{1,0:T(8,128)(2,1)S(1)} %collective-permute-done.4.refs_5_), channel_id=1, source_target_pairs={{0,1},{1,0},{2,3},{3,2},{4,5},{5,4},{6,7},{7,6},{8,9},{9,8},{10,11... | collective-permute-start | bytes 589832 | tf_op jit(solution)/shard_map/ppermute | solution.py:346
  13.8 10.5 %copy-start.4 = (bf16[192,512]{1,0:T(8,128)(2,1)}, bf16[192,512]{1,0:T(8,128)(2,1)S(1)}, u32[]{:S(2)}) copy-start(bf16[192,512]{1,0:T(8,128)(2,1)S(1)} %collective-permute-done.2.refs_3_) | copy-start | bytes 589828
  13.8 6.3 %collective-permute-start.7 = (bf16[192,512]{1,0:T(8,128)(2,1)S(1)}, bf16[192,512]{1,0:T(8,128)(2,1)S(1)}, u32[]{:S(2)}, u32[]{:S(2)}) collective-permute-start(bf16[192,512]{1,0:T(8,128)(2,1)S(1)} %collective-permute-done.1.refs_2_), channel_id=1, source_target_pairs={{0,1},{1,0},{2,3},{3,2},{4,5},{5,4},{6,7},{7,6},{8,9},{9,8},{10,11... | collective-permute-start | bytes 589832 | tf_op jit(solution)/shard_map/ppermute | solution.py:346
  16.6 7.6 %copy-start.5 = (bf16[192,512]{1,0:T(8,128)(2,1)}, bf16[192,512]{1,0:T(8,128)(2,1)S(1)}, u32[]{:S(2)}) copy-start(bf16[192,512]{1,0:T(8,128)(2,1)S(1)} %collective-permute-done.3.refs_4_) | copy-start | bytes 589828
  16.6 7.6 %collective-permute-start = (bf16[2,192,512]{2,1,0:T(8,128)(2,1)}, bf16[2,192,512]{2,1,0:T(8,128)(2,1)S(1)}, u32[]{:S(2)}, u32[]{:S(2)}) collective-permute-start(bf16[2,192,512]{2,1,0:T(8,128)(2,1)} %refs_0_.3), channel_id=1, source_target_pairs={{0,1},{1,0},{2,3},{3,2},{4,5},{5,4},{6,7},{7,6},{8,9},{9,8},{10,11... | collective-permute-start | bytes 1179656 | tf_op jit(solution)/shard_map/ppermute | solution.py:346
  16.9 7.4 %copy-start.6 = (bf16[192,512]{1,0:T(8,128)(2,1)}, bf16[192,512]{1,0:T(8,128)(2,1)S(1)}, u32[]{:S(2)}) copy-start(bf16[192,512]{1,0:T(8,128)(2,1)S(1)} %collective-permute-done.5.refs_6_) | copy-start | bytes 589828
  16.9 7.3 %collective-permute-start.8 = (bf16[192,512]{1,0:T(8,128)(2,1)S(1)}, bf16[192,512]{1,0:T(8,128)(2,1)S(1)}, u32[]{:S(2)}, u32[]{:S(2)}) collective-permute-start(bf16[192,512]{1,0:T(8,128)(2,1)S(1)} %collective-permute-done.2.refs_3_), channel_id=1, source_target_pairs={{0,1},{1,0},{2,3},{3,2},{4,5},{5,4},{6,7},{7,6},{8,9},{9,8},{10,11... | collective-permute-start | bytes 589832 | tf_op jit(solution)/shard_map/ppermute | solution.py:346
  19.6 4.7 %copy-start.7 = (bf16[192,512]{1,0:T(8,128)(2,1)}, bf16[192,512]{1,0:T(8,128)(2,1)S(1)}, u32[]{:S(2)}) copy-start(bf16[192,512]{1,0:T(8,128)(2,1)S(1)} %collective-permute-done.6.refs_7_) | copy-start | bytes 589828
  19.6 4.6 %collective-permute-start.9 = (bf16[192,512]{1,0:T(8,128)(2,1)S(1)}, bf16[192,512]{1,0:T(8,128)(2,1)S(1)}, u32[]{:S(2)}, u32[]{:S(2)}) collective-permute-start(bf16[192,512]{1,0:T(8,128)(2,1)S(1)} %collective-permute-done.3.refs_4_), channel_id=1, source_target_pairs={{0,1},{1,0},{2,3},{3,2},{4,5},{5,4},{6,7},{7,6},{8,9},{9,8},{10,11... | collective-permute-start | bytes 589832 | tf_op jit(solution)/shard_map/ppermute | solution.py:346
  19.6 4.7 %copy-start.8 = (bf16[192,512]{1,0:T(8,128)(2,1)}, bf16[192,512]{1,0:T(8,128)(2,1)S(1)}, u32[]{:S(2)}) copy-start(bf16[192,512]{1,0:T(8,128)(2,1)S(1)} %collective-permute-done.10.refs_11_) | copy-start | bytes 589828
  19.6 4.6 %collective-permute-start.11 = (bf16[192,512]{1,0:T(8,128)(2,1)S(1)}, bf16[192,512]{1,0:T(8,128)(2,1)}, u32[]{:S(2)}, u32[]{:S(2)}) collective-permute-start(bf16[192,512]{1,0:T(8,128)(2,1)S(1)} %collective-permute-done.5.refs_6_), channel_id=1, source_target_pairs={{0,1},{1,0},{2,3},{3,2},{4,5},{5,4},{6,7},{7,6},{8,9},{9,8},{10,11... | collective-permute-start | bytes 589832 | tf_op jit(solution)/shard_map/ppermute | solution.py:346
  20.1 4.1 %collective-permute-start.12 = (bf16[192,512]{1,0:T(8,128)(2,1)S(1)}, bf16[192,512]{1,0:T(8,128)(2,1)}, u32[]{:S(2)}, u32[]{:S(2)}) collective-permute-start(bf16[192,512]{1,0:T(8,128)(2,1)S(1)} %collective-permute-done.6.refs_7_), channel_id=1, source_target_pairs={{0,1},{1,0},{2,3},{3,2},{4,5},{5,4},{6,7},{7,6},{8,9},{9,8},{10,11... | collective-permute-start | bytes 589832 | tf_op jit(solution)/shard_map/ppermute | solution.py:346
  25.1 38.6 %copy-start.16 = (bf16[2,2,128]{2,1,0:T(2,128)(2,1)S(1)}, bf16[2,2,128]{2,1,0:T(2,128)(2,1)}, u32[]{:S(2)}) copy-start(bf16[2,2,128]{2,1,0:T(2,128)(2,1)} %param.25) | copy-start | bytes 3076
  25.1 39.2 %copy-start.17 = (bf16[2,2,128]{2,1,0:T(2,128)(2,1)S(1)}, bf16[2,2,128]{2,1,0:T(2,128)(2,1)}, u32[]{:S(2)}) copy-start(bf16[2,2,128]{2,1,0:T(2,128)(2,1)} %param.26) | copy-start | bytes 3076
  25.1 39.8 %copy-start.18 = (bf16[2,2,128]{2,1,0:T(2,128)(2,1)S(1)}, bf16[2,2,128]{2,1,0:T(2,128)(2,1)}, u32[]{:S(2)}) copy-start(bf16[2,2,128]{2,1,0:T(2,128)(2,1)} %param.27) | copy-start | bytes 3076
  25.1 40.4 %copy-start.21 = (f32[2,2]{1,0:T(2,128)S(1)}, f32[2,2]{1,0:T(2,128)}, u32[]{:S(2)}) copy-start(f32[2,2]{1,0:T(2,128)} %param.28) | copy-start | bytes 52
  25.1 41.1 %copy-start.22 = (f32[2,2]{1,0:T(2,128)S(1)}, f32[2,2]{1,0:T(2,128)}, u32[]{:S(2)}) copy-start(f32[2,2]{1,0:T(2,128)} %param.29) | copy-start | bytes 52
  36.6 13.1 %all-to-all-start = ((bf16[8,208,128]{2,1,0:T(8,128)(2,1)}), bf16[8,208,128]{2,1,0:T(8,128)(2,1)S(1)}, u32[]{:S(2)}, u32[]{:S(2)}) async-start(bf16[8,208,128]{2,1,0:T(8,128)(2,1)} %get-tuple-element.16), calls=%async_computation | async-start | bytes 851968 | tf_op jit(solution)/shard_map/all_to_all | solution.py:398
  52.7 14.0 %collective-permute-start.13 = (bf16[208,128]{1,0:T(8,128)(2,1)}, bf16[208,128]{1,0:T(8,128)(2,1)S(1)}, u32[]{:S(2)}, u32[]{:S(2)}) collective-permute-start(bf16[208,128]{1,0:T(8,128)(2,1)} %get-tuple-element.17.own), channel_id=1, source_target_pairs={{0,64},{64,128},{128,192},{192,0},{1,65},{65,129},{129,193},{193,1... | collective-permute-start | bytes 159752 | tf_op jit(solution)/shard_map/ppermute | solution.py:346
  56.0 10.7 %collective-permute-start.14 = (bf16[208,128]{1,0:T(8,128)(2,1)}, bf16[208,128]{1,0:T(8,128)(2,1)S(1)}, u32[]{:S(2)}, u32[]{:S(2)}) collective-permute-start(bf16[208,128]{1,0:T(8,128)(2,1)} %get-tuple-element.17.own), channel_id=1, source_target_pairs={{0,128},{64,192},{128,0},{192,64},{1,129},{65,193},{129,1},{193,65... | collective-permute-start | bytes 159752 | tf_op jit(solution)/shard_map/ppermute | solution.py:346
  60.5 6.3 %collective-permute-start.15 = (bf16[208,128]{1,0:T(8,128)(2,1)}, bf16[208,128]{1,0:T(8,128)(2,1)S(1)}, u32[]{:S(2)}, u32[]{:S(2)}) collective-permute-start(bf16[208,128]{1,0:T(8,128)(2,1)} %get-tuple-element.17.own), channel_id=1, source_target_pairs={{0,192},{64,0},{128,64},{192,128},{1,193},{65,1},{129,65},{193,129... | collective-permute-start | bytes 159752 | tf_op jit(solution)/shard_map/ppermute | solution.py:346
  70.0 10.2 %all-to-all-start.1 = ((bf16[8,80,128]{2,1,0:T(8,128)(2,1)}), bf16[8,80,128]{2,1,0:T(8,128)(2,1)S(1)}, u32[]{:S(2)}, u32[]{:S(2)}) async-start(bf16[8,80,128]{2,1,0:T(8,128)(2,1)} %spread_states.1), calls=%async_computation.1 | async-start | bytes 327680 | tf_op jit(solution)/shard_map/all_to_all | solution.py:444
  (9 other events, 9.8 us)

commit v2 on v1

--- a/solution.py
+++ b/solution.py
@@ -1,5 +1,3 @@
-import functools
-
 import jax
 import jax.numpy as jnp
 from jax import lax
@@ -11,6 +9,7 @@
 NEAR = ("zl", "x")
 AXES = ("zh", "zl", "x")
 PACK = 16
+LANES = 128
 unit_floor = 1.0
 norm_floor = 0.001
 bf16 = jnp.bfloat16
@@ -51,69 +50,83 @@
     return lax.rsqrt((total / values.shape[-1] if mean else total) + floor)
 
 
-def token_copies(pieces, buffer, sems):
-    own, own_c, *rest = pieces
-    copies = [
-        [pltpu.make_async_copy(ref.at[seq], buffer.at[slot, seq], sems.at[slot]) for seq in range(2)]
-        for slot, ref in enumerate((own, own_c))
-    ]
-    for pair in range(6):
-        first, second = rest[2 * pair : 2 * pair + 2]
-        slot = 2 + pair
-        copies.append(
-            [
-                pltpu.make_async_copy(first, buffer.at[slot, 0], sems.at[slot]),
-                pltpu.make_async_copy(second, buffer.at[slot, 1], sems.at[slot]),
-            ]
-        )
-    return copies
-
-
-def project_pieces(shard_of, pieces, weights, token_buffer, weight_buffers, sems, each):
-    depth = token_buffer.shape[-1]
-    copies = token_copies(pieces, token_buffer, sems)
-    for slot in range(8):
-        start = pl.multiple_of(shard_of[slot] * depth, depth)
-        for weight, buffer in zip(weights, weight_buffers):
-            copies[slot].append(
-                pltpu.make_async_copy(
-                    weight.at[pl.ds(start, depth), :], buffer.at[slot], sems.at[slot]
-                )
-            )
-        for copy in copies[slot]:
-            copy.start()
+def shard_index(ahead, swapped):
+    core = lax.axis_index("c")
+    core = 1 - core if swapped else core
+    return lax.rem(lax.axis_index("y") + ahead, 4) * 2 + core
+
+
+def project_pieces(pieces, slots, weights):
     totals = [None] * len(weights)
-    for slot in range(8):
-        for copy in copies[slot]:
-            copy.wait()
-        rows = token_buffer[slot].reshape(-1, depth)
-        for at, buffer in enumerate(weight_buffers):
-            part = dot(rows, buffer[slot])
+    for piece, slot in zip(pieces, slots):
+        rows = piece() if callable(piece) else piece[...]
+        depth = rows.shape[-1]
+        rows = rows.reshape(-1, depth)
+        start = pl.multiple_of(shard_index(*slot) * depth, depth)
+        for at, weight in enumerate(weights):
+            part = weight(rows, start) if callable(weight) else dot(rows, weight[pl.ds(start, depth), :])
             totals[at] = part if totals[at] is None else totals[at] + part
     return totals
 
 
-def local_kernel(shard_of, *refs):
-    pieces, refs = refs[:14], refs[14:]
-    key_w, value_w, gate_w, bias_ref, rate_ref = refs[:5]
-    send_ref, key_ref, fresh_ref, carry_ref, cols_ref, rows_ref = refs[5:11]
-    token_buffer, key_buffer, value_buffer, gate_buffer, sems = refs[11:]
-    span = token_buffer.shape[2]
+def joined(first, second):
+    return lambda: jnp.concatenate([first[...], second[...]], axis=0)
+
+
+def scalar_gates(beta_w, decay_w):
+    def project(rows, start):
+        depth = rows.shape[-1]
+        beta = beta_w[:, pl.ds(start, depth)].astype(f32)
+        decay = decay_w[:, pl.ds(start, depth)].astype(f32)
+        stacked = row_pack((beta[0:1], beta[1:2], decay[0:1], decay[1:2]), depth)
+        stacked = jnp.concatenate([stacked, jnp.zeros((LANES - PACK, depth), f32)], axis=0)
+        return dot(rows, stacked, ROWS)
+
+    return project
+
+
+NEAR_SLOTS = ((0, False), (0, True))
+NEXT_SLOTS = ((3, False), (1, False))
+LATE_SLOTS = ((3, True), (1, True), (2, False), (2, True))
+
+
+def early_kernel(own, own_c, key_w, value_w, beta_w, decay_w, key_out, value_out, gate_out):
+    weights = (key_w, value_w, scalar_gates(beta_w, decay_w))
+    totals = project_pieces((own, own_c), NEAR_SLOTS, weights)
+    for ref, total in zip((key_out, value_out, gate_out), totals):
+        ref[...] = total
+
+
+def next_kernel(
+    up0, up1, down0, down1, key_w, value_w, beta_w, decay_w, key_in, value_in, gate_in,
+    key_out, value_out, gate_out,
+):
+    weights = (key_w, value_w, scalar_gates(beta_w, decay_w))
+    totals = project_pieces((joined(up0, up1), joined(down0, down1)), NEXT_SLOTS, weights)
+    before = (key_in, value_in, gate_in)
+    for ref, total, old in zip((key_out, value_out, gate_out), totals, before):
+        ref[...] = old[...] + total
+
+
+def lane_pair(ref, first):
+    lanes = iota((1, LANES), 1)
+    return jnp.where(lanes == first, ref[0], jnp.where(lanes == first + 1, ref[1], 0.0))
+
+
+def local_kernel(bias_ref, rate_ref, *refs):
+    pieces, refs = refs[:8], refs[8:]
+    key_w, value_w, beta_w, decay_w, key_in, value_in, gate_in = refs[:7]
+    send_ref, key_ref, fresh_ref, carry_ref, cols_ref, rows_ref = refs[7:]
+    span = pieces[0].shape[0]
     head = send_ref.shape[-1]
-    key_total, value_total, gates = project_pieces(
-        shard_of,
-        pieces,
-        (key_w, value_w, gate_w),
-        token_buffer,
-        (key_buffer, value_buffer, gate_buffer),
-        sems,
-        None,
-    )
-    key_rows = key_total.astype(bf16)
-    value_rows = value_total.astype(bf16)
+    late = [joined(*pieces[at : at + 2]) for at in range(0, 8, 2)]
+    totals = project_pieces(late, LATE_SLOTS, (key_w, value_w, scalar_gates(beta_w, decay_w)))
+    key_rows = (key_in[...] + totals[0]).astype(bf16)
+    value_rows = (value_in[...] + totals[1]).astype(bf16)
+    gates = gate_in[...] + totals[2]
     key_ref[...] = key_rows
-    strength = jax.nn.sigmoid(gates + bias_ref[...])
-    decays = -jnp.exp(rate_ref[...]) * jax.nn.softplus(gates)
+    strength = jax.nn.sigmoid(gates + lane_pair(bias_ref, 0))
+    decays = -jnp.exp(lane_pair(rate_ref, 2)) * jax.nn.softplus(gates)
     wide = cols_ref.shape[1]
     pairs = []
     lanes = iota((wide, head), 1)
@@ -183,16 +196,17 @@
             send_ref[to, head + half :, :] = factor.astype(bf16)
 
 
-def window_kernel(shard_of, *refs):
-    pieces, refs = refs[:14], refs[14:]
+def window_kernel(*refs):
+    own, own_c, up0, up1, down0, down1 = refs[:6]
+    late, refs = refs[6:14], refs[14:]
     query_w, gate_w, gain_ref, key_ref, fresh_ref, carry_ref, cols_ref, rows_ref = refs[:8]
-    out_ref, reach_ref, silu_ref = refs[8:11]
-    token_buffer, query_buffer, gate_buffer, sems = refs[11:]
-    span = token_buffer.shape[2]
+    out_ref, reach_ref, silu_ref = refs[8:]
+    span = up0.shape[0]
     head = fresh_ref.shape[-1]
-    query_total, gate_total = project_pieces(
-        shard_of, pieces, (query_w, gate_w), token_buffer, (query_buffer, gate_buffer), sems, None
-    )
+    pieces = [own, own_c, joined(up0, up1), joined(down0, down1)]
+    pieces += [joined(*late[at : at + 2]) for at in range(0, 8, 2)]
+    slots = NEAR_SLOTS + NEXT_SLOTS + LATE_SLOTS
+    query_total, gate_total = project_pieces(pieces, slots, (query_w, gate_w))
     query_rows = query_total.astype(bf16)
     gate_rows = gate_total.astype(bf16).astype(f32)
     t = iota((span, span), 0)
@@ -257,14 +271,24 @@
 
 
 def spread_kernel(
-    place, beta_ref, decay_ref, own, back1, back2, back3, maps_ref, adds_ref, factors_ref,
+    beta_ref, decay_ref, own, back1, back2, back3, maps_ref, adds_ref, factors_ref,
     query_ref, key_ref, value_ref, send_ref, groups_ref, wide_ref, turned_ref,
 ):
     rows, head = own.shape
     half = head // 2
-    far, near = place[0], place[1]
+    far = lax.axis_index("zh")
+    near = lax.axis_index("zl") * 4 + lax.axis_index("x")
     pair = near // 2
     side = near % 2
+    seq, h = pair // 2, pair % 2
+
+    def chosen(ref):
+        total = jnp.zeros((1, head), f32)
+        for at in range(4):
+            row = ref[at // 2, at % 2 : at % 2 + 1, :].astype(f32)
+            total = jnp.where(pair == at, row, total)
+        return total
+
     for slot, ref in enumerate((own, back1, back2, back3)):
         groups_ref[slot] = ref[...]
     state = jnp.zeros((half, head), f32)
@@ -283,16 +307,16 @@
     padded = wide_ref[...]
     turned_ref[...] = padded.T
     mine = turned_ref[pl.ds(pl.multiple_of(far * 32, 32), 32), :]
-    query = query_ref[pl.ds(pair, 1), :]
-    key = key_ref[pl.ds(pair, 1), :]
+    query = chosen(query_ref)
+    key = chosen(key_ref)
     query = query * rms_scale(query, unit_floor, False)
     key = key * rms_scale(key, unit_floor, False)
     hits = dot(row_pack(thirds(query) + thirds(key), head), padded, ROWS)
     recall = hits[0:1] + hits[1:2] + hits[2:3]
     retrieve = hits[3:4] + hits[4:5] + hits[5:6]
     intersect = jnp.sum(key * query, axis=-1, keepdims=True)
-    fresh = value_ref[pl.ds(pair, 1), :] - decay_ref[pair] * retrieve
-    read = decay_ref[pair] * recall + (beta_ref[pair] * intersect) * fresh
+    fresh = chosen(value_ref) - decay_ref[seq, h] * retrieve
+    read = decay_ref[seq, h] * recall + (beta_ref[seq, h] * intersect) * fresh
     read = jnp.where(iota((1, head), 1) // half == side, read, 0.0)
     zero = jnp.zeros((1, head), f32)
     extra = row_pack((zero, zero, zero, zero) + thirds(read), head)
@@ -333,12 +357,21 @@
     return pl.BlockSpec(memory_space=pltpu.SMEM)
 
 
-def anywhere():
-    return pl.BlockSpec(memory_space=pl.ANY)
-
-
-def shape(dims, dtype):
-    return jax.ShapeDtypeStruct(dims, dtype)
+def kernel(body, name, outputs, smem_count, args, scratch=(), limit=16):
+    placed = [
+        arg if at < smem_count else pltpu.with_memory_space_constraint(arg, pltpu.VMEM)
+        for at, arg in enumerate(args)
+    ]
+    specs = [smem() if at < smem_count else vmem() for at in range(len(args))]
+    return pl.pallas_call(
+        body,
+        name=name,
+        out_shape=tuple(outputs),
+        in_specs=specs,
+        out_specs=tuple(vmem() for _ in outputs),
+        scratch_shapes=list(scratch),
+        compiler_params=pltpu.CompilerParams(vmem_limit_bytes=limit * 1024 * 1024),
+    )(*placed)
 
 
 def shift(value, axis, by):
@@ -355,104 +388,87 @@
     half = head // 2
     wide = 256
     width = query_weight.shape[1]
-    y, core = lax.axis_index("y"), lax.axis_index("c")
+    rows = head + half + PACK
     first, second = tokens[0], tokens[1]
+    swap = lambda value: shift(value, "c", 1)
+    tokens_c = swap(tokens)
     up0 = shift(first, "y", 1)
     down1 = shift(second, "y", -1)
     up1 = shift(second, "y", 1)
     down0 = shift(first, "y", -1)
     far0 = shift(up0, "y", 1)
     far1 = shift(down1, "y", -1)
-    swap = lambda value: shift(value, "c", 1)
-    pieces = [tokens, swap(tokens), up0, up1, down0, down1, far0, far1]
-    pieces += [swap(value) for value in (up0, up1, down0, down1, far0, far1)]
-    ahead = [y, y, y + 3, y + 1, y + 2, y + 3, y + 1, y + 2]
-    cores = [core, 1 - core, core, core, core, 1 - core, 1 - core, 1 - core]
-    shard_of = jnp.stack([(a % 4) * 2 + c for a, c in zip(ahead, cores)]).astype(jnp.int32)
-    scalars = jnp.concatenate([beta_weight, decay_weight], axis=1)
-    scalars = jnp.pad(scalars, ((0, 0), (0, head - scalars.shape[1])))
-    bias = jnp.pad(beta_bias, (0, head - 2))[None]
-    rate = jnp.pad(rate_log, (2, head - 4))[None]
+    swapped = [swap(value) for value in (up0, up1, down0, down1)]
+    late = [*swapped, far0, far1, swap(far0), swap(far1)]
+    gates = (beta_weight.T, decay_weight.T)
     gain = out_gain[None]
-
-    buffers = lambda widths: [pltpu.VMEM((8, 2, span, depth), bf16)] + [
-        pltpu.VMEM((8, depth, w), bf16) for w in widths
-    ] + [pltpu.SemaphoreType.DMA((8,))]
-    rows = head + half + PACK
-    send, key_rows, fresh, carry, cols, turned = pl.pallas_call(
+    on = pltpu.VMEM
+    sums = [on((2 * span, width), f32), on((2 * span, width), f32), on((2 * span, head), f32)]
+    weights = (key_weight, value_weight, *gates)
+    early = kernel(early_kernel, "early", sums, 0, (tokens, tokens_c, *weights))
+    middle = kernel(next_kernel, "middle", sums, 0, (up0, up1, down0, down1, *weights, *early))
+    send, key_rows, fresh, carry, cols, turned = kernel(
         local_kernel,
-        name="local_terms",
-        out_shape=(
-            shape((8, rows, head), bf16),
-            shape((2 * span, width), bf16),
-            shape((4, span, head), bf16),
-            shape((4, span, head), bf16),
-            shape((2, wide, head), f32),
-            shape((2, head, wide), f32),
+        "local_terms",
+        (
+            on((8, rows, head), bf16),
+            on((2 * span, width), bf16),
+            on((4, span, head), bf16),
+            on((4, span, head), bf16),
+            on((2, wide, head), f32),
+            on((2, head, wide), f32),
         ),
-        in_specs=[smem()] + [anywhere()] * 17 + [vmem()] * 2,
-        out_specs=tuple(vmem() for _ in range(6)),
-        scratch_shapes=buffers((width, width, head)),
-    )(shard_of, *pieces, key_weight, value_weight, scalars, bias, rate)
-
+        2,
+        (beta_bias, rate_log, *late, *weights, *middle),
+    )
     arrived = lax.all_to_all(send, NEAR, 0, 0, tiled=True)
-
-    local_out, reach, silu = pl.pallas_call(
+    local_out, reach, silu = kernel(
         window_kernel,
-        name="window_terms",
-        out_shape=(
-            shape((4, span, head), f32),
-            shape((4, span, head), bf16),
-            shape((4, span, head), f32),
+        "window_terms",
+        (on((4, span, head), f32), on((4, span, head), bf16), on((4, span, head), f32)),
+        0,
+        (
+            tokens, tokens_c, up0, up1, down0, down1, *late,
+            query_weight, gate_weight, gain, key_rows, fresh, carry, cols, turned,
         ),
-        in_specs=[smem()] + [anywhere()] * 16 + [vmem()] * 6,
-        out_specs=tuple(vmem() for _ in range(3)),
-        scratch_shapes=buffers((width, width)),
-    )(shard_of, *pieces, query_weight, gate_weight, gain, key_rows, fresh, carry, cols, turned)
-
-    total, maps, adds, factors = pl.pallas_call(
+    )
+    arrived, local_out = lax.optimization_barrier((arrived, local_out))
+    total, maps, adds, factors = kernel(
         compose_kernel,
-        name="compose_near",
-        out_shape=(
-            shape((rows, head), bf16),
-            shape((7, head, head), bf16),
-            shape((7, half, head), f32),
-            shape((7, 8, head), f32),
+        "compose_near",
+        (
+            on((rows, head), bf16),
+            on((7, head, head), bf16),
+            on((7, half, head), f32),
+            on((7, 8, head), f32),
         ),
-        in_specs=[vmem()],
-        out_specs=tuple(vmem() for _ in range(4)),
-    )(arrived)
-
+        0,
+        (arrived,),
+    )
     others = [shift(total, "zh", by) for by in (1, 2, 3)]
-    place = jnp.stack([lax.axis_index("zh"), lax.axis_index(NEAR)]).astype(jnp.int32)
-    flat = lambda value: value.reshape(4, -1).astype(f32)
-    back = pl.pallas_call(
+    (back,) = kernel(
         spread_kernel,
-        name="spread_states",
-        out_shape=shape((8, half + PACK, head), bf16),
-        in_specs=[smem()] * 3 + [vmem()] * 10,
-        out_specs=vmem(),
-        scratch_shapes=[
-            pltpu.VMEM((4, rows, head), bf16),
-            pltpu.VMEM((head, head), f32),
-            pltpu.VMEM((head, head), f32),
-        ],
-    )(
-        place, new_beta.reshape(4), new_decay.reshape(4), total, *others, maps, adds, factors,
-        flat(new_query), flat(new_key), flat(new_value),
+        "spread_states",
+        (on((8, half + PACK, head), bf16),),
+        2,
+        (
+            new_beta, new_decay, total, *others, maps, adds, factors,
+            new_query, new_key, new_value,
+        ),
+        (on((4, rows, head), bf16), on((head, head), f32), on((head, head), f32)),
     )
     returned = lax.all_to_all(back, NEAR, 0, 0, tiled=True)
-    return pl.pallas_call(
+    return kernel(
         finish_kernel,
-        name="finish",
-        out_shape=(
-            shape((2, span, width), bf16),
-            shape((2, 2, 4, head), bf16),
-            shape((2, width), f32),
+        "finish",
+        (
+            jax.ShapeDtypeStruct((2, span, width), bf16),
+            jax.ShapeDtypeStruct((2, 2, 4, head), bf16),
+            jax.ShapeDtypeStruct((2, width), f32),
         ),
-        in_specs=[vmem()] * 5,
-        out_specs=tuple(vmem() for _ in range(3)),
-    )(returned, local_out, reach, silu, gain)
+        0,
+        (returned, local_out, reach, silu, gain),
+    )
 
 
 def solution(mesh):

time: 84.4 us -> 101 us (1.20)
  local copies, waits for them, and re-layouts: 8.09 us -> 33.9 us
  Pallas kernels: 25.4 us -> 14.1 us
  blocking collectives: 0 us -> 10.8 us
  starting transfers between devices: 27.6 us -> 23.3 us
  other arithmetic: 3.08 us -> 0 us
    unnamed x46 -> x114, local copies, waits for them, and re-layouts: 2.86 us -> 32.9 us
    pallas_call x5 -> x7, Pallas kernels: 25.4 us -> 14.1 us  [kernel(): pl.pallas_call(body, name=name, out_shape=tuple(outputs), in_specs=specs,...]
    all_to_all x0 -> x1, blocking collectives: none -> 10.8 us  [shards(): returned = lax.all_to_all(back, NEAR, 0, 0, tiled=True)]
    all_to_all x1, waiting for transfers between devices: 8.89 us -> 0.01 us  [shards(): arrived = lax.all_to_all(send, NEAR, 0, 0, tiled=True)]
    ppermute x16, waiting for transfers between devices: 9.11 us -> 17 us  [shift(): lax.ppermute(value, axis, [(at, (at + by) % length) for at in range(lengt...]
    all_to_all x1 -> x0, starting transfers between devices: 3.38 us -> none  [shards(): returned = lax.all_to_all(back, NEAR, 0, 0, tiled=True)]
    ppermute x16, starting transfers between devices: 20 us -> 17.7 us  [shift(): lax.ppermute(value, axis, [(at, (at + by) % length) for at in range(lengt...]
    convert_element_type x3 -> x0, other arithmetic: 1.76 us -> none  [shards(): flat = lambda value: value.reshape(4, -1).astype(f32)]
  transfers between devices with their start and end apart: 18 -> 17, of which waited for: 6 -> 7; matrix products, arithmetic and copies ran while one was open for 9% -> 0% of each run, Pallas kernels for 8% -> 4%
where the time goes in v2:
time: 101 us; the launch traced here: 100 us
  local copies, waits for them, and re-layouts  33.9 us (34%)
  starting transfers between devices  23.3 us (23%)
  waiting for transfers between devices  17 us (17%)
  Pallas kernels  14.1 us (14%)
  blocking collectives  10.8 us (11%)
  between operations  1.03 us (1%)
    unnamed x114, local copies, waits for them, and re-layouts  32.9 us
    ppermute x16, starting transfers between devices, shift(): lax.ppermute(value, axis, [(at, (at + by) % length) for at in range(lengt...  17.7 us
    ppermute x16, waiting for transfers between devices, shift(): lax.ppermute(value, axis, [(at, (at + by) % length) for at in range(lengt...  17 us
    pallas_call x7, Pallas kernels, kernel(): pl.pallas_call(body, name=name, out_shape=tuple(outputs), in_specs=specs,...  14.1 us
    all_to_all x1, blocking collectives, shards(): returned = lax.all_to_all(back, NEAR, 0, 0, tiled=True)  10.8 us
    all_to_all x1, starting transfers between devices, shards(): arrived = lax.all_to_all(send, NEAR, 0, 0, tiled=True)  5.65 us
  transfers between devices with their start and end apart: 17, of which 7 were waited for; matrix products, arithmetic and copies ran while one was open for 0% of the time, Pallas kernels for 4%

profile of v2, /device:TPU:24, one launch (start us, length us, event | category | flops | bytes accessed | tf_op | source)
XLA Modules:
  0.0 100.1 jit_solution(3625362113473488362)
XLA Ops:
  0.6 1.1 %slice_bitcast_fusion = (bf16[192,512]{1,0:T(8,128)(2,1)S(1)}, bf16[192,512]{1,0:T(8,128)(2,1)S(1)}) fusion(bf16[2,192,512]{2,1,0:T(8,128)(2,1)} %refs_0_.1), kind=kLoop, calls=%fused_computation | loop fusion | bytes 786432 | tf_op jit(solution)/shard_map/squeeze | solution.py:392
  1.7 2.0 %collective-permute-start = (bf16[192,512]{1,0:T(8,128)(2,1)S(1)}, bf16[192,512]{1,0:T(8,128)(2,1)S(1)}, u32[]{:S(2)}, u32[]{:S(2)}) collective-permute-start(bf16[192,512]{1,0:T(8,128)(2,1)S(1)} %get-tuple-element.46), channel_id=1, source_target_pairs={{0,2},{2,4},{4,6},{6,0},{1,3},{3,5},{5,7},{7,1},{8,10},{10,12},{12... | collective-permute-start | bytes 589832 | tf_op jit(solution)/shard_map/ppermute | solution.py:379
  3.8 1.9 %collective-permute-start.6 = (bf16[192,512]{1,0:T(8,128)(2,1)S(1)}, bf16[192,512]{1,0:T(8,128)(2,1)S(1)}, u32[]{:S(2)}, u32[]{:S(2)}) collective-permute-start(bf16[192,512]{1,0:T(8,128)(2,1)S(1)} %get-tuple-element.45), channel_id=1, source_target_pairs={{0,6},{2,0},{4,2},{6,4},{1,7},{3,1},{5,3},{7,5},{8,14},{10,8},{12,... | collective-permute-start | bytes 589832 | tf_op jit(solution)/shard_map/ppermute | solution.py:379
  5.8 3.7 %collective-permute-done.up0.refs_2_ = bf16[192,512]{1,0:T(8,128)(2,1)S(1)} collective-permute-done((bf16[192,512]{1,0:T(8,128)(2,1)S(1)}, bf16[192,512]{1,0:T(8,128)(2,1)S(1)}, u32[]{:S(2)}, u32[]{:S(2)}) %collective-permute-start) | collective-permute-done | bytes 196640 | tf_op jit(solution)/shard_map/ppermute | solution.py:379
  9.5 3.1 %collective-permute-done.2.up1.refs_3_ = bf16[192,512]{1,0:T(8,128)(2,1)S(1)} collective-permute-done((bf16[192,512]{1,0:T(8,128)(2,1)S(1)}, bf16[192,512]{1,0:T(8,128)(2,1)S(1)}, u32[]{:S(2)}, u32[]{:S(2)}) %collective-permute-start.2) | collective-permute-done | bytes 196640 | tf_op jit(solution)/shard_map/ppermute | solution.py:379
  12.6 1.5 %collective-permute-start.8 = (bf16[192,512]{1,0:T(8,128)(2,1)S(1)}, bf16[192,512]{1,0:T(8,128)(2,1)S(1)}, u32[]{:S(2)}, u32[]{:S(2)}) collective-permute-start(bf16[192,512]{1,0:T(8,128)(2,1)S(1)} %collective-permute-done.up0.refs_2_), channel_id=1, source_target_pairs={{0,2},{2,4},{4,6},{6,0},{1,3},{3,5},{5,7},{7,1},{8,10},{10,12},{12... | collective-permute-start | bytes 589832 | tf_op jit(solution)/shard_map/ppermute | solution.py:379
  15.6 2.8 %collective-permute-done.8.refs_4_.refs_10_ = bf16[192,512]{1,0:T(8,128)(2,1)S(1)} collective-permute-done((bf16[192,512]{1,0:T(8,128)(2,1)S(1)}, bf16[192,512]{1,0:T(8,128)(2,1)S(1)}, u32[]{:S(2)}, u32[]{:S(2)}) %collective-permute-start.8) | collective-permute-done | bytes 196640 | tf_op jit(solution)/shard_map/ppermute | solution.py:379
  18.4 2.6 %collective-permute-done.9.refs_5_.refs_11_ = bf16[192,512]{1,0:T(8,128)(2,1)S(1)} collective-permute-done((bf16[192,512]{1,0:T(8,128)(2,1)S(1)}, bf16[192,512]{1,0:T(8,128)(2,1)S(1)}, u32[]{:S(2)}, u32[]{:S(2)}) %collective-permute-start.9) | collective-permute-done | bytes 196640 | tf_op jit(solution)/shard_map/ppermute | solution.py:379
  21.5 1.6 %copy-done = bf16[4096,256]{1,0:T(8,128)(2,1)S(1)} copy-done((bf16[4096,256]{1,0:T(8,128)(2,1)S(1)}, bf16[4096,256]{1,0:T(8,128)(2,1)}, u32[]{:S(2)}) %copy-start) | copy-done | bytes 2097176
  23.1 1.6 %copy-done.2 = bf16[4096,256]{1,0:T(8,128)(2,1)S(1)} copy-done((bf16[4096,256]{1,0:T(8,128)(2,1)S(1)}, bf16[4096,256]{1,0:T(8,128)(2,1)}, u32[]{:S(2)}) %copy-start.2) | copy-done | bytes 2097176
  24.7 1.0 copy-done.4
  30.3 7.1 %local_terms.1 = (bf16[8,208,128]{2,1,0:T(8,128)(2,1)S(1)}, bf16[384,256]{1,0:T(8,128)(2,1)S(1)}, bf16[4,192,128]{2,1,0:T(8,128)(2,1)S(1)}, bf16[4,192,128]{2,1,...) custom-call(f32[2]{0:T(128)S(1)} %copy-done.55, f32[2]{0:T(128)S(1)} %copy-done.56, ...), custom_call_target="tpu_custom_call" | custom-call | tf_op jit(solution)/shard_map/local_terms/pallas_call | solution.py:366
  41.7 5.6 %all-to-all-start = ((bf16[8,208,128]{2,1,0:T(8,128)(2,1)}), bf16[8,208,128]{2,1,0:T(8,128)(2,1)S(1)}, u32[]{:S(2)}, u32[]{:S(2)}) async-start(bf16[8,208,128]{2,1,0:T(8,128)(2,1)} %copy-done.30), calls=%async_computation | async-start | bytes 851968 | tf_op jit(solution)/shard_map/all_to_all | solution.py:424
  47.4 1.6 %copy-done.7 = bf16[4096,256]{1,0:T(8,128)(2,1)S(1)} copy-done((bf16[4096,256]{1,0:T(8,128)(2,1)S(1)}, bf16[4096,256]{1,0:T(8,128)(2,1)}, u32[]{:S(2)}) %copy-start.7) | copy-done | bytes 2097176
  49.0 0.9 copy-done.9
  49.9 0.9 copy-done.11
  50.8 0.9 copy-done.13
  52.7 0.9 copy-done.17
  53.6 0.9 copy-done.19
  59.2 0.9 copy-done.36
  60.1 0.9 copy-done.38
  63.9 2.6 %window_terms.1 = (f32[4,192,128]{2,1,0:T(8,128)S(1)}, bf16[4,192,128]{2,1,0:T(8,128)(2,1)S(1)}, f32[4,192,128]{2,1,0:T(8,128)S(1)}) custom-call(bf16[2,192,512]{2,1,0:T(8,128)(2,1)S(1)} %copy-done.5, bf16[2,192,512]{2,1,0:T(8,128)(2,1)S(1)} %collective-permute-done.12.own_c.refs_1_, bf16[192,512]{1,0:T(8,128)(2,1)S(1)} %collective-permute-done.up0.refs_2_, ...), custom_call_target="tpu_custom_call" | custom-call | tf_op jit(solution)/shard_map/window_terms/pallas_call | solution.py:366
  69.2 3.4 %collective-permute-start.13 = (bf16[208,128]{1,0:T(8,128)(2,1)S(1)}, bf16[208,128]{1,0:T(8,128)(2,1)S(1)}, u32[]{:S(2)}, u32[]{:S(2)}) collective-permute-start(bf16[208,128]{1,0:T(8,128)(2,1)S(1)} %get-tuple-element.38.own), channel_id=1, source_target_pairs={{0,64},{64,128},{128,192},{192,0},{1,65},{65,129},{129,193},{193,1... | collective-permute-start | bytes 159752 | tf_op jit(solution)/shard_map/ppermute | solution.py:379
  72.6 4.5 %collective-permute-start.14 = (bf16[208,128]{1,0:T(8,128)(2,1)S(1)}, bf16[208,128]{1,0:T(8,128)(2,1)S(1)}, u32[]{:S(2)}, u32[]{:S(2)}) collective-permute-start(bf16[208,128]{1,0:T(8,128)(2,1)S(1)} %get-tuple-element.38.own), channel_id=1, source_target_pairs={{0,128},{64,192},{128,0},{192,64},{1,129},{65,193},{129,1},{193,65... | collective-permute-start | bytes 159752 | tf_op jit(solution)/shard_map/ppermute | solution.py:379
  77.0 2.7 %collective-permute-start.15 = (bf16[208,128]{1,0:T(8,128)(2,1)S(1)}, bf16[208,128]{1,0:T(8,128)(2,1)S(1)}, u32[]{:S(2)}, u32[]{:S(2)}) collective-permute-start(bf16[208,128]{1,0:T(8,128)(2,1)S(1)} %get-tuple-element.38.own), channel_id=1, source_target_pairs={{0,192},{64,0},{128,64},{192,128},{1,193},{65,1},{129,65},{193,129... | collective-permute-start | bytes 159752 | tf_op jit(solution)/shard_map/ppermute | solution.py:379
  79.7 1.4 %collective-permute-done.14.back2 = bf16[208,128]{1,0:T(8,128)(2,1)S(1)} collective-permute-done((bf16[208,128]{1,0:T(8,128)(2,1)S(1)}, bf16[208,128]{1,0:T(8,128)(2,1)S(1)}, u32[]{:S(2)}, u32[]{:S(2)}) %collective-permute-start.14) | collective-permute-done | bytes 53280 | tf_op jit(solution)/shard_map/ppermute | solution.py:379
  81.2 2.9 %collective-permute-done.15.back3 = bf16[208,128]{1,0:T(8,128)(2,1)S(1)} collective-permute-done((bf16[208,128]{1,0:T(8,128)(2,1)S(1)}, bf16[208,128]{1,0:T(8,128)(2,1)S(1)}, u32[]{:S(2)}, u32[]{:S(2)}) %collective-permute-start.15) | collective-permute-done | bytes 53280 | tf_op jit(solution)/shard_map/ppermute | solution.py:379
  84.1 1.3 %spread_states.1 = bf16[8,80,128]{2,1,0:T(8,128)(2,1)S(1)} custom-call(f32[2,2]{1,0:T(2,128)S(1)} %copy-done.50, f32[2,2]{1,0:T(2,128)S(1)} %copy-done.51, bf16[208,128]{1,0:T(8,128)(2,1)S(1)} %get-tuple-element.38.own, bf16[208,128]{1,0:T(8,128)(2,1)S(1)} %collective-permute-done.13.back1, bf16[208,128]{1,0:T(8,128)(2,1)S(1)} %collective-permute-done.14.back2, ...), custom_call_target="tpu_custom_call" | custom-call | tf_op jit(solution)/shard_map/spread_states/pallas_call | solution.py:366
  85.4 10.8 %all_to_all.10.in_ref = bf16[8,80,128]{2,1,0:T(8,128)(2,1)S(1)} all-to-all(bf16[8,80,128]{2,1,0:T(8,128)(2,1)S(1)} %spread_states.1), channel_id=1, replica_groups=mesh['zh'=4,'zl'=2,'x'=4,'y'=4,'c'=2] {'zl','x'}, dimensions={0} | all-to-all | bytes 327680 | tf_op jit(solution)/shard_map/all_to_all | solution.py:460
  96.2 1.0 copy-done.32
  97.2 1.0 copy-done.34
  99.1 1.0 %finish.1 = (bf16[2,192,256]{2,1,0:T(8,128)(2,1)}, bf16[2,2,4,128]{3,2,1,0:T(4,128)(2,1)}, f32[2,256]{1,0:T(2,128)}) custom-call(bf16[8,80,128]{2,1,0:T(8,128)(2,1)S(1)} %all_to_all.10.in_ref, f32[4,192,128]{2,1,0:T(8,128)S(1)} %copy-done.32, bf16[4,192,128]{2,1,0:T(8,128)(2,1)S(1)} %copy-done.40, f32[4,192,128]{2,1,0:T(8,128)S(1)} %copy-done.34, ...), custom_call_target="tpu_custom_call" | custom-call | tf_op jit(solution)/shard_map/finish/pallas_call | solution.py:366
  (125 shorter events, 22.9 us)
Async XLA Ops:
  1.7 7.8 %collective-permute-start = (bf16[192,512]{1,0:T(8,128)(2,1)S(1)}, bf16[192,512]{1,0:T(8,128)(2,1)S(1)}, u32[]{:S(2)}, u32[]{:S(2)}) collective-permute-start(bf16[192,512]{1,0:T(8,128)(2,1)S(1)} %get-tuple-element.46), channel_id=1, source_target_pairs={{0,2},{2,4},{4,6},{6,0},{1,3},{3,5},{5,7},{7,1},{8,10},{10,12},{12... | collective-permute-start | bytes 589832 | tf_op jit(solution)/shard_map/ppermute | solution.py:379
  3.7 8.9 %collective-permute-start.2 = (bf16[192,512]{1,0:T(8,128)(2,1)S(1)}, bf16[192,512]{1,0:T(8,128)(2,1)S(1)}, u32[]{:S(2)}, u32[]{:S(2)}) collective-permute-start(bf16[192,512]{1,0:T(8,128)(2,1)S(1)} %get-tuple-element.45), channel_id=1, source_target_pairs={{0,2},{2,4},{4,6},{6,0},{1,3},{3,5},{5,7},{7,1},{8,10},{10,12},{12... | collective-permute-start | bytes 589832 | tf_op jit(solution)/shard_map/ppermute | solution.py:379
  3.8 10.3 %collective-permute-start.6 = (bf16[192,512]{1,0:T(8,128)(2,1)S(1)}, bf16[192,512]{1,0:T(8,128)(2,1)S(1)}, u32[]{:S(2)}, u32[]{:S(2)}) collective-permute-start(bf16[192,512]{1,0:T(8,128)(2,1)S(1)} %get-tuple-element.45), channel_id=1, source_target_pairs={{0,6},{2,0},{4,2},{6,4},{1,7},{3,1},{5,3},{7,5},{8,14},{10,8},{12,... | collective-permute-start | bytes 589832 | tf_op jit(solution)/shard_map/ppermute | solution.py:379
  5.7 15.3 %collective-permute-start.12 = (bf16[2,192,512]{2,1,0:T(8,128)(2,1)}, bf16[2,192,512]{2,1,0:T(8,128)(2,1)S(1)}, u32[]{:S(2)}, u32[]{:S(2)}) collective-permute-start(bf16[2,192,512]{2,1,0:T(8,128)(2,1)} %refs_0_.1), channel_id=1, source_target_pairs={{0,1},{1,0},{2,3},{3,2},{4,5},{5,4},{6,7},{7,6},{8,9},{9,8},{10,11... | collective-permute-start | bytes 1179656 | tf_op jit(solution)/shard_map/ppermute | solution.py:379
  5.7 9.3 %collective-permute-start.4 = (bf16[192,512]{1,0:T(8,128)(2,1)S(1)}, bf16[192,512]{1,0:T(8,128)(2,1)S(1)}, u32[]{:S(2)}, u32[]{:S(2)}) collective-permute-start(bf16[192,512]{1,0:T(8,128)(2,1)S(1)} %get-tuple-element.46), channel_id=1, source_target_pairs={{0,6},{2,0},{4,2},{6,4},{1,7},{3,1},{5,3},{7,5},{8,14},{10,8},{12,... | collective-permute-start | bytes 589832 | tf_op jit(solution)/shard_map/ppermute | solution.py:379
  9.5 5.5 %collective-permute-start.1 = (bf16[192,512]{1,0:T(8,128)(2,1)S(1)}, bf16[192,512]{1,0:T(8,128)(2,1)S(1)}, u32[]{:S(2)}, u32[]{:S(2)}) collective-permute-start(bf16[192,512]{1,0:T(8,128)(2,1)S(1)} %collective-permute-done.up0.refs_2_), channel_id=1, source_target_pairs={{0,1},{1,0},{2,3},{3,2},{4,5},{5,4},{6,7},{7,6},{8,9},{9,8},{10,11... | collective-permute-start | bytes 589832 | tf_op jit(solution)/shard_map/ppermute | solution.py:379
  12.6 15.3 %copy-start.8 = (bf16[192,512]{1,0:T(8,128)(2,1)}, bf16[192,512]{1,0:T(8,128)(2,1)S(1)}, u32[]{:S(2)}) copy-start(bf16[192,512]{1,0:T(8,128)(2,1)S(1)} %collective-permute-done.2.up1.refs_3_) | copy-start | bytes 589828
  12.6 5.8 %collective-permute-start.8 = (bf16[192,512]{1,0:T(8,128)(2,1)S(1)}, bf16[192,512]{1,0:T(8,128)(2,1)S(1)}, u32[]{:S(2)}, u32[]{:S(2)}) collective-permute-start(bf16[192,512]{1,0:T(8,128)(2,1)S(1)} %collective-permute-done.up0.refs_2_), channel_id=1, source_target_pairs={{0,2},{2,4},{4,6},{6,0},{1,3},{3,5},{5,7},{7,1},{8,10},{10,12},{12... | collective-permute-start | bytes 589832 | tf_op jit(solution)/shard_map/ppermute | solution.py:379
  14.1 13.8 %copy-start.10 = (bf16[192,512]{1,0:T(8,128)(2,1)}, bf16[192,512]{1,0:T(8,128)(2,1)S(1)}, u32[]{:S(2)}) copy-start(bf16[192,512]{1,0:T(8,128)(2,1)S(1)} %collective-permute-done.6.down1.refs_5_) | copy-start | bytes 589828
  14.1 6.9 %collective-permute-start.9 = (bf16[192,512]{1,0:T(8,128)(2,1)S(1)}, bf16[192,512]{1,0:T(8,128)(2,1)S(1)}, u32[]{:S(2)}, u32[]{:S(2)}) collective-permute-start(bf16[192,512]{1,0:T(8,128)(2,1)S(1)} %collective-permute-done.6.down1.refs_5_), channel_id=1, source_target_pairs={{0,6},{2,0},{4,2},{6,4},{1,7},{3,1},{5,3},{7,5},{8,14},{10,8},{12,... | collective-permute-start | bytes 589832 | tf_op jit(solution)/shard_map/ppermute | solution.py:379
  15.1 12.9 %copy-start.12 = (bf16[192,512]{1,0:T(8,128)(2,1)}, bf16[192,512]{1,0:T(8,128)(2,1)S(1)}, u32[]{:S(2)}) copy-start(bf16[192,512]{1,0:T(8,128)(2,1)S(1)} %collective-permute-done.4.down0.refs_4_) | copy-start | bytes 589828
  15.1 15.1 %collective-permute-start.7 = (bf16[192,512]{1,0:T(8,128)(2,1)S(1)}, bf16[192,512]{1,0:T(8,128)(2,1)S(1)}, u32[]{:S(2)}, u32[]{:S(2)}) collective-permute-start(bf16[192,512]{1,0:T(8,128)(2,1)S(1)} %collective-permute-done.6.down1.refs_5_), channel_id=1, source_target_pairs={{0,1},{1,0},{2,3},{3,2},{4,5},{5,4},{6,7},{7,6},{8,9},{9,8},{10,11... | collective-permute-start | bytes 589832 | tf_op jit(solution)/shard_map/ppermute | solution.py:379
  15.1 15.2 %copy-start.14 = (bf16[192,512]{1,0:T(8,128)(2,1)}, bf16[192,512]{1,0:T(8,128)(2,1)S(1)}, u32[]{:S(2)}) copy-start(bf16[192,512]{1,0:T(8,128)(2,1)S(1)} %collective-permute-done.1.refs_0_.refs_6_) | copy-start | bytes 589828
  15.1 15.1 %collective-permute-start.3 = (bf16[192,512]{1,0:T(8,128)(2,1)S(1)}, bf16[192,512]{1,0:T(8,128)(2,1)S(1)}, u32[]{:S(2)}, u32[]{:S(2)}) collective-permute-start(bf16[192,512]{1,0:T(8,128)(2,1)S(1)} %collective-permute-done.2.up1.refs_3_), channel_id=1, source_target_pairs={{0,1},{1,0},{2,3},{3,2},{4,5},{5,4},{6,7},{7,6},{8,9},{9,8},{10,11... | collective-permute-start | bytes 589832 | tf_op jit(solution)/shard_map/ppermute | solution.py:379
  18.4 11.9 %copy-start.16 = (bf16[192,512]{1,0:T(8,128)(2,1)}, bf16[192,512]{1,0:T(8,128)(2,1)S(1)}, u32[]{:S(2)}) copy-start(bf16[192,512]{1,0:T(8,128)(2,1)S(1)} %collective-permute-done.8.refs_4_.refs_10_) | copy-start | bytes 589828
  18.4 11.8 %collective-permute-start.5 = (bf16[192,512]{1,0:T(8,128)(2,1)S(1)}, bf16[192,512]{1,0:T(8,128)(2,1)S(1)}, u32[]{:S(2)}, u32[]{:S(2)}) collective-permute-start(bf16[192,512]{1,0:T(8,128)(2,1)S(1)} %collective-permute-done.4.down0.refs_4_), channel_id=1, source_target_pairs={{0,1},{1,0},{2,3},{3,2},{4,5},{5,4},{6,7},{7,6},{8,9},{9,8},{10,11... | collective-permute-start | bytes 589832 | tf_op jit(solution)/shard_map/ppermute | solution.py:379
  21.0 9.3 %copy-start.18 = (bf16[192,512]{1,0:T(8,128)(2,1)}, bf16[192,512]{1,0:T(8,128)(2,1)S(1)}, u32[]{:S(2)}) copy-start(bf16[192,512]{1,0:T(8,128)(2,1)S(1)} %collective-permute-done.9.refs_5_.refs_11_) | copy-start | bytes 589828
  21.0 9.2 %collective-permute-start.10 = (bf16[192,512]{1,0:T(8,128)(2,1)S(1)}, bf16[192,512]{1,0:T(8,128)(2,1)S(1)}, u32[]{:S(2)}, u32[]{:S(2)}) collective-permute-start(bf16[192,512]{1,0:T(8,128)(2,1)S(1)} %collective-permute-done.8.refs_4_.refs_10_), channel_id=1, source_target_pairs={{0,1},{1,0},{2,3},{3,2},{4,5},{5,4},{6,7},{7,6},{8,9},{9,8},{10,11... | collective-permute-start | bytes 589832 | tf_op jit(solution)/shard_map/ppermute | solution.py:379
  21.0 9.2 %collective-permute-start.11 = (bf16[192,512]{1,0:T(8,128)(2,1)S(1)}, bf16[192,512]{1,0:T(8,128)(2,1)S(1)}, u32[]{:S(2)}, u32[]{:S(2)}) collective-permute-start(bf16[192,512]{1,0:T(8,128)(2,1)S(1)} %collective-permute-done.9.refs_5_.refs_11_), channel_id=1, source_target_pairs={{0,1},{1,0},{2,3},{3,2},{4,5},{5,4},{6,7},{7,6},{8,9},{9,8},{10,11... | collective-permute-start | bytes 589832 | tf_op jit(solution)/shard_map/ppermute | solution.py:379
  30.2 7.3 %copy-start.22 = (bf16[192,512]{1,0:T(8,128)(2,1)}, bf16[192,512]{1,0:T(8,128)(2,1)S(1)}, u32[]{:S(2)}) copy-start(bf16[192,512]{1,0:T(8,128)(2,1)S(1)} %collective-permute-done.3.refs_1_.refs_7_) | copy-start | bytes 589828
  30.3 17.1 %copy-start.5 = (bf16[2,192,512]{2,1,0:T(8,128)(2,1)S(1)}, bf16[2,192,512]{2,1,0:T(8,128)(2,1)}, u32[]{:S(2)}) copy-start(bf16[2,192,512]{2,1,0:T(8,128)(2,1)} %refs_0_.1) | copy-start | bytes 1179652
  30.3 17.1 %copy-start.6 = (bf16[4096,256]{1,0:T(8,128)(2,1)S(1)}, bf16[4096,256]{1,0:T(8,128)(2,1)}, u32[]{:S(2)}) copy-start(bf16[4096,256]{1,0:T(8,128)(2,1)} %refs_14_.1) | copy-start | bytes 6291460
  30.3 17.1 %copy-start.49 = (f32[128]{0:T(128)S(1)}, f32[128]{0:T(128)}, u32[]{:S(2)}) copy-start(f32[128]{0:T(128)} %param.24) | copy-start | bytes 1540
  41.7 26.9 %all-to-all-start = ((bf16[8,208,128]{2,1,0:T(8,128)(2,1)}), bf16[8,208,128]{2,1,0:T(8,128)(2,1)S(1)}, u32[]{:S(2)}, u32[]{:S(2)}) async-start(bf16[8,208,128]{2,1,0:T(8,128)(2,1)} %copy-done.30), calls=%async_computation | async-start | bytes 851968 | tf_op jit(solution)/shard_map/all_to_all | solution.py:424
  63.9 20.2 %copy-start.50 = (f32[2,2]{1,0:T(2,128)S(1)}, f32[2,2]{1,0:T(2,128)}, u32[]{:S(2)}) copy-start(f32[2,2]{1,0:T(2,128)} %beta_ref.1) | copy-start | bytes 52
  63.9 20.2 %copy-start.51 = (f32[2,2]{1,0:T(2,128)S(1)}, f32[2,2]{1,0:T(2,128)}, u32[]{:S(2)}) copy-start(f32[2,2]{1,0:T(2,128)} %decay_ref.1) | copy-start | bytes 52
  63.9 20.2 %copy-start.52 = (bf16[2,2,128]{2,1,0:T(2,128)(2,1)S(1)}, bf16[2,2,128]{2,1,0:T(2,128)(2,1)}, u32[]{:S(2)}) copy-start(bf16[2,2,128]{2,1,0:T(2,128)(2,1)} %query_ref.1) | copy-start | bytes 3076
  63.9 20.2 %copy-start.53 = (bf16[2,2,128]{2,1,0:T(2,128)(2,1)S(1)}, bf16[2,2,128]{2,1,0:T(2,128)(2,1)}, u32[]{:S(2)}) copy-start(bf16[2,2,128]{2,1,0:T(2,128)(2,1)} %key_ref.1) | copy-start | bytes 3076
  63.9 20.2 %copy-start.54 = (bf16[2,2,128]{2,1,0:T(2,128)(2,1)S(1)}, bf16[2,2,128]{2,1,0:T(2,128)(2,1)}, u32[]{:S(2)}) copy-start(bf16[2,2,128]{2,1,0:T(2,128)(2,1)} %value_ref.1) | copy-start | bytes 3076
  69.2 10.5 %collective-permute-start.13 = (bf16[208,128]{1,0:T(8,128)(2,1)S(1)}, bf16[208,128]{1,0:T(8,128)(2,1)S(1)}, u32[]{:S(2)}, u32[]{:S(2)}) collective-permute-start(bf16[208,128]{1,0:T(8,128)(2,1)S(1)} %get-tuple-element.38.own), channel_id=1, source_target_pairs={{0,64},{64,128},{128,192},{192,0},{1,65},{65,129},{129,193},{193,1... | collective-permute-start | bytes 159752 | tf_op jit(solution)/shard_map/ppermute | solution.py:379
  72.6 8.6 %collective-permute-start.14 = (bf16[208,128]{1,0:T(8,128)(2,1)S(1)}, bf16[208,128]{1,0:T(8,128)(2,1)S(1)}, u32[]{:S(2)}, u32[]{:S(2)}) collective-permute-start(bf16[208,128]{1,0:T(8,128)(2,1)S(1)} %get-tuple-element.38.own), channel_id=1, source_target_pairs={{0,128},{64,192},{128,0},{192,64},{1,129},{65,193},{129,1},{193,65... | collective-permute-start | bytes 159752 | tf_op jit(solution)/shard_map/ppermute | solution.py:379
  77.0 7.0 %collective-permute-start.15 = (bf16[208,128]{1,0:T(8,128)(2,1)S(1)}, bf16[208,128]{1,0:T(8,128)(2,1)S(1)}, u32[]{:S(2)}, u32[]{:S(2)}) collective-permute-start(bf16[208,128]{1,0:T(8,128)(2,1)S(1)} %get-tuple-element.38.own), channel_id=1, source_target_pairs={{0,192},{64,0},{128,64},{192,128},{1,193},{65,1},{129,65},{193,129... | collective-permute-start | bytes 159752 | tf_op jit(solution)/shard_map/ppermute | solution.py:379
  (42 other events, 66.1 us)

commit v3 on v2

--- a/solution.py
+++ b/solution.py
@@ -56,56 +56,77 @@
     return lax.rem(lax.axis_index("y") + ahead, 4) * 2 + core
 
 
-def project_pieces(pieces, slots, weights):
-    totals = [None] * len(weights)
-    for piece, slot in zip(pieces, slots):
-        rows = piece() if callable(piece) else piece[...]
+def first_row(slot, depth):
+    return pl.multiple_of(shard_index(*slot) * depth, depth)
+
+
+def joined(first, second):
+    return jnp.concatenate([first[...], second[...]], axis=0)
+
+
+def scalar_part(rows, stacked, slot):
+    depth = rows.shape[-1]
+    weight = stacked[:, pl.ds(first_row(slot, depth), depth)]
+    weight = jnp.concatenate([weight, jnp.zeros((LANES - PACK, depth), bf16)], axis=0)
+    return dot(rows, weight, ROWS)
+
+
+SLOTS = (
+    (0, False), (0, True), (3, False), (1, False), (3, True), (1, True), (2, False), (2, True),
+)
+
+
+def early_kernel(
+    own, own_c, beta_w, decay_w, key_w, value_w, sum_ref, gate_ref, rest_ref, stacked_ref,
+    token_buffer, weight_buffer, sems,
+):
+    depth = own.shape[-1]
+    width = key_w.shape[-1]
+    first = [pltpu.make_async_copy(own, token_buffer, sems.at[0])]
+    later = []
+    for at, slot in enumerate(SLOTS):
+        start = first_row(slot, depth)
+        for side, weight in enumerate((key_w, value_w)):
+            lanes = pl.ds(side * width, width)
+            source = weight.at[pl.ds(start, depth), :]
+            if at < 2:
+                to = weight_buffer.at[pl.ds(at * depth, depth), lanes]
+                first.append(pltpu.make_async_copy(source, to, sems.at[0]))
+            else:
+                to = rest_ref.at[pl.ds((at - 2) * depth, depth), lanes]
+                later.append(pltpu.make_async_copy(source, to, sems.at[1]))
+    for copy in first + later:
+        copy.start()
+    rows = [ref[at : at + 1, :].astype(f32) for ref in (beta_w, decay_w) for at in range(2)]
+    stacked_ref[...] = row_pack(rows, stacked_ref.shape[-1]).astype(bf16)
+    for copy in first:
+        copy.wait()
+    total = gates = 0.0
+    for at, piece in enumerate((token_buffer, own_c)):
+        rows = piece[...].reshape(-1, depth)
+        total = total + dot(rows, weight_buffer[at * depth : (at + 1) * depth, :])
+        gates = gates + scalar_part(rows, stacked_ref, SLOTS[at])
+    sum_ref[...] = total
+    gate_ref[...] = gates
+    for copy in later:
+        copy.wait()
+
+
+def add_pieces(pieces, from_slot, rest, stacked, total, gates):
+    for at in range(len(pieces) // 2):
+        rows = joined(*pieces[2 * at : 2 * at + 2])
         depth = rows.shape[-1]
-        rows = rows.reshape(-1, depth)
-        start = pl.multiple_of(shard_index(*slot) * depth, depth)
-        for at, weight in enumerate(weights):
-            part = weight(rows, start) if callable(weight) else dot(rows, weight[pl.ds(start, depth), :])
-            totals[at] = part if totals[at] is None else totals[at] + part
-    return totals
-
-
-def joined(first, second):
-    return lambda: jnp.concatenate([first[...], second[...]], axis=0)
-
-
-def scalar_gates(beta_w, decay_w):
-    def project(rows, start):
-        depth = rows.shape[-1]
-        beta = beta_w[:, pl.ds(start, depth)].astype(f32)
-        decay = decay_w[:, pl.ds(start, depth)].astype(f32)
-        stacked = row_pack((beta[0:1], beta[1:2], decay[0:1], decay[1:2]), depth)
-        stacked = jnp.concatenate([stacked, jnp.zeros((LANES - PACK, depth), f32)], axis=0)
-        return dot(rows, stacked, ROWS)
-
-    return project
-
-
-NEAR_SLOTS = ((0, False), (0, True))
-NEXT_SLOTS = ((3, False), (1, False))
-LATE_SLOTS = ((3, True), (1, True), (2, False), (2, True))
-
-
-def early_kernel(own, own_c, key_w, value_w, beta_w, decay_w, key_out, value_out, gate_out):
-    weights = (key_w, value_w, scalar_gates(beta_w, decay_w))
-    totals = project_pieces((own, own_c), NEAR_SLOTS, weights)
-    for ref, total in zip((key_out, value_out, gate_out), totals):
-        ref[...] = total
-
-
-def next_kernel(
-    up0, up1, down0, down1, key_w, value_w, beta_w, decay_w, key_in, value_in, gate_in,
-    key_out, value_out, gate_out,
-):
-    weights = (key_w, value_w, scalar_gates(beta_w, decay_w))
-    totals = project_pieces((joined(up0, up1), joined(down0, down1)), NEXT_SLOTS, weights)
-    before = (key_in, value_in, gate_in)
-    for ref, total, old in zip((key_out, value_out, gate_out), totals, before):
-        ref[...] = old[...] + total
+        slot = from_slot + at
+        total = total + dot(rows, rest[(slot - 2) * depth : (slot - 1) * depth, :])
+        gates = gates + scalar_part(rows, stacked, SLOTS[slot])
+    return total, gates
+
+
+def middle_kernel(*refs):
+    pieces, (sum_in, gate_in, rest, stacked, sum_ref, gate_ref) = refs[:8], refs[8:]
+    total, gates = add_pieces(pieces, 2, rest, stacked, sum_in[...], gate_in[...])
+    sum_ref[...] = total
+    gate_ref[...] = gates
 
 
 def lane_pair(ref, first):
@@ -114,17 +135,26 @@
 
 
 def local_kernel(bias_ref, rate_ref, *refs):
-    pieces, refs = refs[:8], refs[8:]
-    key_w, value_w, beta_w, decay_w, key_in, value_in, gate_in = refs[:7]
-    send_ref, key_ref, fresh_ref, carry_ref, cols_ref, rows_ref = refs[7:]
+    pieces, (sum_in, gate_in, rest, stacked) = refs[:4], refs[4:8]
+    outputs, buffers, sems = refs[8:14], refs[14:20], refs[20]
+    send_ref, key_ref, fresh_ref, carry_ref, cols_ref, rows_ref = buffers
+    copies = []
+
+    def give(at, part=None):
+        source, to = buffers[at], outputs[at]
+        if part is not None:
+            source, to = source.at[part], to.at[part]
+        copies.append(pltpu.make_async_copy(source, to, sems.at[at]))
+        copies[-1].start()
+
     span = pieces[0].shape[0]
     head = send_ref.shape[-1]
-    late = [joined(*pieces[at : at + 2]) for at in range(0, 8, 2)]
-    totals = project_pieces(late, LATE_SLOTS, (key_w, value_w, scalar_gates(beta_w, decay_w)))
-    key_rows = (key_in[...] + totals[0]).astype(bf16)
-    value_rows = (value_in[...] + totals[1]).astype(bf16)
-    gates = gate_in[...] + totals[2]
+    total, gates = add_pieces(pieces, 6, rest, stacked, sum_in[...], gate_in[...])
+    width = total.shape[-1] // 2
+    key_rows = total[:, :width].astype(bf16)
+    value_rows = total[:, width:].astype(bf16)
     key_ref[...] = key_rows
+    give(1)
     strength = jax.nn.sigmoid(gates + lane_pair(bias_ref, 0))
     decays = -jnp.exp(lane_pair(rate_ref, 2)) * jax.nn.softplus(gates)
     wide = cols_ref.shape[1]
@@ -148,6 +178,8 @@
             table = jnp.where(lanes == 4 + h, unit, table)
         cols_ref[seq] = table
         rows_ref[seq] = table.T
+    give(4)
+    give(5)
     t = iota((span, span), 0)
     s = iota((span, span), 1)
     lower, inverse = [], []
@@ -194,19 +226,38 @@
             send_ref[to, :head, :] = reach.astype(bf16)
             send_ref[to, head : head + half, :] = gain[side * half : (side + 1) * half].astype(bf16)
             send_ref[to, head + half :, :] = factor.astype(bf16)
+        give(0, pl.ds(2 * pair, 2))
+    give(2)
+    give(3)
+    for copy in copies:
+        copy.wait()
 
 
 def window_kernel(*refs):
-    own, own_c, up0, up1, down0, down1 = refs[:6]
-    late, refs = refs[6:14], refs[14:]
+    pieces, refs = refs[:14], refs[14:]
     query_w, gate_w, gain_ref, key_ref, fresh_ref, carry_ref, cols_ref, rows_ref = refs[:8]
-    out_ref, reach_ref, silu_ref = refs[8:]
-    span = up0.shape[0]
+    out_ref, reach_ref, silu_ref, token_buffer, query_buffer, gate_buffer, sems = refs[8:]
+    span, depth = token_buffer.shape[2:]
     head = fresh_ref.shape[-1]
-    pieces = [own, own_c, joined(up0, up1), joined(down0, down1)]
-    pieces += [joined(*late[at : at + 2]) for at in range(0, 8, 2)]
-    slots = NEAR_SLOTS + NEXT_SLOTS + LATE_SLOTS
-    query_total, gate_total = project_pieces(pieces, slots, (query_w, gate_w))
+    weights = ((query_w, query_buffer), (gate_w, gate_buffer))
+    copies = []
+    for at, slot in enumerate(SLOTS):
+        if at < 2:
+            parts = [(pieces[at], token_buffer.at[at])]
+        else:
+            parts = [(pieces[2 * at - 2 + seq], token_buffer.at[at, seq]) for seq in range(2)]
+        for weight, buffer in weights:
+            parts.append((weight.at[pl.ds(first_row(slot, depth), depth), :], buffer.at[at]))
+        copies.append([pltpu.make_async_copy(a, b, sems.at[at]) for a, b in parts])
+        for copy in copies[at]:
+            copy.start()
+    query_total = gate_total = 0.0
+    for at in range(8):
+        for copy in copies[at]:
+            copy.wait()
+        rows = token_buffer[at].reshape(-1, depth)
+        query_total = query_total + dot(rows, query_buffer[at])
+        gate_total = gate_total + dot(rows, gate_buffer[at])
     query_rows = query_total.astype(bf16)
     gate_rows = gate_total.astype(bf16).astype(f32)
     t = iota((span, span), 0)
@@ -272,8 +323,13 @@
 
 def spread_kernel(
     beta_ref, decay_ref, own, back1, back2, back3, maps_ref, adds_ref, factors_ref,
-    query_ref, key_ref, value_ref, send_ref, groups_ref, wide_ref, turned_ref,
+    query_ref, key_ref, value_ref, out_in, reach_in, silu_in,
+    send_ref, out_ref, reach_ref, silu_ref, groups_ref, wide_ref, turned_ref, sems,
 ):
+    moved = ((out_in, out_ref), (reach_in, reach_ref), (silu_in, silu_ref))
+    copies = [pltpu.make_async_copy(a, b, sems.at[at]) for at, (a, b) in enumerate(moved)]
+    for copy in copies:
+        copy.start()
     rows, head = own.shape
     half = head // 2
     far = lax.axis_index("zh")
@@ -331,6 +387,8 @@
         send_ref[member, :half, :] = entry.astype(bf16)
         pick = ((pick_row < 4) & (pick_col == 4 * member + pick_row)).astype(bf16)
         send_ref[member, half:, :] = (dot(pick, mine) + extra).astype(bf16)
+    for copy in copies:
+        copy.wait()
 
 
 def finish_kernel(in_ref, out_ref, reach_ref, silu_ref, gain_ref, mixed_ref, cache_ref, read_ref):
@@ -357,18 +415,21 @@
     return pl.BlockSpec(memory_space=pltpu.SMEM)
 
 
-def kernel(body, name, outputs, smem_count, args, scratch=(), limit=16):
+def kernel(body, name, outputs, kinds, args, scratch=(), limit=16):
+    given = {"s": smem, "v": vmem, "p": vmem, "h": lambda: pl.BlockSpec(memory_space=pl.ANY)}
     placed = [
-        arg if at < smem_count else pltpu.with_memory_space_constraint(arg, pltpu.VMEM)
-        for at, arg in enumerate(args)
+        arg
+        if kind == "s"
+        else pltpu.with_memory_space_constraint(arg, pltpu.VMEM if kind == "p" else pltpu.HBM)
+        for kind, arg in zip(kinds, args, strict=True)
     ]
-    specs = [smem() if at < smem_count else vmem() for at in range(len(args))]
+    plain = lambda out: pltpu.HBM(out.shape, out.dtype)
     return pl.pallas_call(
         body,
         name=name,
-        out_shape=tuple(outputs),
-        in_specs=specs,
-        out_specs=tuple(vmem() for _ in outputs),
+        out_shape=tuple(out if kind == "p" else plain(out) for kind, out in outputs),
+        in_specs=[given[kind]() for kind in kinds],
+        out_specs=tuple(given[kind]() for kind, _ in outputs),
         scratch_shapes=list(scratch),
         compiler_params=pltpu.CompilerParams(vmem_limit_bytes=limit * 1024 * 1024),
     )(*placed)
@@ -389,85 +450,106 @@
     wide = 256
     width = query_weight.shape[1]
     rows = head + half + PACK
-    first, second = tokens[0], tokens[1]
+    on, dma = pltpu.VMEM, pltpu.SemaphoreType.DMA
+    depth = tokens.shape[2]
     swap = lambda value: shift(value, "c", 1)
     tokens_c = swap(tokens)
+    first, second = tokens[0], tokens[1]
     up0 = shift(first, "y", 1)
     down1 = shift(second, "y", -1)
     up1 = shift(second, "y", 1)
     down0 = shift(first, "y", -1)
+    sums = [("p", on((2 * span, 2 * width), f32)), ("p", on((2 * span, head), f32))]
+    early = kernel(
+        early_kernel,
+        "early",
+        sums + [("p", on((6 * depth, 2 * width), bf16)), ("p", on((PACK, 8 * depth), bf16))],
+        "hpvvhh",
+        (tokens, tokens_c, beta_weight.T, decay_weight.T, key_weight, value_weight),
+        (on((2, span, depth), bf16), on((2 * depth, 2 * width), bf16), dma((2,))),
+    )
+    up0, down1, *early = lax.optimization_barrier((up0, down1, *early))
+    rest = early[2:]
     far0 = shift(up0, "y", 1)
     far1 = shift(down1, "y", -1)
-    swapped = [swap(value) for value in (up0, up1, down0, down1)]
-    late = [*swapped, far0, far1, swap(far0), swap(far1)]
-    gates = (beta_weight.T, decay_weight.T)
-    gain = out_gain[None]
-    on = pltpu.VMEM
-    sums = [on((2 * span, width), f32), on((2 * span, width), f32), on((2 * span, head), f32)]
-    weights = (key_weight, value_weight, *gates)
-    early = kernel(early_kernel, "early", sums, 0, (tokens, tokens_c, *weights))
-    middle = kernel(next_kernel, "middle", sums, 0, (up0, up1, down0, down1, *weights, *early))
-    send, key_rows, fresh, carry, cols, turned = kernel(
+    near = (up0, up1, down0, down1)
+    swapped = [swap(value) for value in near]
+    middle = kernel(
+        middle_kernel, "middle", sums, "p" * 12, (*near, *swapped, *early[:2], *rest)
+    )
+    far0, far1, *middle = lax.optimization_barrier((far0, far1, *middle))
+    last = [far0, far1, swap(far0), swap(far1)]
+    local_shapes = [
+        on((8, rows, head), bf16),
+        on((2 * span, width), bf16),
+        on((4, span, head), bf16),
+        on((4, span, head), bf16),
+        on((2, wide, head), f32),
+        on((2, head, wide), f32),
+    ]
+    send, *shared = kernel(
         local_kernel,
         "local_terms",
-        (
-            on((8, rows, head), bf16),
-            on((2 * span, width), bf16),
-            on((4, span, head), bf16),
-            on((4, span, head), bf16),
-            on((2, wide, head), f32),
-            on((2, head, wide), f32),
-        ),
-        2,
-        (beta_bias, rate_log, *late, *weights, *middle),
+        [("h", out) for out in local_shapes],
+        "ss" + "p" * 8,
+        (beta_bias, rate_log, *last, *middle, *rest),
+        (*local_shapes, dma((6,))),
     )
     arrived = lax.all_to_all(send, NEAR, 0, 0, tiled=True)
+    gain = out_gain[None]
+    finals = [on((4, span, head), f32), on((4, span, head), bf16), on((4, span, head), f32)]
     local_out, reach, silu = kernel(
         window_kernel,
         "window_terms",
-        (on((4, span, head), f32), on((4, span, head), bf16), on((4, span, head), f32)),
-        0,
+        [("v", out) for out in finals],
+        "h" * 16 + "v" * 6,
+        (tokens, tokens_c, *near, *swapped, *last, query_weight, gate_weight, gain, *shared),
         (
-            tokens, tokens_c, up0, up1, down0, down1, *late,
-            query_weight, gate_weight, gain, key_rows, fresh, carry, cols, turned,
+            on((8, 2, span, depth), bf16),
+            on((8, depth, width), bf16),
+            on((8, depth, width), bf16),
+            dma((8,)),
         ),
+        24,
     )
     arrived, local_out = lax.optimization_barrier((arrived, local_out))
     total, maps, adds, factors = kernel(
         compose_kernel,
         "compose_near",
-        (
-            on((rows, head), bf16),
-            on((7, head, head), bf16),
-            on((7, half, head), f32),
-            on((7, 8, head), f32),
-        ),
-        0,
+        [
+            ("p", on((rows, head), bf16)),
+            ("p", on((7, head, head), bf16)),
+            ("p", on((7, half, head), f32)),
+            ("p", on((7, 8, head), f32)),
+        ],
+        "p",
         (arrived,),
     )
     others = [shift(total, "zh", by) for by in (1, 2, 3)]
-    (back,) = kernel(
+    back, *finals_in = kernel(
         spread_kernel,
         "spread_states",
-        (on((8, half + PACK, head), bf16),),
-        2,
+        [("p", on((8, half + PACK, head), bf16)), *(("p", out) for out in finals)],
+        "ss" + "p" * 10 + "hhh",
         (
             new_beta, new_decay, total, *others, maps, adds, factors,
-            new_query, new_key, new_value,
+            new_query, new_key, new_value, local_out, reach, silu,
         ),
-        (on((4, rows, head), bf16), on((head, head), f32), on((head, head), f32)),
+        (
+            on((4, rows, head), bf16), on((head, head), f32), on((head, head), f32), dma((3,)),
+        ),
     )
     returned = lax.all_to_all(back, NEAR, 0, 0, tiled=True)
     return kernel(
         finish_kernel,
         "finish",
-        (
-            jax.ShapeDtypeStruct((2, span, width), bf16),
-            jax.ShapeDtypeStruct((2, 2, 4, head), bf16),
-            jax.ShapeDtypeStruct((2, width), f32),
-        ),
-        0,
-        (returned, local_out, reach, silu, gain),
+        [
+            ("v", on((2, span, width), bf16)),
+            ("v", on((2, 2, 4, head), bf16)),
+            ("v", on((2, width), f32)),
+        ],
+        "ppppp",
+        (returned, *finals_in, gain),
     )
 
 

time: 101 us -> 75.7 us (0.75)
  local copies, waits for them, and re-layouts: 33.9 us -> 1.14 us
  Pallas kernels: 14.1 us -> 22.2 us
  waiting for transfers between devices: 17 us -> 19 us
  starting transfers between devices: 23.3 us -> 21.9 us
    unnamed x114 -> x42, local copies, waits for them, and re-layouts: 32.9 us -> 0.09 us
    pallas_call x7, Pallas kernels: 14.1 us -> 22.2 us  [kernel(): pl.pallas_call(body, name=name, out_shape=tuple((out if kind == 'p' else...]
    all_to_all x1, waiting for transfers between devices: 0.01 us -> 2.09 us  [shards(): arrived = lax.all_to_all(send, NEAR, 0, 0, tiled=True)]
    all_to_all x1, starting transfers between devices: 5.65 us -> 4.03 us  [shards(): arrived = lax.all_to_all(send, NEAR, 0, 0, tiled=True)]
  transfers between devices with their start and end apart: 17 -> 17, of which waited for: 7 -> 10; matrix products, arithmetic and copies ran while one was open for 0% -> 1% of each run, Pallas kernels for 4% -> 15%
where the time goes in v3:
time: 75.7 us; the launch traced here: 75.4 us
  Pallas kernels  22.2 us (29%)
  starting transfers between devices  21.9 us (29%)
  waiting for transfers between devices  19 us (25%)
  blocking collectives  10.2 us (13%)
  local copies, waits for them, and re-layouts  1.14 us (2%)
  between operations  0.92 us (1%)
    pallas_call x7, Pallas kernels, kernel(): pl.pallas_call(body, name=name, out_shape=tuple((out if kind == 'p' else...  22.2 us
    ppermute x16, starting transfers between devices, shift(): lax.ppermute(value, axis, [(at, (at + by) % length) for at in range(lengt...  17.9 us
    ppermute x16, waiting for transfers between devices, shift(): lax.ppermute(value, axis, [(at, (at + by) % length) for at in range(lengt...  16.9 us
    all_to_all x1, blocking collectives, shards(): returned = lax.all_to_all(back, NEAR, 0, 0, tiled=True)  10.2 us
    all_to_all x1, starting transfers between devices, shards(): arrived = lax.all_to_all(send, NEAR, 0, 0, tiled=True)  4.03 us
    all_to_all x1, waiting for transfers between devices, shards(): arrived = lax.all_to_all(send, NEAR, 0, 0, tiled=True)  2.09 us
  transfers between devices with their start and end apart: 17, of which 10 were waited for; matrix products, arithmetic and copies ran while one was open for 1% of the time, Pallas kernels for 15%

profile of v3, /device:TPU:24, one launch (start us, length us, event | category | flops | bytes accessed | tf_op | source)
XLA Modules:
  0.0 75.4 jit_solution(4050128938747954823)
XLA Ops:
  0.7 1.0 %slice_bitcast_fusion = (bf16[192,512]{1,0:T(8,128)(2,1)S(1)}, bf16[192,512]{1,0:T(8,128)(2,1)S(1)}) fusion(bf16[2,192,512]{2,1,0:T(8,128)(2,1)} %refs_0_.1), kind=kLoop, calls=%fused_computation | loop fusion | bytes 786432 | tf_op jit(solution)/shard_map/squeeze | solution.py:457
  1.8 2.0 %collective-permute-start.5 = (bf16[192,512]{1,0:T(8,128)(2,1)S(1)}, bf16[192,512]{1,0:T(8,128)(2,1)S(1)}, u32[]{:S(2)}, u32[]{:S(2)}) collective-permute-start(bf16[192,512]{1,0:T(8,128)(2,1)S(1)} %get-tuple-element.73), channel_id=1, source_target_pairs={{0,2},{2,4},{4,6},{6,0},{1,3},{3,5},{5,7},{7,1},{8,10},{10,12},{12... | collective-permute-start | bytes 589832 | tf_op jit(solution)/shard_map/ppermute | solution.py:440
  3.8 0.1 collective-permute-start.6
  3.9 0.7 collective-permute-start.1
  4.6 2.5 %collective-permute-start = (bf16[192,512]{1,0:T(8,128)(2,1)S(1)}, bf16[192,512]{1,0:T(8,128)(2,1)S(1)}, u32[]{:S(2)}, u32[]{:S(2)}) collective-permute-start(bf16[192,512]{1,0:T(8,128)(2,1)S(1)} %get-tuple-element.74), channel_id=1, source_target_pairs={{0,2},{2,4},{4,6},{6,0},{1,3},{3,5},{5,7},{7,1},{8,10},{10,12},{12... | collective-permute-start | bytes 589832 | tf_op jit(solution)/shard_map/ppermute | solution.py:440
  7.1 2.5 %collective-permute-done.5.refs_1_.refs_3_ = bf16[192,512]{1,0:T(8,128)(2,1)S(1)} collective-permute-done((bf16[192,512]{1,0:T(8,128)(2,1)S(1)}, bf16[192,512]{1,0:T(8,128)(2,1)S(1)}, u32[]{:S(2)}, u32[]{:S(2)}) %collective-permute-start.5) | collective-permute-done | bytes 196640 | tf_op jit(solution)/shard_map/ppermute | solution.py:440
  9.6 3.1 %collective-permute-done.6.refs_2_.refs_4_ = bf16[192,512]{1,0:T(8,128)(2,1)S(1)} collective-permute-done((bf16[192,512]{1,0:T(8,128)(2,1)S(1)}, bf16[192,512]{1,0:T(8,128)(2,1)S(1)}, u32[]{:S(2)}, u32[]{:S(2)}) %collective-permute-start.6) | collective-permute-done | bytes 196640 | tf_op jit(solution)/shard_map/ppermute | solution.py:440
  12.8 3.1 %early.1 = (f32[384,512]{1,0:T(8,128)S(1)}, f32[384,128]{1,0:T(8,128)S(1)}, bf16[3072,512]{1,0:T(8,128)(2,1)S(1)}, bf16[16,4096]{1,0:T(8,128)(2,1)S(1)}) custom-call(bf16[2,192,512]{2,1,0:T(8,128)(2,1)} %refs_0_.1, bf16[2,192,512]{2,1,0:T(8,128)(2,1)S(1)} %collective-permute-done.2.own_c.refs_1_, bf16[2,4096]{1,0:T(2,128)(2,1)} %bitcast.9, ...), custom_call_target="tpu_custom_call" | custom-call | tf_op jit(solution)/shard_map/early/pallas_call | solution.py:427
  15.9 0.3 collective-permute-done.1.refs_3_.refs_5_
  16.3 0.3 collective-permute-start.7
  16.5 0.3 collective-permute-start.10
  16.9 0.2 collective-permute-start.3
  17.1 1.8 %collective-permute-start.4 = (bf16[192,512]{1,0:T(8,128)(2,1)S(1)}, bf16[192,512]{1,0:T(8,128)(2,1)S(1)}, u32[]{:S(2)}, u32[]{:S(2)}) collective-permute-start(bf16[192,512]{1,0:T(8,128)(2,1)S(1)} %collective-permute-done.1.refs_3_.refs_5_), channel_id=1, source_target_pairs={{0,6},{2,0},{4,2},{6,4},{1,7},{3,1},{5,3},{7,5},{8,14},{10,8},{12,... | collective-permute-start | bytes 589832 | tf_op jit(solution)/shard_map/ppermute | solution.py:440
  19.0 1.4 %middle.1 = (f32[384,512]{1,0:T(8,128)S(1)}, f32[384,128]{1,0:T(8,128)S(1)}) custom-call(bf16[192,512]{1,0:T(8,128)(2,1)S(1)} %collective-permute-done.refs_0_.refs_2_, bf16[192,512]{1,0:T(8,128)(2,1)S(1)} %collective-permute-done.5.refs_1_.refs_3_, bf16[192,512]{1,0:T(8,128)(2,1)S(1)} %collective-permute-done.6.refs_2_.refs_4_, ...), custom_call_target="tpu_custom_call" | custom-call | tf_op jit(solution)/shard_map/middle/pallas_call | solution.py:427
  20.4 3.4 %collective-permute-done.3.refs_0_.refs_10_ = bf16[192,512]{1,0:T(8,128)(2,1)S(1)} collective-permute-done((bf16[192,512]{1,0:T(8,128)(2,1)S(1)}, bf16[192,512]{1,0:T(8,128)(2,1)S(1)}, u32[]{:S(2)}, u32[]{:S(2)}) %collective-permute-start.3) | collective-permute-done | bytes 196640 | tf_op jit(solution)/shard_map/ppermute | solution.py:440
  23.8 1.3 %collective-permute-done.4.refs_1_.refs_11_ = bf16[192,512]{1,0:T(8,128)(2,1)S(1)} collective-permute-done((bf16[192,512]{1,0:T(8,128)(2,1)S(1)}, bf16[192,512]{1,0:T(8,128)(2,1)S(1)}, u32[]{:S(2)}, u32[]{:S(2)}) %collective-permute-start.4) | collective-permute-done | bytes 196640 | tf_op jit(solution)/shard_map/ppermute | solution.py:440
  25.1 0.5 collective-permute-start.12
  25.7 0.9 %collective-permute-done.11.refs_2_.refs_12_ = bf16[192,512]{1,0:T(8,128)(2,1)S(1)} collective-permute-done((bf16[192,512]{1,0:T(8,128)(2,1)S(1)}, bf16[192,512]{1,0:T(8,128)(2,1)S(1)}, u32[]{:S(2)}, u32[]{:S(2)}) %collective-permute-start.11) | collective-permute-done | bytes 196640 | tf_op jit(solution)/shard_map/ppermute | solution.py:440
  26.6 0.3 collective-permute-done.12.refs_3_.refs_13_
  26.9 7.2 %local_terms.1 = (bf16[8,208,128]{2,1,0:T(8,128)(2,1)}, bf16[384,256]{1,0:T(8,128)(2,1)}, bf16[4,192,128]{2,1,0:T(8,128)(2,1)}, bf16[4,192,128]{2,1,0:T(8,128)(2...) custom-call(f32[2]{0:T(128)S(1)} %copy-done.19, f32[2]{0:T(128)S(1)} %copy-done.20, ...), custom_call_target="tpu_custom_call" | custom-call | tf_op jit(solution)/shard_map/local_terms/pallas_call | solution.py:427
  34.1 4.0 %all-to-all-start = ((bf16[8,208,128]{2,1,0:T(8,128)(2,1)}), bf16[8,208,128]{2,1,0:T(8,128)(2,1)S(1)}, u32[]{:S(2)}, u32[]{:S(2)}) async-start(bf16[8,208,128]{2,1,0:T(8,128)(2,1)} %get-tuple-element.54), calls=%async_computation | async-start | bytes 851968 | tf_op jit(solution)/shard_map/all_to_all | solution.py:498
  38.2 6.7 %window_terms.1 = (f32[4,192,128]{2,1,0:T(8,128)}, bf16[4,192,128]{2,1,0:T(8,128)(2,1)}, f32[4,192,128]{2,1,0:T(8,128)}) custom-call(bf16[2,192,512]{2,1,0:T(8,128)(2,1)} %refs_0_.1, bf16[2,192,512]{2,1,0:T(8,128)(2,1)} %copy-done, bf16[192,512]{1,0:T(8,128)(2,1)} %copy-done.4, bf16[192,512]{1,0:T(8,128)(2,1)} %copy-done.1, bf16[192,512]{1,0:T(8,128)(2,1)} %copy-done.2, ...), custom_call_target="tpu_custom_call" | custom-call | tf_op jit(solution)/shard_map/window_terms/pallas_call | solution.py:427
  44.9 2.1 %all-to-all-done.in_ref = bf16[8,208,128]{2,1,0:T(8,128)(2,1)S(1)} async-done(((bf16[8,208,128]{2,1,0:T(8,128)(2,1)}), bf16[8,208,128]{2,1,0:T(8,128)(2,1)S(1)}, u32[]{:S(2)}, u32[]{:S(2)}) %all-to-all-start) | async-done | bytes 426016 | tf_op jit(solution)/shard_map/all_to_all | solution.py:498
  47.0 0.5 compose_near.1
  47.6 5.5 %collective-permute-start.15 = (bf16[208,128]{1,0:T(8,128)(2,1)S(1)}, bf16[208,128]{1,0:T(8,128)(2,1)S(1)}, u32[]{:S(2)}, u32[]{:S(2)}) collective-permute-start(bf16[208,128]{1,0:T(8,128)(2,1)S(1)} %get-tuple-element.62.own), channel_id=1, source_target_pairs={{0,192},{64,0},{128,64},{192,128},{1,193},{65,1},{129,65},{193,129... | collective-permute-start | bytes 159752 | tf_op jit(solution)/shard_map/ppermute | solution.py:440
  53.0 1.4 %collective-permute-start.14 = (bf16[208,128]{1,0:T(8,128)(2,1)S(1)}, bf16[208,128]{1,0:T(8,128)(2,1)S(1)}, u32[]{:S(2)}, u32[]{:S(2)}) collective-permute-start(bf16[208,128]{1,0:T(8,128)(2,1)S(1)} %get-tuple-element.62.own), channel_id=1, source_target_pairs={{0,128},{64,192},{128,0},{192,64},{1,129},{65,193},{129,1},{193,65... | collective-permute-start | bytes 159752 | tf_op jit(solution)/shard_map/ppermute | solution.py:440
  54.5 2.4 %collective-permute-start.13 = (bf16[208,128]{1,0:T(8,128)(2,1)S(1)}, bf16[208,128]{1,0:T(8,128)(2,1)S(1)}, u32[]{:S(2)}, u32[]{:S(2)}) collective-permute-start(bf16[208,128]{1,0:T(8,128)(2,1)S(1)} %get-tuple-element.62.own), channel_id=1, source_target_pairs={{0,64},{64,128},{128,192},{192,0},{1,65},{65,129},{129,193},{193,1... | collective-permute-start | bytes 159752 | tf_op jit(solution)/shard_map/ppermute | solution.py:440
  56.9 4.6 %collective-permute-done.14.back2 = bf16[208,128]{1,0:T(8,128)(2,1)S(1)} collective-permute-done((bf16[208,128]{1,0:T(8,128)(2,1)S(1)}, bf16[208,128]{1,0:T(8,128)(2,1)S(1)}, u32[]{:S(2)}, u32[]{:S(2)}) %collective-permute-start.14) | collective-permute-done | bytes 53280 | tf_op jit(solution)/shard_map/ppermute | solution.py:440
  61.4 0.4 collective-permute-done.13.back1
  61.9 2.2 %spread_states.1 = (bf16[8,80,128]{2,1,0:T(8,128)(2,1)S(1)}, f32[4,192,128]{2,1,0:T(8,128)S(1)}, bf16[4,192,128]{2,1,0:T(8,128)(2,1)S(1)}, f32[4,192,128]{2,1,0:T(8,128)S(1)}) custom-call(f32[2,2]{1,0:T(2,128)S(1)} %copy-done.14, f32[2,2]{1,0:T(2,128)S(1)} %copy-done.15, bf16[208,128]{1,0:T(8,128)(2,1)S(1)} %get-tuple-element.62.own, ...), custom_call_target="tpu_custom_call" | custom-call | tf_op jit(solution)/shard_map/spread_states/pallas_call | solution.py:427
  64.1 10.2 %all_to_all.10.in_ref = bf16[8,80,128]{2,1,0:T(8,128)(2,1)S(1)} all-to-all(bf16[8,80,128]{2,1,0:T(8,128)(2,1)S(1)} %get-tuple-element.69), channel_id=1, replica_groups=mesh['zh'=4,'zl'=2,'x'=4,'y'=4,'c'=2] {'zl','x'}, dimensions={0} | all-to-all | bytes 327680 | tf_op jit(solution)/shard_map/all_to_all | solution.py:542
  74.3 1.0 %finish.1 = (bf16[2,192,256]{2,1,0:T(8,128)(2,1)}, bf16[2,2,4,128]{3,2,1,0:T(4,128)(2,1)}, f32[2,256]{1,0:T(2,128)}) custom-call(bf16[8,80,128]{2,1,0:T(8,128)(2,1)S(1)} %all_to_all.10.in_ref, f32[4,192,128]{2,1,0:T(8,128)S(1)} %get-tuple-element.70.out_ref, bf16[4,192,128]{2,1,0:T(8,128)(2,1)S(1)} %get-tuple-element.71.reach_ref, ...), custom_call_target="tpu_custom_call" | custom-call | tf_op jit(solution)/shard_map/finish/pallas_call | solution.py:427
  (53 shorter events, 0.2 us)
Async XLA Ops:
  0.6 12.2 %collective-permute-start.2 = (bf16[2,192,512]{2,1,0:T(8,128)(2,1)}, bf16[2,192,512]{2,1,0:T(8,128)(2,1)S(1)}, u32[]{:S(2)}, u32[]{:S(2)}) collective-permute-start(bf16[2,192,512]{2,1,0:T(8,128)(2,1)} %refs_0_.1), channel_id=1, source_target_pairs={{0,1},{1,0},{2,3},{3,2},{4,5},{5,4},{6,7},{7,6},{8,9},{9,8},{10,11... | collective-permute-start | bytes 1179656 | tf_op jit(solution)/shard_map/ppermute | solution.py:440
  1.8 7.9 %collective-permute-start.5 = (bf16[192,512]{1,0:T(8,128)(2,1)S(1)}, bf16[192,512]{1,0:T(8,128)(2,1)S(1)}, u32[]{:S(2)}, u32[]{:S(2)}) collective-permute-start(bf16[192,512]{1,0:T(8,128)(2,1)S(1)} %get-tuple-element.73), channel_id=1, source_target_pairs={{0,2},{2,4},{4,6},{6,0},{1,3},{3,5},{5,7},{7,1},{8,10},{10,12},{12... | collective-permute-start | bytes 589832 | tf_op jit(solution)/shard_map/ppermute | solution.py:440
  3.8 9.0 %collective-permute-start.6 = (bf16[192,512]{1,0:T(8,128)(2,1)S(1)}, bf16[192,512]{1,0:T(8,128)(2,1)S(1)}, u32[]{:S(2)}, u32[]{:S(2)}) collective-permute-start(bf16[192,512]{1,0:T(8,128)(2,1)S(1)} %get-tuple-element.74), channel_id=1, source_target_pairs={{0,6},{2,0},{4,2},{6,4},{1,7},{3,1},{5,3},{7,5},{8,14},{10,8},{12,... | collective-permute-start | bytes 589832 | tf_op jit(solution)/shard_map/ppermute | solution.py:440
  3.9 12.3 %collective-permute-start.1 = (bf16[192,512]{1,0:T(8,128)(2,1)S(1)}, bf16[192,512]{1,0:T(8,128)(2,1)S(1)}, u32[]{:S(2)}, u32[]{:S(2)}) collective-permute-start(bf16[192,512]{1,0:T(8,128)(2,1)S(1)} %get-tuple-element.73), channel_id=1, source_target_pairs={{0,6},{2,0},{4,2},{6,4},{1,7},{3,1},{5,3},{7,5},{8,14},{10,8},{12,... | collective-permute-start | bytes 589832 | tf_op jit(solution)/shard_map/ppermute | solution.py:440
  4.6 11.6 %collective-permute-start = (bf16[192,512]{1,0:T(8,128)(2,1)S(1)}, bf16[192,512]{1,0:T(8,128)(2,1)S(1)}, u32[]{:S(2)}, u32[]{:S(2)}) collective-permute-start(bf16[192,512]{1,0:T(8,128)(2,1)S(1)} %get-tuple-element.74), channel_id=1, source_target_pairs={{0,2},{2,4},{4,6},{6,0},{1,3},{3,5},{5,7},{7,1},{8,10},{10,12},{12... | collective-permute-start | bytes 589832 | tf_op jit(solution)/shard_map/ppermute | solution.py:440
  9.6 9.3 %copy-start.1 = (bf16[192,512]{1,0:T(8,128)(2,1)}, bf16[192,512]{1,0:T(8,128)(2,1)S(1)}, u32[]{:S(2)}) copy-start(bf16[192,512]{1,0:T(8,128)(2,1)S(1)} %collective-permute-done.5.refs_1_.refs_3_) | copy-start | bytes 589828
  9.6 7.4 %collective-permute-start.8 = (bf16[192,512]{1,0:T(8,128)(2,1)S(1)}, bf16[192,512]{1,0:T(8,128)(2,1)S(1)}, u32[]{:S(2)}, u32[]{:S(2)}) collective-permute-start(bf16[192,512]{1,0:T(8,128)(2,1)S(1)} %collective-permute-done.5.refs_1_.refs_3_), channel_id=1, source_target_pairs={{0,1},{1,0},{2,3},{3,2},{4,5},{5,4},{6,7},{7,6},{8,9},{9,8},{10,11... | collective-permute-start | bytes 589832 | tf_op jit(solution)/shard_map/ppermute | solution.py:440
  12.8 6.2 %copy-start.2 = (bf16[192,512]{1,0:T(8,128)(2,1)}, bf16[192,512]{1,0:T(8,128)(2,1)S(1)}, u32[]{:S(2)}) copy-start(bf16[192,512]{1,0:T(8,128)(2,1)S(1)} %collective-permute-done.6.refs_2_.refs_4_) | copy-start | bytes 589828
  12.8 6.1 %collective-permute-start.9 = (bf16[192,512]{1,0:T(8,128)(2,1)S(1)}, bf16[192,512]{1,0:T(8,128)(2,1)S(1)}, u32[]{:S(2)}, u32[]{:S(2)}) collective-permute-start(bf16[192,512]{1,0:T(8,128)(2,1)S(1)} %collective-permute-done.6.refs_2_.refs_4_), channel_id=1, source_target_pairs={{0,1},{1,0},{2,3},{3,2},{4,5},{5,4},{6,7},{7,6},{8,9},{9,8},{10,11... | collective-permute-start | bytes 589832 | tf_op jit(solution)/shard_map/ppermute | solution.py:440
  16.2 4.1 %copy-start.4 = (bf16[192,512]{1,0:T(8,128)(2,1)}, bf16[192,512]{1,0:T(8,128)(2,1)S(1)}, u32[]{:S(2)}) copy-start(bf16[192,512]{1,0:T(8,128)(2,1)S(1)} %collective-permute-done.refs_0_.refs_2_) | copy-start | bytes 589828
  16.2 10.6 %copy-start.19 = (f32[2]{0:T(128)S(1)}, f32[2]{0:T(128)}, u32[]{:S(2)}) copy-start(f32[2]{0:T(128)} %bias_ref.1) | copy-start | bytes 28
  16.2 10.6 %copy-start.20 = (f32[2]{0:T(128)S(1)}, f32[2]{0:T(128)}, u32[]{:S(2)}) copy-start(f32[2]{0:T(128)} %rate_ref.1) | copy-start | bytes 28
  16.3 2.6 %collective-permute-start.7 = (bf16[192,512]{1,0:T(8,128)(2,1)S(1)}, bf16[192,512]{1,0:T(8,128)(2,1)S(1)}, u32[]{:S(2)}, u32[]{:S(2)}) collective-permute-start(bf16[192,512]{1,0:T(8,128)(2,1)S(1)} %collective-permute-done.refs_0_.refs_2_), channel_id=1, source_target_pairs={{0,1},{1,0},{2,3},{3,2},{4,5},{5,4},{6,7},{7,6},{8,9},{9,8},{10,11... | collective-permute-start | bytes 589832 | tf_op jit(solution)/shard_map/ppermute | solution.py:440
  16.5 2.4 %collective-permute-start.10 = (bf16[192,512]{1,0:T(8,128)(2,1)S(1)}, bf16[192,512]{1,0:T(8,128)(2,1)S(1)}, u32[]{:S(2)}, u32[]{:S(2)}) collective-permute-start(bf16[192,512]{1,0:T(8,128)(2,1)S(1)} %collective-permute-done.1.refs_3_.refs_5_), channel_id=1, source_target_pairs={{0,1},{1,0},{2,3},{3,2},{4,5},{5,4},{6,7},{7,6},{8,9},{9,8},{10,11... | collective-permute-start | bytes 589832 | tf_op jit(solution)/shard_map/ppermute | solution.py:440
  16.9 7.0 %collective-permute-start.3 = (bf16[192,512]{1,0:T(8,128)(2,1)S(1)}, bf16[192,512]{1,0:T(8,128)(2,1)S(1)}, u32[]{:S(2)}, u32[]{:S(2)}) collective-permute-start(bf16[192,512]{1,0:T(8,128)(2,1)S(1)} %collective-permute-done.refs_0_.refs_2_), channel_id=1, source_target_pairs={{0,2},{2,4},{4,6},{6,0},{1,3},{3,5},{5,7},{7,1},{8,10},{10,12},{12... | collective-permute-start | bytes 589832 | tf_op jit(solution)/shard_map/ppermute | solution.py:440
  17.1 8.1 %collective-permute-start.4 = (bf16[192,512]{1,0:T(8,128)(2,1)S(1)}, bf16[192,512]{1,0:T(8,128)(2,1)S(1)}, u32[]{:S(2)}, u32[]{:S(2)}) collective-permute-start(bf16[192,512]{1,0:T(8,128)(2,1)S(1)} %collective-permute-done.1.refs_3_.refs_5_), channel_id=1, source_target_pairs={{0,6},{2,0},{4,2},{6,4},{1,7},{3,1},{5,3},{7,5},{8,14},{10,8},{12,... | collective-permute-start | bytes 589832 | tf_op jit(solution)/shard_map/ppermute | solution.py:440
  23.8 10.2 %copy-start.9 = (bf16[192,512]{1,0:T(8,128)(2,1)}, bf16[192,512]{1,0:T(8,128)(2,1)S(1)}, u32[]{:S(2)}) copy-start(bf16[192,512]{1,0:T(8,128)(2,1)S(1)} %collective-permute-done.3.refs_0_.refs_10_) | copy-start | bytes 589828
  25.1 8.9 %copy-start.10 = (bf16[192,512]{1,0:T(8,128)(2,1)}, bf16[192,512]{1,0:T(8,128)(2,1)S(1)}, u32[]{:S(2)}) copy-start(bf16[192,512]{1,0:T(8,128)(2,1)S(1)} %collective-permute-done.4.refs_1_.refs_11_) | copy-start | bytes 589828
  25.1 1.4 %collective-permute-start.11 = (bf16[192,512]{1,0:T(8,128)(2,1)S(1)}, bf16[192,512]{1,0:T(8,128)(2,1)S(1)}, u32[]{:S(2)}, u32[]{:S(2)}) collective-permute-start(bf16[192,512]{1,0:T(8,128)(2,1)S(1)} %collective-permute-done.3.refs_0_.refs_10_), channel_id=1, source_target_pairs={{0,1},{1,0},{2,3},{3,2},{4,5},{5,4},{6,7},{7,6},{8,9},{9,8},{10,11... | collective-permute-start | bytes 589832 | tf_op jit(solution)/shard_map/ppermute | solution.py:440
  25.1 1.7 %collective-permute-start.12 = (bf16[192,512]{1,0:T(8,128)(2,1)S(1)}, bf16[192,512]{1,0:T(8,128)(2,1)S(1)}, u32[]{:S(2)}, u32[]{:S(2)}) collective-permute-start(bf16[192,512]{1,0:T(8,128)(2,1)S(1)} %collective-permute-done.4.refs_1_.refs_11_), channel_id=1, source_target_pairs={{0,1},{1,0},{2,3},{3,2},{4,5},{5,4},{6,7},{7,6},{8,9},{9,8},{10,11... | collective-permute-start | bytes 589832 | tf_op jit(solution)/shard_map/ppermute | solution.py:440
  26.6 7.5 %copy-start.11 = (bf16[192,512]{1,0:T(8,128)(2,1)}, bf16[192,512]{1,0:T(8,128)(2,1)S(1)}, u32[]{:S(2)}) copy-start(bf16[192,512]{1,0:T(8,128)(2,1)S(1)} %collective-permute-done.11.refs_2_.refs_12_) | copy-start | bytes 589828
  26.9 7.2 %copy-start.12 = (bf16[192,512]{1,0:T(8,128)(2,1)}, bf16[192,512]{1,0:T(8,128)(2,1)S(1)}, u32[]{:S(2)}) copy-start(bf16[192,512]{1,0:T(8,128)(2,1)S(1)} %collective-permute-done.12.refs_3_.refs_13_) | copy-start | bytes 589828
  34.1 12.9 %all-to-all-start = ((bf16[8,208,128]{2,1,0:T(8,128)(2,1)}), bf16[8,208,128]{2,1,0:T(8,128)(2,1)S(1)}, u32[]{:S(2)}, u32[]{:S(2)}) async-start(bf16[8,208,128]{2,1,0:T(8,128)(2,1)} %get-tuple-element.54), calls=%async_computation | async-start | bytes 851968 | tf_op jit(solution)/shard_map/all_to_all | solution.py:498
  38.1 23.7 %copy-start.14 = (f32[2,2]{1,0:T(2,128)S(1)}, f32[2,2]{1,0:T(2,128)}, u32[]{:S(2)}) copy-start(f32[2,2]{1,0:T(2,128)} %beta_ref.1) | copy-start | bytes 52
  38.1 23.7 %copy-start.15 = (f32[2,2]{1,0:T(2,128)S(1)}, f32[2,2]{1,0:T(2,128)}, u32[]{:S(2)}) copy-start(f32[2,2]{1,0:T(2,128)} %decay_ref.1) | copy-start | bytes 52
  38.1 23.7 %copy-start.16 = (bf16[2,2,128]{2,1,0:T(2,128)(2,1)S(1)}, bf16[2,2,128]{2,1,0:T(2,128)(2,1)}, u32[]{:S(2)}) copy-start(bf16[2,2,128]{2,1,0:T(2,128)(2,1)} %query_ref.1) | copy-start | bytes 3076
  38.2 23.7 %copy-start.17 = (bf16[2,2,128]{2,1,0:T(2,128)(2,1)S(1)}, bf16[2,2,128]{2,1,0:T(2,128)(2,1)}, u32[]{:S(2)}) copy-start(bf16[2,2,128]{2,1,0:T(2,128)(2,1)} %key_ref.1) | copy-start | bytes 3076
  38.2 23.7 %copy-start.18 = (bf16[2,2,128]{2,1,0:T(2,128)(2,1)S(1)}, bf16[2,2,128]{2,1,0:T(2,128)(2,1)}, u32[]{:S(2)}) copy-start(bf16[2,2,128]{2,1,0:T(2,128)(2,1)} %value_ref.1) | copy-start | bytes 3076
  44.9 29.4 %copy-start.13 = (f32[128]{0:T(128)S(1)}, f32[128]{0:T(128)}, u32[]{:S(2)}) copy-start(f32[128]{0:T(128)} %param.24) | copy-start | bytes 1540
  47.6 9.3 %collective-permute-start.15 = (bf16[208,128]{1,0:T(8,128)(2,1)S(1)}, bf16[208,128]{1,0:T(8,128)(2,1)S(1)}, u32[]{:S(2)}, u32[]{:S(2)}) collective-permute-start(bf16[208,128]{1,0:T(8,128)(2,1)S(1)} %get-tuple-element.62.own), channel_id=1, source_target_pairs={{0,192},{64,0},{128,64},{192,128},{1,193},{65,1},{129,65},{193,129... | collective-permute-start | bytes 159752 | tf_op jit(solution)/shard_map/ppermute | solution.py:440
  53.0 8.4 %collective-permute-start.14 = (bf16[208,128]{1,0:T(8,128)(2,1)S(1)}, bf16[208,128]{1,0:T(8,128)(2,1)S(1)}, u32[]{:S(2)}, u32[]{:S(2)}) collective-permute-start(bf16[208,128]{1,0:T(8,128)(2,1)S(1)} %get-tuple-element.62.own), channel_id=1, source_target_pairs={{0,128},{64,192},{128,0},{192,64},{1,129},{65,193},{129,1},{193,65... | collective-permute-start | bytes 159752 | tf_op jit(solution)/shard_map/ppermute | solution.py:440
  54.5 7.4 %collective-permute-start.13 = (bf16[208,128]{1,0:T(8,128)(2,1)S(1)}, bf16[208,128]{1,0:T(8,128)(2,1)S(1)}, u32[]{:S(2)}, u32[]{:S(2)}) collective-permute-start(bf16[208,128]{1,0:T(8,128)(2,1)S(1)} %get-tuple-element.62.own), channel_id=1, source_target_pairs={{0,64},{64,128},{128,192},{192,0},{1,65},{65,129},{129,193},{193,1... | collective-permute-start | bytes 159752 | tf_op jit(solution)/shard_map/ppermute | solution.py:440
  (6 other events, 14.9 us)

commit v4 on v3

--- a/solution.py
+++ b/solution.py
@@ -1,3 +1,5 @@
+import functools
+
 import jax
 import jax.numpy as jnp
 from jax import lax
@@ -5,6 +7,7 @@
 from jax.experimental.pallas import tpu as pltpu
 from jax.sharding import Mesh
 from jax.sharding import PartitionSpec as P
+
 
 NEAR = ("zl", "x")
 AXES = ("zh", "zl", "x")
@@ -78,11 +81,13 @@
 
 def early_kernel(
     own, own_c, beta_w, decay_w, key_w, value_w, sum_ref, gate_ref, rest_ref, stacked_ref,
-    token_buffer, weight_buffer, sems,
+    token_buffer, weight_buffer, scalar_buffer, sems,
 ):
     depth = own.shape[-1]
     width = key_w.shape[-1]
     first = [pltpu.make_async_copy(own, token_buffer, sems.at[0])]
+    for at, weight in enumerate((beta_w, decay_w)):
+        first.append(pltpu.make_async_copy(weight, scalar_buffer.at[at], sems.at[0]))
     later = []
     for at, slot in enumerate(SLOTS):
         start = first_row(slot, depth)
@@ -97,10 +102,10 @@
                 later.append(pltpu.make_async_copy(source, to, sems.at[1]))
     for copy in first + later:
         copy.start()
-    rows = [ref[at : at + 1, :].astype(f32) for ref in (beta_w, decay_w) for at in range(2)]
-    stacked_ref[...] = row_pack(rows, stacked_ref.shape[-1]).astype(bf16)
     for copy in first:
         copy.wait()
+    rows = [scalar_buffer[at, h : h + 1, :].astype(f32) for at in range(2) for h in range(2)]
+    stacked_ref[...] = row_pack(rows, stacked_ref.shape[-1]).astype(bf16)
     total = gates = 0.0
     for at, piece in enumerate((token_buffer, own_c)):
         rows = piece[...].reshape(-1, depth)
@@ -122,9 +127,9 @@
     return total, gates
 
 
-def middle_kernel(*refs):
-    pieces, (sum_in, gate_in, rest, stacked, sum_ref, gate_ref) = refs[:8], refs[8:]
-    total, gates = add_pieces(pieces, 2, rest, stacked, sum_in[...], gate_in[...])
+def middle_kernel(first_slot, *refs):
+    pieces, (sum_in, gate_in, rest, stacked, sum_ref, gate_ref) = refs[:-6], refs[-6:]
+    total, gates = add_pieces(pieces, first_slot, rest, stacked, sum_in[...], gate_in[...])
     sum_ref[...] = total
     gate_ref[...] = gates
 
@@ -135,8 +140,8 @@
 
 
 def local_kernel(bias_ref, rate_ref, *refs):
-    pieces, (sum_in, gate_in, rest, stacked) = refs[:4], refs[4:8]
-    outputs, buffers, sems = refs[8:14], refs[14:20], refs[20]
+    pieces, (sum_in, gate_in, rest, stacked) = refs[:2], refs[2:6]
+    outputs, buffers, sems = refs[6:12], refs[12:18], refs[18]
     send_ref, key_ref, fresh_ref, carry_ref, cols_ref, rows_ref = buffers
     copies = []
 
@@ -149,7 +154,7 @@
 
     span = pieces[0].shape[0]
     head = send_ref.shape[-1]
-    total, gates = add_pieces(pieces, 6, rest, stacked, sum_in[...], gate_in[...])
+    total, gates = add_pieces(pieces, 7, rest, stacked, sum_in[...], gate_in[...])
     width = total.shape[-1] // 2
     key_rows = total[:, :width].astype(bf16)
     value_rows = total[:, width:].astype(bf16)
@@ -158,7 +163,6 @@
     strength = jax.nn.sigmoid(gates + lane_pair(bias_ref, 0))
     decays = -jnp.exp(lane_pair(rate_ref, 2)) * jax.nn.softplus(gates)
     wide = cols_ref.shape[1]
-    pairs = []
     lanes = iota((wide, head), 1)
     causal_wide = (iota((wide, wide), 0) >= iota((wide, wide), 1)).astype(bf16)
     for seq in range(2):
@@ -182,6 +186,7 @@
     give(5)
     t = iota((span, span), 0)
     s = iota((span, span), 1)
+    apart = t ^ s
     lower, inverse = [], []
     for pair in range(4):
         seq, h = divmod(pair, 2)
@@ -191,10 +196,10 @@
         spread = jnp.where(t >= s, col(2) - row(2), 0.0)
         alike = dot(keys, keys, ROWS) * (col(0) * col(4)) * row(4) * jnp.exp(spread)
         lower.append(jnp.where(t > s, alike, 0.0))
-        inverse.append(jnp.where(t // 2 == s // 2, lower[pair], 0.0))
+        inverse.append(jnp.where(apart < 2, lower[pair], 0.0))
     size = 2
     while size < span:
-        mask = (t // (2 * size) == s // (2 * size)) & (t // size != s // size)
+        mask = (apart >= size) & (apart < 2 * size)
         steps = []
         for pair in range(4):
             block = jnp.where(mask, lower[pair], 0.0)
@@ -323,14 +328,9 @@
 
 def spread_kernel(
     beta_ref, decay_ref, own, back1, back2, back3, maps_ref, adds_ref, factors_ref,
-    query_ref, key_ref, value_ref, out_in, reach_in, silu_in,
-    send_ref, out_ref, reach_ref, silu_ref, groups_ref, wide_ref, turned_ref, sems,
+    query_ref, key_ref, value_ref, send_ref, groups_ref, wide_ref, turned_ref,
 ):
-    moved = ((out_in, out_ref), (reach_in, reach_ref), (silu_in, silu_ref))
-    copies = [pltpu.make_async_copy(a, b, sems.at[at]) for at, (a, b) in enumerate(moved)]
-    for copy in copies:
-        copy.start()
-    rows, head = own.shape
+    _, head = own.shape
     half = head // 2
     far = lax.axis_index("zh")
     near = lax.axis_index("zl") * 4 + lax.axis_index("x")
@@ -387,6 +387,16 @@
         send_ref[member, :half, :] = entry.astype(bf16)
         pick = ((pick_row < 4) & (pick_col == 4 * member + pick_row)).astype(bf16)
         send_ref[member, half:, :] = (dot(pick, mine) + extra).astype(bf16)
+
+
+def load_kernel(_, *refs):
+    count = len(refs) // 2
+    sources, outputs, sems = refs[:count], refs[count : 2 * count], refs[2 * count]
+    copies = [
+        pltpu.make_async_copy(a, b, sems.at[at]) for at, (a, b) in enumerate(zip(sources, outputs))
+    ]
+    for copy in copies:
+        copy.start()
     for copy in copies:
         copy.wait()
 
@@ -415,7 +425,7 @@
     return pl.BlockSpec(memory_space=pltpu.SMEM)
 
 
-def kernel(body, name, outputs, kinds, args, scratch=(), limit=16):
+def kernel(body, outputs, kinds, args, scratch=(), limit=16):
     given = {"s": smem, "v": vmem, "p": vmem, "h": lambda: pl.BlockSpec(memory_space=pl.ANY)}
     placed = [
         arg
@@ -426,7 +436,6 @@
     plain = lambda out: pltpu.HBM(out.shape, out.dtype)
     return pl.pallas_call(
         body,
-        name=name,
         out_shape=tuple(out if kind == "p" else plain(out) for kind, out in outputs),
         in_specs=[given[kind]() for kind in kinds],
         out_specs=tuple(given[kind]() for kind, _ in outputs),
@@ -457,28 +466,42 @@
     first, second = tokens[0], tokens[1]
     up0 = shift(first, "y", 1)
     down1 = shift(second, "y", -1)
+    tokens_c, first, second = lax.optimization_barrier((tokens_c, first, second))
     up1 = shift(second, "y", 1)
     down0 = shift(first, "y", -1)
+    early_c, up0, down1 = lax.optimization_barrier((tokens_c, up0, down1))
     sums = [("p", on((2 * span, 2 * width), f32)), ("p", on((2 * span, head), f32))]
     early = kernel(
         early_kernel,
-        "early",
         sums + [("p", on((6 * depth, 2 * width), bf16)), ("p", on((PACK, 8 * depth), bf16))],
-        "hpvvhh",
-        (tokens, tokens_c, beta_weight.T, decay_weight.T, key_weight, value_weight),
-        (on((2, span, depth), bf16), on((2 * depth, 2 * width), bf16), dma((2,))),
-    )
-    up0, down1, *early = lax.optimization_barrier((up0, down1, *early))
+        "hphhhh",
+        (tokens, early_c, beta_weight.T, decay_weight.T, key_weight, value_weight),
+        (
+            on((2, span, depth), bf16),
+            on((2 * depth, 2 * width), bf16),
+            on((2, 2, 8 * depth), bf16),
+            dma((2,)),
+        ),
+    )
+    early = list(early)
     rest = early[2:]
     far0 = shift(up0, "y", 1)
     far1 = shift(down1, "y", -1)
+    up1, down0, *early[:2] = lax.optimization_barrier((up1, down0, *early[:2]))
     near = (up0, up1, down0, down1)
-    swapped = [swap(value) for value in near]
+    swapped = []
+    for value in near:
+        swapped.append(swap(value))
     middle = kernel(
-        middle_kernel, "middle", sums, "p" * 12, (*near, *swapped, *early[:2], *rest)
+        functools.partial(middle_kernel, 2), sums, "p" * 12, (*near, *swapped, *early[:2], *rest)
     )
     far0, far1, *middle = lax.optimization_barrier((far0, far1, *middle))
     last = [far0, far1, swap(far0), swap(far1)]
+    middle = kernel(
+        functools.partial(middle_kernel, 6), sums, "p" * 6, (far0, far1, *middle, *rest)
+    )
+    far_c0, far_c1, *middle = lax.optimization_barrier((*last[2:], *middle))
+    last[2:] = [far_c0, far_c1]
     local_shapes = [
         on((8, rows, head), bf16),
         on((2 * span, width), bf16),
@@ -489,10 +512,9 @@
     ]
     send, *shared = kernel(
         local_kernel,
-        "local_terms",
         [("h", out) for out in local_shapes],
-        "ss" + "p" * 8,
-        (beta_bias, rate_log, *last, *middle, *rest),
+        "ss" + "p" * 6,
+        (beta_bias, rate_log, *last[2:], *middle, *rest),
         (*local_shapes, dma((6,))),
     )
     arrived = lax.all_to_all(send, NEAR, 0, 0, tiled=True)
@@ -500,7 +522,6 @@
     finals = [on((4, span, head), f32), on((4, span, head), bf16), on((4, span, head), f32)]
     local_out, reach, silu = kernel(
         window_kernel,
-        "window_terms",
         [("v", out) for out in finals],
         "h" * 16 + "v" * 6,
         (tokens, tokens_c, *near, *swapped, *last, query_weight, gate_weight, gain, *shared),
@@ -515,7 +536,6 @@
     arrived, local_out = lax.optimization_barrier((arrived, local_out))
     total, maps, adds, factors = kernel(
         compose_kernel,
-        "compose_near",
         [
             ("p", on((rows, head), bf16)),
             ("p", on((7, head, head), bf16)),
@@ -526,23 +546,28 @@
         (arrived,),
     )
     others = [shift(total, "zh", by) for by in (1, 2, 3)]
-    back, *finals_in = kernel(
+    finals_in = kernel(
+        load_kernel,
+        [("p", out) for out in finals],
+        "phhh",
+        (total, local_out, reach, silu),
+        (dma((3,)),),
+    )
+    *others, loaded = lax.optimization_barrier((*others, finals_in[0]))
+    finals_in = (loaded, *finals_in[1:])
+    (back,) = kernel(
         spread_kernel,
-        "spread_states",
-        [("p", on((8, half + PACK, head), bf16)), *(("p", out) for out in finals)],
-        "ss" + "p" * 10 + "hhh",
+        [("p", on((8, half + PACK, head), bf16))],
+        "ss" + "p" * 10,
         (
             new_beta, new_decay, total, *others, maps, adds, factors,
-            new_query, new_key, new_value, local_out, reach, silu,
+            new_query, new_key, new_value,
         ),
-        (
-            on((4, rows, head), bf16), on((head, head), f32), on((head, head), f32), dma((3,)),
-        ),
+        (on((4, rows, head), bf16), on((head, head), f32), on((head, head), f32)),
     )
     returned = lax.all_to_all(back, NEAR, 0, 0, tiled=True)
     return kernel(
         finish_kernel,
-        "finish",
         [
             ("v", on((2, span, width), bf16)),
             ("v", on((2, 2, 4, head), bf16)),
@@ -565,6 +590,7 @@
         P(None, tp), P(None, tp),
     )
     out_specs = (P(None, sp, tp), P(None, tp, sp, None), P(None, tp))
+
     return jax.shard_map(
         shards, mesh=torus, in_specs=in_specs, out_specs=out_specs, check_vma=False
     )

time: 75.7 us -> 76.7 us (1.013)
  starting transfers between devices: 21.9 us -> 25 us
  waiting for transfers between devices: 19 us -> 17.4 us
    all_to_all x1, starting transfers between devices: 4.03 us -> 5.66 us  [shards(): arrived = lax.all_to_all(send, NEAR, 0, 0, tiled=True)]
    ppermute x16, waiting for transfers between devices: 16.9 us -> 15.3 us  [shift(): lax.ppermute(value, axis, [(at, (at + by) % length) for at in range(lengt...]
    ppermute x16, starting transfers between devices: 17.9 us -> 19.4 us  [shift(): lax.ppermute(value, axis, [(at, (at + by) % length) for at in range(lengt...]
    pallas_call x7 -> x9, Pallas kernels: 22.2 us -> 21.7 us  [kernel(): pl.pallas_call(body, out_shape=tuple((out if kind == 'p' else plain(out)...]
  transfers between devices with their start and end apart: 17 -> 17, of which waited for: 10 -> 10; matrix products, arithmetic and copies ran while one was open for 1% -> 1% of each run, Pallas kernels for 15% -> 16%
where the time goes in v4:
time: 76.7 us; the launch traced here: 76.4 us
  starting transfers between devices  25 us (33%)
  Pallas kernels  21.7 us (28%)
  waiting for transfers between devices  17.4 us (23%)
  blocking collectives  10.2 us (13%)
  local copies, waits for them, and re-layouts  1.14 us (1%)
  between operations  0.95 us (1%)
    pallas_call x9, Pallas kernels, kernel(): pl.pallas_call(body, out_shape=tuple((out if kind == 'p' else plain(out)...  21.7 us
    ppermute x16, starting transfers between devices, shift(): lax.ppermute(value, axis, [(at, (at + by) % length) for at in range(lengt...  19.4 us
    ppermute x16, waiting for transfers between devices, shift(): lax.ppermute(value, axis, [(at, (at + by) % length) for at in range(lengt...  15.3 us
    all_to_all x1, blocking collectives, shards(): returned = lax.all_to_all(back, NEAR, 0, 0, tiled=True)  10.2 us
    all_to_all x1, starting transfers between devices, shards(): arrived = lax.all_to_all(send, NEAR, 0, 0, tiled=True)  5.66 us
    all_to_all x1, waiting for transfers between devices, shards(): arrived = lax.all_to_all(send, NEAR, 0, 0, tiled=True)  2.09 us
  transfers between devices with their start and end apart: 17, of which 10 were waited for; matrix products, arithmetic and copies ran while one was open for 1% of the time, Pallas kernels for 16%

profile of v4, /device:TPU:24, one launch (start us, length us, event | category | flops | bytes accessed | tf_op | source)
XLA Modules:
  0.0 76.4 jit_solution(14333559332407798213)
XLA Ops:
  0.7 1.0 %slice_bitcast_fusion = (bf16[192,512]{1,0:T(8,128)(2,1)S(1)}, bf16[192,512]{1,0:T(8,128)(2,1)S(1)}) fusion(bf16[2,192,512]{2,1,0:T(8,128)(2,1)} %refs_0_.1), kind=kLoop, calls=%fused_computation | loop fusion | bytes 786432 | tf_op jit(solution)/shard_map/squeeze | solution.py:466
  1.8 0.8 %collective-permute-start.2 = (bf16[192,512]{1,0:T(8,128)(2,1)S(1)}, bf16[192,512]{1,0:T(8,128)(2,1)S(1)}, u32[]{:S(2)}, u32[]{:S(2)}) collective-permute-start(bf16[192,512]{1,0:T(8,128)(2,1)S(1)} %get-tuple-element.54), channel_id=1, source_target_pairs={{0,6},{2,0},{4,2},{6,4},{1,7},{3,1},{5,3},{7,5},{8,14},{10,8},{12,... | collective-permute-start | bytes 589832 | tf_op jit(solution)/shard_map/ppermute | solution.py:449
  2.6 2.5 %collective-permute-start.1 = (bf16[192,512]{1,0:T(8,128)(2,1)S(1)}, bf16[192,512]{1,0:T(8,128)(2,1)S(1)}, u32[]{:S(2)}, u32[]{:S(2)}) collective-permute-start(bf16[192,512]{1,0:T(8,128)(2,1)S(1)} %get-tuple-element.55), channel_id=1, source_target_pairs={{0,2},{2,4},{4,6},{6,0},{1,3},{3,5},{5,7},{7,1},{8,10},{10,12},{12... | collective-permute-start | bytes 589832 | tf_op jit(solution)/shard_map/ppermute | solution.py:449
  5.1 0.7 collective-permute-start.5
  5.8 1.3 %collective-permute-start.6 = (bf16[192,512]{1,0:T(8,128)(2,1)S(1)}, bf16[192,512]{1,0:T(8,128)(2,1)S(1)}, u32[]{:S(2)}, u32[]{:S(2)}) collective-permute-start(bf16[192,512]{1,0:T(8,128)(2,1)S(1)} %get-tuple-element.55), channel_id=1, source_target_pairs={{0,6},{2,0},{4,2},{6,4},{1,7},{3,1},{5,3},{7,5},{8,14},{10,8},{12,... | collective-permute-start | bytes 589832 | tf_op jit(solution)/shard_map/ppermute | solution.py:449
  7.1 3.7 %collective-permute-done.2.refs_3_.refs_5_ = bf16[192,512]{1,0:T(8,128)(2,1)S(1)} collective-permute-done((bf16[192,512]{1,0:T(8,128)(2,1)S(1)}, bf16[192,512]{1,0:T(8,128)(2,1)S(1)}, u32[]{:S(2)}, u32[]{:S(2)}) %collective-permute-start.2) | collective-permute-done | bytes 196640 | tf_op jit(solution)/shard_map/ppermute | solution.py:449
  11.0 0.5 collective-permute-start.10
  11.4 2.3 %shard_map.166 = (f32[384,512]{1,0:T(8,128)S(1)}, f32[384,128]{1,0:T(8,128)S(1)}, bf16[3072,512]{1,0:T(8,128)(2,1)S(1)}, bf16[16,4096]{1,0:T(8,128)(2,1)S(1)}) custom-call(bf16[2,192,512]{2,1,0:T(8,128)(2,1)} %refs_0_.1, bf16[2,192,512]{2,1,0:T(8,128)(2,1)S(1)} %collective-permute-done.own_c.refs_1_, bf16[2,4096]{1,0:T(2,128)(2,1)} %bitcast.9, ...), custom_call_target="tpu_custom_call" | custom-call | tf_op jit(solution)/shard_map/pallas_call | solution.py:437
  13.9 0.7 collective-permute-done.6.refs_2_.refs_4_
  14.6 0.5 collective-permute-start.9
  15.1 3.0 %collective-permute-start.3 = (bf16[192,512]{1,0:T(8,128)(2,1)S(1)}, bf16[192,512]{1,0:T(8,128)(2,1)S(1)}, u32[]{:S(2)}, u32[]{:S(2)}) collective-permute-start(bf16[192,512]{1,0:T(8,128)(2,1)S(1)} %collective-permute-done.1.refs_0_.refs_2_), channel_id=1, source_target_pairs={{0,2},{2,4},{4,6},{6,0},{1,3},{3,5},{5,7},{7,1},{8,10},{10,12},{12... | collective-permute-start | bytes 589832 | tf_op jit(solution)/shard_map/ppermute | solution.py:449
  18.2 1.4 %shard_map.167 = (f32[384,512]{1,0:T(8,128)S(1)}, f32[384,128]{1,0:T(8,128)S(1)}) custom-call(bf16[192,512]{1,0:T(8,128)(2,1)S(1)} %collective-permute-done.1.refs_0_.refs_2_, bf16[192,512]{1,0:T(8,128)(2,1)S(1)} %collective-permute-done.5.refs_1_.refs_3_, bf16[192,512]{1,0:T(8,128)(2,1)S(1)} %collective-permute-done.6.refs_2_.refs_4_, ...), custom_call_target="tpu_custom_call" | custom-call | tf_op jit(solution)/shard_map/pallas_call | solution.py:437
  19.7 2.9 %collective-permute-done.3.refs_0_.refs_10_ = bf16[192,512]{1,0:T(8,128)(2,1)S(1)} collective-permute-done((bf16[192,512]{1,0:T(8,128)(2,1)S(1)}, bf16[192,512]{1,0:T(8,128)(2,1)S(1)}, u32[]{:S(2)}, u32[]{:S(2)}) %collective-permute-start.3) | collective-permute-done | bytes 196640 | tf_op jit(solution)/shard_map/ppermute | solution.py:449
  22.6 3.4 %collective-permute-done.4.refs_1_.refs_11_ = bf16[192,512]{1,0:T(8,128)(2,1)S(1)} collective-permute-done((bf16[192,512]{1,0:T(8,128)(2,1)S(1)}, bf16[192,512]{1,0:T(8,128)(2,1)S(1)}, u32[]{:S(2)}, u32[]{:S(2)}) %collective-permute-start.4) | collective-permute-done | bytes 196640 | tf_op jit(solution)/shard_map/ppermute | solution.py:449
  26.0 0.5 collective-permute-start.12
  26.5 0.5 shard_map.168
  27.0 0.4 collective-permute-done.11.refs_0_.refs_12_
  27.4 0.3 collective-permute-done.12.refs_1_.refs_13_
  27.7 6.8 %shard_map.169 = (bf16[8,208,128]{2,1,0:T(8,128)(2,1)}, bf16[384,256]{1,0:T(8,128)(2,1)}, bf16[4,192,128]{2,1,0:T(8,128)(2,1)}, bf16[4,192,128]{2,1,0:T(8,128)(2...) custom-call(f32[2]{0:T(128)S(1)} %copy-done.19, f32[2]{0:T(128)S(1)} %copy-done.20, ...), custom_call_target="tpu_custom_call" | custom-call | tf_op jit(solution)/shard_map/pallas_call | solution.py:437
  34.5 5.7 %all-to-all-start = ((bf16[8,208,128]{2,1,0:T(8,128)(2,1)}), bf16[8,208,128]{2,1,0:T(8,128)(2,1)S(1)}, u32[]{:S(2)}, u32[]{:S(2)}) async-start(bf16[8,208,128]{2,1,0:T(8,128)(2,1)} %get-tuple-element.77), calls=%async_computation | async-start | bytes 851968 | tf_op jit(solution)/shard_map/all_to_all | solution.py:520
  40.2 6.7 %shard_map.170 = (f32[4,192,128]{2,1,0:T(8,128)}, bf16[4,192,128]{2,1,0:T(8,128)(2,1)}, f32[4,192,128]{2,1,0:T(8,128)}) custom-call(bf16[2,192,512]{2,1,0:T(8,128)(2,1)} %refs_0_.1, bf16[2,192,512]{2,1,0:T(8,128)(2,1)} %copy-done, bf16[192,512]{1,0:T(8,128)(2,1)} %copy-done.2, bf16[192,512]{1,0:T(8,128)(2,1)} %copy-done.3, bf16[192,512]{1,0:T(8,128)(2,1)} %copy-done.4, ...), custom_call_target="tpu_custom_call" | custom-call | tf_op jit(solution)/shard_map/pallas_call | solution.py:437
  47.0 2.1 %all-to-all-done.in_ref = bf16[8,208,128]{2,1,0:T(8,128)(2,1)S(1)} async-done(((bf16[8,208,128]{2,1,0:T(8,128)(2,1)}), bf16[8,208,128]{2,1,0:T(8,128)(2,1)S(1)}, u32[]{:S(2)}, u32[]{:S(2)}) %all-to-all-start) | async-done | bytes 426016 | tf_op jit(solution)/shard_map/all_to_all | solution.py:520
  49.1 0.5 shard_map.171
  49.6 5.5 %collective-permute-start.15 = (bf16[208,128]{1,0:T(8,128)(2,1)S(1)}, bf16[208,128]{1,0:T(8,128)(2,1)S(1)}, u32[]{:S(2)}, u32[]{:S(2)}) collective-permute-start(bf16[208,128]{1,0:T(8,128)(2,1)S(1)} %get-tuple-element.85._.own), channel_id=1, source_target_pairs={{0,192},{64,0},{128,64},{192,128},{1,193},{65,1},{129,65},{193,129... | collective-permute-start | bytes 159752 | tf_op jit(solution)/shard_map/ppermute | solution.py:449
  55.1 1.4 %collective-permute-start.14 = (bf16[208,128]{1,0:T(8,128)(2,1)S(1)}, bf16[208,128]{1,0:T(8,128)(2,1)S(1)}, u32[]{:S(2)}, u32[]{:S(2)}) collective-permute-start(bf16[208,128]{1,0:T(8,128)(2,1)S(1)} %get-tuple-element.85._.own), channel_id=1, source_target_pairs={{0,128},{64,192},{128,0},{192,64},{1,129},{65,193},{129,1},{193,65... | collective-permute-start | bytes 159752 | tf_op jit(solution)/shard_map/ppermute | solution.py:449
  56.5 2.4 %collective-permute-start.13 = (bf16[208,128]{1,0:T(8,128)(2,1)S(1)}, bf16[208,128]{1,0:T(8,128)(2,1)S(1)}, u32[]{:S(2)}, u32[]{:S(2)}) collective-permute-start(bf16[208,128]{1,0:T(8,128)(2,1)S(1)} %get-tuple-element.85._.own), channel_id=1, source_target_pairs={{0,64},{64,128},{128,192},{192,0},{1,65},{65,129},{129,193},{193,1... | collective-permute-start | bytes 159752 | tf_op jit(solution)/shard_map/ppermute | solution.py:449
  58.9 1.2 %shard_map.172 = (f32[4,192,128]{2,1,0:T(8,128)S(1)}, bf16[4,192,128]{2,1,0:T(8,128)(2,1)S(1)}, f32[4,192,128]{2,1,0:T(8,128)S(1)}) custom-call(bf16[208,128]{1,0:T(8,128)(2,1)S(1)} %get-tuple-element.85._.own, f32[4,192,128]{2,1,0:T(8,128)} %get-tuple-element.86.refs_0_, bf16[4,192,128]{2,1,0:T(8,128)(2,1)} %get-tuple-element.87.refs_1_, ...), custom_call_target="tpu_custom_call" | custom-call | tf_op jit(solution)/shard_map/pallas_call | solution.py:437
  60.2 3.3 %collective-permute-done.14.back2 = bf16[208,128]{1,0:T(8,128)(2,1)S(1)} collective-permute-done((bf16[208,128]{1,0:T(8,128)(2,1)S(1)}, bf16[208,128]{1,0:T(8,128)(2,1)S(1)}, u32[]{:S(2)}, u32[]{:S(2)}) %collective-permute-start.14) | collective-permute-done | bytes 53280 | tf_op jit(solution)/shard_map/ppermute | solution.py:449
  63.5 0.4 collective-permute-done.13.back1
  63.9 1.3 %shard_map.173 = bf16[8,80,128]{2,1,0:T(8,128)(2,1)S(1)} custom-call(f32[2,2]{1,0:T(2,128)S(1)} %copy-done.14, f32[2,2]{1,0:T(2,128)S(1)} %copy-done.15, bf16[208,128]{1,0:T(8,128)(2,1)S(1)} %get-tuple-element.85._.own, bf16[208,128]{1,0:T(8,128)(2,1)S(1)} %collective-permute-done.13.back1, bf16[208,128]{1,0:T(8,128)(2,1)S(1)} %collective-permute-done.14.back2, ...), custom_call_target="tpu_custom_call" | custom-call | tf_op jit(solution)/shard_map/pallas_call | solution.py:437
  65.2 10.2 %all_to_all.10.in_ref = bf16[8,80,128]{2,1,0:T(8,128)(2,1)S(1)} all-to-all(bf16[8,80,128]{2,1,0:T(8,128)(2,1)S(1)} %shard_map.173), channel_id=1, replica_groups=mesh['zh'=4,'zl'=2,'x'=4,'y'=4,'c'=2] {'zl','x'}, dimensions={0} | all-to-all | bytes 327680 | tf_op jit(solution)/shard_map/all_to_all | solution.py:568
  75.4 1.0 %shard_map.174 = (bf16[2,192,256]{2,1,0:T(8,128)(2,1)}, bf16[2,2,4,128]{3,2,1,0:T(4,128)(2,1)}, f32[2,256]{1,0:T(2,128)}) custom-call(bf16[8,80,128]{2,1,0:T(8,128)(2,1)S(1)} %all_to_all.10.in_ref, f32[4,192,128]{2,1,0:T(8,128)S(1)} %get-tuple-element.96.out_ref, bf16[4,192,128]{2,1,0:T(8,128)(2,1)S(1)} %get-tuple-element.97.reach_ref, ...), custom_call_target="tpu_custom_call" | custom-call | tf_op jit(solution)/shard_map/pallas_call | solution.py:437
  (55 shorter events, 0.4 us)
Async XLA Ops:
  0.6 4.5 %collective-permute-start = (bf16[2,192,512]{2,1,0:T(8,128)(2,1)}, bf16[2,192,512]{2,1,0:T(8,128)(2,1)S(1)}, u32[]{:S(2)}, u32[]{:S(2)}) collective-permute-start(bf16[2,192,512]{2,1,0:T(8,128)(2,1)} %refs_0_.1), channel_id=1, source_target_pairs={{0,1},{1,0},{2,3},{3,2},{4,5},{5,4},{6,7},{7,6},{8,9},{9,8},{10,11... | collective-permute-start | bytes 1179656 | tf_op jit(solution)/shard_map/ppermute | solution.py:449
  1.8 9.1 %collective-permute-start.2 = (bf16[192,512]{1,0:T(8,128)(2,1)S(1)}, bf16[192,512]{1,0:T(8,128)(2,1)S(1)}, u32[]{:S(2)}, u32[]{:S(2)}) collective-permute-start(bf16[192,512]{1,0:T(8,128)(2,1)S(1)} %get-tuple-element.54), channel_id=1, source_target_pairs={{0,6},{2,0},{4,2},{6,4},{1,7},{3,1},{5,3},{7,5},{8,14},{10,8},{12,... | collective-permute-start | bytes 589832 | tf_op jit(solution)/shard_map/ppermute | solution.py:449
  2.6 8.2 %collective-permute-start.1 = (bf16[192,512]{1,0:T(8,128)(2,1)S(1)}, bf16[192,512]{1,0:T(8,128)(2,1)S(1)}, u32[]{:S(2)}, u32[]{:S(2)}) collective-permute-start(bf16[192,512]{1,0:T(8,128)(2,1)S(1)} %get-tuple-element.55), channel_id=1, source_target_pairs={{0,2},{2,4},{4,6},{6,0},{1,3},{3,5},{5,7},{7,1},{8,10},{10,12},{12... | collective-permute-start | bytes 589832 | tf_op jit(solution)/shard_map/ppermute | solution.py:449
  5.1 8.7 %copy-start = (bf16[2,192,512]{2,1,0:T(8,128)(2,1)}, bf16[2,192,512]{2,1,0:T(8,128)(2,1)S(1)}, u32[]{:S(2)}) copy-start(bf16[2,192,512]{2,1,0:T(8,128)(2,1)S(1)} %collective-permute-done.own_c.refs_1_) | copy-start | bytes 1179652
  5.1 8.7 %collective-permute-start.5 = (bf16[192,512]{1,0:T(8,128)(2,1)S(1)}, bf16[192,512]{1,0:T(8,128)(2,1)S(1)}, u32[]{:S(2)}, u32[]{:S(2)}) collective-permute-start(bf16[192,512]{1,0:T(8,128)(2,1)S(1)} %get-tuple-element.54), channel_id=1, source_target_pairs={{0,2},{2,4},{4,6},{6,0},{1,3},{3,5},{5,7},{7,1},{8,10},{10,12},{12... | collective-permute-start | bytes 589832 | tf_op jit(solution)/shard_map/ppermute | solution.py:449
  5.8 8.8 %collective-permute-start.6 = (bf16[192,512]{1,0:T(8,128)(2,1)S(1)}, bf16[192,512]{1,0:T(8,128)(2,1)S(1)}, u32[]{:S(2)}, u32[]{:S(2)}) collective-permute-start(bf16[192,512]{1,0:T(8,128)(2,1)S(1)} %get-tuple-element.55), channel_id=1, source_target_pairs={{0,6},{2,0},{4,2},{6,4},{1,7},{3,1},{5,3},{7,5},{8,14},{10,8},{12,... | collective-permute-start | bytes 589832 | tf_op jit(solution)/shard_map/ppermute | solution.py:449
  10.8 7.4 %copy-start.1 = (bf16[192,512]{1,0:T(8,128)(2,1)}, bf16[192,512]{1,0:T(8,128)(2,1)S(1)}, u32[]{:S(2)}) copy-start(bf16[192,512]{1,0:T(8,128)(2,1)S(1)} %collective-permute-done.2.refs_3_.refs_5_) | copy-start | bytes 589828
  10.9 7.4 %copy-start.2 = (bf16[192,512]{1,0:T(8,128)(2,1)}, bf16[192,512]{1,0:T(8,128)(2,1)S(1)}, u32[]{:S(2)}) copy-start(bf16[192,512]{1,0:T(8,128)(2,1)S(1)} %collective-permute-done.1.refs_0_.refs_2_) | copy-start | bytes 589828
  10.9 7.3 %collective-permute-start.7 = (bf16[192,512]{1,0:T(8,128)(2,1)S(1)}, bf16[192,512]{1,0:T(8,128)(2,1)S(1)}, u32[]{:S(2)}, u32[]{:S(2)}) collective-permute-start(bf16[192,512]{1,0:T(8,128)(2,1)S(1)} %collective-permute-done.1.refs_0_.refs_2_), channel_id=1, source_target_pairs={{0,1},{1,0},{2,3},{3,2},{4,5},{5,4},{6,7},{7,6},{8,9},{9,8},{10,11... | collective-permute-start | bytes 589832 | tf_op jit(solution)/shard_map/ppermute | solution.py:449
  11.0 7.2 %collective-permute-start.10 = (bf16[192,512]{1,0:T(8,128)(2,1)S(1)}, bf16[192,512]{1,0:T(8,128)(2,1)S(1)}, u32[]{:S(2)}, u32[]{:S(2)}) collective-permute-start(bf16[192,512]{1,0:T(8,128)(2,1)S(1)} %collective-permute-done.2.refs_3_.refs_5_), channel_id=1, source_target_pairs={{0,1},{1,0},{2,3},{3,2},{4,5},{5,4},{6,7},{7,6},{8,9},{9,8},{10,11... | collective-permute-start | bytes 589832 | tf_op jit(solution)/shard_map/ppermute | solution.py:449
  13.8 5.8 %copy-start.3 = (bf16[192,512]{1,0:T(8,128)(2,1)}, bf16[192,512]{1,0:T(8,128)(2,1)S(1)}, u32[]{:S(2)}) copy-start(bf16[192,512]{1,0:T(8,128)(2,1)S(1)} %collective-permute-done.5.refs_1_.refs_3_) | copy-start | bytes 589828
  14.6 5.0 %copy-start.4 = (bf16[192,512]{1,0:T(8,128)(2,1)}, bf16[192,512]{1,0:T(8,128)(2,1)S(1)}, u32[]{:S(2)}) copy-start(bf16[192,512]{1,0:T(8,128)(2,1)S(1)} %collective-permute-done.6.refs_2_.refs_4_) | copy-start | bytes 589828
  14.6 3.6 %collective-permute-start.8 = (bf16[192,512]{1,0:T(8,128)(2,1)S(1)}, bf16[192,512]{1,0:T(8,128)(2,1)S(1)}, u32[]{:S(2)}, u32[]{:S(2)}) collective-permute-start(bf16[192,512]{1,0:T(8,128)(2,1)S(1)} %collective-permute-done.5.refs_1_.refs_3_), channel_id=1, source_target_pairs={{0,1},{1,0},{2,3},{3,2},{4,5},{5,4},{6,7},{7,6},{8,9},{9,8},{10,11... | collective-permute-start | bytes 589832 | tf_op jit(solution)/shard_map/ppermute | solution.py:449
  14.6 3.6 %collective-permute-start.9 = (bf16[192,512]{1,0:T(8,128)(2,1)S(1)}, bf16[192,512]{1,0:T(8,128)(2,1)S(1)}, u32[]{:S(2)}, u32[]{:S(2)}) collective-permute-start(bf16[192,512]{1,0:T(8,128)(2,1)S(1)} %collective-permute-done.6.refs_2_.refs_4_), channel_id=1, source_target_pairs={{0,1},{1,0},{2,3},{3,2},{4,5},{5,4},{6,7},{7,6},{8,9},{9,8},{10,11... | collective-permute-start | bytes 589832 | tf_op jit(solution)/shard_map/ppermute | solution.py:449
  15.1 7.5 %collective-permute-start.3 = (bf16[192,512]{1,0:T(8,128)(2,1)S(1)}, bf16[192,512]{1,0:T(8,128)(2,1)S(1)}, u32[]{:S(2)}, u32[]{:S(2)}) collective-permute-start(bf16[192,512]{1,0:T(8,128)(2,1)S(1)} %collective-permute-done.1.refs_0_.refs_2_), channel_id=1, source_target_pairs={{0,2},{2,4},{4,6},{6,0},{1,3},{3,5},{5,7},{7,1},{8,10},{10,12},{12... | collective-permute-start | bytes 589832 | tf_op jit(solution)/shard_map/ppermute | solution.py:449
  18.1 7.8 %collective-permute-start.4 = (bf16[192,512]{1,0:T(8,128)(2,1)S(1)}, bf16[192,512]{1,0:T(8,128)(2,1)S(1)}, u32[]{:S(2)}, u32[]{:S(2)}) collective-permute-start(bf16[192,512]{1,0:T(8,128)(2,1)S(1)} %collective-permute-done.2.refs_3_.refs_5_), channel_id=1, source_target_pairs={{0,6},{2,0},{4,2},{6,4},{1,7},{3,1},{5,3},{7,5},{8,14},{10,8},{12,... | collective-permute-start | bytes 589832 | tf_op jit(solution)/shard_map/ppermute | solution.py:449
  22.6 4.4 %copy-start.9 = (bf16[192,512]{1,0:T(8,128)(2,1)}, bf16[192,512]{1,0:T(8,128)(2,1)S(1)}, u32[]{:S(2)}) copy-start(bf16[192,512]{1,0:T(8,128)(2,1)S(1)} %collective-permute-done.3.refs_0_.refs_10_) | copy-start | bytes 589828
  26.0 1.7 %copy-start.20 = (f32[2]{0:T(128)S(1)}, f32[2]{0:T(128)}, u32[]{:S(2)}) copy-start(f32[2]{0:T(128)} %rate_ref.1) | copy-start | bytes 28
  26.0 1.4 %collective-permute-start.11 = (bf16[192,512]{1,0:T(8,128)(2,1)S(1)}, bf16[192,512]{1,0:T(8,128)(2,1)S(1)}, u32[]{:S(2)}, u32[]{:S(2)}) collective-permute-start(bf16[192,512]{1,0:T(8,128)(2,1)S(1)} %collective-permute-done.3.refs_0_.refs_10_), channel_id=1, source_target_pairs={{0,1},{1,0},{2,3},{3,2},{4,5},{5,4},{6,7},{7,6},{8,9},{9,8},{10,11... | collective-permute-start | bytes 589832 | tf_op jit(solution)/shard_map/ppermute | solution.py:449
  26.0 1.7 %collective-permute-start.12 = (bf16[192,512]{1,0:T(8,128)(2,1)S(1)}, bf16[192,512]{1,0:T(8,128)(2,1)S(1)}, u32[]{:S(2)}, u32[]{:S(2)}) collective-permute-start(bf16[192,512]{1,0:T(8,128)(2,1)S(1)} %collective-permute-done.4.refs_1_.refs_11_), channel_id=1, source_target_pairs={{0,1},{1,0},{2,3},{3,2},{4,5},{5,4},{6,7},{7,6},{8,9},{9,8},{10,11... | collective-permute-start | bytes 589832 | tf_op jit(solution)/shard_map/ppermute | solution.py:449
  27.4 7.0 %copy-start.11 = (bf16[192,512]{1,0:T(8,128)(2,1)}, bf16[192,512]{1,0:T(8,128)(2,1)S(1)}, u32[]{:S(2)}) copy-start(bf16[192,512]{1,0:T(8,128)(2,1)S(1)} %collective-permute-done.11.refs_0_.refs_12_) | copy-start | bytes 589828
  27.7 6.8 %copy-start.12 = (bf16[192,512]{1,0:T(8,128)(2,1)}, bf16[192,512]{1,0:T(8,128)(2,1)S(1)}, u32[]{:S(2)}) copy-start(bf16[192,512]{1,0:T(8,128)(2,1)S(1)} %collective-permute-done.12.refs_1_.refs_13_) | copy-start | bytes 589828
  34.5 14.6 %all-to-all-start = ((bf16[8,208,128]{2,1,0:T(8,128)(2,1)}), bf16[8,208,128]{2,1,0:T(8,128)(2,1)S(1)}, u32[]{:S(2)}, u32[]{:S(2)}) async-start(bf16[8,208,128]{2,1,0:T(8,128)(2,1)} %get-tuple-element.77), calls=%async_computation | async-start | bytes 851968 | tf_op jit(solution)/shard_map/all_to_all | solution.py:520
  40.2 23.7 %copy-start.14 = (f32[2,2]{1,0:T(2,128)S(1)}, f32[2,2]{1,0:T(2,128)}, u32[]{:S(2)}) copy-start(f32[2,2]{1,0:T(2,128)} %beta_ref.1) | copy-start | bytes 52
  40.2 23.7 %copy-start.15 = (f32[2,2]{1,0:T(2,128)S(1)}, f32[2,2]{1,0:T(2,128)}, u32[]{:S(2)}) copy-start(f32[2,2]{1,0:T(2,128)} %decay_ref.1) | copy-start | bytes 52
  40.2 23.7 %copy-start.16 = (bf16[2,2,128]{2,1,0:T(2,128)(2,1)S(1)}, bf16[2,2,128]{2,1,0:T(2,128)(2,1)}, u32[]{:S(2)}) copy-start(bf16[2,2,128]{2,1,0:T(2,128)(2,1)} %query_ref.1) | copy-start | bytes 3076
  40.2 23.7 %copy-start.17 = (bf16[2,2,128]{2,1,0:T(2,128)(2,1)S(1)}, bf16[2,2,128]{2,1,0:T(2,128)(2,1)}, u32[]{:S(2)}) copy-start(bf16[2,2,128]{2,1,0:T(2,128)(2,1)} %key_ref.1) | copy-start | bytes 3076
  40.2 23.7 %copy-start.18 = (bf16[2,2,128]{2,1,0:T(2,128)(2,1)S(1)}, bf16[2,2,128]{2,1,0:T(2,128)(2,1)}, u32[]{:S(2)}) copy-start(bf16[2,2,128]{2,1,0:T(2,128)(2,1)} %value_ref.1) | copy-start | bytes 3076
  47.0 28.4 %copy-start.13 = (f32[128]{0:T(128)S(1)}, f32[128]{0:T(128)}, u32[]{:S(2)}) copy-start(f32[128]{0:T(128)} %param.24) | copy-start | bytes 1540
  49.6 10.5 %collective-permute-start.15 = (bf16[208,128]{1,0:T(8,128)(2,1)S(1)}, bf16[208,128]{1,0:T(8,128)(2,1)S(1)}, u32[]{:S(2)}, u32[]{:S(2)}) collective-permute-start(bf16[208,128]{1,0:T(8,128)(2,1)S(1)} %get-tuple-element.85._.own), channel_id=1, source_target_pairs={{0,192},{64,0},{128,64},{192,128},{1,193},{65,1},{129,65},{193,129... | collective-permute-start | bytes 159752 | tf_op jit(solution)/shard_map/ppermute | solution.py:449
  55.1 8.4 %collective-permute-start.14 = (bf16[208,128]{1,0:T(8,128)(2,1)S(1)}, bf16[208,128]{1,0:T(8,128)(2,1)S(1)}, u32[]{:S(2)}, u32[]{:S(2)}) collective-permute-start(bf16[208,128]{1,0:T(8,128)(2,1)S(1)} %get-tuple-element.85._.own), channel_id=1, source_target_pairs={{0,128},{64,192},{128,0},{192,64},{1,129},{65,193},{129,1},{193,65... | collective-permute-start | bytes 159752 | tf_op jit(solution)/shard_map/ppermute | solution.py:449
  56.5 7.4 %collective-permute-start.13 = (bf16[208,128]{1,0:T(8,128)(2,1)S(1)}, bf16[208,128]{1,0:T(8,128)(2,1)S(1)}, u32[]{:S(2)}, u32[]{:S(2)}) collective-permute-start(bf16[208,128]{1,0:T(8,128)(2,1)S(1)} %get-tuple-element.85._.own), channel_id=1, source_target_pairs={{0,64},{64,128},{128,192},{192,0},{1,65},{65,129},{129,193},{193,1... | collective-permute-start | bytes 159752 | tf_op jit(solution)/shard_map/ppermute | solution.py:449
  (6 other events, 8.7 us)

commit v5 on v4

--- a/solution.py
+++ b/solution.py
@@ -466,16 +466,12 @@
     first, second = tokens[0], tokens[1]
     up0 = shift(first, "y", 1)
     down1 = shift(second, "y", -1)
-    tokens_c, first, second = lax.optimization_barrier((tokens_c, first, second))
-    up1 = shift(second, "y", 1)
-    down0 = shift(first, "y", -1)
-    early_c, up0, down1 = lax.optimization_barrier((tokens_c, up0, down1))
     sums = [("p", on((2 * span, 2 * width), f32)), ("p", on((2 * span, head), f32))]
     early = kernel(
         early_kernel,
         sums + [("p", on((6 * depth, 2 * width), bf16)), ("p", on((PACK, 8 * depth), bf16))],
         "hphhhh",
-        (tokens, early_c, beta_weight.T, decay_weight.T, key_weight, value_weight),
+        (tokens, tokens_c, beta_weight.T, decay_weight.T, key_weight, value_weight),
         (
             on((2, span, depth), bf16),
             on((2 * depth, 2 * width), bf16),
@@ -484,10 +480,12 @@
         ),
     )
     early = list(early)
+    first, second, *early[:2] = lax.optimization_barrier((first, second, *early[:2]))
+    up1 = shift(second, "y", 1)
+    down0 = shift(first, "y", -1)
     rest = early[2:]
     far0 = shift(up0, "y", 1)
     far1 = shift(down1, "y", -1)
-    up1, down0, *early[:2] = lax.optimization_barrier((up1, down0, *early[:2]))
     near = (up0, up1, down0, down1)
     swapped = []
     for value in near:

time: 76.7 us -> 76.6 us (level)
  the two profiles are of different devices: /device:TPU:24 before, /device:TPU:2 now
where the time goes in v5:
time: 76.6 us; the launch traced here: 76.3 us
  starting transfers between devices  25.1 us (33%)
  Pallas kernels  21.9 us (29%)
  waiting for transfers between devices  16.9 us (22%)
  blocking collectives  10.4 us (14%)
  local copies, waits for them, and re-layouts  1.14 us (1%)
  between operations  0.93 us (1%)
    pallas_call x9, Pallas kernels, kernel(): pl.pallas_call(body, out_shape=tuple((out if kind == 'p' else plain(out)...  21.9 us
    ppermute x16, starting transfers between devices, shift(): lax.ppermute(value, axis, [(at, (at + by) % length) for at in range(lengt...  18.9 us
    ppermute x16, waiting for transfers between devices, shift(): lax.ppermute(value, axis, [(at, (at + by) % length) for at in range(lengt...  16.3 us
    all_to_all x1, blocking collectives, shards(): returned = lax.all_to_all(back, NEAR, 0, 0, tiled=True)  10.4 us
    all_to_all x1, starting transfers between devices, shards(): arrived = lax.all_to_all(send, NEAR, 0, 0, tiled=True)  6.19 us
  transfers between devices with their start and end apart: 17, of which 9 were waited for; matrix products, arithmetic and copies ran while one was open for 1% of the time, Pallas kernels for 16%

profile of v5, /device:TPU:2, one launch (start us, length us, event | category | flops | bytes accessed | tf_op | source)
XLA Modules:
  0.0 76.3 jit_solution(8843236128346011985)
XLA Ops:
  0.6 0.1 collective-permute-start.4
  0.7 1.0 %slice_bitcast_fusion = (bf16[192,512]{1,0:T(8,128)(2,1)S(1)}, bf16[192,512]{1,0:T(8,128)(2,1)S(1)}) fusion(bf16[2,192,512]{2,1,0:T(8,128)(2,1)} %refs_0_.1), kind=kLoop, calls=%fused_computation | loop fusion | bytes 786432 | tf_op jit(solution)/shard_map/squeeze | solution.py:466
  1.8 3.1 %collective-permute-start.2 = (bf16[192,512]{1,0:T(8,128)(2,1)S(1)}, bf16[192,512]{1,0:T(8,128)(2,1)S(1)}, u32[]{:S(2)}, u32[]{:S(2)}) collective-permute-start(bf16[192,512]{1,0:T(8,128)(2,1)S(1)} %get-tuple-element.47), channel_id=1, source_target_pairs={{0,6},{2,0},{4,2},{6,4},{1,7},{3,1},{5,3},{7,5},{8,14},{10,8},{12,... | collective-permute-start | bytes 589832 | tf_op jit(solution)/shard_map/ppermute | solution.py:449
  4.9 2.4 %shard_map.166 = (f32[384,512]{1,0:T(8,128)S(1)}, f32[384,128]{1,0:T(8,128)S(1)}, bf16[3072,512]{1,0:T(8,128)(2,1)S(1)}, bf16[16,4096]{1,0:T(8,128)(2,1)S(1)}) custom-call(bf16[2,192,512]{2,1,0:T(8,128)(2,1)} %refs_0_.1, bf16[2,192,512]{2,1,0:T(8,128)(2,1)S(1)} %collective-permute-done.4.own_c.refs_1_, bf16[2,4096]{1,0:T(2,128)(2,1)} %bitcast.9, ...), custom_call_target="tpu_custom_call" | custom-call | tf_op jit(solution)/shard_map/pallas_call | solution.py:437
  7.3 0.7 collective-permute-start.5
  8.0 2.7 %collective-permute-start.6 = (bf16[192,512]{1,0:T(8,128)(2,1)S(1)}, bf16[192,512]{1,0:T(8,128)(2,1)S(1)}, u32[]{:S(2)}, u32[]{:S(2)}) collective-permute-start(bf16[192,512]{1,0:T(8,128)(2,1)S(1)} %get-tuple-element.48), channel_id=1, source_target_pairs={{0,6},{2,0},{4,2},{6,4},{1,7},{3,1},{5,3},{7,5},{8,14},{10,8},{12,... | collective-permute-start | bytes 589832 | tf_op jit(solution)/shard_map/ppermute | solution.py:449
  10.8 3.1 %collective-permute-done.refs_0_.refs_2_ = bf16[192,512]{1,0:T(8,128)(2,1)S(1)} collective-permute-done((bf16[192,512]{1,0:T(8,128)(2,1)S(1)}, bf16[192,512]{1,0:T(8,128)(2,1)S(1)}, u32[]{:S(2)}, u32[]{:S(2)}) %collective-permute-start) | collective-permute-done | bytes 196640 | tf_op jit(solution)/shard_map/ppermute | solution.py:449
  13.9 3.5 %collective-permute-done.5.refs_1_.refs_3_ = bf16[192,512]{1,0:T(8,128)(2,1)S(1)} collective-permute-done((bf16[192,512]{1,0:T(8,128)(2,1)S(1)}, bf16[192,512]{1,0:T(8,128)(2,1)S(1)}, u32[]{:S(2)}, u32[]{:S(2)}) %collective-permute-start.5) | collective-permute-done | bytes 196640 | tf_op jit(solution)/shard_map/ppermute | solution.py:449
  17.3 0.5 collective-permute-start.9
  17.8 0.9 %collective-permute-start.3 = (bf16[192,512]{1,0:T(8,128)(2,1)S(1)}, bf16[192,512]{1,0:T(8,128)(2,1)S(1)}, u32[]{:S(2)}, u32[]{:S(2)}) collective-permute-start(bf16[192,512]{1,0:T(8,128)(2,1)S(1)} %collective-permute-done.2.refs_3_.refs_5_), channel_id=1, source_target_pairs={{0,6},{2,0},{4,2},{6,4},{1,7},{3,1},{5,3},{7,5},{8,14},{10,8},{12,... | collective-permute-start | bytes 589832 | tf_op jit(solution)/shard_map/ppermute | solution.py:449
  18.7 1.2 %collective-permute-start.1 = (bf16[192,512]{1,0:T(8,128)(2,1)S(1)}, bf16[192,512]{1,0:T(8,128)(2,1)S(1)}, u32[]{:S(2)}, u32[]{:S(2)}) collective-permute-start(bf16[192,512]{1,0:T(8,128)(2,1)S(1)} %collective-permute-done.refs_0_.refs_2_), channel_id=1, source_target_pairs={{0,2},{2,4},{4,6},{6,0},{1,3},{3,5},{5,7},{7,1},{8,10},{10,12},{12... | collective-permute-start | bytes 589832 | tf_op jit(solution)/shard_map/ppermute | solution.py:449
  19.9 1.4 %shard_map.167 = (f32[384,512]{1,0:T(8,128)S(1)}, f32[384,128]{1,0:T(8,128)S(1)}) custom-call(bf16[192,512]{1,0:T(8,128)(2,1)S(1)} %collective-permute-done.refs_0_.refs_2_, bf16[192,512]{1,0:T(8,128)(2,1)S(1)} %collective-permute-done.5.refs_1_.refs_3_, bf16[192,512]{1,0:T(8,128)(2,1)S(1)} %collective-permute-done.6.refs_2_.refs_4_, ...), custom_call_target="tpu_custom_call" | custom-call | tf_op jit(solution)/shard_map/pallas_call | solution.py:437
  21.4 3.4 %collective-permute-done.3.refs_1_.refs_11_ = bf16[192,512]{1,0:T(8,128)(2,1)S(1)} collective-permute-done((bf16[192,512]{1,0:T(8,128)(2,1)S(1)}, bf16[192,512]{1,0:T(8,128)(2,1)S(1)}, u32[]{:S(2)}, u32[]{:S(2)}) %collective-permute-start.3) | collective-permute-done | bytes 196640 | tf_op jit(solution)/shard_map/ppermute | solution.py:449
  24.7 2.2 %collective-permute-done.1.refs_0_.refs_10_ = bf16[192,512]{1,0:T(8,128)(2,1)S(1)} collective-permute-done((bf16[192,512]{1,0:T(8,128)(2,1)S(1)}, bf16[192,512]{1,0:T(8,128)(2,1)S(1)}, u32[]{:S(2)}, u32[]{:S(2)}) %collective-permute-start.1) | collective-permute-done | bytes 196640 | tf_op jit(solution)/shard_map/ppermute | solution.py:449
  27.0 0.5 collective-permute-start.12
  27.5 0.5 shard_map.168
  28.0 0.4 collective-permute-done.11.refs_0_.refs_12_
  28.4 0.3 collective-permute-done.12.refs_1_.refs_13_
  28.7 6.8 %shard_map.169 = (bf16[8,208,128]{2,1,0:T(8,128)(2,1)}, bf16[384,256]{1,0:T(8,128)(2,1)}, bf16[4,192,128]{2,1,0:T(8,128)(2,1)}, bf16[4,192,128]{2,1,0:T(8,128)(2...) custom-call(f32[2]{0:T(128)S(1)} %copy-done.19, f32[2]{0:T(128)S(1)} %copy-done.20, ...), custom_call_target="tpu_custom_call" | custom-call | tf_op jit(solution)/shard_map/pallas_call | solution.py:437
  35.5 6.2 %all-to-all-start = ((bf16[8,208,128]{2,1,0:T(8,128)(2,1)}), bf16[8,208,128]{2,1,0:T(8,128)(2,1)S(1)}, u32[]{:S(2)}, u32[]{:S(2)}) async-start(bf16[8,208,128]{2,1,0:T(8,128)(2,1)} %get-tuple-element.65), calls=%async_computation | async-start | bytes 851968 | tf_op jit(solution)/shard_map/all_to_all | solution.py:518
  41.7 6.8 %shard_map.170 = (f32[4,192,128]{2,1,0:T(8,128)}, bf16[4,192,128]{2,1,0:T(8,128)(2,1)}, f32[4,192,128]{2,1,0:T(8,128)}) custom-call(bf16[2,192,512]{2,1,0:T(8,128)(2,1)} %refs_0_.1, bf16[2,192,512]{2,1,0:T(8,128)(2,1)} %copy-done, bf16[192,512]{1,0:T(8,128)(2,1)} %copy-done.2, bf16[192,512]{1,0:T(8,128)(2,1)} %copy-done.3, bf16[192,512]{1,0:T(8,128)(2,1)} %copy-done.4, ...), custom_call_target="tpu_custom_call" | custom-call | tf_op jit(solution)/shard_map/pallas_call | solution.py:437
  48.5 0.5 all-to-all-done.in_ref
  49.0 0.5 shard_map.171
  49.5 5.5 %collective-permute-start.15 = (bf16[208,128]{1,0:T(8,128)(2,1)S(1)}, bf16[208,128]{1,0:T(8,128)(2,1)S(1)}, u32[]{:S(2)}, u32[]{:S(2)}) collective-permute-start(bf16[208,128]{1,0:T(8,128)(2,1)S(1)} %get-tuple-element.73._.own), channel_id=1, source_target_pairs={{0,192},{64,0},{128,64},{192,128},{1,193},{65,1},{129,65},{193,129... | collective-permute-start | bytes 159752 | tf_op jit(solution)/shard_map/ppermute | solution.py:449
  55.0 1.4 %collective-permute-start.14 = (bf16[208,128]{1,0:T(8,128)(2,1)S(1)}, bf16[208,128]{1,0:T(8,128)(2,1)S(1)}, u32[]{:S(2)}, u32[]{:S(2)}) collective-permute-start(bf16[208,128]{1,0:T(8,128)(2,1)S(1)} %get-tuple-element.73._.own), channel_id=1, source_target_pairs={{0,128},{64,192},{128,0},{192,64},{1,129},{65,193},{129,1},{193,65... | collective-permute-start | bytes 159752 | tf_op jit(solution)/shard_map/ppermute | solution.py:449
  56.5 2.4 %collective-permute-start.13 = (bf16[208,128]{1,0:T(8,128)(2,1)S(1)}, bf16[208,128]{1,0:T(8,128)(2,1)S(1)}, u32[]{:S(2)}, u32[]{:S(2)}) collective-permute-start(bf16[208,128]{1,0:T(8,128)(2,1)S(1)} %get-tuple-element.73._.own), channel_id=1, source_target_pairs={{0,64},{64,128},{128,192},{192,0},{1,65},{65,129},{129,193},{193,1... | collective-permute-start | bytes 159752 | tf_op jit(solution)/shard_map/ppermute | solution.py:449
  58.8 1.2 %shard_map.172 = (f32[4,192,128]{2,1,0:T(8,128)S(1)}, bf16[4,192,128]{2,1,0:T(8,128)(2,1)S(1)}, f32[4,192,128]{2,1,0:T(8,128)S(1)}) custom-call(bf16[208,128]{1,0:T(8,128)(2,1)S(1)} %get-tuple-element.73._.own, f32[4,192,128]{2,1,0:T(8,128)} %get-tuple-element.74.refs_0_, bf16[4,192,128]{2,1,0:T(8,128)(2,1)} %get-tuple-element.75.refs_1_, ...), custom_call_target="tpu_custom_call" | custom-call | tf_op jit(solution)/shard_map/pallas_call | solution.py:437
  60.1 3.0 %collective-permute-done.14.back2 = bf16[208,128]{1,0:T(8,128)(2,1)S(1)} collective-permute-done((bf16[208,128]{1,0:T(8,128)(2,1)S(1)}, bf16[208,128]{1,0:T(8,128)(2,1)S(1)}, u32[]{:S(2)}, u32[]{:S(2)}) %collective-permute-start.14) | collective-permute-done | bytes 53280 | tf_op jit(solution)/shard_map/ppermute | solution.py:449
  63.1 0.5 collective-permute-done.13.back1
  63.6 1.3 %shard_map.173 = bf16[8,80,128]{2,1,0:T(8,128)(2,1)S(1)} custom-call(f32[2,2]{1,0:T(2,128)S(1)} %copy-done.14, f32[2,2]{1,0:T(2,128)S(1)} %copy-done.15, bf16[208,128]{1,0:T(8,128)(2,1)S(1)} %get-tuple-element.73._.own, bf16[208,128]{1,0:T(8,128)(2,1)S(1)} %collective-permute-done.13.back1, bf16[208,128]{1,0:T(8,128)(2,1)S(1)} %collective-permute-done.14.back2, ...), custom_call_target="tpu_custom_call" | custom-call | tf_op jit(solution)/shard_map/pallas_call | solution.py:437
  64.9 10.4 %all_to_all.10.in_ref = bf16[8,80,128]{2,1,0:T(8,128)(2,1)S(1)} all-to-all(bf16[8,80,128]{2,1,0:T(8,128)(2,1)S(1)} %shard_map.173), channel_id=1, replica_groups=mesh['zh'=4,'zl'=2,'x'=4,'y'=4,'c'=2] {'zl','x'}, dimensions={0} | all-to-all | bytes 327680 | tf_op jit(solution)/shard_map/all_to_all | solution.py:566
  75.3 1.0 %shard_map.174 = (bf16[2,192,256]{2,1,0:T(8,128)(2,1)}, bf16[2,2,4,128]{3,2,1,0:T(4,128)(2,1)}, f32[2,256]{1,0:T(2,128)}) custom-call(bf16[8,80,128]{2,1,0:T(8,128)(2,1)S(1)} %all_to_all.10.in_ref, f32[4,192,128]{2,1,0:T(8,128)S(1)} %get-tuple-element.84.out_ref, bf16[4,192,128]{2,1,0:T(8,128)(2,1)S(1)} %get-tuple-element.85.reach_ref, ...), custom_call_target="tpu_custom_call" | custom-call | tf_op jit(solution)/shard_map/pallas_call | solution.py:437
  (55 shorter events, 0.1 us)
Async XLA Ops:
  0.6 4.3 %collective-permute-start.4 = (bf16[2,192,512]{2,1,0:T(8,128)(2,1)}, bf16[2,192,512]{2,1,0:T(8,128)(2,1)S(1)}, u32[]{:S(2)}, u32[]{:S(2)}) collective-permute-start(bf16[2,192,512]{2,1,0:T(8,128)(2,1)} %refs_0_.1), channel_id=1, source_target_pairs={{0,1},{1,0},{2,3},{3,2},{4,5},{5,4},{6,7},{7,6},{8,9},{9,8},{10,11... | collective-permute-start | bytes 1179656 | tf_op jit(solution)/shard_map/ppermute | solution.py:449
  1.8 9.0 %collective-permute-start.2 = (bf16[192,512]{1,0:T(8,128)(2,1)S(1)}, bf16[192,512]{1,0:T(8,128)(2,1)S(1)}, u32[]{:S(2)}, u32[]{:S(2)}) collective-permute-start(bf16[192,512]{1,0:T(8,128)(2,1)S(1)} %get-tuple-element.47), channel_id=1, source_target_pairs={{0,6},{2,0},{4,2},{6,4},{1,7},{3,1},{5,3},{7,5},{8,14},{10,8},{12,... | collective-permute-start | bytes 589832 | tf_op jit(solution)/shard_map/ppermute | solution.py:449
  4.9 9.0 %collective-permute-start = (bf16[192,512]{1,0:T(8,128)(2,1)S(1)}, bf16[192,512]{1,0:T(8,128)(2,1)S(1)}, u32[]{:S(2)}, u32[]{:S(2)}) collective-permute-start(bf16[192,512]{1,0:T(8,128)(2,1)S(1)} %get-tuple-element.48), channel_id=1, source_target_pairs={{0,2},{2,4},{4,6},{6,0},{1,3},{3,5},{5,7},{7,1},{8,10},{10,12},{12... | collective-permute-start | bytes 589832 | tf_op jit(solution)/shard_map/ppermute | solution.py:449
  4.9 2.5 %copy-start = (bf16[2,192,512]{2,1,0:T(8,128)(2,1)}, bf16[2,192,512]{2,1,0:T(8,128)(2,1)S(1)}, u32[]{:S(2)}) copy-start(bf16[2,192,512]{2,1,0:T(8,128)(2,1)S(1)} %collective-permute-done.4.own_c.refs_1_) | copy-start | bytes 1179652
  7.3 10.0 %collective-permute-start.5 = (bf16[192,512]{1,0:T(8,128)(2,1)S(1)}, bf16[192,512]{1,0:T(8,128)(2,1)S(1)}, u32[]{:S(2)}, u32[]{:S(2)}) collective-permute-start(bf16[192,512]{1,0:T(8,128)(2,1)S(1)} %get-tuple-element.47), channel_id=1, source_target_pairs={{0,2},{2,4},{4,6},{6,0},{1,3},{3,5},{5,7},{7,1},{8,10},{10,12},{12... | collective-permute-start | bytes 589832 | tf_op jit(solution)/shard_map/ppermute | solution.py:449
  8.0 9.3 %collective-permute-start.6 = (bf16[192,512]{1,0:T(8,128)(2,1)S(1)}, bf16[192,512]{1,0:T(8,128)(2,1)S(1)}, u32[]{:S(2)}, u32[]{:S(2)}) collective-permute-start(bf16[192,512]{1,0:T(8,128)(2,1)S(1)} %get-tuple-element.48), channel_id=1, source_target_pairs={{0,6},{2,0},{4,2},{6,4},{1,7},{3,1},{5,3},{7,5},{8,14},{10,8},{12,... | collective-permute-start | bytes 589832 | tf_op jit(solution)/shard_map/ppermute | solution.py:449
  10.7 10.6 %copy-start.1 = (bf16[192,512]{1,0:T(8,128)(2,1)}, bf16[192,512]{1,0:T(8,128)(2,1)S(1)}, u32[]{:S(2)}) copy-start(bf16[192,512]{1,0:T(8,128)(2,1)S(1)} %collective-permute-done.2.refs_3_.refs_5_) | copy-start | bytes 589828
  10.7 8.0 %collective-permute-start.10 = (bf16[192,512]{1,0:T(8,128)(2,1)S(1)}, bf16[192,512]{1,0:T(8,128)(2,1)S(1)}, u32[]{:S(2)}, u32[]{:S(2)}) collective-permute-start(bf16[192,512]{1,0:T(8,128)(2,1)S(1)} %collective-permute-done.2.refs_3_.refs_5_), channel_id=1, source_target_pairs={{0,1},{1,0},{2,3},{3,2},{4,5},{5,4},{6,7},{7,6},{8,9},{9,8},{10,11... | collective-permute-start | bytes 589832 | tf_op jit(solution)/shard_map/ppermute | solution.py:449
  13.9 7.4 %copy-start.2 = (bf16[192,512]{1,0:T(8,128)(2,1)}, bf16[192,512]{1,0:T(8,128)(2,1)S(1)}, u32[]{:S(2)}) copy-start(bf16[192,512]{1,0:T(8,128)(2,1)S(1)} %collective-permute-done.refs_0_.refs_2_) | copy-start | bytes 589828
  13.9 6.0 %collective-permute-start.7 = (bf16[192,512]{1,0:T(8,128)(2,1)S(1)}, bf16[192,512]{1,0:T(8,128)(2,1)S(1)}, u32[]{:S(2)}, u32[]{:S(2)}) collective-permute-start(bf16[192,512]{1,0:T(8,128)(2,1)S(1)} %collective-permute-done.refs_0_.refs_2_), channel_id=1, source_target_pairs={{0,1},{1,0},{2,3},{3,2},{4,5},{5,4},{6,7},{7,6},{8,9},{9,8},{10,11... | collective-permute-start | bytes 589832 | tf_op jit(solution)/shard_map/ppermute | solution.py:449
  17.3 4.0 %copy-start.3 = (bf16[192,512]{1,0:T(8,128)(2,1)}, bf16[192,512]{1,0:T(8,128)(2,1)S(1)}, u32[]{:S(2)}) copy-start(bf16[192,512]{1,0:T(8,128)(2,1)S(1)} %collective-permute-done.5.refs_1_.refs_3_) | copy-start | bytes 589828
  17.3 2.6 %collective-permute-start.8 = (bf16[192,512]{1,0:T(8,128)(2,1)S(1)}, bf16[192,512]{1,0:T(8,128)(2,1)S(1)}, u32[]{:S(2)}, u32[]{:S(2)}) collective-permute-start(bf16[192,512]{1,0:T(8,128)(2,1)S(1)} %collective-permute-done.5.refs_1_.refs_3_), channel_id=1, source_target_pairs={{0,1},{1,0},{2,3},{3,2},{4,5},{5,4},{6,7},{7,6},{8,9},{9,8},{10,11... | collective-permute-start | bytes 589832 | tf_op jit(solution)/shard_map/ppermute | solution.py:449
  17.3 4.0 %copy-start.4 = (bf16[192,512]{1,0:T(8,128)(2,1)}, bf16[192,512]{1,0:T(8,128)(2,1)S(1)}, u32[]{:S(2)}) copy-start(bf16[192,512]{1,0:T(8,128)(2,1)S(1)} %collective-permute-done.6.refs_2_.refs_4_) | copy-start | bytes 589828
  17.3 2.6 %collective-permute-start.9 = (bf16[192,512]{1,0:T(8,128)(2,1)S(1)}, bf16[192,512]{1,0:T(8,128)(2,1)S(1)}, u32[]{:S(2)}, u32[]{:S(2)}) collective-permute-start(bf16[192,512]{1,0:T(8,128)(2,1)S(1)} %collective-permute-done.6.refs_2_.refs_4_), channel_id=1, source_target_pairs={{0,1},{1,0},{2,3},{3,2},{4,5},{5,4},{6,7},{7,6},{8,9},{9,8},{10,11... | collective-permute-start | bytes 589832 | tf_op jit(solution)/shard_map/ppermute | solution.py:449
  17.8 6.9 %collective-permute-start.3 = (bf16[192,512]{1,0:T(8,128)(2,1)S(1)}, bf16[192,512]{1,0:T(8,128)(2,1)S(1)}, u32[]{:S(2)}, u32[]{:S(2)}) collective-permute-start(bf16[192,512]{1,0:T(8,128)(2,1)S(1)} %collective-permute-done.2.refs_3_.refs_5_), channel_id=1, source_target_pairs={{0,6},{2,0},{4,2},{6,4},{1,7},{3,1},{5,3},{7,5},{8,14},{10,8},{12,... | collective-permute-start | bytes 589832 | tf_op jit(solution)/shard_map/ppermute | solution.py:449
  18.7 2.6 %copy-start.5 = (bf16[192,512]{1,0:T(8,128)(2,1)}, bf16[192,512]{1,0:T(8,128)(2,1)S(1)}, u32[]{:S(2)}) copy-start(bf16[192,512]{1,0:T(8,128)(2,1)S(1)} %collective-permute-done.10.refs_7_.refs_9_) | copy-start | bytes 589828
  18.7 8.2 %collective-permute-start.1 = (bf16[192,512]{1,0:T(8,128)(2,1)S(1)}, bf16[192,512]{1,0:T(8,128)(2,1)S(1)}, u32[]{:S(2)}, u32[]{:S(2)}) collective-permute-start(bf16[192,512]{1,0:T(8,128)(2,1)S(1)} %collective-permute-done.refs_0_.refs_2_), channel_id=1, source_target_pairs={{0,2},{2,4},{4,6},{6,0},{1,3},{3,5},{5,7},{7,1},{8,10},{10,12},{12... | collective-permute-start | bytes 589832 | tf_op jit(solution)/shard_map/ppermute | solution.py:449
  24.7 3.2 %copy-start.9 = (bf16[192,512]{1,0:T(8,128)(2,1)}, bf16[192,512]{1,0:T(8,128)(2,1)S(1)}, u32[]{:S(2)}) copy-start(bf16[192,512]{1,0:T(8,128)(2,1)S(1)} %collective-permute-done.3.refs_1_.refs_11_) | copy-start | bytes 589828
  27.0 1.4 %collective-permute-start.11 = (bf16[192,512]{1,0:T(8,128)(2,1)S(1)}, bf16[192,512]{1,0:T(8,128)(2,1)S(1)}, u32[]{:S(2)}, u32[]{:S(2)}) collective-permute-start(bf16[192,512]{1,0:T(8,128)(2,1)S(1)} %collective-permute-done.1.refs_0_.refs_10_), channel_id=1, source_target_pairs={{0,1},{1,0},{2,3},{3,2},{4,5},{5,4},{6,7},{7,6},{8,9},{9,8},{10,11... | collective-permute-start | bytes 589832 | tf_op jit(solution)/shard_map/ppermute | solution.py:449
  27.0 1.7 %collective-permute-start.12 = (bf16[192,512]{1,0:T(8,128)(2,1)S(1)}, bf16[192,512]{1,0:T(8,128)(2,1)S(1)}, u32[]{:S(2)}, u32[]{:S(2)}) collective-permute-start(bf16[192,512]{1,0:T(8,128)(2,1)S(1)} %collective-permute-done.3.refs_1_.refs_11_), channel_id=1, source_target_pairs={{0,1},{1,0},{2,3},{3,2},{4,5},{5,4},{6,7},{7,6},{8,9},{9,8},{10,11... | collective-permute-start | bytes 589832 | tf_op jit(solution)/shard_map/ppermute | solution.py:449
  28.4 7.1 %copy-start.11 = (bf16[192,512]{1,0:T(8,128)(2,1)}, bf16[192,512]{1,0:T(8,128)(2,1)S(1)}, u32[]{:S(2)}) copy-start(bf16[192,512]{1,0:T(8,128)(2,1)S(1)} %collective-permute-done.11.refs_0_.refs_12_) | copy-start | bytes 589828
  28.7 6.8 %copy-start.12 = (bf16[192,512]{1,0:T(8,128)(2,1)}, bf16[192,512]{1,0:T(8,128)(2,1)S(1)}, u32[]{:S(2)}) copy-start(bf16[192,512]{1,0:T(8,128)(2,1)S(1)} %collective-permute-done.12.refs_1_.refs_13_) | copy-start | bytes 589828
  35.5 13.5 %all-to-all-start = ((bf16[8,208,128]{2,1,0:T(8,128)(2,1)}), bf16[8,208,128]{2,1,0:T(8,128)(2,1)S(1)}, u32[]{:S(2)}, u32[]{:S(2)}) async-start(bf16[8,208,128]{2,1,0:T(8,128)(2,1)} %get-tuple-element.65), calls=%async_computation | async-start | bytes 851968 | tf_op jit(solution)/shard_map/all_to_all | solution.py:518
  41.7 21.9 %copy-start.14 = (f32[2,2]{1,0:T(2,128)S(1)}, f32[2,2]{1,0:T(2,128)}, u32[]{:S(2)}) copy-start(f32[2,2]{1,0:T(2,128)} %beta_ref.1) | copy-start | bytes 52
  41.7 21.9 %copy-start.15 = (f32[2,2]{1,0:T(2,128)S(1)}, f32[2,2]{1,0:T(2,128)}, u32[]{:S(2)}) copy-start(f32[2,2]{1,0:T(2,128)} %decay_ref.1) | copy-start | bytes 52
  41.7 21.9 %copy-start.16 = (bf16[2,2,128]{2,1,0:T(2,128)(2,1)S(1)}, bf16[2,2,128]{2,1,0:T(2,128)(2,1)}, u32[]{:S(2)}) copy-start(bf16[2,2,128]{2,1,0:T(2,128)(2,1)} %query_ref.1) | copy-start | bytes 3076
  41.7 21.9 %copy-start.17 = (bf16[2,2,128]{2,1,0:T(2,128)(2,1)S(1)}, bf16[2,2,128]{2,1,0:T(2,128)(2,1)}, u32[]{:S(2)}) copy-start(bf16[2,2,128]{2,1,0:T(2,128)(2,1)} %key_ref.1) | copy-start | bytes 3076
  41.7 21.9 %copy-start.18 = (bf16[2,2,128]{2,1,0:T(2,128)(2,1)S(1)}, bf16[2,2,128]{2,1,0:T(2,128)(2,1)}, u32[]{:S(2)}) copy-start(bf16[2,2,128]{2,1,0:T(2,128)(2,1)} %value_ref.1) | copy-start | bytes 3076
  48.5 26.8 %copy-start.13 = (f32[128]{0:T(128)S(1)}, f32[128]{0:T(128)}, u32[]{:S(2)}) copy-start(f32[128]{0:T(128)} %param.24) | copy-start | bytes 1540
  49.5 10.5 %collective-permute-start.15 = (bf16[208,128]{1,0:T(8,128)(2,1)S(1)}, bf16[208,128]{1,0:T(8,128)(2,1)S(1)}, u32[]{:S(2)}, u32[]{:S(2)}) collective-permute-start(bf16[208,128]{1,0:T(8,128)(2,1)S(1)} %get-tuple-element.73._.own), channel_id=1, source_target_pairs={{0,192},{64,0},{128,64},{192,128},{1,193},{65,1},{129,65},{193,129... | collective-permute-start | bytes 159752 | tf_op jit(solution)/shard_map/ppermute | solution.py:449
  55.0 8.1 %collective-permute-start.14 = (bf16[208,128]{1,0:T(8,128)(2,1)S(1)}, bf16[208,128]{1,0:T(8,128)(2,1)S(1)}, u32[]{:S(2)}, u32[]{:S(2)}) collective-permute-start(bf16[208,128]{1,0:T(8,128)(2,1)S(1)} %get-tuple-element.73._.own), channel_id=1, source_target_pairs={{0,128},{64,192},{128,0},{192,64},{1,129},{65,193},{129,1},{193,65... | collective-permute-start | bytes 159752 | tf_op jit(solution)/shard_map/ppermute | solution.py:449
  56.5 7.1 %collective-permute-start.13 = (bf16[208,128]{1,0:T(8,128)(2,1)S(1)}, bf16[208,128]{1,0:T(8,128)(2,1)S(1)}, u32[]{:S(2)}, u32[]{:S(2)}) collective-permute-start(bf16[208,128]{1,0:T(8,128)(2,1)S(1)} %get-tuple-element.73._.own), channel_id=1, source_target_pairs={{0,64},{64,128},{128,192},{192,0},{1,65},{65,129},{129,193},{193,1... | collective-permute-start | bytes 159752 | tf_op jit(solution)/shard_map/ppermute | solution.py:449
  (6 other events, 8.9 us)

commit v6 on v5

--- a/solution.py
+++ b/solution.py
@@ -136,7 +136,10 @@
 
 def lane_pair(ref, first):
     lanes = iota((1, LANES), 1)
-    return jnp.where(lanes == first, ref[0], jnp.where(lanes == first + 1, ref[1], 0.0))
+    pair = ref[...]
+    return jnp.where(
+        lanes == first, pair[:, 0:1], jnp.where(lanes == first + 1, pair[:, 1:2], 0.0)
+    )
 
 
 def local_kernel(bias_ref, rate_ref, *refs):
@@ -184,29 +187,56 @@
         rows_ref[seq] = table.T
     give(4)
     give(5)
-    t = iota((span, span), 0)
-    s = iota((span, span), 1)
+    half = head // 2
+    t = iota((head, head), 0)
+    s = iota((head, head), 1)
     apart = t ^ s
-    lower, inverse = [], []
+    upper, lower = slice(0, head), slice(head, span)
+    blocks = []
     for pair in range(4):
         seq, h = divmod(pair, 2)
         keys = key_rows[seq * span : (seq + 1) * span, h * head : (h + 1) * head]
-        col = lambda at: cols_ref[seq, :span, at + h : at + h + 1]
-        row = lambda at: rows_ref[seq, at + h : at + h + 1, :span]
-        spread = jnp.where(t >= s, col(2) - row(2), 0.0)
-        alike = dot(keys, keys, ROWS) * (col(0) * col(4)) * row(4) * jnp.exp(spread)
-        lower.append(jnp.where(t > s, alike, 0.0))
-        inverse.append(jnp.where(apart < 2, lower[pair], 0.0))
+
+        def alike(of, with_, mask):
+            col = lambda at: cols_ref[seq, of, at + h : at + h + 1]
+            row = lambda at: rows_ref[seq, at + h : at + h + 1, with_]
+            spread = col(2) - row(2)
+            if mask is not None:
+                spread = jnp.where(mask, spread, 0.0)
+            product = dot(keys[of], keys[with_], ROWS)
+            product = product * (col(0) * col(4)) * row(4) * jnp.exp(spread)
+            return product if mask is None else jnp.where(mask, product, 0.0)
+
+        def started(block):
+            size = block.shape[0]
+            near, same = apart[:size, :size] < 2, (t == s)[:size, :size]
+            return jnp.where(same, 1.0, jnp.where(near, -block, 0.0)).astype(bf16)
+
+        first = alike(upper, upper, t > s)
+        second = alike(lower, lower, (t > s)[:half, :half])
+        across = alike(lower, upper, None)
+        blocks.append(
+            [first.astype(bf16), second.astype(bf16), across.astype(bf16)]
+            + [started(first), started(second)]
+        )
     size = 2
-    while size < span:
-        mask = (apart >= size) & (apart < 2 * size)
+    while size < half:
+        mask = jnp.where((apart >= size) & (apart < 2 * size), 1.0, 0.0).astype(bf16)
         steps = []
-        for pair in range(4):
-            block = jnp.where(mask, lower[pair], 0.0)
-            steps.append(block - dot(block, inverse[pair]))
-        for pair in range(4):
-            inverse[pair] = inverse[pair] + steps[pair] - dot(inverse[pair], steps[pair])
+        for first, second, _, x_first, x_second in blocks:
+            step = dot(first * mask, x_first).astype(bf16)
+            steps.append((step, dot(second * mask[:half, :half], x_second).astype(bf16)))
+        for block, (step_first, step_second) in zip(blocks, steps):
+            block[3] = block[3] - dot(block[3], step_first).astype(bf16)
+            block[4] = block[4] - dot(block[4], step_second).astype(bf16)
         size *= 2
+    left = jnp.where(iota((half, head), 1) < half, 1.0, 0.0).astype(bf16)
+    blank = jnp.zeros((half, head), bf16)
+    steps = [dot(block[0][half:] * left, block[3]).astype(bf16) for block in blocks]
+    for block, step in zip(blocks, steps):
+        change = dot(block[3][half:], jnp.concatenate([blank, step], axis=0)).astype(bf16)
+        block[3] = jnp.concatenate([block[3][:half], block[3][half:] - change], axis=0)
+    steps = [dot(block[2], block[3]).astype(bf16) for block in blocks]
     for pair in range(4):
         seq, h = divmod(pair, 2)
         take = slice(seq * span, (seq + 1) * span)
@@ -214,9 +244,19 @@
         values = value_rows[take, h * head : (h + 1) * head]
         col = lambda at: cols_ref[seq, :span, at + h : at + h + 1]
         row = lambda at: rows_ref[seq, at + h : at + h + 1, :span]
-        fresh = col(0) * values.astype(f32) - dot(inverse[pair] * row(0), values)
-        carry = (col(0) * col(4) * jnp.exp(col(2))) * keys.astype(f32) - dot(
-            inverse[pair] * (row(0) * row(4) * jnp.exp(row(2))), keys
+        off_first = jnp.where(t == s, 0.0, blocks[pair][3].astype(f32))
+        off_second = jnp.where((t == s)[:half, :half], 0.0, blocks[pair][4].astype(f32))
+        off_across = -dot(blocks[pair][4], steps[pair])
+
+        def applied(weight, right):
+            top = dot(off_first * weight[:, upper], right[upper])
+            low = dot(off_across * weight[:, upper], right[upper])
+            low = low + dot(off_second * weight[:, lower], right[lower])
+            return jnp.concatenate([top, low], axis=0)
+
+        fresh = col(0) * values.astype(f32) + applied(row(0), values)
+        carry = (col(0) * col(4) * jnp.exp(col(2))) * keys.astype(f32) + applied(
+            row(0) * row(4) * jnp.exp(row(2)), keys
         )
         last = cols_ref[seq, span - 1 : span, 2 + h : 3 + h]
         late = col(4) * jnp.exp(last - col(2))
@@ -225,7 +265,6 @@
         fresh_ref[pair] = fresh.astype(bf16)
         carry_ref[pair] = carry.astype(bf16)
         factor = row_pack(thirds(jnp.broadcast_to(jnp.exp(last), (1, head))), head)
-        half = head // 2
         for side in range(2):
             to = 2 * pair + side
             send_ref[to, :head, :] = reach.astype(bf16)
@@ -336,7 +375,13 @@
     near = lax.axis_index("zl") * 4 + lax.axis_index("x")
     pair = near // 2
     side = near % 2
-    seq, h = pair // 2, pair % 2
+
+    def scalar(ref):
+        total = jnp.zeros((1, 1), f32)
+        for at in range(4):
+            entry = ref[at // 2 : at // 2 + 1, at % 2 : at % 2 + 1]
+            total = jnp.where(pair == at, entry, total)
+        return total
 
     def chosen(ref):
         total = jnp.zeros((1, head), f32)
@@ -351,7 +396,7 @@
     begin = state
     for group in range(4):
         begin = jnp.where(far == group, state, begin)
-        block = groups_ref[lax.rem(far - group + 4, 4)]
+        block = groups_ref[lax.bitwise_xor(far, group)]
         added = block[head : head + half].astype(f32)
         if group:
             state = unpack_factor(block[head + half :]) * state - dot(state, block[:head]) + added
@@ -370,9 +415,10 @@
     hits = dot(row_pack(thirds(query) + thirds(key), head), padded, ROWS)
     recall = hits[0:1] + hits[1:2] + hits[2:3]
     retrieve = hits[3:4] + hits[4:5] + hits[5:6]
+    decay = scalar(decay_ref)
     intersect = jnp.sum(key * query, axis=-1, keepdims=True)
-    fresh = chosen(value_ref) - decay_ref[seq, h] * retrieve
-    read = decay_ref[seq, h] * recall + (beta_ref[seq, h] * intersect) * fresh
+    fresh = chosen(value_ref) - decay * retrieve
+    read = decay * recall + (scalar(beta_ref) * intersect) * fresh
     read = jnp.where(iota((1, head), 1) // half == side, read, 0.0)
     zero = jnp.zeros((1, head), f32)
     extra = row_pack((zero, zero, zero, zero) + thirds(read), head)
@@ -511,8 +557,8 @@
     send, *shared = kernel(
         local_kernel,
         [("h", out) for out in local_shapes],
-        "ss" + "p" * 6,
-        (beta_bias, rate_log, *last[2:], *middle, *rest),
+        "p" * 8,
+        (beta_bias[None], rate_log[None], *last[2:], *middle, *rest),
         (*local_shapes, dma((6,))),
     )
     arrived = lax.all_to_all(send, NEAR, 0, 0, tiled=True)
@@ -543,7 +589,9 @@
         "p",
         (arrived,),
     )
-    others = [shift(total, "zh", by) for by in (1, 2, 3)]
+    others = [
+        lax.ppermute(total, "zh", [(at, at ^ by) for at in range(4)]) for by in (1, 2, 3)
+    ]
     finals_in = kernel(
         load_kernel,
         [("p", out) for out in finals],
@@ -556,7 +604,7 @@
     (back,) = kernel(
         spread_kernel,
         [("p", on((8, half + PACK, head), bf16))],
-        "ss" + "p" * 10,
+        "p" * 12,
         (
             new_beta, new_decay, total, *others, maps, adds, factors,
             new_query, new_key, new_value,

time: 76.6 us -> 74.8 us (0.977)
  waiting for transfers between devices: 16.9 us -> 18.7 us
  Pallas kernels: 21.9 us -> 20.2 us
  starting transfers between devices: 25.1 us -> 23.8 us
    ppermute x16 -> x13, starting transfers between devices: 18.9 us -> 9.62 us  [shift(): lax.ppermute(value, axis, [(at, (at + by) % length) for at in range(lengt...]
    ppermute x0 -> x3, starting transfers between devices: none -> 7.95 us  [shards(): lax.ppermute(total, 'zh', [(at, at ^ by) for at in range(4)])]
    ppermute x0 -> x3, waiting for transfers between devices: none -> 5.32 us  [shards(): lax.ppermute(total, 'zh', [(at, at ^ by) for at in range(4)])]
    ppermute x16 -> x13, waiting for transfers between devices: 16.3 us -> 12.9 us  [shift(): lax.ppermute(value, axis, [(at, (at + by) % length) for at in range(lengt...]
    pallas_call x9, Pallas kernels: 21.9 us -> 20.2 us  [kernel(): pl.pallas_call(body, out_shape=tuple((out if kind == 'p' else plain(out)...]
  transfers between devices with their start and end apart: 17 -> 17, of which waited for: 9 -> 8; matrix products, arithmetic and copies ran while one was open for 1% -> 1% of each run, Pallas kernels for 16% -> 16%
where the time goes in v6:
time: 74.8 us; the launch traced here: 74.5 us
  starting transfers between devices  23.8 us (32%)
  Pallas kernels  20.2 us (27%)
  waiting for transfers between devices  18.7 us (25%)
  blocking collectives  9.73 us (13%)
  local copies, waits for them, and re-layouts  1.14 us (2%)
  between operations  0.94 us (1%)
    pallas_call x9, Pallas kernels, kernel(): pl.pallas_call(body, out_shape=tuple((out if kind == 'p' else plain(out)...  20.2 us
    ppermute x13, waiting for transfers between devices, shift(): lax.ppermute(value, axis, [(at, (at + by) % length) for at in range(lengt...  12.9 us
    all_to_all x1, blocking collectives, shards(): returned = lax.all_to_all(back, NEAR, 0, 0, tiled=True)  9.73 us
    ppermute x13, starting transfers between devices, shift(): lax.ppermute(value, axis, [(at, (at + by) % length) for at in range(lengt...  9.62 us
    ppermute x3, starting transfers between devices, shards(): lax.ppermute(total, 'zh', [(at, at ^ by) for at in range(4)])  7.95 us
    all_to_all x1, starting transfers between devices, shards(): arrived = lax.all_to_all(send, NEAR, 0, 0, tiled=True)  6.2 us
    ppermute x3, waiting for transfers between devices, shards(): lax.ppermute(total, 'zh', [(at, at ^ by) for at in range(4)])  5.32 us
  transfers between devices with their start and end apart: 17, of which 8 were waited for; matrix products, arithmetic and copies ran while one was open for 1% of the time, Pallas kernels for 16%

profile of v6, /device:TPU:2, one launch (start us, length us, event | category | flops | bytes accessed | tf_op | source)
XLA Modules:
  0.0 74.5 jit_solution(7568588156686102776)
XLA Ops:
  0.6 0.1 collective-permute-start.4
  0.7 1.0 %slice_bitcast_fusion = (bf16[192,512]{1,0:T(8,128)(2,1)S(1)}, bf16[192,512]{1,0:T(8,128)(2,1)S(1)}) fusion(bf16[2,192,512]{2,1,0:T(8,128)(2,1)} %refs_0_.1), kind=kLoop, calls=%fused_computation | loop fusion | bytes 786432 | tf_op jit(solution)/shard_map/squeeze | solution.py:512
  1.8 3.1 %collective-permute-start.2 = (bf16[192,512]{1,0:T(8,128)(2,1)S(1)}, bf16[192,512]{1,0:T(8,128)(2,1)S(1)}, u32[]{:S(2)}, u32[]{:S(2)}) collective-permute-start(bf16[192,512]{1,0:T(8,128)(2,1)S(1)} %get-tuple-element.47), channel_id=1, source_target_pairs={{0,6},{2,0},{4,2},{6,4},{1,7},{3,1},{5,3},{7,5},{8,14},{10,8},{12,... | collective-permute-start | bytes 589832 | tf_op jit(solution)/shard_map/ppermute | solution.py:495
  4.9 2.4 %shard_map.166 = (f32[384,512]{1,0:T(8,128)S(1)}, f32[384,128]{1,0:T(8,128)S(1)}, bf16[3072,512]{1,0:T(8,128)(2,1)S(1)}, bf16[16,4096]{1,0:T(8,128)(2,1)S(1)}) custom-call(bf16[2,192,512]{2,1,0:T(8,128)(2,1)} %refs_0_.1, bf16[2,192,512]{2,1,0:T(8,128)(2,1)S(1)} %collective-permute-done.4.own_c.refs_1_, bf16[2,4096]{1,0:T(2,128)(2,1)} %bitcast.13, ...), custom_call_target="tpu_custom_call" | custom-call | tf_op jit(solution)/shard_map/pallas_call | solution.py:483
  7.3 0.7 collective-permute-start.5
  8.0 2.7 %collective-permute-start.6 = (bf16[192,512]{1,0:T(8,128)(2,1)S(1)}, bf16[192,512]{1,0:T(8,128)(2,1)S(1)}, u32[]{:S(2)}, u32[]{:S(2)}) collective-permute-start(bf16[192,512]{1,0:T(8,128)(2,1)S(1)} %get-tuple-element.48), channel_id=1, source_target_pairs={{0,6},{2,0},{4,2},{6,4},{1,7},{3,1},{5,3},{7,5},{8,14},{10,8},{12,... | collective-permute-start | bytes 589832 | tf_op jit(solution)/shard_map/ppermute | solution.py:495
  10.8 3.1 %collective-permute-done.refs_0_.refs_2_ = bf16[192,512]{1,0:T(8,128)(2,1)S(1)} collective-permute-done((bf16[192,512]{1,0:T(8,128)(2,1)S(1)}, bf16[192,512]{1,0:T(8,128)(2,1)S(1)}, u32[]{:S(2)}, u32[]{:S(2)}) %collective-permute-start) | collective-permute-done | bytes 196640 | tf_op jit(solution)/shard_map/ppermute | solution.py:495
  13.9 3.5 %collective-permute-done.5.refs_1_.refs_3_ = bf16[192,512]{1,0:T(8,128)(2,1)S(1)} collective-permute-done((bf16[192,512]{1,0:T(8,128)(2,1)S(1)}, bf16[192,512]{1,0:T(8,128)(2,1)S(1)}, u32[]{:S(2)}, u32[]{:S(2)}) %collective-permute-start.5) | collective-permute-done | bytes 196640 | tf_op jit(solution)/shard_map/ppermute | solution.py:495
  17.3 0.5 collective-permute-start.9
  17.8 0.9 %collective-permute-start.3 = (bf16[192,512]{1,0:T(8,128)(2,1)S(1)}, bf16[192,512]{1,0:T(8,128)(2,1)S(1)}, u32[]{:S(2)}, u32[]{:S(2)}) collective-permute-start(bf16[192,512]{1,0:T(8,128)(2,1)S(1)} %collective-permute-done.2.refs_3_.refs_5_), channel_id=1, source_target_pairs={{0,6},{2,0},{4,2},{6,4},{1,7},{3,1},{5,3},{7,5},{8,14},{10,8},{12,... | collective-permute-start | bytes 589832 | tf_op jit(solution)/shard_map/ppermute | solution.py:495
  18.7 1.2 %collective-permute-start.1 = (bf16[192,512]{1,0:T(8,128)(2,1)S(1)}, bf16[192,512]{1,0:T(8,128)(2,1)S(1)}, u32[]{:S(2)}, u32[]{:S(2)}) collective-permute-start(bf16[192,512]{1,0:T(8,128)(2,1)S(1)} %collective-permute-done.refs_0_.refs_2_), channel_id=1, source_target_pairs={{0,2},{2,4},{4,6},{6,0},{1,3},{3,5},{5,7},{7,1},{8,10},{10,12},{12... | collective-permute-start | bytes 589832 | tf_op jit(solution)/shard_map/ppermute | solution.py:495
  19.9 1.4 %shard_map.167 = (f32[384,512]{1,0:T(8,128)S(1)}, f32[384,128]{1,0:T(8,128)S(1)}) custom-call(bf16[192,512]{1,0:T(8,128)(2,1)S(1)} %collective-permute-done.refs_0_.refs_2_, bf16[192,512]{1,0:T(8,128)(2,1)S(1)} %collective-permute-done.5.refs_1_.refs_3_, bf16[192,512]{1,0:T(8,128)(2,1)S(1)} %collective-permute-done.6.refs_2_.refs_4_, ...), custom_call_target="tpu_custom_call" | custom-call | tf_op jit(solution)/shard_map/pallas_call | solution.py:483
  21.4 3.4 %collective-permute-done.3.refs_1_.refs_11_ = bf16[192,512]{1,0:T(8,128)(2,1)S(1)} collective-permute-done((bf16[192,512]{1,0:T(8,128)(2,1)S(1)}, bf16[192,512]{1,0:T(8,128)(2,1)S(1)}, u32[]{:S(2)}, u32[]{:S(2)}) %collective-permute-start.3) | collective-permute-done | bytes 196640 | tf_op jit(solution)/shard_map/ppermute | solution.py:495
  24.7 2.2 %collective-permute-done.1.refs_0_.refs_10_ = bf16[192,512]{1,0:T(8,128)(2,1)S(1)} collective-permute-done((bf16[192,512]{1,0:T(8,128)(2,1)S(1)}, bf16[192,512]{1,0:T(8,128)(2,1)S(1)}, u32[]{:S(2)}, u32[]{:S(2)}) %collective-permute-start.1) | collective-permute-done | bytes 196640 | tf_op jit(solution)/shard_map/ppermute | solution.py:495
  27.0 0.5 collective-permute-start.12
  27.5 0.5 shard_map.168
  28.0 0.4 collective-permute-done.11.refs_0_.refs_12_
  28.4 0.3 collective-permute-done.12.refs_1_.refs_13_
  28.7 5.6 %shard_map.169 = (bf16[8,208,128]{2,1,0:T(8,128)(2,1)}, bf16[384,256]{1,0:T(8,128)(2,1)}, bf16[4,192,128]{2,1,0:T(8,128)(2,1)}, bf16[4,192,128]{2,1,0:T(8,128)(2...) custom-call(f32[1,2]{1,0:T(1,128)S(1)} %bitcast.11, f32[1,2]{1,0:T(1,128)S(1)} %bitcast.12, ...), custom_call_target="tpu_custom_call" | custom-call | tf_op jit(solution)/shard_map/pallas_call | solution.py:483
  34.3 6.2 %all-to-all-start = ((bf16[8,208,128]{2,1,0:T(8,128)(2,1)}), bf16[8,208,128]{2,1,0:T(8,128)(2,1)S(1)}, u32[]{:S(2)}, u32[]{:S(2)}) async-start(bf16[8,208,128]{2,1,0:T(8,128)(2,1)} %get-tuple-element.65), calls=%async_computation | async-start | bytes 851968 | tf_op jit(solution)/shard_map/all_to_all | solution.py:564
  40.5 0.0 copy-start.17
  40.6 6.8 %shard_map.170 = (f32[4,192,128]{2,1,0:T(8,128)}, bf16[4,192,128]{2,1,0:T(8,128)(2,1)}, f32[4,192,128]{2,1,0:T(8,128)}) custom-call(bf16[2,192,512]{2,1,0:T(8,128)(2,1)} %refs_0_.1, bf16[2,192,512]{2,1,0:T(8,128)(2,1)} %copy-done, bf16[192,512]{1,0:T(8,128)(2,1)} %copy-done.2, bf16[192,512]{1,0:T(8,128)(2,1)} %copy-done.3, bf16[192,512]{1,0:T(8,128)(2,1)} %copy-done.4, ...), custom_call_target="tpu_custom_call" | custom-call | tf_op jit(solution)/shard_map/pallas_call | solution.py:483
  47.3 0.5 all-to-all-done.in_ref
  47.9 0.5 shard_map.171
  48.4 5.5 %collective-permute-start.15 = (bf16[208,128]{1,0:T(8,128)(2,1)S(1)}, bf16[208,128]{1,0:T(8,128)(2,1)S(1)}, u32[]{:S(2)}, u32[]{:S(2)}) collective-permute-start(bf16[208,128]{1,0:T(8,128)(2,1)S(1)} %get-tuple-element.73._.own), channel_id=1, source_target_pairs={{0,192},{64,128},{128,64},{192,0},{1,193},{65,129},{129,65},{193,1... | collective-permute-start | bytes 159752 | tf_op jit(solution)/shard_map/ppermute | solution.py:593
  53.9 1.4 %collective-permute-start.14 = (bf16[208,128]{1,0:T(8,128)(2,1)S(1)}, bf16[208,128]{1,0:T(8,128)(2,1)S(1)}, u32[]{:S(2)}, u32[]{:S(2)}) collective-permute-start(bf16[208,128]{1,0:T(8,128)(2,1)S(1)} %get-tuple-element.73._.own), channel_id=1, source_target_pairs={{0,128},{64,192},{128,0},{192,64},{1,129},{65,193},{129,1},{193,65... | collective-permute-start | bytes 159752 | tf_op jit(solution)/shard_map/ppermute | solution.py:593
  55.4 1.0 %collective-permute-start.13 = (bf16[208,128]{1,0:T(8,128)(2,1)S(1)}, bf16[208,128]{1,0:T(8,128)(2,1)S(1)}, u32[]{:S(2)}, u32[]{:S(2)}) collective-permute-start(bf16[208,128]{1,0:T(8,128)(2,1)S(1)} %get-tuple-element.73._.own), channel_id=1, source_target_pairs={{0,64},{64,0},{128,192},{192,128},{1,65},{65,1},{129,193},{193,129... | collective-permute-start | bytes 159752 | tf_op jit(solution)/shard_map/ppermute | solution.py:593
  56.4 1.2 %shard_map.172 = (f32[4,192,128]{2,1,0:T(8,128)S(1)}, bf16[4,192,128]{2,1,0:T(8,128)(2,1)S(1)}, f32[4,192,128]{2,1,0:T(8,128)S(1)}) custom-call(bf16[208,128]{1,0:T(8,128)(2,1)S(1)} %get-tuple-element.73._.own, f32[4,192,128]{2,1,0:T(8,128)} %get-tuple-element.74.refs_0_, bf16[4,192,128]{2,1,0:T(8,128)(2,1)} %get-tuple-element.75.refs_1_, ...), custom_call_target="tpu_custom_call" | custom-call | tf_op jit(solution)/shard_map/pallas_call | solution.py:483
  57.6 5.3 %collective-permute-done.14.back2 = bf16[208,128]{1,0:T(8,128)(2,1)S(1)} collective-permute-done((bf16[208,128]{1,0:T(8,128)(2,1)S(1)}, bf16[208,128]{1,0:T(8,128)(2,1)S(1)}, u32[]{:S(2)}, u32[]{:S(2)}) %collective-permute-start.14) | collective-permute-done | bytes 53280 | tf_op jit(solution)/shard_map/ppermute | solution.py:593
  63.0 0.7 shard_map.173
  63.7 9.7 %all_to_all.10.in_ref = bf16[8,80,128]{2,1,0:T(8,128)(2,1)S(1)} all-to-all(bf16[8,80,128]{2,1,0:T(8,128)(2,1)S(1)} %shard_map.173), channel_id=1, replica_groups=mesh['zh'=4,'zl'=2,'x'=4,'y'=4,'c'=2] {'zl','x'}, dimensions={0} | all-to-all | bytes 327680 | tf_op jit(solution)/shard_map/all_to_all | solution.py:614
  73.4 1.0 %shard_map.174 = (bf16[2,192,256]{2,1,0:T(8,128)(2,1)}, bf16[2,2,4,128]{3,2,1,0:T(4,128)(2,1)}, f32[2,256]{1,0:T(2,128)}) custom-call(bf16[8,80,128]{2,1,0:T(8,128)(2,1)S(1)} %all_to_all.10.in_ref, f32[4,192,128]{2,1,0:T(8,128)S(1)} %get-tuple-element.84.out_ref, bf16[4,192,128]{2,1,0:T(8,128)(2,1)S(1)} %get-tuple-element.85.reach_ref, ...), custom_call_target="tpu_custom_call" | custom-call | tf_op jit(solution)/shard_map/pallas_call | solution.py:483
  (55 shorter events, 0.1 us)
Async XLA Ops:
  0.6 4.3 %collective-permute-start.4 = (bf16[2,192,512]{2,1,0:T(8,128)(2,1)}, bf16[2,192,512]{2,1,0:T(8,128)(2,1)S(1)}, u32[]{:S(2)}, u32[]{:S(2)}) collective-permute-start(bf16[2,192,512]{2,1,0:T(8,128)(2,1)} %refs_0_.1), channel_id=1, source_target_pairs={{0,1},{1,0},{2,3},{3,2},{4,5},{5,4},{6,7},{7,6},{8,9},{9,8},{10,11... | collective-permute-start | bytes 1179656 | tf_op jit(solution)/shard_map/ppermute | solution.py:495
  1.8 9.0 %collective-permute-start.2 = (bf16[192,512]{1,0:T(8,128)(2,1)S(1)}, bf16[192,512]{1,0:T(8,128)(2,1)S(1)}, u32[]{:S(2)}, u32[]{:S(2)}) collective-permute-start(bf16[192,512]{1,0:T(8,128)(2,1)S(1)} %get-tuple-element.47), channel_id=1, source_target_pairs={{0,6},{2,0},{4,2},{6,4},{1,7},{3,1},{5,3},{7,5},{8,14},{10,8},{12,... | collective-permute-start | bytes 589832 | tf_op jit(solution)/shard_map/ppermute | solution.py:495
  4.9 9.0 %collective-permute-start = (bf16[192,512]{1,0:T(8,128)(2,1)S(1)}, bf16[192,512]{1,0:T(8,128)(2,1)S(1)}, u32[]{:S(2)}, u32[]{:S(2)}) collective-permute-start(bf16[192,512]{1,0:T(8,128)(2,1)S(1)} %get-tuple-element.48), channel_id=1, source_target_pairs={{0,2},{2,4},{4,6},{6,0},{1,3},{3,5},{5,7},{7,1},{8,10},{10,12},{12... | collective-permute-start | bytes 589832 | tf_op jit(solution)/shard_map/ppermute | solution.py:495
  4.9 2.5 %copy-start = (bf16[2,192,512]{2,1,0:T(8,128)(2,1)}, bf16[2,192,512]{2,1,0:T(8,128)(2,1)S(1)}, u32[]{:S(2)}) copy-start(bf16[2,192,512]{2,1,0:T(8,128)(2,1)S(1)} %collective-permute-done.4.own_c.refs_1_) | copy-start | bytes 1179652
  7.3 10.0 %collective-permute-start.5 = (bf16[192,512]{1,0:T(8,128)(2,1)S(1)}, bf16[192,512]{1,0:T(8,128)(2,1)S(1)}, u32[]{:S(2)}, u32[]{:S(2)}) collective-permute-start(bf16[192,512]{1,0:T(8,128)(2,1)S(1)} %get-tuple-element.47), channel_id=1, source_target_pairs={{0,2},{2,4},{4,6},{6,0},{1,3},{3,5},{5,7},{7,1},{8,10},{10,12},{12... | collective-permute-start | bytes 589832 | tf_op jit(solution)/shard_map/ppermute | solution.py:495
  8.0 9.3 %collective-permute-start.6 = (bf16[192,512]{1,0:T(8,128)(2,1)S(1)}, bf16[192,512]{1,0:T(8,128)(2,1)S(1)}, u32[]{:S(2)}, u32[]{:S(2)}) collective-permute-start(bf16[192,512]{1,0:T(8,128)(2,1)S(1)} %get-tuple-element.48), channel_id=1, source_target_pairs={{0,6},{2,0},{4,2},{6,4},{1,7},{3,1},{5,3},{7,5},{8,14},{10,8},{12,... | collective-permute-start | bytes 589832 | tf_op jit(solution)/shard_map/ppermute | solution.py:495
  10.7 10.6 %copy-start.1 = (bf16[192,512]{1,0:T(8,128)(2,1)}, bf16[192,512]{1,0:T(8,128)(2,1)S(1)}, u32[]{:S(2)}) copy-start(bf16[192,512]{1,0:T(8,128)(2,1)S(1)} %collective-permute-done.2.refs_3_.refs_5_) | copy-start | bytes 589828
  10.7 8.0 %collective-permute-start.10 = (bf16[192,512]{1,0:T(8,128)(2,1)S(1)}, bf16[192,512]{1,0:T(8,128)(2,1)S(1)}, u32[]{:S(2)}, u32[]{:S(2)}) collective-permute-start(bf16[192,512]{1,0:T(8,128)(2,1)S(1)} %collective-permute-done.2.refs_3_.refs_5_), channel_id=1, source_target_pairs={{0,1},{1,0},{2,3},{3,2},{4,5},{5,4},{6,7},{7,6},{8,9},{9,8},{10,11... | collective-permute-start | bytes 589832 | tf_op jit(solution)/shard_map/ppermute | solution.py:495
  13.9 7.4 %copy-start.2 = (bf16[192,512]{1,0:T(8,128)(2,1)}, bf16[192,512]{1,0:T(8,128)(2,1)S(1)}, u32[]{:S(2)}) copy-start(bf16[192,512]{1,0:T(8,128)(2,1)S(1)} %collective-permute-done.refs_0_.refs_2_) | copy-start | bytes 589828
  13.9 6.0 %collective-permute-start.7 = (bf16[192,512]{1,0:T(8,128)(2,1)S(1)}, bf16[192,512]{1,0:T(8,128)(2,1)S(1)}, u32[]{:S(2)}, u32[]{:S(2)}) collective-permute-start(bf16[192,512]{1,0:T(8,128)(2,1)S(1)} %collective-permute-done.refs_0_.refs_2_), channel_id=1, source_target_pairs={{0,1},{1,0},{2,3},{3,2},{4,5},{5,4},{6,7},{7,6},{8,9},{9,8},{10,11... | collective-permute-start | bytes 589832 | tf_op jit(solution)/shard_map/ppermute | solution.py:495
  17.3 4.0 %copy-start.3 = (bf16[192,512]{1,0:T(8,128)(2,1)}, bf16[192,512]{1,0:T(8,128)(2,1)S(1)}, u32[]{:S(2)}) copy-start(bf16[192,512]{1,0:T(8,128)(2,1)S(1)} %collective-permute-done.5.refs_1_.refs_3_) | copy-start | bytes 589828
  17.3 2.6 %collective-permute-start.8 = (bf16[192,512]{1,0:T(8,128)(2,1)S(1)}, bf16[192,512]{1,0:T(8,128)(2,1)S(1)}, u32[]{:S(2)}, u32[]{:S(2)}) collective-permute-start(bf16[192,512]{1,0:T(8,128)(2,1)S(1)} %collective-permute-done.5.refs_1_.refs_3_), channel_id=1, source_target_pairs={{0,1},{1,0},{2,3},{3,2},{4,5},{5,4},{6,7},{7,6},{8,9},{9,8},{10,11... | collective-permute-start | bytes 589832 | tf_op jit(solution)/shard_map/ppermute | solution.py:495
  17.3 4.0 %copy-start.4 = (bf16[192,512]{1,0:T(8,128)(2,1)}, bf16[192,512]{1,0:T(8,128)(2,1)S(1)}, u32[]{:S(2)}) copy-start(bf16[192,512]{1,0:T(8,128)(2,1)S(1)} %collective-permute-done.6.refs_2_.refs_4_) | copy-start | bytes 589828
  17.3 2.6 %collective-permute-start.9 = (bf16[192,512]{1,0:T(8,128)(2,1)S(1)}, bf16[192,512]{1,0:T(8,128)(2,1)S(1)}, u32[]{:S(2)}, u32[]{:S(2)}) collective-permute-start(bf16[192,512]{1,0:T(8,128)(2,1)S(1)} %collective-permute-done.6.refs_2_.refs_4_), channel_id=1, source_target_pairs={{0,1},{1,0},{2,3},{3,2},{4,5},{5,4},{6,7},{7,6},{8,9},{9,8},{10,11... | collective-permute-start | bytes 589832 | tf_op jit(solution)/shard_map/ppermute | solution.py:495
  17.8 6.9 %collective-permute-start.3 = (bf16[192,512]{1,0:T(8,128)(2,1)S(1)}, bf16[192,512]{1,0:T(8,128)(2,1)S(1)}, u32[]{:S(2)}, u32[]{:S(2)}) collective-permute-start(bf16[192,512]{1,0:T(8,128)(2,1)S(1)} %collective-permute-done.2.refs_3_.refs_5_), channel_id=1, source_target_pairs={{0,6},{2,0},{4,2},{6,4},{1,7},{3,1},{5,3},{7,5},{8,14},{10,8},{12,... | collective-permute-start | bytes 589832 | tf_op jit(solution)/shard_map/ppermute | solution.py:495
  18.7 2.6 %copy-start.5 = (bf16[192,512]{1,0:T(8,128)(2,1)}, bf16[192,512]{1,0:T(8,128)(2,1)S(1)}, u32[]{:S(2)}) copy-start(bf16[192,512]{1,0:T(8,128)(2,1)S(1)} %collective-permute-done.10.refs_7_.refs_9_) | copy-start | bytes 589828
  18.7 8.2 %collective-permute-start.1 = (bf16[192,512]{1,0:T(8,128)(2,1)S(1)}, bf16[192,512]{1,0:T(8,128)(2,1)S(1)}, u32[]{:S(2)}, u32[]{:S(2)}) collective-permute-start(bf16[192,512]{1,0:T(8,128)(2,1)S(1)} %collective-permute-done.refs_0_.refs_2_), channel_id=1, source_target_pairs={{0,2},{2,4},{4,6},{6,0},{1,3},{3,5},{5,7},{7,1},{8,10},{10,12},{12... | collective-permute-start | bytes 589832 | tf_op jit(solution)/shard_map/ppermute | solution.py:495
  24.7 3.2 %copy-start.9 = (bf16[192,512]{1,0:T(8,128)(2,1)}, bf16[192,512]{1,0:T(8,128)(2,1)S(1)}, u32[]{:S(2)}) copy-start(bf16[192,512]{1,0:T(8,128)(2,1)S(1)} %collective-permute-done.3.refs_1_.refs_11_) | copy-start | bytes 589828
  27.0 1.4 %collective-permute-start.11 = (bf16[192,512]{1,0:T(8,128)(2,1)S(1)}, bf16[192,512]{1,0:T(8,128)(2,1)S(1)}, u32[]{:S(2)}, u32[]{:S(2)}) collective-permute-start(bf16[192,512]{1,0:T(8,128)(2,1)S(1)} %collective-permute-done.1.refs_0_.refs_10_), channel_id=1, source_target_pairs={{0,1},{1,0},{2,3},{3,2},{4,5},{5,4},{6,7},{7,6},{8,9},{9,8},{10,11... | collective-permute-start | bytes 589832 | tf_op jit(solution)/shard_map/ppermute | solution.py:495
  27.0 1.7 %collective-permute-start.12 = (bf16[192,512]{1,0:T(8,128)(2,1)S(1)}, bf16[192,512]{1,0:T(8,128)(2,1)S(1)}, u32[]{:S(2)}, u32[]{:S(2)}) collective-permute-start(bf16[192,512]{1,0:T(8,128)(2,1)S(1)} %collective-permute-done.3.refs_1_.refs_11_), channel_id=1, source_target_pairs={{0,1},{1,0},{2,3},{3,2},{4,5},{5,4},{6,7},{7,6},{8,9},{9,8},{10,11... | collective-permute-start | bytes 589832 | tf_op jit(solution)/shard_map/ppermute | solution.py:495
  28.4 5.9 %copy-start.11 = (bf16[192,512]{1,0:T(8,128)(2,1)}, bf16[192,512]{1,0:T(8,128)(2,1)S(1)}, u32[]{:S(2)}) copy-start(bf16[192,512]{1,0:T(8,128)(2,1)S(1)} %collective-permute-done.11.refs_0_.refs_12_) | copy-start | bytes 589828
  28.7 5.6 %copy-start.12 = (bf16[192,512]{1,0:T(8,128)(2,1)}, bf16[192,512]{1,0:T(8,128)(2,1)S(1)}, u32[]{:S(2)}) copy-start(bf16[192,512]{1,0:T(8,128)(2,1)S(1)} %collective-permute-done.12.refs_1_.refs_13_) | copy-start | bytes 589828
  34.3 13.6 %all-to-all-start = ((bf16[8,208,128]{2,1,0:T(8,128)(2,1)}), bf16[8,208,128]{2,1,0:T(8,128)(2,1)S(1)}, u32[]{:S(2)}, u32[]{:S(2)}) async-start(bf16[8,208,128]{2,1,0:T(8,128)(2,1)} %get-tuple-element.65), calls=%async_computation | async-start | bytes 851968 | tf_op jit(solution)/shard_map/all_to_all | solution.py:564
  40.5 22.4 %copy-start.14 = (f32[2,2]{1,0:T(2,128)S(1)}, f32[2,2]{1,0:T(2,128)}, u32[]{:S(2)}) copy-start(f32[2,2]{1,0:T(2,128)} %beta_ref.1) | copy-start | bytes 52
  40.5 22.4 %copy-start.15 = (f32[2,2]{1,0:T(2,128)S(1)}, f32[2,2]{1,0:T(2,128)}, u32[]{:S(2)}) copy-start(f32[2,2]{1,0:T(2,128)} %decay_ref.1) | copy-start | bytes 52
  40.5 22.4 %copy-start.16 = (bf16[2,2,128]{2,1,0:T(2,128)(2,1)S(1)}, bf16[2,2,128]{2,1,0:T(2,128)(2,1)}, u32[]{:S(2)}) copy-start(bf16[2,2,128]{2,1,0:T(2,128)(2,1)} %query_ref.1) | copy-start | bytes 3076
  40.5 22.4 %copy-start.17 = (bf16[2,2,128]{2,1,0:T(2,128)(2,1)S(1)}, bf16[2,2,128]{2,1,0:T(2,128)(2,1)}, u32[]{:S(2)}) copy-start(bf16[2,2,128]{2,1,0:T(2,128)(2,1)} %key_ref.1) | copy-start | bytes 3076
  40.6 22.4 %copy-start.18 = (bf16[2,2,128]{2,1,0:T(2,128)(2,1)S(1)}, bf16[2,2,128]{2,1,0:T(2,128)(2,1)}, u32[]{:S(2)}) copy-start(bf16[2,2,128]{2,1,0:T(2,128)(2,1)} %value_ref.1) | copy-start | bytes 3076
  47.3 26.1 %copy-start.13 = (f32[128]{0:T(128)S(1)}, f32[128]{0:T(128)}, u32[]{:S(2)}) copy-start(f32[128]{0:T(128)} %param.24) | copy-start | bytes 1540
  48.4 9.2 %collective-permute-start.15 = (bf16[208,128]{1,0:T(8,128)(2,1)S(1)}, bf16[208,128]{1,0:T(8,128)(2,1)S(1)}, u32[]{:S(2)}, u32[]{:S(2)}) collective-permute-start(bf16[208,128]{1,0:T(8,128)(2,1)S(1)} %get-tuple-element.73._.own), channel_id=1, source_target_pairs={{0,192},{64,128},{128,64},{192,0},{1,193},{65,129},{129,65},{193,1... | collective-permute-start | bytes 159752 | tf_op jit(solution)/shard_map/ppermute | solution.py:593
  53.9 9.0 %collective-permute-start.14 = (bf16[208,128]{1,0:T(8,128)(2,1)S(1)}, bf16[208,128]{1,0:T(8,128)(2,1)S(1)}, u32[]{:S(2)}, u32[]{:S(2)}) collective-permute-start(bf16[208,128]{1,0:T(8,128)(2,1)S(1)} %get-tuple-element.73._.own), channel_id=1, source_target_pairs={{0,128},{64,192},{128,0},{192,64},{1,129},{65,193},{129,1},{193,65... | collective-permute-start | bytes 159752 | tf_op jit(solution)/shard_map/ppermute | solution.py:593
  55.4 7.6 %collective-permute-start.13 = (bf16[208,128]{1,0:T(8,128)(2,1)S(1)}, bf16[208,128]{1,0:T(8,128)(2,1)S(1)}, u32[]{:S(2)}, u32[]{:S(2)}) collective-permute-start(bf16[208,128]{1,0:T(8,128)(2,1)S(1)} %get-tuple-element.73._.own), channel_id=1, source_target_pairs={{0,64},{64,0},{128,192},{192,128},{1,65},{65,1},{129,193},{193,129... | collective-permute-start | bytes 159752 | tf_op jit(solution)/shard_map/ppermute | solution.py:593
  (6 other events, 8.9 us)

commit v7 on v6

--- a/solution.py
+++ b/solution.py
@@ -279,8 +279,12 @@
 
 def window_kernel(*refs):
     pieces, refs = refs[:14], refs[14:]
-    query_w, gate_w, gain_ref, key_ref, fresh_ref, carry_ref, cols_ref, rows_ref = refs[:8]
-    out_ref, reach_ref, silu_ref, token_buffer, query_buffer, gate_buffer, sems = refs[8:]
+    query_w, gate_w, gain_ref, shared, refs = refs[0], refs[1], refs[2], refs[3:8], refs[8:]
+    outputs, refs = refs[:3], refs[3:]
+    token_buffer, query_buffer, gate_buffer, sems, more_sems = refs[:5]
+    shared_buffers, output_buffers = refs[5:10], refs[10:]
+    key_ref, fresh_ref, carry_ref, cols_ref, rows_ref = shared_buffers
+    out_ref, reach_ref, silu_ref = output_buffers
     span, depth = token_buffer.shape[2:]
     head = fresh_ref.shape[-1]
     weights = ((query_w, query_buffer), (gate_w, gate_buffer))
@@ -295,6 +299,12 @@
         copies.append([pltpu.make_async_copy(a, b, sems.at[at]) for a, b in parts])
         for copy in copies[at]:
             copy.start()
+    given = [
+        pltpu.make_async_copy(a, b, more_sems.at[at])
+        for at, (a, b) in enumerate(zip(shared, shared_buffers))
+    ]
+    for copy in given:
+        copy.start()
     query_total = gate_total = 0.0
     for at in range(8):
         for copy in copies[at]:
@@ -302,10 +312,13 @@
         rows = token_buffer[at].reshape(-1, depth)
         query_total = query_total + dot(rows, query_buffer[at])
         gate_total = gate_total + dot(rows, gate_buffer[at])
+    for copy in given:
+        copy.wait()
     query_rows = query_total.astype(bf16)
     gate_rows = gate_total.astype(bf16).astype(f32)
     t = iota((span, span), 0)
     s = iota((span, span), 1)
+    taken = []
     for pair in range(4):
         seq, h = divmod(pair, 2)
         take = slice(seq * span, (seq + 1) * span)
@@ -322,6 +335,11 @@
         reach_ref[pair] = reach.astype(bf16)
         gate = gate_rows[take, part]
         silu_ref[pair] = gain_ref[...] * gate * jax.nn.sigmoid(gate)
+        for at, (a, b) in enumerate(zip(output_buffers, outputs)):
+            taken.append(pltpu.make_async_copy(a.at[pair], b.at[pair], more_sems.at[5 + at]))
+            taken[-1].start()
+    for copy in taken:
+        copy.wait()
 
 
 def unpack_factor(block):
@@ -536,13 +554,13 @@
     swapped = []
     for value in near:
         swapped.append(swap(value))
+    middle = kernel(functools.partial(middle_kernel, 2), sums, "p" * 8, (*near, *early[:2], *rest))
+    far0, far1, *middle = lax.optimization_barrier((far0, far1, *middle))
+    last = [far0, far1]
+    for at in range(2):
+        last.append(swap(last[at]))
     middle = kernel(
-        functools.partial(middle_kernel, 2), sums, "p" * 12, (*near, *swapped, *early[:2], *rest)
-    )
-    far0, far1, *middle = lax.optimization_barrier((far0, far1, *middle))
-    last = [far0, far1, swap(far0), swap(far1)]
-    middle = kernel(
-        functools.partial(middle_kernel, 6), sums, "p" * 6, (far0, far1, *middle, *rest)
+        functools.partial(middle_kernel, 4), sums, "p" * 10, (*swapped, far0, far1, *middle, *rest)
     )
     far_c0, far_c1, *middle = lax.optimization_barrier((*last[2:], *middle))
     last[2:] = [far_c0, far_c1]
@@ -566,14 +584,17 @@
     finals = [on((4, span, head), f32), on((4, span, head), bf16), on((4, span, head), f32)]
     local_out, reach, silu = kernel(
         window_kernel,
-        [("v", out) for out in finals],
-        "h" * 16 + "v" * 6,
+        [("h", out) for out in finals],
+        "h" * 16 + "v" + "h" * 5,
         (tokens, tokens_c, *near, *swapped, *last, query_weight, gate_weight, gain, *shared),
         (
             on((8, 2, span, depth), bf16),
             on((8, depth, width), bf16),
             on((8, depth, width), bf16),
             dma((8,)),
+            dma((8,)),
+            *local_shapes[1:],
+            *finals,
         ),
         24,
     )

time: 74.8 us -> 70.3 us (0.940)
  the two profiles are of different devices: /device:TPU:2 before, /device:TPU:24 now
where the time goes in v7:
time: 70.3 us; the launch traced here: 69.5 us
  starting transfers between devices  23.6 us (34%)
  Pallas kernels  19.6 us (28%)
  waiting for transfers between devices  14.2 us (20%)
  blocking collectives  10 us (14%)
  local copies, waits for them, and re-layouts  1.15 us (2%)
  between operations  0.96 us (1%)
    pallas_call x9, Pallas kernels, kernel(): pl.pallas_call(body, out_shape=tuple((out if kind == 'p' else plain(out)...  19.6 us
    ppermute x13, starting transfers between devices, shift(): lax.ppermute(value, axis, [(at, (at + by) % length) for at in range(lengt...  10.3 us
    all_to_all x1, blocking collectives, shards(): returned = lax.all_to_all(back, NEAR, 0, 0, tiled=True)  10 us
    ppermute x3, starting transfers between devices, shards(): lax.ppermute(total, 'zh', [(at, at ^ by) for at in range(4)])  7.94 us
    ppermute x13, waiting for transfers between devices, shift(): lax.ppermute(value, axis, [(at, (at + by) % length) for at in range(lengt...  6.78 us
    all_to_all x1, starting transfers between devices, shards(): arrived = lax.all_to_all(send, NEAR, 0, 0, tiled=True)  5.32 us
    ppermute x3, waiting for transfers between devices, shards(): lax.ppermute(total, 'zh', [(at, at ^ by) for at in range(4)])  4.77 us
    all_to_all x1, waiting for transfers between devices, shards(): arrived = lax.all_to_all(send, NEAR, 0, 0, tiled=True)  2.65 us
  transfers between devices with their start and end apart: 17, of which 8 were waited for; matrix products, arithmetic and copies ran while one was open for 2% of the time, Pallas kernels for 17%

profile of v7, /device:TPU:24, one launch (start us, length us, event | category | flops | bytes accessed | tf_op | source)
XLA Modules:
  0.0 69.5 jit_solution(16539235348034561672)
XLA Ops:
  0.6 0.1 collective-permute-start.4
  0.7 1.0 %slice_bitcast_fusion = (bf16[192,512]{1,0:T(8,128)(2,1)S(1)}, bf16[192,512]{1,0:T(8,128)(2,1)S(1)}) fusion(bf16[2,192,512]{2,1,0:T(8,128)(2,1)} %refs_0_.1), kind=kLoop, calls=%fused_computation | loop fusion | bytes 786432 | tf_op jit(solution)/shard_map/squeeze | solution.py:530
  1.8 0.8 %collective-permute-start.2 = (bf16[192,512]{1,0:T(8,128)(2,1)S(1)}, bf16[192,512]{1,0:T(8,128)(2,1)S(1)}, u32[]{:S(2)}, u32[]{:S(2)}) collective-permute-start(bf16[192,512]{1,0:T(8,128)(2,1)S(1)} %get-tuple-element.47), channel_id=1, source_target_pairs={{0,6},{2,0},{4,2},{6,4},{1,7},{3,1},{5,3},{7,5},{8,14},{10,8},{12,... | collective-permute-start | bytes 589832 | tf_op jit(solution)/shard_map/ppermute | solution.py:513
  2.6 2.5 %collective-permute-start = (bf16[192,512]{1,0:T(8,128)(2,1)S(1)}, bf16[192,512]{1,0:T(8,128)(2,1)S(1)}, u32[]{:S(2)}, u32[]{:S(2)}) collective-permute-start(bf16[192,512]{1,0:T(8,128)(2,1)S(1)} %get-tuple-element.48), channel_id=1, source_target_pairs={{0,2},{2,4},{4,6},{6,0},{1,3},{3,5},{5,7},{7,1},{8,10},{10,12},{12... | collective-permute-start | bytes 589832 | tf_op jit(solution)/shard_map/ppermute | solution.py:513
  5.1 2.4 %shard_map.166 = (f32[384,512]{1,0:T(8,128)S(1)}, f32[384,128]{1,0:T(8,128)S(1)}, bf16[3072,512]{1,0:T(8,128)(2,1)S(1)}, bf16[16,4096]{1,0:T(8,128)(2,1)S(1)}) custom-call(bf16[2,192,512]{2,1,0:T(8,128)(2,1)} %refs_0_.1, bf16[2,192,512]{2,1,0:T(8,128)(2,1)S(1)} %collective-permute-done.4.own_c.refs_1_, bf16[2,4096]{1,0:T(2,128)(2,1)} %bitcast.13, ...), custom_call_target="tpu_custom_call" | custom-call | tf_op jit(solution)/shard_map/pallas_call | solution.py:501
  7.6 0.8 %collective-permute-start.5 = (bf16[192,512]{1,0:T(8,128)(2,1)S(1)}, bf16[192,512]{1,0:T(8,128)(2,1)S(1)}, u32[]{:S(2)}, u32[]{:S(2)}) collective-permute-start(bf16[192,512]{1,0:T(8,128)(2,1)S(1)} %get-tuple-element.47), channel_id=1, source_target_pairs={{0,2},{2,4},{4,6},{6,0},{1,3},{3,5},{5,7},{7,1},{8,10},{10,12},{12... | collective-permute-start | bytes 589832 | tf_op jit(solution)/shard_map/ppermute | solution.py:513
  8.4 1.3 %collective-permute-start.6 = (bf16[192,512]{1,0:T(8,128)(2,1)S(1)}, bf16[192,512]{1,0:T(8,128)(2,1)S(1)}, u32[]{:S(2)}, u32[]{:S(2)}) collective-permute-start(bf16[192,512]{1,0:T(8,128)(2,1)S(1)} %get-tuple-element.48), channel_id=1, source_target_pairs={{0,6},{2,0},{4,2},{6,4},{1,7},{3,1},{5,3},{7,5},{8,14},{10,8},{12,... | collective-permute-start | bytes 589832 | tf_op jit(solution)/shard_map/ppermute | solution.py:513
  9.7 0.7 %collective-permute-done.2.refs_3_.refs_5_ = bf16[192,512]{1,0:T(8,128)(2,1)S(1)} collective-permute-done((bf16[192,512]{1,0:T(8,128)(2,1)S(1)}, bf16[192,512]{1,0:T(8,128)(2,1)S(1)}, u32[]{:S(2)}, u32[]{:S(2)}) %collective-permute-start.2) | collective-permute-done | bytes 196640 | tf_op jit(solution)/shard_map/ppermute | solution.py:513
  10.4 3.7 %collective-permute-start.1 = (bf16[192,512]{1,0:T(8,128)(2,1)S(1)}, bf16[192,512]{1,0:T(8,128)(2,1)S(1)}, u32[]{:S(2)}, u32[]{:S(2)}) collective-permute-start(bf16[192,512]{1,0:T(8,128)(2,1)S(1)} %collective-permute-done.refs_0_.refs_2_), channel_id=1, source_target_pairs={{0,2},{2,4},{4,6},{6,0},{1,3},{3,5},{5,7},{7,1},{8,10},{10,12},{12... | collective-permute-start | bytes 589832 | tf_op jit(solution)/shard_map/ppermute | solution.py:513
  14.1 1.3 %collective-permute-done.5.refs_1_.refs_3_ = bf16[192,512]{1,0:T(8,128)(2,1)S(1)} collective-permute-done((bf16[192,512]{1,0:T(8,128)(2,1)S(1)}, bf16[192,512]{1,0:T(8,128)(2,1)S(1)}, u32[]{:S(2)}, u32[]{:S(2)}) %collective-permute-start.5) | collective-permute-done | bytes 196640 | tf_op jit(solution)/shard_map/ppermute | solution.py:513
  15.4 1.9 %collective-permute-done.6.refs_2_.refs_4_ = bf16[192,512]{1,0:T(8,128)(2,1)S(1)} collective-permute-done((bf16[192,512]{1,0:T(8,128)(2,1)S(1)}, bf16[192,512]{1,0:T(8,128)(2,1)S(1)}, u32[]{:S(2)}, u32[]{:S(2)}) %collective-permute-start.6) | collective-permute-done | bytes 196640 | tf_op jit(solution)/shard_map/ppermute | solution.py:513
  17.3 0.8 %shard_map.167 = (f32[384,512]{1,0:T(8,128)S(1)}, f32[384,128]{1,0:T(8,128)S(1)}) custom-call(bf16[192,512]{1,0:T(8,128)(2,1)S(1)} %collective-permute-done.refs_0_.refs_2_, bf16[192,512]{1,0:T(8,128)(2,1)S(1)} %collective-permute-done.5.refs_1_.refs_3_, bf16[192,512]{1,0:T(8,128)(2,1)S(1)} %collective-permute-done.6.refs_2_.refs_4_, ...), custom_call_target="tpu_custom_call" | custom-call | tf_op jit(solution)/shard_map/pallas_call | solution.py:501
  18.1 2.1 %collective-permute-done.3.refs_5_.refs_11_ = bf16[192,512]{1,0:T(8,128)(2,1)S(1)} collective-permute-done((bf16[192,512]{1,0:T(8,128)(2,1)S(1)}, bf16[192,512]{1,0:T(8,128)(2,1)S(1)}, u32[]{:S(2)}, u32[]{:S(2)}) %collective-permute-start.3) | collective-permute-done | bytes 196640 | tf_op jit(solution)/shard_map/ppermute | solution.py:513
  20.4 0.5 collective-permute-start.11
  20.9 0.1 collective-permute-start.7
  21.0 0.4 collective-permute-start.8
  21.4 0.4 collective-permute-done.10.refs_1_.refs_7_
  21.8 0.3 collective-permute-done.11.refs_2_.refs_8_
  22.1 1.1 %shard_map.168 = (f32[384,512]{1,0:T(8,128)S(1)}, f32[384,128]{1,0:T(8,128)S(1)}) custom-call(bf16[192,512]{1,0:T(8,128)(2,1)S(1)} %collective-permute-done.9.refs_0_.refs_6_, bf16[192,512]{1,0:T(8,128)(2,1)S(1)} %collective-permute-done.10.refs_1_.refs_7_, bf16[192,512]{1,0:T(8,128)(2,1)S(1)} %collective-permute-done.11.refs_2_.refs_8_, ...), custom_call_target="tpu_custom_call" | custom-call | tf_op jit(solution)/shard_map/pallas_call | solution.py:501
  23.3 5.6 %shard_map.169 = (bf16[8,208,128]{2,1,0:T(8,128)(2,1)}, bf16[384,256]{1,0:T(8,128)(2,1)}, bf16[4,192,128]{2,1,0:T(8,128)(2,1)}, bf16[4,192,128]{2,1,0:T(8,128)(2...) custom-call(f32[1,2]{1,0:T(1,128)S(1)} %bitcast.11, f32[1,2]{1,0:T(1,128)S(1)} %bitcast.12, ...), custom_call_target="tpu_custom_call" | custom-call | tf_op jit(solution)/shard_map/pallas_call | solution.py:501
  28.9 5.3 %all-to-all-start = ((bf16[8,208,128]{2,1,0:T(8,128)(2,1)}), bf16[8,208,128]{2,1,0:T(8,128)(2,1)S(1)}, u32[]{:S(2)}, u32[]{:S(2)}) async-start(bf16[8,208,128]{2,1,0:T(8,128)(2,1)} %get-tuple-element.65), calls=%async_computation | async-start | bytes 851968 | tf_op jit(solution)/shard_map/all_to_all | solution.py:582
  34.3 6.2 %shard_map.170 = (f32[4,192,128]{2,1,0:T(8,128)}, bf16[4,192,128]{2,1,0:T(8,128)(2,1)}, f32[4,192,128]{2,1,0:T(8,128)}) custom-call(bf16[2,192,512]{2,1,0:T(8,128)(2,1)} %refs_0_.1, bf16[2,192,512]{2,1,0:T(8,128)(2,1)} %copy-done, bf16[192,512]{1,0:T(8,128)(2,1)} %copy-done.2, bf16[192,512]{1,0:T(8,128)(2,1)} %copy-done.3, bf16[192,512]{1,0:T(8,128)(2,1)} %copy-done.4, ...), custom_call_target="tpu_custom_call" | custom-call | tf_op jit(solution)/shard_map/pallas_call | solution.py:501
  40.5 2.7 %all-to-all-done.in_ref = bf16[8,208,128]{2,1,0:T(8,128)(2,1)S(1)} async-done(((bf16[8,208,128]{2,1,0:T(8,128)(2,1)}), bf16[8,208,128]{2,1,0:T(8,128)(2,1)S(1)}, u32[]{:S(2)}, u32[]{:S(2)}) %all-to-all-start) | async-done | bytes 426016 | tf_op jit(solution)/shard_map/all_to_all | solution.py:582
  43.2 0.5 shard_map.171
  43.7 5.5 %collective-permute-start.15 = (bf16[208,128]{1,0:T(8,128)(2,1)S(1)}, bf16[208,128]{1,0:T(8,128)(2,1)S(1)}, u32[]{:S(2)}, u32[]{:S(2)}) collective-permute-start(bf16[208,128]{1,0:T(8,128)(2,1)S(1)} %get-tuple-element.73._.own), channel_id=1, source_target_pairs={{0,192},{64,128},{128,64},{192,0},{1,193},{65,129},{129,65},{193,1... | collective-permute-start | bytes 159752 | tf_op jit(solution)/shard_map/ppermute | solution.py:614
  49.2 1.4 %collective-permute-start.14 = (bf16[208,128]{1,0:T(8,128)(2,1)S(1)}, bf16[208,128]{1,0:T(8,128)(2,1)S(1)}, u32[]{:S(2)}, u32[]{:S(2)}) collective-permute-start(bf16[208,128]{1,0:T(8,128)(2,1)S(1)} %get-tuple-element.73._.own), channel_id=1, source_target_pairs={{0,128},{64,192},{128,0},{192,64},{1,129},{65,193},{129,1},{193,65... | collective-permute-start | bytes 159752 | tf_op jit(solution)/shard_map/ppermute | solution.py:614
  50.6 1.0 %collective-permute-start.13 = (bf16[208,128]{1,0:T(8,128)(2,1)S(1)}, bf16[208,128]{1,0:T(8,128)(2,1)S(1)}, u32[]{:S(2)}, u32[]{:S(2)}) collective-permute-start(bf16[208,128]{1,0:T(8,128)(2,1)S(1)} %get-tuple-element.73._.own), channel_id=1, source_target_pairs={{0,64},{64,0},{128,192},{192,128},{1,65},{65,1},{129,193},{193,129... | collective-permute-start | bytes 159752 | tf_op jit(solution)/shard_map/ppermute | solution.py:614
  51.6 1.2 %shard_map.172 = (f32[4,192,128]{2,1,0:T(8,128)S(1)}, bf16[4,192,128]{2,1,0:T(8,128)(2,1)S(1)}, f32[4,192,128]{2,1,0:T(8,128)S(1)}) custom-call(bf16[208,128]{1,0:T(8,128)(2,1)S(1)} %get-tuple-element.73._.own, f32[4,192,128]{2,1,0:T(8,128)} %get-tuple-element.74.refs_0_, bf16[4,192,128]{2,1,0:T(8,128)(2,1)} %get-tuple-element.75.refs_1_, ...), custom_call_target="tpu_custom_call" | custom-call | tf_op jit(solution)/shard_map/pallas_call | solution.py:501
  52.9 4.8 %collective-permute-done.14.back2 = bf16[208,128]{1,0:T(8,128)(2,1)S(1)} collective-permute-done((bf16[208,128]{1,0:T(8,128)(2,1)S(1)}, bf16[208,128]{1,0:T(8,128)(2,1)S(1)}, u32[]{:S(2)}, u32[]{:S(2)}) %collective-permute-start.14) | collective-permute-done | bytes 53280 | tf_op jit(solution)/shard_map/ppermute | solution.py:614
  57.7 0.7 %shard_map.173 = bf16[8,80,128]{2,1,0:T(8,128)(2,1)S(1)} custom-call(f32[2,2]{1,0:T(2,128)S(1)} %copy-done.14, f32[2,2]{1,0:T(2,128)S(1)} %copy-done.15, bf16[208,128]{1,0:T(8,128)(2,1)S(1)} %get-tuple-element.73._.own, bf16[208,128]{1,0:T(8,128)(2,1)S(1)} %collective-permute-done.13.back1, bf16[208,128]{1,0:T(8,128)(2,1)S(1)} %collective-permute-done.14.back2, ...), custom_call_target="tpu_custom_call" | custom-call | tf_op jit(solution)/shard_map/pallas_call | solution.py:501
  58.4 10.0 %all_to_all.10.in_ref = bf16[8,80,128]{2,1,0:T(8,128)(2,1)S(1)} all-to-all(bf16[8,80,128]{2,1,0:T(8,128)(2,1)S(1)} %shard_map.173), channel_id=1, replica_groups=mesh['zh'=4,'zl'=2,'x'=4,'y'=4,'c'=2] {'zl','x'}, dimensions={0} | all-to-all | bytes 327680 | tf_op jit(solution)/shard_map/all_to_all | solution.py:635
  68.4 1.1 %shard_map.174 = (bf16[2,192,256]{2,1,0:T(8,128)(2,1)}, bf16[2,2,4,128]{3,2,1,0:T(4,128)(2,1)}, f32[2,256]{1,0:T(2,128)}) custom-call(bf16[8,80,128]{2,1,0:T(8,128)(2,1)S(1)} %all_to_all.10.in_ref, f32[4,192,128]{2,1,0:T(8,128)S(1)} %get-tuple-element.84.out_ref, bf16[4,192,128]{2,1,0:T(8,128)(2,1)S(1)} %get-tuple-element.85.reach_ref, ...), custom_call_target="tpu_custom_call" | custom-call | tf_op jit(solution)/shard_map/pallas_call | solution.py:501
  (55 shorter events, 0.2 us)
Async XLA Ops:
  0.6 4.5 %collective-permute-start.4 = (bf16[2,192,512]{2,1,0:T(8,128)(2,1)}, bf16[2,192,512]{2,1,0:T(8,128)(2,1)S(1)}, u32[]{:S(2)}, u32[]{:S(2)}) collective-permute-start(bf16[2,192,512]{2,1,0:T(8,128)(2,1)} %refs_0_.1), channel_id=1, source_target_pairs={{0,1},{1,0},{2,3},{3,2},{4,5},{5,4},{6,7},{7,6},{8,9},{9,8},{10,11... | collective-permute-start | bytes 1179656 | tf_op jit(solution)/shard_map/ppermute | solution.py:513
  1.8 8.6 %collective-permute-start.2 = (bf16[192,512]{1,0:T(8,128)(2,1)S(1)}, bf16[192,512]{1,0:T(8,128)(2,1)S(1)}, u32[]{:S(2)}, u32[]{:S(2)}) collective-permute-start(bf16[192,512]{1,0:T(8,128)(2,1)S(1)} %get-tuple-element.47), channel_id=1, source_target_pairs={{0,6},{2,0},{4,2},{6,4},{1,7},{3,1},{5,3},{7,5},{8,14},{10,8},{12,... | collective-permute-start | bytes 589832 | tf_op jit(solution)/shard_map/ppermute | solution.py:513
  2.6 7.8 %collective-permute-start = (bf16[192,512]{1,0:T(8,128)(2,1)S(1)}, bf16[192,512]{1,0:T(8,128)(2,1)S(1)}, u32[]{:S(2)}, u32[]{:S(2)}) collective-permute-start(bf16[192,512]{1,0:T(8,128)(2,1)S(1)} %get-tuple-element.48), channel_id=1, source_target_pairs={{0,2},{2,4},{4,6},{6,0},{1,3},{3,5},{5,7},{7,1},{8,10},{10,12},{12... | collective-permute-start | bytes 589832 | tf_op jit(solution)/shard_map/ppermute | solution.py:513
  7.6 7.9 %collective-permute-start.5 = (bf16[192,512]{1,0:T(8,128)(2,1)S(1)}, bf16[192,512]{1,0:T(8,128)(2,1)S(1)}, u32[]{:S(2)}, u32[]{:S(2)}) collective-permute-start(bf16[192,512]{1,0:T(8,128)(2,1)S(1)} %get-tuple-element.47), channel_id=1, source_target_pairs={{0,2},{2,4},{4,6},{6,0},{1,3},{3,5},{5,7},{7,1},{8,10},{10,12},{12... | collective-permute-start | bytes 589832 | tf_op jit(solution)/shard_map/ppermute | solution.py:513
  8.4 9.0 %collective-permute-start.6 = (bf16[192,512]{1,0:T(8,128)(2,1)S(1)}, bf16[192,512]{1,0:T(8,128)(2,1)S(1)}, u32[]{:S(2)}, u32[]{:S(2)}) collective-permute-start(bf16[192,512]{1,0:T(8,128)(2,1)S(1)} %get-tuple-element.48), channel_id=1, source_target_pairs={{0,6},{2,0},{4,2},{6,4},{1,7},{3,1},{5,3},{7,5},{8,14},{10,8},{12,... | collective-permute-start | bytes 589832 | tf_op jit(solution)/shard_map/ppermute | solution.py:513
  10.4 7.7 %copy-start.1 = (bf16[192,512]{1,0:T(8,128)(2,1)}, bf16[192,512]{1,0:T(8,128)(2,1)S(1)}, u32[]{:S(2)}) copy-start(bf16[192,512]{1,0:T(8,128)(2,1)S(1)} %collective-permute-done.2.refs_3_.refs_5_) | copy-start | bytes 589828
  10.4 9.9 %collective-permute-start.3 = (bf16[192,512]{1,0:T(8,128)(2,1)S(1)}, bf16[192,512]{1,0:T(8,128)(2,1)S(1)}, u32[]{:S(2)}, u32[]{:S(2)}) collective-permute-start(bf16[192,512]{1,0:T(8,128)(2,1)S(1)} %collective-permute-done.2.refs_3_.refs_5_), channel_id=1, source_target_pairs={{0,6},{2,0},{4,2},{6,4},{1,7},{3,1},{5,3},{7,5},{8,14},{10,8},{12,... | collective-permute-start | bytes 589832 | tf_op jit(solution)/shard_map/ppermute | solution.py:513
  10.4 7.7 %copy-start.2 = (bf16[192,512]{1,0:T(8,128)(2,1)}, bf16[192,512]{1,0:T(8,128)(2,1)S(1)}, u32[]{:S(2)}) copy-start(bf16[192,512]{1,0:T(8,128)(2,1)S(1)} %collective-permute-done.refs_0_.refs_2_) | copy-start | bytes 589828
  10.4 9.8 %collective-permute-start.1 = (bf16[192,512]{1,0:T(8,128)(2,1)S(1)}, bf16[192,512]{1,0:T(8,128)(2,1)S(1)}, u32[]{:S(2)}, u32[]{:S(2)}) collective-permute-start(bf16[192,512]{1,0:T(8,128)(2,1)S(1)} %collective-permute-done.refs_0_.refs_2_), channel_id=1, source_target_pairs={{0,2},{2,4},{4,6},{6,0},{1,3},{3,5},{5,7},{7,1},{8,10},{10,12},{12... | collective-permute-start | bytes 589832 | tf_op jit(solution)/shard_map/ppermute | solution.py:513
  14.1 6.9 %collective-permute-start.12 = (bf16[192,512]{1,0:T(8,128)(2,1)S(1)}, bf16[192,512]{1,0:T(8,128)(2,1)S(1)}, u32[]{:S(2)}, u32[]{:S(2)}) collective-permute-start(bf16[192,512]{1,0:T(8,128)(2,1)S(1)} %collective-permute-done.2.refs_3_.refs_5_), channel_id=1, source_target_pairs={{0,1},{1,0},{2,3},{3,2},{4,5},{5,4},{6,7},{7,6},{8,9},{9,8},{10,11... | collective-permute-start | bytes 589832 | tf_op jit(solution)/shard_map/ppermute | solution.py:513
  15.4 4.8 %copy-start.3 = (bf16[192,512]{1,0:T(8,128)(2,1)}, bf16[192,512]{1,0:T(8,128)(2,1)S(1)}, u32[]{:S(2)}) copy-start(bf16[192,512]{1,0:T(8,128)(2,1)S(1)} %collective-permute-done.5.refs_1_.refs_3_) | copy-start | bytes 589828
  15.4 6.0 %collective-permute-start.9 = (bf16[192,512]{1,0:T(8,128)(2,1)S(1)}, bf16[192,512]{1,0:T(8,128)(2,1)S(1)}, u32[]{:S(2)}, u32[]{:S(2)}) collective-permute-start(bf16[192,512]{1,0:T(8,128)(2,1)S(1)} %collective-permute-done.refs_0_.refs_2_), channel_id=1, source_target_pairs={{0,1},{1,0},{2,3},{3,2},{4,5},{5,4},{6,7},{7,6},{8,9},{9,8},{10,11... | collective-permute-start | bytes 589832 | tf_op jit(solution)/shard_map/ppermute | solution.py:513
  17.3 3.0 %copy-start.4 = (bf16[192,512]{1,0:T(8,128)(2,1)}, bf16[192,512]{1,0:T(8,128)(2,1)S(1)}, u32[]{:S(2)}) copy-start(bf16[192,512]{1,0:T(8,128)(2,1)S(1)} %collective-permute-done.6.refs_2_.refs_4_) | copy-start | bytes 589828
  20.2 2.9 %copy-start.8 = (bf16[192,512]{1,0:T(8,128)(2,1)}, bf16[192,512]{1,0:T(8,128)(2,1)S(1)}, u32[]{:S(2)}) copy-start(bf16[192,512]{1,0:T(8,128)(2,1)S(1)} %collective-permute-done.1.refs_4_.refs_10_) | copy-start | bytes 589828
  20.2 3.0 %copy-start.19 = (f32[2]{0:T(128)S(1)}, f32[2]{0:T(128)}, u32[]{:S(2)}) copy-start(f32[2]{0:T(128)} %param.22) | copy-start | bytes 28
  20.3 3.0 %copy-start.20 = (f32[2]{0:T(128)S(1)}, f32[2]{0:T(128)}, u32[]{:S(2)}) copy-start(f32[2]{0:T(128)} %param.23) | copy-start | bytes 28
  20.3 1.5 %collective-permute-start.10 = (bf16[192,512]{1,0:T(8,128)(2,1)S(1)}, bf16[192,512]{1,0:T(8,128)(2,1)S(1)}, u32[]{:S(2)}, u32[]{:S(2)}) collective-permute-start(bf16[192,512]{1,0:T(8,128)(2,1)S(1)} %collective-permute-done.5.refs_1_.refs_3_), channel_id=1, source_target_pairs={{0,1},{1,0},{2,3},{3,2},{4,5},{5,4},{6,7},{7,6},{8,9},{9,8},{10,11... | collective-permute-start | bytes 589832 | tf_op jit(solution)/shard_map/ppermute | solution.py:513
  20.4 1.7 %collective-permute-start.11 = (bf16[192,512]{1,0:T(8,128)(2,1)S(1)}, bf16[192,512]{1,0:T(8,128)(2,1)S(1)}, u32[]{:S(2)}, u32[]{:S(2)}) collective-permute-start(bf16[192,512]{1,0:T(8,128)(2,1)S(1)} %collective-permute-done.6.refs_2_.refs_4_), channel_id=1, source_target_pairs={{0,1},{1,0},{2,3},{3,2},{4,5},{5,4},{6,7},{7,6},{8,9},{9,8},{10,11... | collective-permute-start | bytes 589832 | tf_op jit(solution)/shard_map/ppermute | solution.py:513
  20.9 2.4 %collective-permute-start.7 = (bf16[192,512]{1,0:T(8,128)(2,1)S(1)}, bf16[192,512]{1,0:T(8,128)(2,1)S(1)}, u32[]{:S(2)}, u32[]{:S(2)}) collective-permute-start(bf16[192,512]{1,0:T(8,128)(2,1)S(1)} %collective-permute-done.1.refs_4_.refs_10_), channel_id=1, source_target_pairs={{0,1},{1,0},{2,3},{3,2},{4,5},{5,4},{6,7},{7,6},{8,9},{9,8},{10,11... | collective-permute-start | bytes 589832 | tf_op jit(solution)/shard_map/ppermute | solution.py:513
  21.0 2.3 %collective-permute-start.8 = (bf16[192,512]{1,0:T(8,128)(2,1)S(1)}, bf16[192,512]{1,0:T(8,128)(2,1)S(1)}, u32[]{:S(2)}, u32[]{:S(2)}) collective-permute-start(bf16[192,512]{1,0:T(8,128)(2,1)S(1)} %collective-permute-done.3.refs_5_.refs_11_), channel_id=1, source_target_pairs={{0,1},{1,0},{2,3},{3,2},{4,5},{5,4},{6,7},{7,6},{8,9},{9,8},{10,11... | collective-permute-start | bytes 589832 | tf_op jit(solution)/shard_map/ppermute | solution.py:513
  23.2 5.7 %copy-start.5 = (bf16[192,512]{1,0:T(8,128)(2,1)}, bf16[192,512]{1,0:T(8,128)(2,1)S(1)}, u32[]{:S(2)}) copy-start(bf16[192,512]{1,0:T(8,128)(2,1)S(1)} %collective-permute-done.7.refs_0_.refs_12_) | copy-start | bytes 589828
  23.3 5.7 %copy-start.6 = (bf16[192,512]{1,0:T(8,128)(2,1)}, bf16[192,512]{1,0:T(8,128)(2,1)S(1)}, u32[]{:S(2)}) copy-start(bf16[192,512]{1,0:T(8,128)(2,1)S(1)} %collective-permute-done.8.refs_1_.refs_13_) | copy-start | bytes 589828
  28.9 14.2 %all-to-all-start = ((bf16[8,208,128]{2,1,0:T(8,128)(2,1)}), bf16[8,208,128]{2,1,0:T(8,128)(2,1)S(1)}, u32[]{:S(2)}, u32[]{:S(2)}) async-start(bf16[8,208,128]{2,1,0:T(8,128)(2,1)} %get-tuple-element.65), calls=%async_computation | async-start | bytes 851968 | tf_op jit(solution)/shard_map/all_to_all | solution.py:582
  34.3 23.4 %copy-start.14 = (f32[2,2]{1,0:T(2,128)S(1)}, f32[2,2]{1,0:T(2,128)}, u32[]{:S(2)}) copy-start(f32[2,2]{1,0:T(2,128)} %beta_ref.1) | copy-start | bytes 52
  34.3 23.4 %copy-start.15 = (f32[2,2]{1,0:T(2,128)S(1)}, f32[2,2]{1,0:T(2,128)}, u32[]{:S(2)}) copy-start(f32[2,2]{1,0:T(2,128)} %decay_ref.1) | copy-start | bytes 52
  34.3 23.4 %copy-start.16 = (bf16[2,2,128]{2,1,0:T(2,128)(2,1)S(1)}, bf16[2,2,128]{2,1,0:T(2,128)(2,1)}, u32[]{:S(2)}) copy-start(bf16[2,2,128]{2,1,0:T(2,128)(2,1)} %query_ref.1) | copy-start | bytes 3076
  34.3 23.4 %copy-start.17 = (bf16[2,2,128]{2,1,0:T(2,128)(2,1)S(1)}, bf16[2,2,128]{2,1,0:T(2,128)(2,1)}, u32[]{:S(2)}) copy-start(bf16[2,2,128]{2,1,0:T(2,128)(2,1)} %key_ref.1) | copy-start | bytes 3076
  34.3 23.4 %copy-start.18 = (bf16[2,2,128]{2,1,0:T(2,128)(2,1)S(1)}, bf16[2,2,128]{2,1,0:T(2,128)(2,1)}, u32[]{:S(2)}) copy-start(bf16[2,2,128]{2,1,0:T(2,128)(2,1)} %value_ref.1) | copy-start | bytes 3076
  40.5 28.0 %copy-start.13 = (f32[128]{0:T(128)S(1)}, f32[128]{0:T(128)}, u32[]{:S(2)}) copy-start(f32[128]{0:T(128)} %param.24) | copy-start | bytes 1540
  43.7 9.2 %collective-permute-start.15 = (bf16[208,128]{1,0:T(8,128)(2,1)S(1)}, bf16[208,128]{1,0:T(8,128)(2,1)S(1)}, u32[]{:S(2)}, u32[]{:S(2)}) collective-permute-start(bf16[208,128]{1,0:T(8,128)(2,1)S(1)} %get-tuple-element.73._.own), channel_id=1, source_target_pairs={{0,192},{64,128},{128,64},{192,0},{1,193},{65,129},{129,65},{193,1... | collective-permute-start | bytes 159752 | tf_op jit(solution)/shard_map/ppermute | solution.py:614
  49.2 8.5 %collective-permute-start.14 = (bf16[208,128]{1,0:T(8,128)(2,1)S(1)}, bf16[208,128]{1,0:T(8,128)(2,1)S(1)}, u32[]{:S(2)}, u32[]{:S(2)}) collective-permute-start(bf16[208,128]{1,0:T(8,128)(2,1)S(1)} %get-tuple-element.73._.own), channel_id=1, source_target_pairs={{0,128},{64,192},{128,0},{192,64},{1,129},{65,193},{129,1},{193,65... | collective-permute-start | bytes 159752 | tf_op jit(solution)/shard_map/ppermute | solution.py:614
  50.6 7.0 %collective-permute-start.13 = (bf16[208,128]{1,0:T(8,128)(2,1)S(1)}, bf16[208,128]{1,0:T(8,128)(2,1)S(1)}, u32[]{:S(2)}, u32[]{:S(2)}) collective-permute-start(bf16[208,128]{1,0:T(8,128)(2,1)S(1)} %get-tuple-element.73._.own), channel_id=1, source_target_pairs={{0,64},{64,0},{128,192},{192,128},{1,65},{65,1},{129,193},{193,129... | collective-permute-start | bytes 159752 | tf_op jit(solution)/shard_map/ppermute | solution.py:614
  (6 other events, 11.9 us)

commit v8 on v7

--- a/solution.py
+++ b/solution.py
@@ -264,6 +264,8 @@
         gain = dot(fresh * late, keys, COLS)
         fresh_ref[pair] = fresh.astype(bf16)
         carry_ref[pair] = carry.astype(bf16)
+        give(2, pair)
+        give(3, pair)
         factor = row_pack(thirds(jnp.broadcast_to(jnp.exp(last), (1, head))), head)
         for side in range(2):
             to = 2 * pair + side
@@ -271,8 +273,6 @@
             send_ref[to, head : head + half, :] = gain[side * half : (side + 1) * half].astype(bf16)
             send_ref[to, head + half :, :] = factor.astype(bf16)
         give(0, pl.ds(2 * pair, 2))
-    give(2)
-    give(3)
     for copy in copies:
         copy.wait()
 
@@ -465,20 +465,34 @@
         copy.wait()
 
 
-def finish_kernel(in_ref, out_ref, reach_ref, silu_ref, gain_ref, mixed_ref, cache_ref, read_ref):
+def finish_kernel(
+    in_ref, out_ref, reach_ref, silu_ref, gain_ref, mixed_out, cache_ref, read_ref, mixed_ref, sems
+):
     head = in_ref.shape[-1]
     half = head // 2
+    copies = []
     for pair in range(4):
         seq, h = divmod(pair, 2)
         incoming = jnp.concatenate([in_ref[2 * pair, :half, :], in_ref[2 * pair + 1, :half, :]], 0)
         whole = out_ref[pair] + dot(reach_ref[pair], incoming, ROWS)
         mixed = whole * rms_scale(whole, norm_floor, True) * silu_ref[pair]
+        lanes = pl.ds(h * head, head)
         mixed_ref[seq, :, h * head : (h + 1) * head] = mixed.astype(bf16)
+        copies.append(
+            pltpu.make_async_copy(
+                mixed_ref.at[seq, :, lanes], mixed_out.at[seq, :, lanes], sems.at[pair]
+            )
+        )
+        copies[-1].start()
+    for pair in range(4):
+        seq, h = divmod(pair, 2)
         extra = in_ref[2 * pair, half:, :].astype(f32) + in_ref[2 * pair + 1, half:, :].astype(f32)
         cache_ref[seq, h] = extra[:4].astype(bf16)
         read = extra[4:5] + extra[5:6] + extra[6:7]
         read = read * rms_scale(read, norm_floor, True) * gain_ref[...]
         read_ref[seq : seq + 1, h * head : (h + 1) * head] = read
+    for copy in copies:
+        copy.wait()
 
 
 def vmem():
@@ -554,13 +568,13 @@
     swapped = []
     for value in near:
         swapped.append(swap(value))
-    middle = kernel(functools.partial(middle_kernel, 2), sums, "p" * 8, (*near, *early[:2], *rest))
+    middle = kernel(
+        functools.partial(middle_kernel, 2), sums, "p" * 12, (*near, *swapped, *early[:2], *rest)
+    )
     far0, far1, *middle = lax.optimization_barrier((far0, far1, *middle))
-    last = [far0, far1]
-    for at in range(2):
-        last.append(swap(last[at]))
+    last = [far0, far1, swap(far0), swap(far1)]
     middle = kernel(
-        functools.partial(middle_kernel, 4), sums, "p" * 10, (*swapped, far0, far1, *middle, *rest)
+        functools.partial(middle_kernel, 6), sums, "p" * 6, (far0, far1, *middle, *rest)
     )
     far_c0, far_c1, *middle = lax.optimization_barrier((*last[2:], *middle))
     last[2:] = [far_c0, far_c1]
@@ -636,12 +650,13 @@
     return kernel(
         finish_kernel,
         [
-            ("v", on((2, span, width), bf16)),
+            ("h", on((2, span, width), bf16)),
             ("v", on((2, 2, 4, head), bf16)),
             ("v", on((2, width), f32)),
         ],
         "ppppp",
         (returned, *finals_in, gain),
+        (on((2, span, width), bf16), dma((4,))),
     )
 
 

time: 70.3 us -> 75.1 us (1.068)
  the two profiles are of different devices: /device:TPU:24 before, /device:TPU:2 now
where the time goes in v8:
time: 75.1 us; the launch traced here: 74.9 us
  starting transfers between devices  23.8 us (32%)
  Pallas kernels  20.2 us (27%)
  waiting for transfers between devices  19.1 us (25%)
  blocking collectives  9.6 us (13%)
  local copies, waits for them, and re-layouts  1.14 us (2%)
  between operations  1.1 us (1%)
    pallas_call x9, Pallas kernels, kernel(): pl.pallas_call(body, out_shape=tuple((out if kind == 'p' else plain(out)...  20.2 us
    ppermute x13, waiting for transfers between devices, shift(): lax.ppermute(value, axis, [(at, (at + by) % length) for at in range(lengt...  12.9 us
    ppermute x13, starting transfers between devices, shift(): lax.ppermute(value, axis, [(at, (at + by) % length) for at in range(lengt...  9.62 us
    all_to_all x1, blocking collectives, shards(): returned = lax.all_to_all(back, NEAR, 0, 0, tiled=True)  9.6 us
    ppermute x3, starting transfers between devices, shards(): lax.ppermute(total, 'zh', [(at, at ^ by) for at in range(4)])  7.95 us
    all_to_all x1, starting transfers between devices, shards(): arrived = lax.all_to_all(send, NEAR, 0, 0, tiled=True)  6.2 us
    ppermute x3, waiting for transfers between devices, shards(): lax.ppermute(total, 'zh', [(at, at ^ by) for at in range(4)])  5.12 us
  transfers between devices with their start and end apart: 17, of which 8 were waited for; matrix products, arithmetic and copies ran while one was open for 1% of the time, Pallas kernels for 16%

profile of v8, /device:TPU:2, one launch (start us, length us, event | category | flops | bytes accessed | tf_op | source)
XLA Modules:
  0.0 74.9 jit_solution(5534309762406914370)
XLA Ops:
  0.6 0.1 collective-permute-start.4
  0.7 1.0 %slice_bitcast_fusion = (bf16[192,512]{1,0:T(8,128)(2,1)S(1)}, bf16[192,512]{1,0:T(8,128)(2,1)S(1)}) fusion(bf16[2,192,512]{2,1,0:T(8,128)(2,1)} %refs_0_.1), kind=kLoop, calls=%fused_computation | loop fusion | bytes 786432 | tf_op jit(solution)/shard_map/squeeze | solution.py:544
  1.8 3.1 %collective-permute-start.2 = (bf16[192,512]{1,0:T(8,128)(2,1)S(1)}, bf16[192,512]{1,0:T(8,128)(2,1)S(1)}, u32[]{:S(2)}, u32[]{:S(2)}) collective-permute-start(bf16[192,512]{1,0:T(8,128)(2,1)S(1)} %get-tuple-element.47), channel_id=1, source_target_pairs={{0,6},{2,0},{4,2},{6,4},{1,7},{3,1},{5,3},{7,5},{8,14},{10,8},{12,... | collective-permute-start | bytes 589832 | tf_op jit(solution)/shard_map/ppermute | solution.py:527
  4.9 2.4 %shard_map.166 = (f32[384,512]{1,0:T(8,128)S(1)}, f32[384,128]{1,0:T(8,128)S(1)}, bf16[3072,512]{1,0:T(8,128)(2,1)S(1)}, bf16[16,4096]{1,0:T(8,128)(2,1)S(1)}) custom-call(bf16[2,192,512]{2,1,0:T(8,128)(2,1)} %refs_0_.1, bf16[2,192,512]{2,1,0:T(8,128)(2,1)S(1)} %collective-permute-done.4.own_c.refs_1_, bf16[2,4096]{1,0:T(2,128)(2,1)} %bitcast.13, ...), custom_call_target="tpu_custom_call" | custom-call | tf_op jit(solution)/shard_map/pallas_call | solution.py:515
  7.3 0.7 collective-permute-start.5
  8.0 2.7 %collective-permute-start.6 = (bf16[192,512]{1,0:T(8,128)(2,1)S(1)}, bf16[192,512]{1,0:T(8,128)(2,1)S(1)}, u32[]{:S(2)}, u32[]{:S(2)}) collective-permute-start(bf16[192,512]{1,0:T(8,128)(2,1)S(1)} %get-tuple-element.48), channel_id=1, source_target_pairs={{0,6},{2,0},{4,2},{6,4},{1,7},{3,1},{5,3},{7,5},{8,14},{10,8},{12,... | collective-permute-start | bytes 589832 | tf_op jit(solution)/shard_map/ppermute | solution.py:527
  10.8 3.1 %collective-permute-done.refs_0_.refs_2_ = bf16[192,512]{1,0:T(8,128)(2,1)S(1)} collective-permute-done((bf16[192,512]{1,0:T(8,128)(2,1)S(1)}, bf16[192,512]{1,0:T(8,128)(2,1)S(1)}, u32[]{:S(2)}, u32[]{:S(2)}) %collective-permute-start) | collective-permute-done | bytes 196640 | tf_op jit(solution)/shard_map/ppermute | solution.py:527
  13.9 3.5 %collective-permute-done.5.refs_1_.refs_3_ = bf16[192,512]{1,0:T(8,128)(2,1)S(1)} collective-permute-done((bf16[192,512]{1,0:T(8,128)(2,1)S(1)}, bf16[192,512]{1,0:T(8,128)(2,1)S(1)}, u32[]{:S(2)}, u32[]{:S(2)}) %collective-permute-start.5) | collective-permute-done | bytes 196640 | tf_op jit(solution)/shard_map/ppermute | solution.py:527
  17.3 0.5 collective-permute-start.9
  17.8 0.9 %collective-permute-start.3 = (bf16[192,512]{1,0:T(8,128)(2,1)S(1)}, bf16[192,512]{1,0:T(8,128)(2,1)S(1)}, u32[]{:S(2)}, u32[]{:S(2)}) collective-permute-start(bf16[192,512]{1,0:T(8,128)(2,1)S(1)} %collective-permute-done.2.refs_3_.refs_5_), channel_id=1, source_target_pairs={{0,6},{2,0},{4,2},{6,4},{1,7},{3,1},{5,3},{7,5},{8,14},{10,8},{12,... | collective-permute-start | bytes 589832 | tf_op jit(solution)/shard_map/ppermute | solution.py:527
  18.7 1.2 %collective-permute-start.1 = (bf16[192,512]{1,0:T(8,128)(2,1)S(1)}, bf16[192,512]{1,0:T(8,128)(2,1)S(1)}, u32[]{:S(2)}, u32[]{:S(2)}) collective-permute-start(bf16[192,512]{1,0:T(8,128)(2,1)S(1)} %collective-permute-done.refs_0_.refs_2_), channel_id=1, source_target_pairs={{0,2},{2,4},{4,6},{6,0},{1,3},{3,5},{5,7},{7,1},{8,10},{10,12},{12... | collective-permute-start | bytes 589832 | tf_op jit(solution)/shard_map/ppermute | solution.py:527
  19.9 1.4 %shard_map.167 = (f32[384,512]{1,0:T(8,128)S(1)}, f32[384,128]{1,0:T(8,128)S(1)}) custom-call(bf16[192,512]{1,0:T(8,128)(2,1)S(1)} %collective-permute-done.refs_0_.refs_2_, bf16[192,512]{1,0:T(8,128)(2,1)S(1)} %collective-permute-done.5.refs_1_.refs_3_, bf16[192,512]{1,0:T(8,128)(2,1)S(1)} %collective-permute-done.6.refs_2_.refs_4_, ...), custom_call_target="tpu_custom_call" | custom-call | tf_op jit(solution)/shard_map/pallas_call | solution.py:515
  21.4 3.4 %collective-permute-done.3.refs_1_.refs_11_ = bf16[192,512]{1,0:T(8,128)(2,1)S(1)} collective-permute-done((bf16[192,512]{1,0:T(8,128)(2,1)S(1)}, bf16[192,512]{1,0:T(8,128)(2,1)S(1)}, u32[]{:S(2)}, u32[]{:S(2)}) %collective-permute-start.3) | collective-permute-done | bytes 196640 | tf_op jit(solution)/shard_map/ppermute | solution.py:527
  24.7 2.2 %collective-permute-done.1.refs_0_.refs_10_ = bf16[192,512]{1,0:T(8,128)(2,1)S(1)} collective-permute-done((bf16[192,512]{1,0:T(8,128)(2,1)S(1)}, bf16[192,512]{1,0:T(8,128)(2,1)S(1)}, u32[]{:S(2)}, u32[]{:S(2)}) %collective-permute-start.1) | collective-permute-done | bytes 196640 | tf_op jit(solution)/shard_map/ppermute | solution.py:527
  27.0 0.5 collective-permute-start.12
  27.5 0.5 shard_map.168
  28.0 0.4 collective-permute-done.11.refs_0_.refs_12_
  28.4 0.3 collective-permute-done.12.refs_1_.refs_13_
  28.7 5.6 %shard_map.169 = (bf16[8,208,128]{2,1,0:T(8,128)(2,1)}, bf16[384,256]{1,0:T(8,128)(2,1)}, bf16[4,192,128]{2,1,0:T(8,128)(2,1)}, bf16[4,192,128]{2,1,0:T(8,128)(2...) custom-call(f32[1,2]{1,0:T(1,128)S(1)} %bitcast.11, f32[1,2]{1,0:T(1,128)S(1)} %bitcast.12, ...), custom_call_target="tpu_custom_call" | custom-call | tf_op jit(solution)/shard_map/pallas_call | solution.py:515
  34.3 6.2 %all-to-all-start = ((bf16[8,208,128]{2,1,0:T(8,128)(2,1)}), bf16[8,208,128]{2,1,0:T(8,128)(2,1)S(1)}, u32[]{:S(2)}, u32[]{:S(2)}) async-start(bf16[8,208,128]{2,1,0:T(8,128)(2,1)} %get-tuple-element.65), calls=%async_computation | async-start | bytes 851968 | tf_op jit(solution)/shard_map/all_to_all | solution.py:596
  40.5 0.0 copy-start.17
  40.5 6.2 %shard_map.170 = (f32[4,192,128]{2,1,0:T(8,128)}, bf16[4,192,128]{2,1,0:T(8,128)(2,1)}, f32[4,192,128]{2,1,0:T(8,128)}) custom-call(bf16[2,192,512]{2,1,0:T(8,128)(2,1)} %refs_0_.1, bf16[2,192,512]{2,1,0:T(8,128)(2,1)} %copy-done, bf16[192,512]{1,0:T(8,128)(2,1)} %copy-done.2, bf16[192,512]{1,0:T(8,128)(2,1)} %copy-done.3, bf16[192,512]{1,0:T(8,128)(2,1)} %copy-done.4, ...), custom_call_target="tpu_custom_call" | custom-call | tf_op jit(solution)/shard_map/pallas_call | solution.py:515
  46.7 1.1 %all-to-all-done.in_ref = bf16[8,208,128]{2,1,0:T(8,128)(2,1)S(1)} async-done(((bf16[8,208,128]{2,1,0:T(8,128)(2,1)}), bf16[8,208,128]{2,1,0:T(8,128)(2,1)S(1)}, u32[]{:S(2)}, u32[]{:S(2)}) %all-to-all-start) | async-done | bytes 426016 | tf_op jit(solution)/shard_map/all_to_all | solution.py:596
  47.8 0.5 shard_map.171
  48.4 5.5 %collective-permute-start.15 = (bf16[208,128]{1,0:T(8,128)(2,1)S(1)}, bf16[208,128]{1,0:T(8,128)(2,1)S(1)}, u32[]{:S(2)}, u32[]{:S(2)}) collective-permute-start(bf16[208,128]{1,0:T(8,128)(2,1)S(1)} %get-tuple-element.73._.own), channel_id=1, source_target_pairs={{0,192},{64,128},{128,64},{192,0},{1,193},{65,129},{129,65},{193,1... | collective-permute-start | bytes 159752 | tf_op jit(solution)/shard_map/ppermute | solution.py:628
  53.9 1.4 %collective-permute-start.14 = (bf16[208,128]{1,0:T(8,128)(2,1)S(1)}, bf16[208,128]{1,0:T(8,128)(2,1)S(1)}, u32[]{:S(2)}, u32[]{:S(2)}) collective-permute-start(bf16[208,128]{1,0:T(8,128)(2,1)S(1)} %get-tuple-element.73._.own), channel_id=1, source_target_pairs={{0,128},{64,192},{128,0},{192,64},{1,129},{65,193},{129,1},{193,65... | collective-permute-start | bytes 159752 | tf_op jit(solution)/shard_map/ppermute | solution.py:628
  55.3 1.0 %collective-permute-start.13 = (bf16[208,128]{1,0:T(8,128)(2,1)S(1)}, bf16[208,128]{1,0:T(8,128)(2,1)S(1)}, u32[]{:S(2)}, u32[]{:S(2)}) collective-permute-start(bf16[208,128]{1,0:T(8,128)(2,1)S(1)} %get-tuple-element.73._.own), channel_id=1, source_target_pairs={{0,64},{64,0},{128,192},{192,128},{1,65},{65,1},{129,193},{193,129... | collective-permute-start | bytes 159752 | tf_op jit(solution)/shard_map/ppermute | solution.py:628
  56.3 1.2 %shard_map.172 = (f32[4,192,128]{2,1,0:T(8,128)S(1)}, bf16[4,192,128]{2,1,0:T(8,128)(2,1)S(1)}, f32[4,192,128]{2,1,0:T(8,128)S(1)}) custom-call(bf16[208,128]{1,0:T(8,128)(2,1)S(1)} %get-tuple-element.73._.own, f32[4,192,128]{2,1,0:T(8,128)} %get-tuple-element.74.refs_0_, bf16[4,192,128]{2,1,0:T(8,128)(2,1)} %get-tuple-element.75.refs_1_, ...), custom_call_target="tpu_custom_call" | custom-call | tf_op jit(solution)/shard_map/pallas_call | solution.py:515
  57.6 5.1 %collective-permute-done.14.back2 = bf16[208,128]{1,0:T(8,128)(2,1)S(1)} collective-permute-done((bf16[208,128]{1,0:T(8,128)(2,1)S(1)}, bf16[208,128]{1,0:T(8,128)(2,1)S(1)}, u32[]{:S(2)}, u32[]{:S(2)}) %collective-permute-start.14) | collective-permute-done | bytes 53280 | tf_op jit(solution)/shard_map/ppermute | solution.py:628
  62.7 0.7 shard_map.173
  63.5 9.6 %all_to_all.10.in_ref = bf16[8,80,128]{2,1,0:T(8,128)(2,1)S(1)} all-to-all(bf16[8,80,128]{2,1,0:T(8,128)(2,1)S(1)} %shard_map.173), channel_id=1, replica_groups=mesh['zh'=4,'zl'=2,'x'=4,'y'=4,'c'=2] {'zl','x'}, dimensions={0} | all-to-all | bytes 327680 | tf_op jit(solution)/shard_map/all_to_all | solution.py:649
  73.1 1.6 %shard_map.174 = (bf16[2,192,256]{2,1,0:T(8,128)(2,1)}, bf16[2,2,4,128]{3,2,1,0:T(4,128)(2,1)}, f32[2,256]{1,0:T(2,128)}) custom-call(bf16[8,80,128]{2,1,0:T(8,128)(2,1)S(1)} %all_to_all.10.in_ref, f32[4,192,128]{2,1,0:T(8,128)S(1)} %get-tuple-element.84.out_ref, bf16[4,192,128]{2,1,0:T(8,128)(2,1)S(1)} %get-tuple-element.85.reach_ref, ...), custom_call_target="tpu_custom_call" | custom-call | tf_op jit(solution)/shard_map/pallas_call | solution.py:515
  (55 shorter events, 0.1 us)
Async XLA Ops:
  0.6 4.3 %collective-permute-start.4 = (bf16[2,192,512]{2,1,0:T(8,128)(2,1)}, bf16[2,192,512]{2,1,0:T(8,128)(2,1)S(1)}, u32[]{:S(2)}, u32[]{:S(2)}) collective-permute-start(bf16[2,192,512]{2,1,0:T(8,128)(2,1)} %refs_0_.1), channel_id=1, source_target_pairs={{0,1},{1,0},{2,3},{3,2},{4,5},{5,4},{6,7},{7,6},{8,9},{9,8},{10,11... | collective-permute-start | bytes 1179656 | tf_op jit(solution)/shard_map/ppermute | solution.py:527
  1.8 9.0 %collective-permute-start.2 = (bf16[192,512]{1,0:T(8,128)(2,1)S(1)}, bf16[192,512]{1,0:T(8,128)(2,1)S(1)}, u32[]{:S(2)}, u32[]{:S(2)}) collective-permute-start(bf16[192,512]{1,0:T(8,128)(2,1)S(1)} %get-tuple-element.47), channel_id=1, source_target_pairs={{0,6},{2,0},{4,2},{6,4},{1,7},{3,1},{5,3},{7,5},{8,14},{10,8},{12,... | collective-permute-start | bytes 589832 | tf_op jit(solution)/shard_map/ppermute | solution.py:527
  4.9 9.0 %collective-permute-start = (bf16[192,512]{1,0:T(8,128)(2,1)S(1)}, bf16[192,512]{1,0:T(8,128)(2,1)S(1)}, u32[]{:S(2)}, u32[]{:S(2)}) collective-permute-start(bf16[192,512]{1,0:T(8,128)(2,1)S(1)} %get-tuple-element.48), channel_id=1, source_target_pairs={{0,2},{2,4},{4,6},{6,0},{1,3},{3,5},{5,7},{7,1},{8,10},{10,12},{12... | collective-permute-start | bytes 589832 | tf_op jit(solution)/shard_map/ppermute | solution.py:527
  4.9 2.5 %copy-start = (bf16[2,192,512]{2,1,0:T(8,128)(2,1)}, bf16[2,192,512]{2,1,0:T(8,128)(2,1)S(1)}, u32[]{:S(2)}) copy-start(bf16[2,192,512]{2,1,0:T(8,128)(2,1)S(1)} %collective-permute-done.4.own_c.refs_1_) | copy-start | bytes 1179652
  7.3 10.0 %collective-permute-start.5 = (bf16[192,512]{1,0:T(8,128)(2,1)S(1)}, bf16[192,512]{1,0:T(8,128)(2,1)S(1)}, u32[]{:S(2)}, u32[]{:S(2)}) collective-permute-start(bf16[192,512]{1,0:T(8,128)(2,1)S(1)} %get-tuple-element.47), channel_id=1, source_target_pairs={{0,2},{2,4},{4,6},{6,0},{1,3},{3,5},{5,7},{7,1},{8,10},{10,12},{12... | collective-permute-start | bytes 589832 | tf_op jit(solution)/shard_map/ppermute | solution.py:527
  8.0 9.3 %collective-permute-start.6 = (bf16[192,512]{1,0:T(8,128)(2,1)S(1)}, bf16[192,512]{1,0:T(8,128)(2,1)S(1)}, u32[]{:S(2)}, u32[]{:S(2)}) collective-permute-start(bf16[192,512]{1,0:T(8,128)(2,1)S(1)} %get-tuple-element.48), channel_id=1, source_target_pairs={{0,6},{2,0},{4,2},{6,4},{1,7},{3,1},{5,3},{7,5},{8,14},{10,8},{12,... | collective-permute-start | bytes 589832 | tf_op jit(solution)/shard_map/ppermute | solution.py:527
  10.7 10.6 %copy-start.1 = (bf16[192,512]{1,0:T(8,128)(2,1)}, bf16[192,512]{1,0:T(8,128)(2,1)S(1)}, u32[]{:S(2)}) copy-start(bf16[192,512]{1,0:T(8,128)(2,1)S(1)} %collective-permute-done.2.refs_3_.refs_5_) | copy-start | bytes 589828
  10.7 8.0 %collective-permute-start.10 = (bf16[192,512]{1,0:T(8,128)(2,1)S(1)}, bf16[192,512]{1,0:T(8,128)(2,1)S(1)}, u32[]{:S(2)}, u32[]{:S(2)}) collective-permute-start(bf16[192,512]{1,0:T(8,128)(2,1)S(1)} %collective-permute-done.2.refs_3_.refs_5_), channel_id=1, source_target_pairs={{0,1},{1,0},{2,3},{3,2},{4,5},{5,4},{6,7},{7,6},{8,9},{9,8},{10,11... | collective-permute-start | bytes 589832 | tf_op jit(solution)/shard_map/ppermute | solution.py:527
  13.9 7.4 %copy-start.2 = (bf16[192,512]{1,0:T(8,128)(2,1)}, bf16[192,512]{1,0:T(8,128)(2,1)S(1)}, u32[]{:S(2)}) copy-start(bf16[192,512]{1,0:T(8,128)(2,1)S(1)} %collective-permute-done.refs_0_.refs_2_) | copy-start | bytes 589828
  13.9 6.0 %collective-permute-start.7 = (bf16[192,512]{1,0:T(8,128)(2,1)S(1)}, bf16[192,512]{1,0:T(8,128)(2,1)S(1)}, u32[]{:S(2)}, u32[]{:S(2)}) collective-permute-start(bf16[192,512]{1,0:T(8,128)(2,1)S(1)} %collective-permute-done.refs_0_.refs_2_), channel_id=1, source_target_pairs={{0,1},{1,0},{2,3},{3,2},{4,5},{5,4},{6,7},{7,6},{8,9},{9,8},{10,11... | collective-permute-start | bytes 589832 | tf_op jit(solution)/shard_map/ppermute | solution.py:527
  17.3 4.0 %copy-start.3 = (bf16[192,512]{1,0:T(8,128)(2,1)}, bf16[192,512]{1,0:T(8,128)(2,1)S(1)}, u32[]{:S(2)}) copy-start(bf16[192,512]{1,0:T(8,128)(2,1)S(1)} %collective-permute-done.5.refs_1_.refs_3_) | copy-start | bytes 589828
  17.3 2.6 %collective-permute-start.8 = (bf16[192,512]{1,0:T(8,128)(2,1)S(1)}, bf16[192,512]{1,0:T(8,128)(2,1)S(1)}, u32[]{:S(2)}, u32[]{:S(2)}) collective-permute-start(bf16[192,512]{1,0:T(8,128)(2,1)S(1)} %collective-permute-done.5.refs_1_.refs_3_), channel_id=1, source_target_pairs={{0,1},{1,0},{2,3},{3,2},{4,5},{5,4},{6,7},{7,6},{8,9},{9,8},{10,11... | collective-permute-start | bytes 589832 | tf_op jit(solution)/shard_map/ppermute | solution.py:527
  17.3 4.0 %copy-start.4 = (bf16[192,512]{1,0:T(8,128)(2,1)}, bf16[192,512]{1,0:T(8,128)(2,1)S(1)}, u32[]{:S(2)}) copy-start(bf16[192,512]{1,0:T(8,128)(2,1)S(1)} %collective-permute-done.6.refs_2_.refs_4_) | copy-start | bytes 589828
  17.3 2.6 %collective-permute-start.9 = (bf16[192,512]{1,0:T(8,128)(2,1)S(1)}, bf16[192,512]{1,0:T(8,128)(2,1)S(1)}, u32[]{:S(2)}, u32[]{:S(2)}) collective-permute-start(bf16[192,512]{1,0:T(8,128)(2,1)S(1)} %collective-permute-done.6.refs_2_.refs_4_), channel_id=1, source_target_pairs={{0,1},{1,0},{2,3},{3,2},{4,5},{5,4},{6,7},{7,6},{8,9},{9,8},{10,11... | collective-permute-start | bytes 589832 | tf_op jit(solution)/shard_map/ppermute | solution.py:527
  17.8 6.9 %collective-permute-start.3 = (bf16[192,512]{1,0:T(8,128)(2,1)S(1)}, bf16[192,512]{1,0:T(8,128)(2,1)S(1)}, u32[]{:S(2)}, u32[]{:S(2)}) collective-permute-start(bf16[192,512]{1,0:T(8,128)(2,1)S(1)} %collective-permute-done.2.refs_3_.refs_5_), channel_id=1, source_target_pairs={{0,6},{2,0},{4,2},{6,4},{1,7},{3,1},{5,3},{7,5},{8,14},{10,8},{12,... | collective-permute-start | bytes 589832 | tf_op jit(solution)/shard_map/ppermute | solution.py:527
  18.7 2.6 %copy-start.5 = (bf16[192,512]{1,0:T(8,128)(2,1)}, bf16[192,512]{1,0:T(8,128)(2,1)S(1)}, u32[]{:S(2)}) copy-start(bf16[192,512]{1,0:T(8,128)(2,1)S(1)} %collective-permute-done.10.refs_7_.refs_9_) | copy-start | bytes 589828
  18.7 8.2 %collective-permute-start.1 = (bf16[192,512]{1,0:T(8,128)(2,1)S(1)}, bf16[192,512]{1,0:T(8,128)(2,1)S(1)}, u32[]{:S(2)}, u32[]{:S(2)}) collective-permute-start(bf16[192,512]{1,0:T(8,128)(2,1)S(1)} %collective-permute-done.refs_0_.refs_2_), channel_id=1, source_target_pairs={{0,2},{2,4},{4,6},{6,0},{1,3},{3,5},{5,7},{7,1},{8,10},{10,12},{12... | collective-permute-start | bytes 589832 | tf_op jit(solution)/shard_map/ppermute | solution.py:527
  24.7 3.2 %copy-start.9 = (bf16[192,512]{1,0:T(8,128)(2,1)}, bf16[192,512]{1,0:T(8,128)(2,1)S(1)}, u32[]{:S(2)}) copy-start(bf16[192,512]{1,0:T(8,128)(2,1)S(1)} %collective-permute-done.3.refs_1_.refs_11_) | copy-start | bytes 589828
  27.0 1.4 %collective-permute-start.11 = (bf16[192,512]{1,0:T(8,128)(2,1)S(1)}, bf16[192,512]{1,0:T(8,128)(2,1)S(1)}, u32[]{:S(2)}, u32[]{:S(2)}) collective-permute-start(bf16[192,512]{1,0:T(8,128)(2,1)S(1)} %collective-permute-done.1.refs_0_.refs_10_), channel_id=1, source_target_pairs={{0,1},{1,0},{2,3},{3,2},{4,5},{5,4},{6,7},{7,6},{8,9},{9,8},{10,11... | collective-permute-start | bytes 589832 | tf_op jit(solution)/shard_map/ppermute | solution.py:527
  27.0 1.7 %collective-permute-start.12 = (bf16[192,512]{1,0:T(8,128)(2,1)S(1)}, bf16[192,512]{1,0:T(8,128)(2,1)S(1)}, u32[]{:S(2)}, u32[]{:S(2)}) collective-permute-start(bf16[192,512]{1,0:T(8,128)(2,1)S(1)} %collective-permute-done.3.refs_1_.refs_11_), channel_id=1, source_target_pairs={{0,1},{1,0},{2,3},{3,2},{4,5},{5,4},{6,7},{7,6},{8,9},{9,8},{10,11... | collective-permute-start | bytes 589832 | tf_op jit(solution)/shard_map/ppermute | solution.py:527
  28.4 5.9 %copy-start.11 = (bf16[192,512]{1,0:T(8,128)(2,1)}, bf16[192,512]{1,0:T(8,128)(2,1)S(1)}, u32[]{:S(2)}) copy-start(bf16[192,512]{1,0:T(8,128)(2,1)S(1)} %collective-permute-done.11.refs_0_.refs_12_) | copy-start | bytes 589828
  28.7 5.6 %copy-start.12 = (bf16[192,512]{1,0:T(8,128)(2,1)}, bf16[192,512]{1,0:T(8,128)(2,1)S(1)}, u32[]{:S(2)}) copy-start(bf16[192,512]{1,0:T(8,128)(2,1)S(1)} %collective-permute-done.12.refs_1_.refs_13_) | copy-start | bytes 589828
  34.3 13.6 %all-to-all-start = ((bf16[8,208,128]{2,1,0:T(8,128)(2,1)}), bf16[8,208,128]{2,1,0:T(8,128)(2,1)S(1)}, u32[]{:S(2)}, u32[]{:S(2)}) async-start(bf16[8,208,128]{2,1,0:T(8,128)(2,1)} %get-tuple-element.65), calls=%async_computation | async-start | bytes 851968 | tf_op jit(solution)/shard_map/all_to_all | solution.py:596
  40.5 22.2 %copy-start.14 = (f32[2,2]{1,0:T(2,128)S(1)}, f32[2,2]{1,0:T(2,128)}, u32[]{:S(2)}) copy-start(f32[2,2]{1,0:T(2,128)} %beta_ref.1) | copy-start | bytes 52
  40.5 22.2 %copy-start.15 = (f32[2,2]{1,0:T(2,128)S(1)}, f32[2,2]{1,0:T(2,128)}, u32[]{:S(2)}) copy-start(f32[2,2]{1,0:T(2,128)} %decay_ref.1) | copy-start | bytes 52
  40.5 22.2 %copy-start.16 = (bf16[2,2,128]{2,1,0:T(2,128)(2,1)S(1)}, bf16[2,2,128]{2,1,0:T(2,128)(2,1)}, u32[]{:S(2)}) copy-start(bf16[2,2,128]{2,1,0:T(2,128)(2,1)} %query_ref.1) | copy-start | bytes 3076
  40.5 22.2 %copy-start.17 = (bf16[2,2,128]{2,1,0:T(2,128)(2,1)S(1)}, bf16[2,2,128]{2,1,0:T(2,128)(2,1)}, u32[]{:S(2)}) copy-start(bf16[2,2,128]{2,1,0:T(2,128)(2,1)} %key_ref.1) | copy-start | bytes 3076
  40.5 22.2 %copy-start.18 = (bf16[2,2,128]{2,1,0:T(2,128)(2,1)S(1)}, bf16[2,2,128]{2,1,0:T(2,128)(2,1)}, u32[]{:S(2)}) copy-start(bf16[2,2,128]{2,1,0:T(2,128)(2,1)} %value_ref.1) | copy-start | bytes 3076
  46.7 26.3 %copy-start.13 = (f32[128]{0:T(128)S(1)}, f32[128]{0:T(128)}, u32[]{:S(2)}) copy-start(f32[128]{0:T(128)} %param.24) | copy-start | bytes 1540
  48.4 9.2 %collective-permute-start.15 = (bf16[208,128]{1,0:T(8,128)(2,1)S(1)}, bf16[208,128]{1,0:T(8,128)(2,1)S(1)}, u32[]{:S(2)}, u32[]{:S(2)}) collective-permute-start(bf16[208,128]{1,0:T(8,128)(2,1)S(1)} %get-tuple-element.73._.own), channel_id=1, source_target_pairs={{0,192},{64,128},{128,64},{192,0},{1,193},{65,129},{129,65},{193,1... | collective-permute-start | bytes 159752 | tf_op jit(solution)/shard_map/ppermute | solution.py:628
  53.9 8.8 %collective-permute-start.14 = (bf16[208,128]{1,0:T(8,128)(2,1)S(1)}, bf16[208,128]{1,0:T(8,128)(2,1)S(1)}, u32[]{:S(2)}, u32[]{:S(2)}) collective-permute-start(bf16[208,128]{1,0:T(8,128)(2,1)S(1)} %get-tuple-element.73._.own), channel_id=1, source_target_pairs={{0,128},{64,192},{128,0},{192,64},{1,129},{65,193},{129,1},{193,65... | collective-permute-start | bytes 159752 | tf_op jit(solution)/shard_map/ppermute | solution.py:628
  55.3 7.4 %collective-permute-start.13 = (bf16[208,128]{1,0:T(8,128)(2,1)S(1)}, bf16[208,128]{1,0:T(8,128)(2,1)S(1)}, u32[]{:S(2)}, u32[]{:S(2)}) collective-permute-start(bf16[208,128]{1,0:T(8,128)(2,1)S(1)} %get-tuple-element.73._.own), channel_id=1, source_target_pairs={{0,64},{64,0},{128,192},{192,128},{1,65},{65,1},{129,193},{193,129... | collective-permute-start | bytes 159752 | tf_op jit(solution)/shard_map/ppermute | solution.py:628
  (6 other events, 8.9 us)

commit v9 on v7

--- a/solution.py
+++ b/solution.py
@@ -79,13 +79,23 @@
 )
 
 
+def split_kernel(source, first, second, sems):
+    copies = [
+        pltpu.make_async_copy(source.at[at], to, sems.at[at]) for at, to in enumerate((first, second))
+    ]
+    for copy in copies:
+        copy.start()
+    for copy in copies:
+        copy.wait()
+
+
 def early_kernel(
-    own, own_c, beta_w, decay_w, key_w, value_w, sum_ref, gate_ref, rest_ref, stacked_ref,
-    token_buffer, weight_buffer, scalar_buffer, sems,
+    own_first, own_second, own_c, beta_w, decay_w, key_w, value_w, sum_ref, gate_ref, rest_ref, stacked_ref,
+    weight_buffer, scalar_buffer, sems,
 ):
-    depth = own.shape[-1]
+    depth = own_c.shape[-1]
     width = key_w.shape[-1]
-    first = [pltpu.make_async_copy(own, token_buffer, sems.at[0])]
+    first = []
     for at, weight in enumerate((beta_w, decay_w)):
         first.append(pltpu.make_async_copy(weight, scalar_buffer.at[at], sems.at[0]))
     later = []
@@ -107,8 +117,8 @@
     rows = [scalar_buffer[at, h : h + 1, :].astype(f32) for at in range(2) for h in range(2)]
     stacked_ref[...] = row_pack(rows, stacked_ref.shape[-1]).astype(bf16)
     total = gates = 0.0
-    for at, piece in enumerate((token_buffer, own_c)):
-        rows = piece[...].reshape(-1, depth)
+    for at in range(2):
+        rows = own_c[...].reshape(-1, depth) if at else joined(own_first, own_second)
         total = total + dot(rows, weight_buffer[at * depth : (at + 1) * depth, :])
         gates = gates + scalar_part(rows, stacked_ref, SLOTS[at])
     sum_ref[...] = total
@@ -264,6 +274,8 @@
         gain = dot(fresh * late, keys, COLS)
         fresh_ref[pair] = fresh.astype(bf16)
         carry_ref[pair] = carry.astype(bf16)
+        give(2, pair)
+        give(3, pair)
         factor = row_pack(thirds(jnp.broadcast_to(jnp.exp(last), (1, head))), head)
         for side in range(2):
             to = 2 * pair + side
@@ -271,8 +283,6 @@
             send_ref[to, head : head + half, :] = gain[side * half : (side + 1) * half].astype(bf16)
             send_ref[to, head + half :, :] = factor.astype(bf16)
         give(0, pl.ds(2 * pair, 2))
-    give(2)
-    give(3)
     for copy in copies:
         copy.wait()
 
@@ -347,40 +357,52 @@
     return block[0:1] + block[1:2] + block[2:3]
 
 
-def compose_kernel(in_ref, total_ref, maps_ref, adds_ref, factors_ref):
-    count, rows, head = in_ref.shape
-    body = rows - PACK
-
-    def load(at):
-        return in_ref[at, :body, :].astype(f32), unpack_factor(in_ref[at, body:, :])
-
-    def join(first, second):
-        both, factor = first
-        later, later_factor = second
-        tail = jnp.concatenate([factor * later[:head], later[head:]], axis=0)
-        return later_factor * both - dot(both, later[:head]) + tail, factor * later_factor
-
-    member = [load(at) for at in range(count)]
-    upto = [None] * (count + 1)
-    upto[1] = member[0]
-    c23, c45, c67 = (join(member[at], member[at + 1]) for at in (2, 4, 6))
-    upto[2] = join(member[0], member[1])
-    c456 = join(c45, member[6])
-    c4567 = join(c45, c67)
-    upto[4] = join(upto[2], c23)
-    upto[8] = join(upto[4], c4567)
-    both, factor = upto[8]
+def load_member(in_ref, at):
+    body = in_ref.shape[1] - PACK
+    return in_ref[at, :body, :].astype(f32), unpack_factor(in_ref[at, body:, :])
+
+
+def join(first, second):
+    both, factor = first
+    later, later_factor = second
+    head = later.shape[-1]
+    tail = jnp.concatenate([factor * later[:head], later[head:]], axis=0)
+    return later_factor * both - dot(both, later[:head]) + tail, factor * later_factor
+
+
+def total_kernel(in_ref, total_ref):
+    parts = [load_member(in_ref, at) for at in range(in_ref.shape[0])]
+    while len(parts) > 1:
+        parts = [join(parts[at], parts[at + 1]) for at in range(0, len(parts), 2)]
+    both, factor = parts[0]
+    body, head = both.shape
     total_ref[:body, :] = both.astype(bf16)
     total_ref[body:, :] = row_pack(thirds(factor), head).astype(bf16)
-    upto[3] = join(upto[2], member[2])
-    upto[5] = join(upto[4], member[4])
-    upto[6] = join(upto[4], c45)
-    upto[7] = join(upto[4], c456)
+
+
+def prefix_kernel(_, in_ref, out_in, reach_in, silu_in, *refs):
+    maps_ref, adds_ref, factors_ref, out_ref, reach_ref, silu_ref, sems = refs
+    moved = ((out_in, out_ref), (reach_in, reach_ref), (silu_in, silu_ref))
+    copies = [pltpu.make_async_copy(a, b, sems.at[at]) for at, (a, b) in enumerate(moved)]
+    for copy in copies:
+        copy.start()
+    count, _, head = in_ref.shape
+    member = [load_member(in_ref, at) for at in range(count - 1)]
+    c23, c45 = (join(member[at], member[at + 1]) for at in (2, 4))
+    upto = [None, member[0], join(member[0], member[1])]
+    c456 = join(c45, member[6])
+    upto.append(join(upto[2], member[2]))
+    upto.append(join(upto[2], c23))
+    upto.append(join(upto[4], member[4]))
+    upto.append(join(upto[4], c45))
+    upto.append(join(upto[4], c456))
     for at in range(1, count):
         both, factor = upto[at]
         maps_ref[at - 1] = both[:head].astype(bf16)
         adds_ref[at - 1] = both[head:]
         factors_ref[at - 1] = jnp.broadcast_to(factor, (8, head))
+    for copy in copies:
+        copy.wait()
 
 
 def spread_kernel(
@@ -453,18 +475,6 @@
         send_ref[member, half:, :] = (dot(pick, mine) + extra).astype(bf16)
 
 
-def load_kernel(_, *refs):
-    count = len(refs) // 2
-    sources, outputs, sems = refs[:count], refs[count : 2 * count], refs[2 * count]
-    copies = [
-        pltpu.make_async_copy(a, b, sems.at[at]) for at, (a, b) in enumerate(zip(sources, outputs))
-    ]
-    for copy in copies:
-        copy.start()
-    for copy in copies:
-        copy.wait()
-
-
 def finish_kernel(in_ref, out_ref, reach_ref, silu_ref, gain_ref, mixed_ref, cache_ref, read_ref):
     head = in_ref.shape[-1]
     half = head // 2
@@ -527,17 +537,17 @@
     depth = tokens.shape[2]
     swap = lambda value: shift(value, "c", 1)
     tokens_c = swap(tokens)
-    first, second = tokens[0], tokens[1]
+    half_span = ("p", on((span, depth), bf16))
+    first, second = kernel(split_kernel, [half_span, half_span], "h", (tokens,), (dma((2,)),))
     up0 = shift(first, "y", 1)
     down1 = shift(second, "y", -1)
     sums = [("p", on((2 * span, 2 * width), f32)), ("p", on((2 * span, head), f32))]
     early = kernel(
         early_kernel,
         sums + [("p", on((6 * depth, 2 * width), bf16)), ("p", on((PACK, 8 * depth), bf16))],
-        "hphhhh",
-        (tokens, tokens_c, beta_weight.T, decay_weight.T, key_weight, value_weight),
+        "ppphhhh",
+        (first, second, tokens_c, beta_weight.T, decay_weight.T, key_weight, value_weight),
         (
-            on((2, span, depth), bf16),
             on((2 * depth, 2 * width), bf16),
             on((2, 2, 8 * depth), bf16),
             dma((2,)),
@@ -554,13 +564,13 @@
     swapped = []
     for value in near:
         swapped.append(swap(value))
-    middle = kernel(functools.partial(middle_kernel, 2), sums, "p" * 8, (*near, *early[:2], *rest))
+    middle = kernel(
+        functools.partial(middle_kernel, 2), sums, "p" * 12, (*near, *swapped, *early[:2], *rest)
+    )
     far0, far1, *middle = lax.optimization_barrier((far0, far1, *middle))
-    last = [far0, far1]
-    for at in range(2):
-        last.append(swap(last[at]))
+    last = [far0, far1, swap(far0), swap(far1)]
     middle = kernel(
-        functools.partial(middle_kernel, 4), sums, "p" * 10, (*swapped, far0, far1, *middle, *rest)
+        functools.partial(middle_kernel, 6), sums, "p" * 6, (far0, far1, *middle, *rest)
     )
     far_c0, far_c1, *middle = lax.optimization_barrier((*last[2:], *middle))
     last[2:] = [far_c0, far_c1]
@@ -599,29 +609,23 @@
         24,
     )
     arrived, local_out = lax.optimization_barrier((arrived, local_out))
-    total, maps, adds, factors = kernel(
-        compose_kernel,
+    (total,) = kernel(total_kernel, [("p", on((rows, head), bf16))], "p", (arrived,))
+    others = [
+        lax.ppermute(total, "zh", [(at, at ^ by) for at in range(4)]) for by in (1, 2, 3)
+    ]
+    maps, adds, factors, *finals_in = kernel(
+        prefix_kernel,
         [
-            ("p", on((rows, head), bf16)),
             ("p", on((7, head, head), bf16)),
             ("p", on((7, half, head), f32)),
             ("p", on((7, 8, head), f32)),
+            *(("p", out) for out in finals),
         ],
-        "p",
-        (arrived,),
-    )
-    others = [
-        lax.ppermute(total, "zh", [(at, at ^ by) for at in range(4)]) for by in (1, 2, 3)
-    ]
-    finals_in = kernel(
-        load_kernel,
-        [("p", out) for out in finals],
-        "phhh",
-        (total, local_out, reach, silu),
+        "pphhh",
+        (total, arrived, local_out, reach, silu),
         (dma((3,)),),
     )
-    *others, loaded = lax.optimization_barrier((*others, finals_in[0]))
-    finals_in = (loaded, *finals_in[1:])
+    *others, maps = lax.optimization_barrier((*others, maps))
     (back,) = kernel(
         spread_kernel,
         [("p", on((8, half + PACK, head), bf16))],

time: 70.3 us -> 72.6 us (1.033)
  waiting for transfers between devices: 14.2 us -> 20.8 us
  starting transfers between devices: 23.6 us -> 20.1 us
  local copies, waits for them, and re-layouts: 1.15 us -> 0.09 us
  Pallas kernels: 19.6 us -> 20.4 us
    ppermute x13, waiting for transfers between devices: 6.78 us -> 13.4 us  [shift(): lax.ppermute(value, axis, [(at, (at + by) % length) for at in range(lengt...]
    ppermute x13, starting transfers between devices: 10.3 us -> 8.05 us  [shift(): lax.ppermute(value, axis, [(at, (at + by) % length) for at in range(lengt...]
    all_to_all x1, starting transfers between devices: 5.32 us -> 4.11 us  [shards(): arrived = lax.all_to_all(send, NEAR, 0, 0, tiled=True)]
    squeeze x1 -> x0, local copies, waits for them, and re-layouts: 1.05 us -> none  [shards(): first, second = (tokens[0], tokens[1])]
    pallas_call x9 -> x10, Pallas kernels: 19.6 us -> 20.4 us  [kernel(): pl.pallas_call(body, out_shape=tuple((out if kind == 'p' else plain(out)...]
  transfers between devices with their start and end apart: 17 -> 17, of which waited for: 8 -> 9; matrix products, arithmetic and copies ran while one was open for 2% -> 0% of each run, Pallas kernels for 17% -> 17%
where the time goes in v9:
time: 72.6 us; the launch traced here: 72.4 us
  waiting for transfers between devices  20.8 us (29%)
  Pallas kernels  20.4 us (28%)
  starting transfers between devices  20.1 us (28%)
  blocking collectives  10 us (14%)
  between operations  0.95 us (1%)
    pallas_call x10, Pallas kernels, kernel(): pl.pallas_call(body, out_shape=tuple((out if kind == 'p' else plain(out)...  20.4 us
    ppermute x13, waiting for transfers between devices, shift(): lax.ppermute(value, axis, [(at, (at + by) % length) for at in range(lengt...  13.4 us
    all_to_all x1, blocking collectives, shards(): returned = lax.all_to_all(back, NEAR, 0, 0, tiled=True)  10 us
    ppermute x13, starting transfers between devices, shift(): lax.ppermute(value, axis, [(at, (at + by) % length) for at in range(lengt...  8.05 us
    ppermute x3, starting transfers between devices, shards(): lax.ppermute(total, 'zh', [(at, at ^ by) for at in range(4)])  7.94 us
    ppermute x3, waiting for transfers between devices, shards(): lax.ppermute(total, 'zh', [(at, at ^ by) for at in range(4)])  4.77 us
    all_to_all x1, starting transfers between devices, shards(): arrived = lax.all_to_all(send, NEAR, 0, 0, tiled=True)  4.11 us
    all_to_all x1, waiting for transfers between devices, shards(): arrived = lax.all_to_all(send, NEAR, 0, 0, tiled=True)  2.7 us
  transfers between devices with their start and end apart: 17, of which 9 were waited for; matrix products, arithmetic and copies ran while one was open for 0% of the time, Pallas kernels for 17%

profile of v9, /device:TPU:24, one launch (start us, length us, event | category | flops | bytes accessed | tf_op | source)
XLA Modules:
  0.0 72.4 jit_solution(4044257823263174515)
XLA Ops:
  0.6 0.1 collective-permute-start.4
  0.7 1.0 %shard_map.166 = (bf16[192,512]{1,0:T(8,128)(2,1)S(1)}, bf16[192,512]{1,0:T(8,128)(2,1)S(1)}) custom-call(bf16[2,192,512]{2,1,0:T(8,128)(2,1)} %refs_0_.1), custom_call_target="tpu_custom_call" | custom-call | tf_op jit(solution)/shard_map/pallas_call | solution.py:511
  1.8 2.0 %collective-permute-start = (bf16[192,512]{1,0:T(8,128)(2,1)S(1)}, bf16[192,512]{1,0:T(8,128)(2,1)S(1)}, u32[]{:S(2)}, u32[]{:S(2)}) collective-permute-start(bf16[192,512]{1,0:T(8,128)(2,1)S(1)} %get-tuple-element.51.own_first), channel_id=1, source_target_pairs={{0,2},{2,4},{4,6},{6,0},{1,3},{3,5},{5,7},{7,1},{8,10},{10,12},{12... | collective-permute-start | bytes 589832 | tf_op jit(solution)/shard_map/ppermute | solution.py:523
  3.8 0.1 collective-permute-start.2
  3.9 2.3 %shard_map.167 = (f32[384,512]{1,0:T(8,128)S(1)}, f32[384,128]{1,0:T(8,128)S(1)}, bf16[3072,512]{1,0:T(8,128)(2,1)S(1)}, bf16[16,4096]{1,0:T(8,128)(2,1)S(1)}) custom-call(bf16[192,512]{1,0:T(8,128)(2,1)S(1)} %get-tuple-element.51.own_first, bf16[192,512]{1,0:T(8,128)(2,1)S(1)} %get-tuple-element.50.own_second, ...), custom_call_target="tpu_custom_call" | custom-call | tf_op jit(solution)/shard_map/pallas_call | solution.py:511
  6.2 3.2 %collective-permute-start.5 = (bf16[192,512]{1,0:T(8,128)(2,1)S(1)}, bf16[192,512]{1,0:T(8,128)(2,1)S(1)}, u32[]{:S(2)}, u32[]{:S(2)}) collective-permute-start(bf16[192,512]{1,0:T(8,128)(2,1)S(1)} %get-tuple-element.50.own_second), channel_id=1, source_target_pairs={{0,2},{2,4},{4,6},{6,0},{1,3},{3,5},{5,7},{7,1},{8,10},{10,12},{12... | collective-permute-start | bytes 589832 | tf_op jit(solution)/shard_map/ppermute | solution.py:523
  9.5 0.1 collective-permute-start.7
  9.6 2.5 %collective-permute-done.2.refs_3_.refs_5_ = bf16[192,512]{1,0:T(8,128)(2,1)S(1)} collective-permute-done((bf16[192,512]{1,0:T(8,128)(2,1)S(1)}, bf16[192,512]{1,0:T(8,128)(2,1)S(1)}, u32[]{:S(2)}, u32[]{:S(2)}) %collective-permute-start.2) | collective-permute-done | bytes 196640 | tf_op jit(solution)/shard_map/ppermute | solution.py:523
  12.0 1.7 %collective-permute-done.5.refs_1_.refs_3_ = bf16[192,512]{1,0:T(8,128)(2,1)S(1)} collective-permute-done((bf16[192,512]{1,0:T(8,128)(2,1)S(1)}, bf16[192,512]{1,0:T(8,128)(2,1)S(1)}, u32[]{:S(2)}, u32[]{:S(2)}) %collective-permute-start.5) | collective-permute-done | bytes 196640 | tf_op jit(solution)/shard_map/ppermute | solution.py:523
  13.7 3.4 %collective-permute-done.6.refs_2_.refs_4_ = bf16[192,512]{1,0:T(8,128)(2,1)S(1)} collective-permute-done((bf16[192,512]{1,0:T(8,128)(2,1)S(1)}, bf16[192,512]{1,0:T(8,128)(2,1)S(1)}, u32[]{:S(2)}, u32[]{:S(2)}) %collective-permute-start.6) | collective-permute-done | bytes 196640 | tf_op jit(solution)/shard_map/ppermute | solution.py:523
  17.1 0.8 %collective-permute-start.1 = (bf16[192,512]{1,0:T(8,128)(2,1)S(1)}, bf16[192,512]{1,0:T(8,128)(2,1)S(1)}, u32[]{:S(2)}, u32[]{:S(2)}) collective-permute-start(bf16[192,512]{1,0:T(8,128)(2,1)S(1)} %collective-permute-done.refs_0_.refs_2_), channel_id=1, source_target_pairs={{0,2},{2,4},{4,6},{6,0},{1,3},{3,5},{5,7},{7,1},{8,10},{10,12},{12... | collective-permute-start | bytes 589832 | tf_op jit(solution)/shard_map/ppermute | solution.py:523
  17.9 1.2 %collective-permute-start.3 = (bf16[192,512]{1,0:T(8,128)(2,1)S(1)}, bf16[192,512]{1,0:T(8,128)(2,1)S(1)}, u32[]{:S(2)}, u32[]{:S(2)}) collective-permute-start(bf16[192,512]{1,0:T(8,128)(2,1)S(1)} %collective-permute-done.2.refs_3_.refs_5_), channel_id=1, source_target_pairs={{0,6},{2,0},{4,2},{6,4},{1,7},{3,1},{5,3},{7,5},{8,14},{10,8},{12,... | collective-permute-start | bytes 589832 | tf_op jit(solution)/shard_map/ppermute | solution.py:523
  19.2 1.4 %shard_map.168 = (f32[384,512]{1,0:T(8,128)S(1)}, f32[384,128]{1,0:T(8,128)S(1)}) custom-call(bf16[192,512]{1,0:T(8,128)(2,1)S(1)} %collective-permute-done.refs_0_.refs_2_, bf16[192,512]{1,0:T(8,128)(2,1)S(1)} %collective-permute-done.5.refs_1_.refs_3_, bf16[192,512]{1,0:T(8,128)(2,1)S(1)} %collective-permute-done.6.refs_2_.refs_4_, ...), custom_call_target="tpu_custom_call" | custom-call | tf_op jit(solution)/shard_map/pallas_call | solution.py:511
  20.7 3.8 %collective-permute-done.1.refs_0_.refs_10_ = bf16[192,512]{1,0:T(8,128)(2,1)S(1)} collective-permute-done((bf16[192,512]{1,0:T(8,128)(2,1)S(1)}, bf16[192,512]{1,0:T(8,128)(2,1)S(1)}, u32[]{:S(2)}, u32[]{:S(2)}) %collective-permute-start.1) | collective-permute-done | bytes 196640 | tf_op jit(solution)/shard_map/ppermute | solution.py:523
  24.4 1.3 %collective-permute-done.3.refs_1_.refs_11_ = bf16[192,512]{1,0:T(8,128)(2,1)S(1)} collective-permute-done((bf16[192,512]{1,0:T(8,128)(2,1)S(1)}, bf16[192,512]{1,0:T(8,128)(2,1)S(1)}, u32[]{:S(2)}, u32[]{:S(2)}) %collective-permute-start.3) | collective-permute-done | bytes 196640 | tf_op jit(solution)/shard_map/ppermute | solution.py:523
  25.8 0.5 collective-permute-start.12
  26.3 0.5 shard_map.169
  26.8 0.4 collective-permute-done.11.refs_0_.refs_12_
  27.2 0.3 collective-permute-done.12.refs_1_.refs_13_
  27.5 5.6 %shard_map.170 = (bf16[8,208,128]{2,1,0:T(8,128)(2,1)}, bf16[384,256]{1,0:T(8,128)(2,1)}, bf16[4,192,128]{2,1,0:T(8,128)(2,1)}, bf16[4,192,128]{2,1,0:T(8,128)(2...) custom-call(f32[1,2]{1,0:T(1,128)S(1)} %bitcast.7, f32[1,2]{1,0:T(1,128)S(1)} %bitcast.8, ...), custom_call_target="tpu_custom_call" | custom-call | tf_op jit(solution)/shard_map/pallas_call | solution.py:511
  33.1 4.1 %all-to-all-start = ((bf16[8,208,128]{2,1,0:T(8,128)(2,1)}), bf16[8,208,128]{2,1,0:T(8,128)(2,1)S(1)}, u32[]{:S(2)}, u32[]{:S(2)}) async-start(bf16[8,208,128]{2,1,0:T(8,128)(2,1)} %get-tuple-element.68), calls=%async_computation | async-start | bytes 851968 | tf_op jit(solution)/shard_map/all_to_all | solution.py:592
  37.3 6.1 %shard_map.171 = (f32[4,192,128]{2,1,0:T(8,128)}, bf16[4,192,128]{2,1,0:T(8,128)(2,1)}, f32[4,192,128]{2,1,0:T(8,128)}) custom-call(bf16[2,192,512]{2,1,0:T(8,128)(2,1)} %refs_0_.1, bf16[2,192,512]{2,1,0:T(8,128)(2,1)} %copy-done, bf16[192,512]{1,0:T(8,128)(2,1)} %copy-done.1, bf16[192,512]{1,0:T(8,128)(2,1)} %copy-done.3, bf16[192,512]{1,0:T(8,128)(2,1)} %copy-done.4, ...), custom_call_target="tpu_custom_call" | custom-call | tf_op jit(solution)/shard_map/pallas_call | solution.py:511
  43.4 2.7 %all-to-all-done.in_ref = bf16[8,208,128]{2,1,0:T(8,128)(2,1)S(1)} async-done(((bf16[8,208,128]{2,1,0:T(8,128)(2,1)}), bf16[8,208,128]{2,1,0:T(8,128)(2,1)S(1)}, u32[]{:S(2)}, u32[]{:S(2)}) %all-to-all-start) | async-done | bytes 426016 | tf_op jit(solution)/shard_map/all_to_all | solution.py:592
  46.1 0.5 shard_map.172._.own
  46.6 5.5 %collective-permute-start.15 = (bf16[208,128]{1,0:T(8,128)(2,1)S(1)}, bf16[208,128]{1,0:T(8,128)(2,1)S(1)}, u32[]{:S(2)}, u32[]{:S(2)}) collective-permute-start(bf16[208,128]{1,0:T(8,128)(2,1)S(1)} %shard_map.172._.own), channel_id=1, source_target_pairs={{0,192},{64,128},{128,64},{192,0},{1,193},{65,129},{129,65},{193,1... | collective-permute-start | bytes 159752 | tf_op jit(solution)/shard_map/ppermute | solution.py:614
  52.1 1.4 %collective-permute-start.14 = (bf16[208,128]{1,0:T(8,128)(2,1)S(1)}, bf16[208,128]{1,0:T(8,128)(2,1)S(1)}, u32[]{:S(2)}, u32[]{:S(2)}) collective-permute-start(bf16[208,128]{1,0:T(8,128)(2,1)S(1)} %shard_map.172._.own), channel_id=1, source_target_pairs={{0,128},{64,192},{128,0},{192,64},{1,129},{65,193},{129,1},{193,65... | collective-permute-start | bytes 159752 | tf_op jit(solution)/shard_map/ppermute | solution.py:614
  53.5 1.0 %collective-permute-start.13 = (bf16[208,128]{1,0:T(8,128)(2,1)S(1)}, bf16[208,128]{1,0:T(8,128)(2,1)S(1)}, u32[]{:S(2)}, u32[]{:S(2)}) collective-permute-start(bf16[208,128]{1,0:T(8,128)(2,1)S(1)} %shard_map.172._.own), channel_id=1, source_target_pairs={{0,64},{64,0},{128,192},{192,128},{1,65},{65,1},{129,193},{193,129... | collective-permute-start | bytes 159752 | tf_op jit(solution)/shard_map/ppermute | solution.py:614
  54.5 1.2 %shard_map.173 = (bf16[7,128,128]{2,1,0:T(8,128)(2,1)S(1)}, f32[7,64,128]{2,1,0:T(8,128)S(1)}, f32[7,8,128]{2,1,0:T(8,128)S(1)}, f32[4,192,128]{2,1,0:T(8,128)S(...) custom-call(bf16[208,128]{1,0:T(8,128)(2,1)S(1)} %shard_map.172._.own, ...), custom_call_target="tpu_custom_call" | custom-call | tf_op jit(solution)/shard_map/pallas_call | solution.py:511
  55.8 4.8 %collective-permute-done.14.back2 = bf16[208,128]{1,0:T(8,128)(2,1)S(1)} collective-permute-done((bf16[208,128]{1,0:T(8,128)(2,1)S(1)}, bf16[208,128]{1,0:T(8,128)(2,1)S(1)}, u32[]{:S(2)}, u32[]{:S(2)}) %collective-permute-start.14) | collective-permute-done | bytes 53280 | tf_op jit(solution)/shard_map/ppermute | solution.py:614
  60.6 0.7 %shard_map.174 = bf16[8,80,128]{2,1,0:T(8,128)(2,1)S(1)} custom-call(f32[2,2]{1,0:T(2,128)S(1)} %copy-done.14, f32[2,2]{1,0:T(2,128)S(1)} %copy-done.15, bf16[208,128]{1,0:T(8,128)(2,1)S(1)} %shard_map.172._.own, bf16[208,128]{1,0:T(8,128)(2,1)S(1)} %collective-permute-done.13.back1, bf16[208,128]{1,0:T(8,128)(2,1)S(1)} %collective-permute-done.14.back2, ...), custom_call_target="tpu_custom_call" | custom-call | tf_op jit(solution)/shard_map/pallas_call | solution.py:511
  61.3 10.0 %all_to_all.10.in_ref = bf16[8,80,128]{2,1,0:T(8,128)(2,1)S(1)} all-to-all(bf16[8,80,128]{2,1,0:T(8,128)(2,1)S(1)} %shard_map.174), channel_id=1, replica_groups=mesh['zh'=4,'zl'=2,'x'=4,'y'=4,'c'=2] {'zl','x'}, dimensions={0} | all-to-all | bytes 327680 | tf_op jit(solution)/shard_map/all_to_all | solution.py:639
  71.3 1.0 %shard_map.175 = (bf16[2,192,256]{2,1,0:T(8,128)(2,1)}, bf16[2,2,4,128]{3,2,1,0:T(4,128)(2,1)}, f32[2,256]{1,0:T(2,128)}) custom-call(bf16[8,80,128]{2,1,0:T(8,128)(2,1)S(1)} %all_to_all.10.in_ref, f32[4,192,128]{2,1,0:T(8,128)S(1)} %get-tuple-element.86.out_ref, bf16[4,192,128]{2,1,0:T(8,128)(2,1)S(1)} %get-tuple-element.87.reach_ref, ...), custom_call_target="tpu_custom_call" | custom-call | tf_op jit(solution)/shard_map/pallas_call | solution.py:511
  (55 shorter events, 0.1 us)
Async XLA Ops:
  0.6 3.3 %collective-permute-start.4 = (bf16[2,192,512]{2,1,0:T(8,128)(2,1)}, bf16[2,192,512]{2,1,0:T(8,128)(2,1)S(1)}, u32[]{:S(2)}, u32[]{:S(2)}) collective-permute-start(bf16[2,192,512]{2,1,0:T(8,128)(2,1)} %refs_0_.1), channel_id=1, source_target_pairs={{0,1},{1,0},{2,3},{3,2},{4,5},{5,4},{6,7},{7,6},{8,9},{9,8},{10,11... | collective-permute-start | bytes 1179656 | tf_op jit(solution)/shard_map/ppermute | solution.py:523
  1.8 7.7 %collective-permute-start = (bf16[192,512]{1,0:T(8,128)(2,1)S(1)}, bf16[192,512]{1,0:T(8,128)(2,1)S(1)}, u32[]{:S(2)}, u32[]{:S(2)}) collective-permute-start(bf16[192,512]{1,0:T(8,128)(2,1)S(1)} %get-tuple-element.51.own_first), channel_id=1, source_target_pairs={{0,2},{2,4},{4,6},{6,0},{1,3},{3,5},{5,7},{7,1},{8,10},{10,12},{12... | collective-permute-start | bytes 589832 | tf_op jit(solution)/shard_map/ppermute | solution.py:523
  3.8 8.2 %collective-permute-start.2 = (bf16[192,512]{1,0:T(8,128)(2,1)S(1)}, bf16[192,512]{1,0:T(8,128)(2,1)S(1)}, u32[]{:S(2)}, u32[]{:S(2)}) collective-permute-start(bf16[192,512]{1,0:T(8,128)(2,1)S(1)} %get-tuple-element.50.own_second), channel_id=1, source_target_pairs={{0,6},{2,0},{4,2},{6,4},{1,7},{3,1},{5,3},{7,5},{8,14},{10,8},{12,... | collective-permute-start | bytes 589832 | tf_op jit(solution)/shard_map/ppermute | solution.py:523
  3.9 2.3 %copy-start = (bf16[2,192,512]{2,1,0:T(8,128)(2,1)}, bf16[2,192,512]{2,1,0:T(8,128)(2,1)S(1)}, u32[]{:S(2)}) copy-start(bf16[2,192,512]{2,1,0:T(8,128)(2,1)S(1)} %collective-permute-done.4.own_c.refs_1_) | copy-start | bytes 1179652
  6.2 7.5 %collective-permute-start.5 = (bf16[192,512]{1,0:T(8,128)(2,1)S(1)}, bf16[192,512]{1,0:T(8,128)(2,1)S(1)}, u32[]{:S(2)}, u32[]{:S(2)}) collective-permute-start(bf16[192,512]{1,0:T(8,128)(2,1)S(1)} %get-tuple-element.50.own_second), channel_id=1, source_target_pairs={{0,2},{2,4},{4,6},{6,0},{1,3},{3,5},{5,7},{7,1},{8,10},{10,12},{12... | collective-permute-start | bytes 589832 | tf_op jit(solution)/shard_map/ppermute | solution.py:523
  9.4 7.7 %collective-permute-start.6 = (bf16[192,512]{1,0:T(8,128)(2,1)S(1)}, bf16[192,512]{1,0:T(8,128)(2,1)S(1)}, u32[]{:S(2)}, u32[]{:S(2)}) collective-permute-start(bf16[192,512]{1,0:T(8,128)(2,1)S(1)} %get-tuple-element.51.own_first), channel_id=1, source_target_pairs={{0,6},{2,0},{4,2},{6,4},{1,7},{3,1},{5,3},{7,5},{8,14},{10,8},{12,... | collective-permute-start | bytes 589832 | tf_op jit(solution)/shard_map/ppermute | solution.py:523
  9.4 11.1 %copy-start.1 = (bf16[192,512]{1,0:T(8,128)(2,1)}, bf16[192,512]{1,0:T(8,128)(2,1)S(1)}, u32[]{:S(2)}) copy-start(bf16[192,512]{1,0:T(8,128)(2,1)S(1)} %collective-permute-done.refs_0_.refs_2_) | copy-start | bytes 589828
  9.5 8.5 %collective-permute-start.7 = (bf16[192,512]{1,0:T(8,128)(2,1)S(1)}, bf16[192,512]{1,0:T(8,128)(2,1)S(1)}, u32[]{:S(2)}, u32[]{:S(2)}) collective-permute-start(bf16[192,512]{1,0:T(8,128)(2,1)S(1)} %collective-permute-done.refs_0_.refs_2_), channel_id=1, source_target_pairs={{0,1},{1,0},{2,3},{3,2},{4,5},{5,4},{6,7},{7,6},{8,9},{9,8},{10,11... | collective-permute-start | bytes 589832 | tf_op jit(solution)/shard_map/ppermute | solution.py:523
  12.0 8.6 %copy-start.2 = (bf16[192,512]{1,0:T(8,128)(2,1)}, bf16[192,512]{1,0:T(8,128)(2,1)S(1)}, u32[]{:S(2)}) copy-start(bf16[192,512]{1,0:T(8,128)(2,1)S(1)} %collective-permute-done.2.refs_3_.refs_5_) | copy-start | bytes 589828
  12.0 7.1 %collective-permute-start.10 = (bf16[192,512]{1,0:T(8,128)(2,1)S(1)}, bf16[192,512]{1,0:T(8,128)(2,1)S(1)}, u32[]{:S(2)}, u32[]{:S(2)}) collective-permute-start(bf16[192,512]{1,0:T(8,128)(2,1)S(1)} %collective-permute-done.2.refs_3_.refs_5_), channel_id=1, source_target_pairs={{0,1},{1,0},{2,3},{3,2},{4,5},{5,4},{6,7},{7,6},{8,9},{9,8},{10,11... | collective-permute-start | bytes 589832 | tf_op jit(solution)/shard_map/ppermute | solution.py:523
  13.7 6.9 %copy-start.3 = (bf16[192,512]{1,0:T(8,128)(2,1)}, bf16[192,512]{1,0:T(8,128)(2,1)S(1)}, u32[]{:S(2)}) copy-start(bf16[192,512]{1,0:T(8,128)(2,1)S(1)} %collective-permute-done.5.refs_1_.refs_3_) | copy-start | bytes 589828
  13.7 5.5 %collective-permute-start.8 = (bf16[192,512]{1,0:T(8,128)(2,1)S(1)}, bf16[192,512]{1,0:T(8,128)(2,1)S(1)}, u32[]{:S(2)}, u32[]{:S(2)}) collective-permute-start(bf16[192,512]{1,0:T(8,128)(2,1)S(1)} %collective-permute-done.5.refs_1_.refs_3_), channel_id=1, source_target_pairs={{0,1},{1,0},{2,3},{3,2},{4,5},{5,4},{6,7},{7,6},{8,9},{9,8},{10,11... | collective-permute-start | bytes 589832 | tf_op jit(solution)/shard_map/ppermute | solution.py:523
  17.1 3.5 %copy-start.4 = (bf16[192,512]{1,0:T(8,128)(2,1)}, bf16[192,512]{1,0:T(8,128)(2,1)S(1)}, u32[]{:S(2)}) copy-start(bf16[192,512]{1,0:T(8,128)(2,1)S(1)} %collective-permute-done.6.refs_2_.refs_4_) | copy-start | bytes 589828
  17.1 2.1 %collective-permute-start.9 = (bf16[192,512]{1,0:T(8,128)(2,1)S(1)}, bf16[192,512]{1,0:T(8,128)(2,1)S(1)}, u32[]{:S(2)}, u32[]{:S(2)}) collective-permute-start(bf16[192,512]{1,0:T(8,128)(2,1)S(1)} %collective-permute-done.6.refs_2_.refs_4_), channel_id=1, source_target_pairs={{0,1},{1,0},{2,3},{3,2},{4,5},{5,4},{6,7},{7,6},{8,9},{9,8},{10,11... | collective-permute-start | bytes 589832 | tf_op jit(solution)/shard_map/ppermute | solution.py:523
  17.1 7.3 %collective-permute-start.1 = (bf16[192,512]{1,0:T(8,128)(2,1)S(1)}, bf16[192,512]{1,0:T(8,128)(2,1)S(1)}, u32[]{:S(2)}, u32[]{:S(2)}) collective-permute-start(bf16[192,512]{1,0:T(8,128)(2,1)S(1)} %collective-permute-done.refs_0_.refs_2_), channel_id=1, source_target_pairs={{0,2},{2,4},{4,6},{6,0},{1,3},{3,5},{5,7},{7,1},{8,10},{10,12},{12... | collective-permute-start | bytes 589832 | tf_op jit(solution)/shard_map/ppermute | solution.py:523
  17.9 2.7 %copy-start.5 = (bf16[192,512]{1,0:T(8,128)(2,1)}, bf16[192,512]{1,0:T(8,128)(2,1)S(1)}, u32[]{:S(2)}) copy-start(bf16[192,512]{1,0:T(8,128)(2,1)S(1)} %collective-permute-done.7.refs_4_.refs_6_) | copy-start | bytes 589828
  17.9 7.8 %collective-permute-start.3 = (bf16[192,512]{1,0:T(8,128)(2,1)S(1)}, bf16[192,512]{1,0:T(8,128)(2,1)S(1)}, u32[]{:S(2)}, u32[]{:S(2)}) collective-permute-start(bf16[192,512]{1,0:T(8,128)(2,1)S(1)} %collective-permute-done.2.refs_3_.refs_5_), channel_id=1, source_target_pairs={{0,6},{2,0},{4,2},{6,4},{1,7},{3,1},{5,3},{7,5},{8,14},{10,8},{12,... | collective-permute-start | bytes 589832 | tf_op jit(solution)/shard_map/ppermute | solution.py:523
  24.4 2.3 %copy-start.9 = (bf16[192,512]{1,0:T(8,128)(2,1)}, bf16[192,512]{1,0:T(8,128)(2,1)S(1)}, u32[]{:S(2)}) copy-start(bf16[192,512]{1,0:T(8,128)(2,1)S(1)} %collective-permute-done.1.refs_0_.refs_10_) | copy-start | bytes 589828
  25.8 1.4 %collective-permute-start.11 = (bf16[192,512]{1,0:T(8,128)(2,1)S(1)}, bf16[192,512]{1,0:T(8,128)(2,1)S(1)}, u32[]{:S(2)}, u32[]{:S(2)}) collective-permute-start(bf16[192,512]{1,0:T(8,128)(2,1)S(1)} %collective-permute-done.1.refs_0_.refs_10_), channel_id=1, source_target_pairs={{0,1},{1,0},{2,3},{3,2},{4,5},{5,4},{6,7},{7,6},{8,9},{9,8},{10,11... | collective-permute-start | bytes 589832 | tf_op jit(solution)/shard_map/ppermute | solution.py:523
  25.8 1.7 %collective-permute-start.12 = (bf16[192,512]{1,0:T(8,128)(2,1)S(1)}, bf16[192,512]{1,0:T(8,128)(2,1)S(1)}, u32[]{:S(2)}, u32[]{:S(2)}) collective-permute-start(bf16[192,512]{1,0:T(8,128)(2,1)S(1)} %collective-permute-done.3.refs_1_.refs_11_), channel_id=1, source_target_pairs={{0,1},{1,0},{2,3},{3,2},{4,5},{5,4},{6,7},{7,6},{8,9},{9,8},{10,11... | collective-permute-start | bytes 589832 | tf_op jit(solution)/shard_map/ppermute | solution.py:523
  27.2 5.9 %copy-start.11 = (bf16[192,512]{1,0:T(8,128)(2,1)}, bf16[192,512]{1,0:T(8,128)(2,1)S(1)}, u32[]{:S(2)}) copy-start(bf16[192,512]{1,0:T(8,128)(2,1)S(1)} %collective-permute-done.11.refs_0_.refs_12_) | copy-start | bytes 589828
  27.5 5.6 %copy-start.12 = (bf16[192,512]{1,0:T(8,128)(2,1)}, bf16[192,512]{1,0:T(8,128)(2,1)S(1)}, u32[]{:S(2)}) copy-start(bf16[192,512]{1,0:T(8,128)(2,1)S(1)} %collective-permute-done.12.refs_1_.refs_13_) | copy-start | bytes 589828
  33.1 13.0 %all-to-all-start = ((bf16[8,208,128]{2,1,0:T(8,128)(2,1)}), bf16[8,208,128]{2,1,0:T(8,128)(2,1)S(1)}, u32[]{:S(2)}, u32[]{:S(2)}) async-start(bf16[8,208,128]{2,1,0:T(8,128)(2,1)} %get-tuple-element.68), calls=%async_computation | async-start | bytes 851968 | tf_op jit(solution)/shard_map/all_to_all | solution.py:592
  37.2 23.3 %copy-start.14 = (f32[2,2]{1,0:T(2,128)S(1)}, f32[2,2]{1,0:T(2,128)}, u32[]{:S(2)}) copy-start(f32[2,2]{1,0:T(2,128)} %beta_ref.1) | copy-start | bytes 52
  37.2 23.3 %copy-start.15 = (f32[2,2]{1,0:T(2,128)S(1)}, f32[2,2]{1,0:T(2,128)}, u32[]{:S(2)}) copy-start(f32[2,2]{1,0:T(2,128)} %decay_ref.1) | copy-start | bytes 52
  37.2 23.3 %copy-start.16 = (bf16[2,2,128]{2,1,0:T(2,128)(2,1)S(1)}, bf16[2,2,128]{2,1,0:T(2,128)(2,1)}, u32[]{:S(2)}) copy-start(bf16[2,2,128]{2,1,0:T(2,128)(2,1)} %query_ref.1) | copy-start | bytes 3076
  37.2 23.3 %copy-start.17 = (bf16[2,2,128]{2,1,0:T(2,128)(2,1)S(1)}, bf16[2,2,128]{2,1,0:T(2,128)(2,1)}, u32[]{:S(2)}) copy-start(bf16[2,2,128]{2,1,0:T(2,128)(2,1)} %key_ref.1) | copy-start | bytes 3076
  37.2 23.3 %copy-start.18 = (bf16[2,2,128]{2,1,0:T(2,128)(2,1)S(1)}, bf16[2,2,128]{2,1,0:T(2,128)(2,1)}, u32[]{:S(2)}) copy-start(bf16[2,2,128]{2,1,0:T(2,128)(2,1)} %value_ref.1) | copy-start | bytes 3076
  43.4 27.9 %copy-start.13 = (f32[128]{0:T(128)S(1)}, f32[128]{0:T(128)}, u32[]{:S(2)}) copy-start(f32[128]{0:T(128)} %param.24) | copy-start | bytes 1540
  46.6 9.2 %collective-permute-start.15 = (bf16[208,128]{1,0:T(8,128)(2,1)S(1)}, bf16[208,128]{1,0:T(8,128)(2,1)S(1)}, u32[]{:S(2)}, u32[]{:S(2)}) collective-permute-start(bf16[208,128]{1,0:T(8,128)(2,1)S(1)} %shard_map.172._.own), channel_id=1, source_target_pairs={{0,192},{64,128},{128,64},{192,0},{1,193},{65,129},{129,65},{193,1... | collective-permute-start | bytes 159752 | tf_op jit(solution)/shard_map/ppermute | solution.py:614
  52.1 8.5 %collective-permute-start.14 = (bf16[208,128]{1,0:T(8,128)(2,1)S(1)}, bf16[208,128]{1,0:T(8,128)(2,1)S(1)}, u32[]{:S(2)}, u32[]{:S(2)}) collective-permute-start(bf16[208,128]{1,0:T(8,128)(2,1)S(1)} %shard_map.172._.own), channel_id=1, source_target_pairs={{0,128},{64,192},{128,0},{192,64},{1,129},{65,193},{129,1},{193,65... | collective-permute-start | bytes 159752 | tf_op jit(solution)/shard_map/ppermute | solution.py:614
  53.5 7.0 %collective-permute-start.13 = (bf16[208,128]{1,0:T(8,128)(2,1)S(1)}, bf16[208,128]{1,0:T(8,128)(2,1)S(1)}, u32[]{:S(2)}, u32[]{:S(2)}) collective-permute-start(bf16[208,128]{1,0:T(8,128)(2,1)S(1)} %shard_map.172._.own), channel_id=1, source_target_pairs={{0,64},{64,0},{128,192},{192,128},{1,65},{65,1},{129,193},{193,129... | collective-permute-start | bytes 159752 | tf_op jit(solution)/shard_map/ppermute | solution.py:614
  (6 other events, 8.9 us)

commit v10 on v9

--- a/solution.py
+++ b/solution.py
@@ -405,11 +405,29 @@
         copy.wait()
 
 
+def split_total(ref):
+    body = ref.shape[0] - PACK
+    return ref[:body, :].astype(f32), unpack_factor(ref[body:, :])
+
+
+def chosen_total(flag, first, second):
+    return tuple(jnp.where(flag, a, b) for a, b in zip(first, second))
+
+
+def pair_kernel(own_ref, near_ref, pair_ref):
+    odd = lax.axis_index("zh") % 2 == 1
+    own, near = split_total(own_ref), split_total(near_ref)
+    both, factor = join(chosen_total(odd, near, own), chosen_total(odd, own, near))
+    body, head = both.shape
+    pair_ref[:body, :] = both.astype(bf16)
+    pair_ref[body:, :] = row_pack(thirds(factor), head).astype(bf16)
+
+
 def spread_kernel(
-    beta_ref, decay_ref, own, back1, back2, back3, maps_ref, adds_ref, factors_ref,
-    query_ref, key_ref, value_ref, send_ref, groups_ref, wide_ref, turned_ref,
+    beta_ref, decay_ref, near_ref, pair_ref, other_ref, maps_ref, adds_ref, factors_ref,
+    query_ref, key_ref, value_ref, send_ref, wide_ref, turned_ref,
 ):
-    _, head = own.shape
+    head = pair_ref.shape[1]
     half = head // 2
     far = lax.axis_index("zh")
     near = lax.axis_index("zl") * 4 + lax.axis_index("x")
@@ -430,18 +448,16 @@
             total = jnp.where(pair == at, row, total)
         return total
 
-    for slot, ref in enumerate((own, back1, back2, back3)):
-        groups_ref[slot] = ref[...]
-    state = jnp.zeros((half, head), f32)
-    begin = state
-    for group in range(4):
-        begin = jnp.where(far == group, state, begin)
-        block = groups_ref[lax.bitwise_xor(far, group)]
-        added = block[head : head + half].astype(f32)
-        if group:
-            state = unpack_factor(block[head + half :]) * state - dot(state, block[:head]) + added
-        else:
-            state = added
+    def after(step, state):
+        both, factor = step
+        return factor * state - dot(state, both[:head]) + both[head:]
+
+    low = far < 2
+    mine, theirs = split_total(pair_ref), split_total(other_ref)
+    begin = jnp.where(low, 0.0, theirs[0][head:])
+    begin = jnp.where(far % 2 == 1, after(split_total(near_ref), begin), begin)
+    first, last = chosen_total(low, mine, theirs), chosen_total(low, theirs, mine)
+    state = after(last, first[0][head:])
     final = state.astype(bf16).astype(f32)
     wide_ref[...] = jnp.zeros((head, head), f32)
     wide_ref[pl.ds(pl.multiple_of(side * half, half), half), :] = final
@@ -610,9 +626,8 @@
     )
     arrived, local_out = lax.optimization_barrier((arrived, local_out))
     (total,) = kernel(total_kernel, [("p", on((rows, head), bf16))], "p", (arrived,))
-    others = [
-        lax.ppermute(total, "zh", [(at, at ^ by) for at in range(4)]) for by in (1, 2, 3)
-    ]
+    exchange = lambda value, by: lax.ppermute(value, "zh", [(at, at ^ by) for at in range(4)])
+    beside = exchange(total, 1)
     maps, adds, factors, *finals_in = kernel(
         prefix_kernel,
         [
@@ -625,16 +640,18 @@
         (total, arrived, local_out, reach, silu),
         (dma((3,)),),
     )
-    *others, maps = lax.optimization_barrier((*others, maps))
+    beside, maps = lax.optimization_barrier((beside, maps))
+    (pair,) = kernel(pair_kernel, [("p", on((rows, head), bf16))], "pp", (total, beside))
+    other = exchange(pair, 3)
     (back,) = kernel(
         spread_kernel,
         [("p", on((8, half + PACK, head), bf16))],
-        "p" * 12,
+        "p" * 11,
         (
-            new_beta, new_decay, total, *others, maps, adds, factors,
+            new_beta, new_decay, beside, pair, other, maps, adds, factors,
             new_query, new_key, new_value,
         ),
-        (on((4, rows, head), bf16), on((head, head), f32), on((head, head), f32)),
+        (on((head, head), f32), on((head, head), f32)),
     )
     returned = lax.all_to_all(back, NEAR, 0, 0, tiled=True)
     return kernel(

time: 72.6 us -> 72 us (level)
  waiting for transfers between devices: 20.8 us -> 19.1 us
    ppermute x3 -> x2, waiting for transfers between devices: 4.77 us -> 3.05 us  [shards(): lax.ppermute(value, 'zh', [(at, at ^ by) for at in range(4)])]
    ppermute x3 -> x2, starting transfers between devices: 7.94 us -> 8.58 us  [shards(): lax.ppermute(value, 'zh', [(at, at ^ by) for at in range(4)])]
    pallas_call x10 -> x11, Pallas kernels: 20.4 us -> 20.3 us  [kernel(): pl.pallas_call(body, out_shape=tuple((out if kind == 'p' else plain(out)...]
  transfers between devices with their start and end apart: 17 -> 16, of which waited for: 9 -> 10; matrix products, arithmetic and copies ran while one was open for 0% -> 0% of each run, Pallas kernels for 17% -> 17%
where the time goes in v10:
time: 72 us; the launch traced here: 71.7 us
  starting transfers between devices  20.7 us (29%)
  Pallas kernels  20.3 us (28%)
  waiting for transfers between devices  19.1 us (27%)
  blocking collectives  10.5 us (15%)
  between operations  0.94 us (1%)
    pallas_call x11, Pallas kernels, kernel(): pl.pallas_call(body, out_shape=tuple((out if kind == 'p' else plain(out)...  20.3 us
    ppermute x13, waiting for transfers between devices, shift(): lax.ppermute(value, axis, [(at, (at + by) % length) for at in range(lengt...  13.4 us
    all_to_all x1, blocking collectives, shards(): returned = lax.all_to_all(back, NEAR, 0, 0, tiled=True)  10.5 us
    ppermute x2, starting transfers between devices, shards(): lax.ppermute(value, 'zh', [(at, at ^ by) for at in range(4)])  8.58 us
    ppermute x13, starting transfers between devices, shift(): lax.ppermute(value, axis, [(at, (at + by) % length) for at in range(lengt...  8.05 us
    all_to_all x1, starting transfers between devices, shards(): arrived = lax.all_to_all(send, NEAR, 0, 0, tiled=True)  4.11 us
    ppermute x2, waiting for transfers between devices, shards(): lax.ppermute(value, 'zh', [(at, at ^ by) for at in range(4)])  3.05 us
    all_to_all x1, waiting for transfers between devices, shards(): arrived = lax.all_to_all(send, NEAR, 0, 0, tiled=True)  2.73 us
  transfers between devices with their start and end apart: 16, of which 10 were waited for; matrix products, arithmetic and copies ran while one was open for 0% of the time, Pallas kernels for 17%

profile of v10, /device:TPU:24, one launch (start us, length us, event | category | flops | bytes accessed | tf_op | source)
XLA Modules:
  0.0 71.7 jit_solution(9733563737419699120)
XLA Ops:
  0.6 0.1 collective-permute-start.4
  0.7 1.0 %shard_map.166 = (bf16[192,512]{1,0:T(8,128)(2,1)S(1)}, bf16[192,512]{1,0:T(8,128)(2,1)S(1)}) custom-call(bf16[2,192,512]{2,1,0:T(8,128)(2,1)} %refs_0_.1), custom_call_target="tpu_custom_call" | custom-call | tf_op jit(solution)/shard_map/pallas_call | solution.py:527
  1.8 2.0 %collective-permute-start = (bf16[192,512]{1,0:T(8,128)(2,1)S(1)}, bf16[192,512]{1,0:T(8,128)(2,1)S(1)}, u32[]{:S(2)}, u32[]{:S(2)}) collective-permute-start(bf16[192,512]{1,0:T(8,128)(2,1)S(1)} %get-tuple-element.49.own_first), channel_id=1, source_target_pairs={{0,2},{2,4},{4,6},{6,0},{1,3},{3,5},{5,7},{7,1},{8,10},{10,12},{12... | collective-permute-start | bytes 589832 | tf_op jit(solution)/shard_map/ppermute | solution.py:539
  3.8 0.1 collective-permute-start.2
  3.9 2.3 %shard_map.167 = (f32[384,512]{1,0:T(8,128)S(1)}, f32[384,128]{1,0:T(8,128)S(1)}, bf16[3072,512]{1,0:T(8,128)(2,1)S(1)}, bf16[16,4096]{1,0:T(8,128)(2,1)S(1)}) custom-call(bf16[192,512]{1,0:T(8,128)(2,1)S(1)} %get-tuple-element.49.own_first, bf16[192,512]{1,0:T(8,128)(2,1)S(1)} %get-tuple-element.48.own_second, ...), custom_call_target="tpu_custom_call" | custom-call | tf_op jit(solution)/shard_map/pallas_call | solution.py:527
  6.2 3.2 %collective-permute-start.5 = (bf16[192,512]{1,0:T(8,128)(2,1)S(1)}, bf16[192,512]{1,0:T(8,128)(2,1)S(1)}, u32[]{:S(2)}, u32[]{:S(2)}) collective-permute-start(bf16[192,512]{1,0:T(8,128)(2,1)S(1)} %get-tuple-element.48.own_second), channel_id=1, source_target_pairs={{0,2},{2,4},{4,6},{6,0},{1,3},{3,5},{5,7},{7,1},{8,10},{10,12},{12... | collective-permute-start | bytes 589832 | tf_op jit(solution)/shard_map/ppermute | solution.py:539
  9.6 2.5 %collective-permute-done.2.refs_3_.refs_5_ = bf16[192,512]{1,0:T(8,128)(2,1)S(1)} collective-permute-done((bf16[192,512]{1,0:T(8,128)(2,1)S(1)}, bf16[192,512]{1,0:T(8,128)(2,1)S(1)}, u32[]{:S(2)}, u32[]{:S(2)}) %collective-permute-start.2) | collective-permute-done | bytes 196640 | tf_op jit(solution)/shard_map/ppermute | solution.py:539
  12.0 1.7 %collective-permute-done.5.refs_1_.refs_3_ = bf16[192,512]{1,0:T(8,128)(2,1)S(1)} collective-permute-done((bf16[192,512]{1,0:T(8,128)(2,1)S(1)}, bf16[192,512]{1,0:T(8,128)(2,1)S(1)}, u32[]{:S(2)}, u32[]{:S(2)}) %collective-permute-start.5) | collective-permute-done | bytes 196640 | tf_op jit(solution)/shard_map/ppermute | solution.py:539
  13.7 3.4 %collective-permute-done.6.refs_2_.refs_4_ = bf16[192,512]{1,0:T(8,128)(2,1)S(1)} collective-permute-done((bf16[192,512]{1,0:T(8,128)(2,1)S(1)}, bf16[192,512]{1,0:T(8,128)(2,1)S(1)}, u32[]{:S(2)}, u32[]{:S(2)}) %collective-permute-start.6) | collective-permute-done | bytes 196640 | tf_op jit(solution)/shard_map/ppermute | solution.py:539
  17.1 0.8 %collective-permute-start.1 = (bf16[192,512]{1,0:T(8,128)(2,1)S(1)}, bf16[192,512]{1,0:T(8,128)(2,1)S(1)}, u32[]{:S(2)}, u32[]{:S(2)}) collective-permute-start(bf16[192,512]{1,0:T(8,128)(2,1)S(1)} %collective-permute-done.refs_0_.refs_2_), channel_id=1, source_target_pairs={{0,2},{2,4},{4,6},{6,0},{1,3},{3,5},{5,7},{7,1},{8,10},{10,12},{12... | collective-permute-start | bytes 589832 | tf_op jit(solution)/shard_map/ppermute | solution.py:539
  17.9 1.2 %collective-permute-start.3 = (bf16[192,512]{1,0:T(8,128)(2,1)S(1)}, bf16[192,512]{1,0:T(8,128)(2,1)S(1)}, u32[]{:S(2)}, u32[]{:S(2)}) collective-permute-start(bf16[192,512]{1,0:T(8,128)(2,1)S(1)} %collective-permute-done.2.refs_3_.refs_5_), channel_id=1, source_target_pairs={{0,6},{2,0},{4,2},{6,4},{1,7},{3,1},{5,3},{7,5},{8,14},{10,8},{12,... | collective-permute-start | bytes 589832 | tf_op jit(solution)/shard_map/ppermute | solution.py:539
  19.2 1.4 %shard_map.168 = (f32[384,512]{1,0:T(8,128)S(1)}, f32[384,128]{1,0:T(8,128)S(1)}) custom-call(bf16[192,512]{1,0:T(8,128)(2,1)S(1)} %collective-permute-done.refs_0_.refs_2_, bf16[192,512]{1,0:T(8,128)(2,1)S(1)} %collective-permute-done.5.refs_1_.refs_3_, bf16[192,512]{1,0:T(8,128)(2,1)S(1)} %collective-permute-done.6.refs_2_.refs_4_, ...), custom_call_target="tpu_custom_call" | custom-call | tf_op jit(solution)/shard_map/pallas_call | solution.py:527
  20.7 3.8 %collective-permute-done.1.refs_0_.refs_10_ = bf16[192,512]{1,0:T(8,128)(2,1)S(1)} collective-permute-done((bf16[192,512]{1,0:T(8,128)(2,1)S(1)}, bf16[192,512]{1,0:T(8,128)(2,1)S(1)}, u32[]{:S(2)}, u32[]{:S(2)}) %collective-permute-start.1) | collective-permute-done | bytes 196640 | tf_op jit(solution)/shard_map/ppermute | solution.py:539
  24.4 1.3 %collective-permute-done.3.refs_1_.refs_11_ = bf16[192,512]{1,0:T(8,128)(2,1)S(1)} collective-permute-done((bf16[192,512]{1,0:T(8,128)(2,1)S(1)}, bf16[192,512]{1,0:T(8,128)(2,1)S(1)}, u32[]{:S(2)}, u32[]{:S(2)}) %collective-permute-start.3) | collective-permute-done | bytes 196640 | tf_op jit(solution)/shard_map/ppermute | solution.py:539
  25.8 0.5 collective-permute-start.12
  26.3 0.5 shard_map.169
  26.8 0.4 collective-permute-done.11.refs_0_.refs_12_
  27.2 0.3 collective-permute-done.12.refs_1_.refs_13_
  27.5 5.6 %shard_map.170 = (bf16[8,208,128]{2,1,0:T(8,128)(2,1)}, bf16[384,256]{1,0:T(8,128)(2,1)}, bf16[4,192,128]{2,1,0:T(8,128)(2,1)}, bf16[4,192,128]{2,1,0:T(8,128)(2...) custom-call(f32[1,2]{1,0:T(1,128)S(1)} %bitcast.7, f32[1,2]{1,0:T(1,128)S(1)} %bitcast.8, ...), custom_call_target="tpu_custom_call" | custom-call | tf_op jit(solution)/shard_map/pallas_call | solution.py:527
  33.1 4.1 %all-to-all-start = ((bf16[8,208,128]{2,1,0:T(8,128)(2,1)}), bf16[8,208,128]{2,1,0:T(8,128)(2,1)S(1)}, u32[]{:S(2)}, u32[]{:S(2)}) async-start(bf16[8,208,128]{2,1,0:T(8,128)(2,1)} %get-tuple-element.66), calls=%async_computation | async-start | bytes 851968 | tf_op jit(solution)/shard_map/all_to_all | solution.py:608
  37.2 6.1 %shard_map.171 = (f32[4,192,128]{2,1,0:T(8,128)}, bf16[4,192,128]{2,1,0:T(8,128)(2,1)}, f32[4,192,128]{2,1,0:T(8,128)}) custom-call(bf16[2,192,512]{2,1,0:T(8,128)(2,1)} %refs_0_.1, bf16[2,192,512]{2,1,0:T(8,128)(2,1)} %copy-done, bf16[192,512]{1,0:T(8,128)(2,1)} %copy-done.1, bf16[192,512]{1,0:T(8,128)(2,1)} %copy-done.3, bf16[192,512]{1,0:T(8,128)(2,1)} %copy-done.4, ...), custom_call_target="tpu_custom_call" | custom-call | tf_op jit(solution)/shard_map/pallas_call | solution.py:527
  43.4 2.7 %all-to-all-done.in_ref = bf16[8,208,128]{2,1,0:T(8,128)(2,1)S(1)} async-done(((bf16[8,208,128]{2,1,0:T(8,128)(2,1)}), bf16[8,208,128]{2,1,0:T(8,128)(2,1)S(1)}, u32[]{:S(2)}, u32[]{:S(2)}) %all-to-all-start) | async-done | bytes 426016 | tf_op jit(solution)/shard_map/all_to_all | solution.py:608
  46.1 0.5 shard_map.172._.own_ref
  46.6 3.4 %collective-permute-start.13 = (bf16[208,128]{1,0:T(8,128)(2,1)S(1)}, bf16[208,128]{1,0:T(8,128)(2,1)S(1)}, u32[]{:S(2)}, u32[]{:S(2)}) collective-permute-start(bf16[208,128]{1,0:T(8,128)(2,1)S(1)} %shard_map.172._.own_ref), channel_id=1, source_target_pairs={{0,64},{64,0},{128,192},{192,128},{1,65},{65,1},{129,193},{193,129... | collective-permute-start | bytes 159752 | tf_op jit(solution)/shard_map/ppermute | solution.py:629
  50.0 1.2 %shard_map.173 = (bf16[7,128,128]{2,1,0:T(8,128)(2,1)S(1)}, f32[7,64,128]{2,1,0:T(8,128)S(1)}, f32[7,8,128]{2,1,0:T(8,128)S(1)}, f32[4,192,128]{2,1,0:T(8,128)S(...) custom-call(bf16[208,128]{1,0:T(8,128)(2,1)S(1)} %shard_map.172._.own_ref, ...), custom_call_target="tpu_custom_call" | custom-call | tf_op jit(solution)/shard_map/pallas_call | solution.py:527
  51.2 0.9 %collective-permute-done.13.near_ref = bf16[208,128]{1,0:T(8,128)(2,1)S(1)} collective-permute-done((bf16[208,128]{1,0:T(8,128)(2,1)S(1)}, bf16[208,128]{1,0:T(8,128)(2,1)S(1)}, u32[]{:S(2)}, u32[]{:S(2)}) %collective-permute-start.13) | collective-permute-done | bytes 53280 | tf_op jit(solution)/shard_map/ppermute | solution.py:629
  52.1 0.1 shard_map.174.pair_ref
  52.2 5.2 %collective-permute-start.14 = (bf16[208,128]{1,0:T(8,128)(2,1)S(1)}, bf16[208,128]{1,0:T(8,128)(2,1)S(1)}, u32[]{:S(2)}, u32[]{:S(2)}) collective-permute-start(bf16[208,128]{1,0:T(8,128)(2,1)S(1)} %shard_map.174.pair_ref), channel_id=1, source_target_pairs={{0,192},{64,128},{128,64},{192,0},{1,193},{65,129},{129,65},{193,1... | collective-permute-start | bytes 159752 | tf_op jit(solution)/shard_map/ppermute | solution.py:629
  57.5 2.2 %collective-permute-done.14.other_ref = bf16[208,128]{1,0:T(8,128)(2,1)S(1)} collective-permute-done((bf16[208,128]{1,0:T(8,128)(2,1)S(1)}, bf16[208,128]{1,0:T(8,128)(2,1)S(1)}, u32[]{:S(2)}, u32[]{:S(2)}) %collective-permute-start.14) | collective-permute-done | bytes 53280 | tf_op jit(solution)/shard_map/ppermute | solution.py:629
  59.7 0.5 shard_map.175
  60.2 10.5 %all_to_all.10.in_ref = bf16[8,80,128]{2,1,0:T(8,128)(2,1)S(1)} all-to-all(bf16[8,80,128]{2,1,0:T(8,128)(2,1)S(1)} %shard_map.175), channel_id=1, replica_groups=mesh['zh'=4,'zl'=2,'x'=4,'y'=4,'c'=2] {'zl','x'}, dimensions={0} | all-to-all | bytes 327680 | tf_op jit(solution)/shard_map/all_to_all | solution.py:656
  70.7 1.0 %shard_map.176 = (bf16[2,192,256]{2,1,0:T(8,128)(2,1)}, bf16[2,2,4,128]{3,2,1,0:T(4,128)(2,1)}, f32[2,256]{1,0:T(2,128)}) custom-call(bf16[8,80,128]{2,1,0:T(8,128)(2,1)S(1)} %all_to_all.10.in_ref, f32[4,192,128]{2,1,0:T(8,128)S(1)} %get-tuple-element.82.out_ref, bf16[4,192,128]{2,1,0:T(8,128)(2,1)S(1)} %get-tuple-element.83.reach_ref, ...), custom_call_target="tpu_custom_call" | custom-call | tf_op jit(solution)/shard_map/pallas_call | solution.py:527
  (54 shorter events, 0.2 us)
Async XLA Ops:
  0.6 3.3 %collective-permute-start.4 = (bf16[2,192,512]{2,1,0:T(8,128)(2,1)}, bf16[2,192,512]{2,1,0:T(8,128)(2,1)S(1)}, u32[]{:S(2)}, u32[]{:S(2)}) collective-permute-start(bf16[2,192,512]{2,1,0:T(8,128)(2,1)} %refs_0_.1), channel_id=1, source_target_pairs={{0,1},{1,0},{2,3},{3,2},{4,5},{5,4},{6,7},{7,6},{8,9},{9,8},{10,11... | collective-permute-start | bytes 1179656 | tf_op jit(solution)/shard_map/ppermute | solution.py:539
  1.8 7.7 %collective-permute-start = (bf16[192,512]{1,0:T(8,128)(2,1)S(1)}, bf16[192,512]{1,0:T(8,128)(2,1)S(1)}, u32[]{:S(2)}, u32[]{:S(2)}) collective-permute-start(bf16[192,512]{1,0:T(8,128)(2,1)S(1)} %get-tuple-element.49.own_first), channel_id=1, source_target_pairs={{0,2},{2,4},{4,6},{6,0},{1,3},{3,5},{5,7},{7,1},{8,10},{10,12},{12... | collective-permute-start | bytes 589832 | tf_op jit(solution)/shard_map/ppermute | solution.py:539
  3.8 8.2 %collective-permute-start.2 = (bf16[192,512]{1,0:T(8,128)(2,1)S(1)}, bf16[192,512]{1,0:T(8,128)(2,1)S(1)}, u32[]{:S(2)}, u32[]{:S(2)}) collective-permute-start(bf16[192,512]{1,0:T(8,128)(2,1)S(1)} %get-tuple-element.48.own_second), channel_id=1, source_target_pairs={{0,6},{2,0},{4,2},{6,4},{1,7},{3,1},{5,3},{7,5},{8,14},{10,8},{12,... | collective-permute-start | bytes 589832 | tf_op jit(solution)/shard_map/ppermute | solution.py:539
  3.9 2.3 %copy-start = (bf16[2,192,512]{2,1,0:T(8,128)(2,1)}, bf16[2,192,512]{2,1,0:T(8,128)(2,1)S(1)}, u32[]{:S(2)}) copy-start(bf16[2,192,512]{2,1,0:T(8,128)(2,1)S(1)} %collective-permute-done.4.own_c.refs_1_) | copy-start | bytes 1179652
  6.2 7.5 %collective-permute-start.5 = (bf16[192,512]{1,0:T(8,128)(2,1)S(1)}, bf16[192,512]{1,0:T(8,128)(2,1)S(1)}, u32[]{:S(2)}, u32[]{:S(2)}) collective-permute-start(bf16[192,512]{1,0:T(8,128)(2,1)S(1)} %get-tuple-element.48.own_second), channel_id=1, source_target_pairs={{0,2},{2,4},{4,6},{6,0},{1,3},{3,5},{5,7},{7,1},{8,10},{10,12},{12... | collective-permute-start | bytes 589832 | tf_op jit(solution)/shard_map/ppermute | solution.py:539
  9.4 7.7 %collective-permute-start.6 = (bf16[192,512]{1,0:T(8,128)(2,1)S(1)}, bf16[192,512]{1,0:T(8,128)(2,1)S(1)}, u32[]{:S(2)}, u32[]{:S(2)}) collective-permute-start(bf16[192,512]{1,0:T(8,128)(2,1)S(1)} %get-tuple-element.49.own_first), channel_id=1, source_target_pairs={{0,6},{2,0},{4,2},{6,4},{1,7},{3,1},{5,3},{7,5},{8,14},{10,8},{12,... | collective-permute-start | bytes 589832 | tf_op jit(solution)/shard_map/ppermute | solution.py:539
  9.4 11.1 %copy-start.1 = (bf16[192,512]{1,0:T(8,128)(2,1)}, bf16[192,512]{1,0:T(8,128)(2,1)S(1)}, u32[]{:S(2)}) copy-start(bf16[192,512]{1,0:T(8,128)(2,1)S(1)} %collective-permute-done.refs_0_.refs_2_) | copy-start | bytes 589828
  9.5 8.5 %collective-permute-start.7 = (bf16[192,512]{1,0:T(8,128)(2,1)S(1)}, bf16[192,512]{1,0:T(8,128)(2,1)S(1)}, u32[]{:S(2)}, u32[]{:S(2)}) collective-permute-start(bf16[192,512]{1,0:T(8,128)(2,1)S(1)} %collective-permute-done.refs_0_.refs_2_), channel_id=1, source_target_pairs={{0,1},{1,0},{2,3},{3,2},{4,5},{5,4},{6,7},{7,6},{8,9},{9,8},{10,11... | collective-permute-start | bytes 589832 | tf_op jit(solution)/shard_map/ppermute | solution.py:539
  12.0 8.6 %copy-start.2 = (bf16[192,512]{1,0:T(8,128)(2,1)}, bf16[192,512]{1,0:T(8,128)(2,1)S(1)}, u32[]{:S(2)}) copy-start(bf16[192,512]{1,0:T(8,128)(2,1)S(1)} %collective-permute-done.2.refs_3_.refs_5_) | copy-start | bytes 589828
  12.0 7.1 %collective-permute-start.10 = (bf16[192,512]{1,0:T(8,128)(2,1)S(1)}, bf16[192,512]{1,0:T(8,128)(2,1)S(1)}, u32[]{:S(2)}, u32[]{:S(2)}) collective-permute-start(bf16[192,512]{1,0:T(8,128)(2,1)S(1)} %collective-permute-done.2.refs_3_.refs_5_), channel_id=1, source_target_pairs={{0,1},{1,0},{2,3},{3,2},{4,5},{5,4},{6,7},{7,6},{8,9},{9,8},{10,11... | collective-permute-start | bytes 589832 | tf_op jit(solution)/shard_map/ppermute | solution.py:539
  13.7 6.9 %copy-start.3 = (bf16[192,512]{1,0:T(8,128)(2,1)}, bf16[192,512]{1,0:T(8,128)(2,1)S(1)}, u32[]{:S(2)}) copy-start(bf16[192,512]{1,0:T(8,128)(2,1)S(1)} %collective-permute-done.5.refs_1_.refs_3_) | copy-start | bytes 589828
  13.7 5.5 %collective-permute-start.8 = (bf16[192,512]{1,0:T(8,128)(2,1)S(1)}, bf16[192,512]{1,0:T(8,128)(2,1)S(1)}, u32[]{:S(2)}, u32[]{:S(2)}) collective-permute-start(bf16[192,512]{1,0:T(8,128)(2,1)S(1)} %collective-permute-done.5.refs_1_.refs_3_), channel_id=1, source_target_pairs={{0,1},{1,0},{2,3},{3,2},{4,5},{5,4},{6,7},{7,6},{8,9},{9,8},{10,11... | collective-permute-start | bytes 589832 | tf_op jit(solution)/shard_map/ppermute | solution.py:539
  17.1 3.5 %copy-start.4 = (bf16[192,512]{1,0:T(8,128)(2,1)}, bf16[192,512]{1,0:T(8,128)(2,1)S(1)}, u32[]{:S(2)}) copy-start(bf16[192,512]{1,0:T(8,128)(2,1)S(1)} %collective-permute-done.6.refs_2_.refs_4_) | copy-start | bytes 589828
  17.1 2.1 %collective-permute-start.9 = (bf16[192,512]{1,0:T(8,128)(2,1)S(1)}, bf16[192,512]{1,0:T(8,128)(2,1)S(1)}, u32[]{:S(2)}, u32[]{:S(2)}) collective-permute-start(bf16[192,512]{1,0:T(8,128)(2,1)S(1)} %collective-permute-done.6.refs_2_.refs_4_), channel_id=1, source_target_pairs={{0,1},{1,0},{2,3},{3,2},{4,5},{5,4},{6,7},{7,6},{8,9},{9,8},{10,11... | collective-permute-start | bytes 589832 | tf_op jit(solution)/shard_map/ppermute | solution.py:539
  17.1 7.3 %collective-permute-start.1 = (bf16[192,512]{1,0:T(8,128)(2,1)S(1)}, bf16[192,512]{1,0:T(8,128)(2,1)S(1)}, u32[]{:S(2)}, u32[]{:S(2)}) collective-permute-start(bf16[192,512]{1,0:T(8,128)(2,1)S(1)} %collective-permute-done.refs_0_.refs_2_), channel_id=1, source_target_pairs={{0,2},{2,4},{4,6},{6,0},{1,3},{3,5},{5,7},{7,1},{8,10},{10,12},{12... | collective-permute-start | bytes 589832 | tf_op jit(solution)/shard_map/ppermute | solution.py:539
  17.9 2.7 %copy-start.5 = (bf16[192,512]{1,0:T(8,128)(2,1)}, bf16[192,512]{1,0:T(8,128)(2,1)S(1)}, u32[]{:S(2)}) copy-start(bf16[192,512]{1,0:T(8,128)(2,1)S(1)} %collective-permute-done.7.refs_4_.refs_6_) | copy-start | bytes 589828
  17.9 7.8 %collective-permute-start.3 = (bf16[192,512]{1,0:T(8,128)(2,1)S(1)}, bf16[192,512]{1,0:T(8,128)(2,1)S(1)}, u32[]{:S(2)}, u32[]{:S(2)}) collective-permute-start(bf16[192,512]{1,0:T(8,128)(2,1)S(1)} %collective-permute-done.2.refs_3_.refs_5_), channel_id=1, source_target_pairs={{0,6},{2,0},{4,2},{6,4},{1,7},{3,1},{5,3},{7,5},{8,14},{10,8},{12,... | collective-permute-start | bytes 589832 | tf_op jit(solution)/shard_map/ppermute | solution.py:539
  24.4 2.3 %copy-start.9 = (bf16[192,512]{1,0:T(8,128)(2,1)}, bf16[192,512]{1,0:T(8,128)(2,1)S(1)}, u32[]{:S(2)}) copy-start(bf16[192,512]{1,0:T(8,128)(2,1)S(1)} %collective-permute-done.1.refs_0_.refs_10_) | copy-start | bytes 589828
  25.8 1.7 %copy-start.20 = (f32[2]{0:T(128)S(1)}, f32[2]{0:T(128)}, u32[]{:S(2)}) copy-start(f32[2]{0:T(128)} %param.23) | copy-start | bytes 28
  25.8 1.4 %collective-permute-start.11 = (bf16[192,512]{1,0:T(8,128)(2,1)S(1)}, bf16[192,512]{1,0:T(8,128)(2,1)S(1)}, u32[]{:S(2)}, u32[]{:S(2)}) collective-permute-start(bf16[192,512]{1,0:T(8,128)(2,1)S(1)} %collective-permute-done.1.refs_0_.refs_10_), channel_id=1, source_target_pairs={{0,1},{1,0},{2,3},{3,2},{4,5},{5,4},{6,7},{7,6},{8,9},{9,8},{10,11... | collective-permute-start | bytes 589832 | tf_op jit(solution)/shard_map/ppermute | solution.py:539
  25.8 1.7 %collective-permute-start.12 = (bf16[192,512]{1,0:T(8,128)(2,1)S(1)}, bf16[192,512]{1,0:T(8,128)(2,1)S(1)}, u32[]{:S(2)}, u32[]{:S(2)}) collective-permute-start(bf16[192,512]{1,0:T(8,128)(2,1)S(1)} %collective-permute-done.3.refs_1_.refs_11_), channel_id=1, source_target_pairs={{0,1},{1,0},{2,3},{3,2},{4,5},{5,4},{6,7},{7,6},{8,9},{9,8},{10,11... | collective-permute-start | bytes 589832 | tf_op jit(solution)/shard_map/ppermute | solution.py:539
  27.2 5.9 %copy-start.11 = (bf16[192,512]{1,0:T(8,128)(2,1)}, bf16[192,512]{1,0:T(8,128)(2,1)S(1)}, u32[]{:S(2)}) copy-start(bf16[192,512]{1,0:T(8,128)(2,1)S(1)} %collective-permute-done.11.refs_0_.refs_12_) | copy-start | bytes 589828
  27.5 5.6 %copy-start.12 = (bf16[192,512]{1,0:T(8,128)(2,1)}, bf16[192,512]{1,0:T(8,128)(2,1)S(1)}, u32[]{:S(2)}) copy-start(bf16[192,512]{1,0:T(8,128)(2,1)S(1)} %collective-permute-done.12.refs_1_.refs_13_) | copy-start | bytes 589828
  33.1 13.0 %all-to-all-start = ((bf16[8,208,128]{2,1,0:T(8,128)(2,1)}), bf16[8,208,128]{2,1,0:T(8,128)(2,1)S(1)}, u32[]{:S(2)}, u32[]{:S(2)}) async-start(bf16[8,208,128]{2,1,0:T(8,128)(2,1)} %get-tuple-element.66), calls=%async_computation | async-start | bytes 851968 | tf_op jit(solution)/shard_map/all_to_all | solution.py:608
  43.3 16.3 %copy-start.14 = (f32[2,2]{1,0:T(2,128)S(1)}, f32[2,2]{1,0:T(2,128)}, u32[]{:S(2)}) copy-start(f32[2,2]{1,0:T(2,128)} %beta_ref.1) | copy-start | bytes 52
  43.4 16.3 %copy-start.15 = (f32[2,2]{1,0:T(2,128)S(1)}, f32[2,2]{1,0:T(2,128)}, u32[]{:S(2)}) copy-start(f32[2,2]{1,0:T(2,128)} %decay_ref.1) | copy-start | bytes 52
  43.4 16.3 %copy-start.16 = (bf16[2,2,128]{2,1,0:T(2,128)(2,1)S(1)}, bf16[2,2,128]{2,1,0:T(2,128)(2,1)}, u32[]{:S(2)}) copy-start(bf16[2,2,128]{2,1,0:T(2,128)(2,1)} %query_ref.1) | copy-start | bytes 3076
  43.4 16.3 %copy-start.17 = (bf16[2,2,128]{2,1,0:T(2,128)(2,1)S(1)}, bf16[2,2,128]{2,1,0:T(2,128)(2,1)}, u32[]{:S(2)}) copy-start(bf16[2,2,128]{2,1,0:T(2,128)(2,1)} %key_ref.1) | copy-start | bytes 3076
  43.4 16.3 %copy-start.18 = (bf16[2,2,128]{2,1,0:T(2,128)(2,1)S(1)}, bf16[2,2,128]{2,1,0:T(2,128)(2,1)}, u32[]{:S(2)}) copy-start(bf16[2,2,128]{2,1,0:T(2,128)(2,1)} %value_ref.1) | copy-start | bytes 3076
  43.4 27.3 %copy-start.13 = (f32[128]{0:T(128)S(1)}, f32[128]{0:T(128)}, u32[]{:S(2)}) copy-start(f32[128]{0:T(128)} %param.24) | copy-start | bytes 1540
  46.6 5.5 %collective-permute-start.13 = (bf16[208,128]{1,0:T(8,128)(2,1)S(1)}, bf16[208,128]{1,0:T(8,128)(2,1)S(1)}, u32[]{:S(2)}, u32[]{:S(2)}) collective-permute-start(bf16[208,128]{1,0:T(8,128)(2,1)S(1)} %shard_map.172._.own_ref), channel_id=1, source_target_pairs={{0,64},{64,0},{128,192},{192,128},{1,65},{65,1},{129,193},{193,129... | collective-permute-start | bytes 159752 | tf_op jit(solution)/shard_map/ppermute | solution.py:629
  52.2 7.4 %collective-permute-start.14 = (bf16[208,128]{1,0:T(8,128)(2,1)S(1)}, bf16[208,128]{1,0:T(8,128)(2,1)S(1)}, u32[]{:S(2)}, u32[]{:S(2)}) collective-permute-start(bf16[208,128]{1,0:T(8,128)(2,1)S(1)} %shard_map.174.pair_ref), channel_id=1, source_target_pairs={{0,192},{64,128},{128,64},{192,0},{1,193},{65,129},{129,65},{193,1... | collective-permute-start | bytes 159752 | tf_op jit(solution)/shard_map/ppermute | solution.py:629
  (5 other events, 7.2 us)

commit v11 on v10

--- a/solution.py
+++ b/solution.py
@@ -11,7 +11,7 @@
 
 NEAR = ("zl", "x")
 AXES = ("zh", "zl", "x")
-PACK = 16
+PACK = 8
 LANES = 128
 unit_floor = 1.0
 norm_floor = 0.001
@@ -70,7 +70,7 @@
 def scalar_part(rows, stacked, slot):
     depth = rows.shape[-1]
     weight = stacked[:, pl.ds(first_row(slot, depth), depth)]
-    weight = jnp.concatenate([weight, jnp.zeros((LANES - PACK, depth), bf16)], axis=0)
+    weight = jnp.concatenate([weight, jnp.zeros((LANES - 16, depth), bf16)], axis=0)
     return dot(rows, weight, ROWS)
 
 
@@ -115,7 +115,7 @@
     for copy in first:
         copy.wait()
     rows = [scalar_buffer[at, h : h + 1, :].astype(f32) for at in range(2) for h in range(2)]
-    stacked_ref[...] = row_pack(rows, stacked_ref.shape[-1]).astype(bf16)
+    stacked_ref[...] = jnp.concatenate([row_pack(rows, stacked_ref.shape[-1]), jnp.zeros((8, stacked_ref.shape[-1]), f32)], axis=0).astype(bf16)
     total = gates = 0.0
     for at in range(2):
         rows = own_c[...].reshape(-1, depth) if at else joined(own_first, own_second)
@@ -560,7 +560,7 @@
     sums = [("p", on((2 * span, 2 * width), f32)), ("p", on((2 * span, head), f32))]
     early = kernel(
         early_kernel,
-        sums + [("p", on((6 * depth, 2 * width), bf16)), ("p", on((PACK, 8 * depth), bf16))],
+        sums + [("p", on((6 * depth, 2 * width), bf16)), ("p", on((16, 8 * depth), bf16))],
         "ppphhhh",
         (first, second, tokens_c, beta_weight.T, decay_weight.T, key_weight, value_weight),
         (

time: 72 us -> 71.8 us (level)
  transfers between devices with their start and end apart: 16 -> 16, of which waited for: 10 -> 10; matrix products, arithmetic and copies ran while one was open for 0% -> 0% of each run, Pallas kernels for 17% -> 18%
where the time goes in v11:
time: 71.8 us; the launch traced here: 71.5 us
  starting transfers between devices  20.7 us (29%)
  Pallas kernels  20.3 us (28%)
  waiting for transfers between devices  19 us (26%)
  blocking collectives  10.5 us (15%)
  between operations  0.93 us (1%)
    pallas_call x11, Pallas kernels, kernel(): pl.pallas_call(body, out_shape=tuple((out if kind == 'p' else plain(out)...  20.3 us
    ppermute x13, waiting for transfers between devices, shift(): lax.ppermute(value, axis, [(at, (at + by) % length) for at in range(lengt...  13.4 us
    all_to_all x1, blocking collectives, shards(): returned = lax.all_to_all(back, NEAR, 0, 0, tiled=True)  10.5 us
    ppermute x2, starting transfers between devices, shards(): lax.ppermute(value, 'zh', [(at, at ^ by) for at in range(4)])  8.58 us
    ppermute x13, starting transfers between devices, shift(): lax.ppermute(value, axis, [(at, (at + by) % length) for at in range(lengt...  8.05 us
    all_to_all x1, starting transfers between devices, shards(): arrived = lax.all_to_all(send, NEAR, 0, 0, tiled=True)  4.11 us
    ppermute x2, waiting for transfers between devices, shards(): lax.ppermute(value, 'zh', [(at, at ^ by) for at in range(4)])  3.01 us
    all_to_all x1, waiting for transfers between devices, shards(): arrived = lax.all_to_all(send, NEAR, 0, 0, tiled=True)  2.61 us
  transfers between devices with their start and end apart: 16, of which 10 were waited for; matrix products, arithmetic and copies ran while one was open for 0% of the time, Pallas kernels for 18%

profile of v11, /device:TPU:24, one launch (start us, length us, event | category | flops | bytes accessed | tf_op | source)
XLA Modules:
  0.0 71.5 jit_solution(6632259331593512693)
XLA Ops:
  0.6 0.1 collective-permute-start.4
  0.7 1.0 %shard_map.166 = (bf16[192,512]{1,0:T(8,128)(2,1)S(1)}, bf16[192,512]{1,0:T(8,128)(2,1)S(1)}) custom-call(bf16[2,192,512]{2,1,0:T(8,128)(2,1)} %refs_0_.1), custom_call_target="tpu_custom_call" | custom-call | tf_op jit(solution)/shard_map/pallas_call | solution.py:527
  1.8 2.0 %collective-permute-start = (bf16[192,512]{1,0:T(8,128)(2,1)S(1)}, bf16[192,512]{1,0:T(8,128)(2,1)S(1)}, u32[]{:S(2)}, u32[]{:S(2)}) collective-permute-start(bf16[192,512]{1,0:T(8,128)(2,1)S(1)} %get-tuple-element.49.own_first), channel_id=1, source_target_pairs={{0,2},{2,4},{4,6},{6,0},{1,3},{3,5},{5,7},{7,1},{8,10},{10,12},{12... | collective-permute-start | bytes 589832 | tf_op jit(solution)/shard_map/ppermute | solution.py:539
  3.8 0.1 collective-permute-start.2
  3.9 2.3 %shard_map.167 = (f32[384,512]{1,0:T(8,128)S(1)}, f32[384,128]{1,0:T(8,128)S(1)}, bf16[3072,512]{1,0:T(8,128)(2,1)S(1)}, bf16[16,4096]{1,0:T(8,128)(2,1)S(1)}) custom-call(bf16[192,512]{1,0:T(8,128)(2,1)S(1)} %get-tuple-element.49.own_first, bf16[192,512]{1,0:T(8,128)(2,1)S(1)} %get-tuple-element.48.own_second, ...), custom_call_target="tpu_custom_call" | custom-call | tf_op jit(solution)/shard_map/pallas_call | solution.py:527
  6.2 3.2 %collective-permute-start.5 = (bf16[192,512]{1,0:T(8,128)(2,1)S(1)}, bf16[192,512]{1,0:T(8,128)(2,1)S(1)}, u32[]{:S(2)}, u32[]{:S(2)}) collective-permute-start(bf16[192,512]{1,0:T(8,128)(2,1)S(1)} %get-tuple-element.48.own_second), channel_id=1, source_target_pairs={{0,2},{2,4},{4,6},{6,0},{1,3},{3,5},{5,7},{7,1},{8,10},{10,12},{12... | collective-permute-start | bytes 589832 | tf_op jit(solution)/shard_map/ppermute | solution.py:539
  9.6 2.5 %collective-permute-done.2.refs_3_.refs_5_ = bf16[192,512]{1,0:T(8,128)(2,1)S(1)} collective-permute-done((bf16[192,512]{1,0:T(8,128)(2,1)S(1)}, bf16[192,512]{1,0:T(8,128)(2,1)S(1)}, u32[]{:S(2)}, u32[]{:S(2)}) %collective-permute-start.2) | collective-permute-done | bytes 196640 | tf_op jit(solution)/shard_map/ppermute | solution.py:539
  12.0 1.7 %collective-permute-done.5.refs_1_.refs_3_ = bf16[192,512]{1,0:T(8,128)(2,1)S(1)} collective-permute-done((bf16[192,512]{1,0:T(8,128)(2,1)S(1)}, bf16[192,512]{1,0:T(8,128)(2,1)S(1)}, u32[]{:S(2)}, u32[]{:S(2)}) %collective-permute-start.5) | collective-permute-done | bytes 196640 | tf_op jit(solution)/shard_map/ppermute | solution.py:539
  13.7 3.4 %collective-permute-done.6.refs_2_.refs_4_ = bf16[192,512]{1,0:T(8,128)(2,1)S(1)} collective-permute-done((bf16[192,512]{1,0:T(8,128)(2,1)S(1)}, bf16[192,512]{1,0:T(8,128)(2,1)S(1)}, u32[]{:S(2)}, u32[]{:S(2)}) %collective-permute-start.6) | collective-permute-done | bytes 196640 | tf_op jit(solution)/shard_map/ppermute | solution.py:539
  17.1 0.8 %collective-permute-start.1 = (bf16[192,512]{1,0:T(8,128)(2,1)S(1)}, bf16[192,512]{1,0:T(8,128)(2,1)S(1)}, u32[]{:S(2)}, u32[]{:S(2)}) collective-permute-start(bf16[192,512]{1,0:T(8,128)(2,1)S(1)} %collective-permute-done.refs_0_.refs_2_), channel_id=1, source_target_pairs={{0,2},{2,4},{4,6},{6,0},{1,3},{3,5},{5,7},{7,1},{8,10},{10,12},{12... | collective-permute-start | bytes 589832 | tf_op jit(solution)/shard_map/ppermute | solution.py:539
  17.9 1.2 %collective-permute-start.3 = (bf16[192,512]{1,0:T(8,128)(2,1)S(1)}, bf16[192,512]{1,0:T(8,128)(2,1)S(1)}, u32[]{:S(2)}, u32[]{:S(2)}) collective-permute-start(bf16[192,512]{1,0:T(8,128)(2,1)S(1)} %collective-permute-done.2.refs_3_.refs_5_), channel_id=1, source_target_pairs={{0,6},{2,0},{4,2},{6,4},{1,7},{3,1},{5,3},{7,5},{8,14},{10,8},{12,... | collective-permute-start | bytes 589832 | tf_op jit(solution)/shard_map/ppermute | solution.py:539
  19.2 1.4 %shard_map.168 = (f32[384,512]{1,0:T(8,128)S(1)}, f32[384,128]{1,0:T(8,128)S(1)}) custom-call(bf16[192,512]{1,0:T(8,128)(2,1)S(1)} %collective-permute-done.refs_0_.refs_2_, bf16[192,512]{1,0:T(8,128)(2,1)S(1)} %collective-permute-done.5.refs_1_.refs_3_, bf16[192,512]{1,0:T(8,128)(2,1)S(1)} %collective-permute-done.6.refs_2_.refs_4_, ...), custom_call_target="tpu_custom_call" | custom-call | tf_op jit(solution)/shard_map/pallas_call | solution.py:527
  20.7 3.8 %collective-permute-done.1.refs_0_.refs_10_ = bf16[192,512]{1,0:T(8,128)(2,1)S(1)} collective-permute-done((bf16[192,512]{1,0:T(8,128)(2,1)S(1)}, bf16[192,512]{1,0:T(8,128)(2,1)S(1)}, u32[]{:S(2)}, u32[]{:S(2)}) %collective-permute-start.1) | collective-permute-done | bytes 196640 | tf_op jit(solution)/shard_map/ppermute | solution.py:539
  24.4 1.3 %collective-permute-done.3.refs_1_.refs_11_ = bf16[192,512]{1,0:T(8,128)(2,1)S(1)} collective-permute-done((bf16[192,512]{1,0:T(8,128)(2,1)S(1)}, bf16[192,512]{1,0:T(8,128)(2,1)S(1)}, u32[]{:S(2)}, u32[]{:S(2)}) %collective-permute-start.3) | collective-permute-done | bytes 196640 | tf_op jit(solution)/shard_map/ppermute | solution.py:539
  25.8 0.5 collective-permute-start.12
  26.3 0.5 shard_map.169
  26.8 0.4 collective-permute-done.11.refs_0_.refs_12_
  27.2 0.3 collective-permute-done.12.refs_1_.refs_13_
  27.5 5.6 %shard_map.170 = (bf16[8,200,128]{2,1,0:T(8,128)(2,1)}, bf16[384,256]{1,0:T(8,128)(2,1)}, bf16[4,192,128]{2,1,0:T(8,128)(2,1)}, bf16[4,192,128]{2,1,0:T(8,128)(2...) custom-call(f32[1,2]{1,0:T(1,128)S(1)} %bitcast.7, f32[1,2]{1,0:T(1,128)S(1)} %bitcast.8, ...), custom_call_target="tpu_custom_call" | custom-call | tf_op jit(solution)/shard_map/pallas_call | solution.py:527
  33.1 4.1 %all-to-all-start = ((bf16[8,200,128]{2,1,0:T(8,128)(2,1)}), bf16[8,200,128]{2,1,0:T(8,128)(2,1)S(1)}, u32[]{:S(2)}, u32[]{:S(2)}) async-start(bf16[8,200,128]{2,1,0:T(8,128)(2,1)} %get-tuple-element.66), calls=%async_computation | async-start | bytes 819200 | tf_op jit(solution)/shard_map/all_to_all | solution.py:608
  37.3 6.1 %shard_map.171 = (f32[4,192,128]{2,1,0:T(8,128)}, bf16[4,192,128]{2,1,0:T(8,128)(2,1)}, f32[4,192,128]{2,1,0:T(8,128)}) custom-call(bf16[2,192,512]{2,1,0:T(8,128)(2,1)} %refs_0_.1, bf16[2,192,512]{2,1,0:T(8,128)(2,1)} %copy-done, bf16[192,512]{1,0:T(8,128)(2,1)} %copy-done.1, bf16[192,512]{1,0:T(8,128)(2,1)} %copy-done.3, bf16[192,512]{1,0:T(8,128)(2,1)} %copy-done.4, ...), custom_call_target="tpu_custom_call" | custom-call | tf_op jit(solution)/shard_map/pallas_call | solution.py:527
  43.4 2.6 %all-to-all-done.in_ref = bf16[8,200,128]{2,1,0:T(8,128)(2,1)S(1)} async-done(((bf16[8,200,128]{2,1,0:T(8,128)(2,1)}), bf16[8,200,128]{2,1,0:T(8,128)(2,1)S(1)}, u32[]{:S(2)}, u32[]{:S(2)}) %all-to-all-start) | async-done | bytes 409632 | tf_op jit(solution)/shard_map/all_to_all | solution.py:608
  46.0 0.5 shard_map.172._.own_ref
  46.5 3.4 %collective-permute-start.13 = (bf16[200,128]{1,0:T(8,128)(2,1)S(1)}, bf16[200,128]{1,0:T(8,128)(2,1)S(1)}, u32[]{:S(2)}, u32[]{:S(2)}) collective-permute-start(bf16[200,128]{1,0:T(8,128)(2,1)S(1)} %shard_map.172._.own_ref), channel_id=1, source_target_pairs={{0,64},{64,0},{128,192},{192,128},{1,65},{65,1},{129,193},{193,129... | collective-permute-start | bytes 153608 | tf_op jit(solution)/shard_map/ppermute | solution.py:629
  49.8 1.2 %shard_map.173 = (bf16[7,128,128]{2,1,0:T(8,128)(2,1)S(1)}, f32[7,64,128]{2,1,0:T(8,128)S(1)}, f32[7,8,128]{2,1,0:T(8,128)S(1)}, f32[4,192,128]{2,1,0:T(8,128)S(...) custom-call(bf16[200,128]{1,0:T(8,128)(2,1)S(1)} %shard_map.172._.own_ref, ...), custom_call_target="tpu_custom_call" | custom-call | tf_op jit(solution)/shard_map/pallas_call | solution.py:527
  51.1 0.9 %collective-permute-done.13.near_ref = bf16[200,128]{1,0:T(8,128)(2,1)S(1)} collective-permute-done((bf16[200,128]{1,0:T(8,128)(2,1)S(1)}, bf16[200,128]{1,0:T(8,128)(2,1)S(1)}, u32[]{:S(2)}, u32[]{:S(2)}) %collective-permute-start.13) | collective-permute-done | bytes 51232 | tf_op jit(solution)/shard_map/ppermute | solution.py:629
  51.9 0.1 shard_map.174.pair_ref
  52.1 5.2 %collective-permute-start.14 = (bf16[200,128]{1,0:T(8,128)(2,1)S(1)}, bf16[200,128]{1,0:T(8,128)(2,1)S(1)}, u32[]{:S(2)}, u32[]{:S(2)}) collective-permute-start(bf16[200,128]{1,0:T(8,128)(2,1)S(1)} %shard_map.174.pair_ref), channel_id=1, source_target_pairs={{0,192},{64,128},{128,64},{192,0},{1,193},{65,129},{129,65},{193,1... | collective-permute-start | bytes 153608 | tf_op jit(solution)/shard_map/ppermute | solution.py:629
  57.3 2.1 %collective-permute-done.14.other_ref = bf16[200,128]{1,0:T(8,128)(2,1)S(1)} collective-permute-done((bf16[200,128]{1,0:T(8,128)(2,1)S(1)}, bf16[200,128]{1,0:T(8,128)(2,1)S(1)}, u32[]{:S(2)}, u32[]{:S(2)}) %collective-permute-start.14) | collective-permute-done | bytes 51232 | tf_op jit(solution)/shard_map/ppermute | solution.py:629
  59.5 0.5 shard_map.175
  60.0 10.5 %all_to_all.10.in_ref = bf16[8,72,128]{2,1,0:T(8,128)(2,1)S(1)} all-to-all(bf16[8,72,128]{2,1,0:T(8,128)(2,1)S(1)} %shard_map.175), channel_id=1, replica_groups=mesh['zh'=4,'zl'=2,'x'=4,'y'=4,'c'=2] {'zl','x'}, dimensions={0} | all-to-all | bytes 294912 | tf_op jit(solution)/shard_map/all_to_all | solution.py:656
  70.4 1.0 %shard_map.176 = (bf16[2,192,256]{2,1,0:T(8,128)(2,1)}, bf16[2,2,4,128]{3,2,1,0:T(4,128)(2,1)}, f32[2,256]{1,0:T(2,128)}) custom-call(bf16[8,72,128]{2,1,0:T(8,128)(2,1)S(1)} %all_to_all.10.in_ref, f32[4,192,128]{2,1,0:T(8,128)S(1)} %get-tuple-element.82.out_ref, bf16[4,192,128]{2,1,0:T(8,128)(2,1)S(1)} %get-tuple-element.83.reach_ref, ...), custom_call_target="tpu_custom_call" | custom-call | tf_op jit(solution)/shard_map/pallas_call | solution.py:527
  (54 shorter events, 0.2 us)
Async XLA Ops:
  0.6 3.3 %collective-permute-start.4 = (bf16[2,192,512]{2,1,0:T(8,128)(2,1)}, bf16[2,192,512]{2,1,0:T(8,128)(2,1)S(1)}, u32[]{:S(2)}, u32[]{:S(2)}) collective-permute-start(bf16[2,192,512]{2,1,0:T(8,128)(2,1)} %refs_0_.1), channel_id=1, source_target_pairs={{0,1},{1,0},{2,3},{3,2},{4,5},{5,4},{6,7},{7,6},{8,9},{9,8},{10,11... | collective-permute-start | bytes 1179656 | tf_op jit(solution)/shard_map/ppermute | solution.py:539
  1.8 7.7 %collective-permute-start = (bf16[192,512]{1,0:T(8,128)(2,1)S(1)}, bf16[192,512]{1,0:T(8,128)(2,1)S(1)}, u32[]{:S(2)}, u32[]{:S(2)}) collective-permute-start(bf16[192,512]{1,0:T(8,128)(2,1)S(1)} %get-tuple-element.49.own_first), channel_id=1, source_target_pairs={{0,2},{2,4},{4,6},{6,0},{1,3},{3,5},{5,7},{7,1},{8,10},{10,12},{12... | collective-permute-start | bytes 589832 | tf_op jit(solution)/shard_map/ppermute | solution.py:539
  3.8 8.2 %collective-permute-start.2 = (bf16[192,512]{1,0:T(8,128)(2,1)S(1)}, bf16[192,512]{1,0:T(8,128)(2,1)S(1)}, u32[]{:S(2)}, u32[]{:S(2)}) collective-permute-start(bf16[192,512]{1,0:T(8,128)(2,1)S(1)} %get-tuple-element.48.own_second), channel_id=1, source_target_pairs={{0,6},{2,0},{4,2},{6,4},{1,7},{3,1},{5,3},{7,5},{8,14},{10,8},{12,... | collective-permute-start | bytes 589832 | tf_op jit(solution)/shard_map/ppermute | solution.py:539
  3.9 2.3 %copy-start = (bf16[2,192,512]{2,1,0:T(8,128)(2,1)}, bf16[2,192,512]{2,1,0:T(8,128)(2,1)S(1)}, u32[]{:S(2)}) copy-start(bf16[2,192,512]{2,1,0:T(8,128)(2,1)S(1)} %collective-permute-done.4.own_c.refs_1_) | copy-start | bytes 1179652
  6.2 7.5 %collective-permute-start.5 = (bf16[192,512]{1,0:T(8,128)(2,1)S(1)}, bf16[192,512]{1,0:T(8,128)(2,1)S(1)}, u32[]{:S(2)}, u32[]{:S(2)}) collective-permute-start(bf16[192,512]{1,0:T(8,128)(2,1)S(1)} %get-tuple-element.48.own_second), channel_id=1, source_target_pairs={{0,2},{2,4},{4,6},{6,0},{1,3},{3,5},{5,7},{7,1},{8,10},{10,12},{12... | collective-permute-start | bytes 589832 | tf_op jit(solution)/shard_map/ppermute | solution.py:539
  9.4 7.7 %collective-permute-start.6 = (bf16[192,512]{1,0:T(8,128)(2,1)S(1)}, bf16[192,512]{1,0:T(8,128)(2,1)S(1)}, u32[]{:S(2)}, u32[]{:S(2)}) collective-permute-start(bf16[192,512]{1,0:T(8,128)(2,1)S(1)} %get-tuple-element.49.own_first), channel_id=1, source_target_pairs={{0,6},{2,0},{4,2},{6,4},{1,7},{3,1},{5,3},{7,5},{8,14},{10,8},{12,... | collective-permute-start | bytes 589832 | tf_op jit(solution)/shard_map/ppermute | solution.py:539
  9.4 11.1 %copy-start.1 = (bf16[192,512]{1,0:T(8,128)(2,1)}, bf16[192,512]{1,0:T(8,128)(2,1)S(1)}, u32[]{:S(2)}) copy-start(bf16[192,512]{1,0:T(8,128)(2,1)S(1)} %collective-permute-done.refs_0_.refs_2_) | copy-start | bytes 589828
  9.5 8.5 %collective-permute-start.7 = (bf16[192,512]{1,0:T(8,128)(2,1)S(1)}, bf16[192,512]{1,0:T(8,128)(2,1)S(1)}, u32[]{:S(2)}, u32[]{:S(2)}) collective-permute-start(bf16[192,512]{1,0:T(8,128)(2,1)S(1)} %collective-permute-done.refs_0_.refs_2_), channel_id=1, source_target_pairs={{0,1},{1,0},{2,3},{3,2},{4,5},{5,4},{6,7},{7,6},{8,9},{9,8},{10,11... | collective-permute-start | bytes 589832 | tf_op jit(solution)/shard_map/ppermute | solution.py:539
  12.0 8.6 %copy-start.2 = (bf16[192,512]{1,0:T(8,128)(2,1)}, bf16[192,512]{1,0:T(8,128)(2,1)S(1)}, u32[]{:S(2)}) copy-start(bf16[192,512]{1,0:T(8,128)(2,1)S(1)} %collective-permute-done.2.refs_3_.refs_5_) | copy-start | bytes 589828
  12.0 7.1 %collective-permute-start.10 = (bf16[192,512]{1,0:T(8,128)(2,1)S(1)}, bf16[192,512]{1,0:T(8,128)(2,1)S(1)}, u32[]{:S(2)}, u32[]{:S(2)}) collective-permute-start(bf16[192,512]{1,0:T(8,128)(2,1)S(1)} %collective-permute-done.2.refs_3_.refs_5_), channel_id=1, source_target_pairs={{0,1},{1,0},{2,3},{3,2},{4,5},{5,4},{6,7},{7,6},{8,9},{9,8},{10,11... | collective-permute-start | bytes 589832 | tf_op jit(solution)/shard_map/ppermute | solution.py:539
  13.7 6.9 %copy-start.3 = (bf16[192,512]{1,0:T(8,128)(2,1)}, bf16[192,512]{1,0:T(8,128)(2,1)S(1)}, u32[]{:S(2)}) copy-start(bf16[192,512]{1,0:T(8,128)(2,1)S(1)} %collective-permute-done.5.refs_1_.refs_3_) | copy-start | bytes 589828
  13.7 5.5 %collective-permute-start.8 = (bf16[192,512]{1,0:T(8,128)(2,1)S(1)}, bf16[192,512]{1,0:T(8,128)(2,1)S(1)}, u32[]{:S(2)}, u32[]{:S(2)}) collective-permute-start(bf16[192,512]{1,0:T(8,128)(2,1)S(1)} %collective-permute-done.5.refs_1_.refs_3_), channel_id=1, source_target_pairs={{0,1},{1,0},{2,3},{3,2},{4,5},{5,4},{6,7},{7,6},{8,9},{9,8},{10,11... | collective-permute-start | bytes 589832 | tf_op jit(solution)/shard_map/ppermute | solution.py:539
  17.1 3.5 %copy-start.4 = (bf16[192,512]{1,0:T(8,128)(2,1)}, bf16[192,512]{1,0:T(8,128)(2,1)S(1)}, u32[]{:S(2)}) copy-start(bf16[192,512]{1,0:T(8,128)(2,1)S(1)} %collective-permute-done.6.refs_2_.refs_4_) | copy-start | bytes 589828
  17.1 2.1 %collective-permute-start.9 = (bf16[192,512]{1,0:T(8,128)(2,1)S(1)}, bf16[192,512]{1,0:T(8,128)(2,1)S(1)}, u32[]{:S(2)}, u32[]{:S(2)}) collective-permute-start(bf16[192,512]{1,0:T(8,128)(2,1)S(1)} %collective-permute-done.6.refs_2_.refs_4_), channel_id=1, source_target_pairs={{0,1},{1,0},{2,3},{3,2},{4,5},{5,4},{6,7},{7,6},{8,9},{9,8},{10,11... | collective-permute-start | bytes 589832 | tf_op jit(solution)/shard_map/ppermute | solution.py:539
  17.1 7.3 %collective-permute-start.1 = (bf16[192,512]{1,0:T(8,128)(2,1)S(1)}, bf16[192,512]{1,0:T(8,128)(2,1)S(1)}, u32[]{:S(2)}, u32[]{:S(2)}) collective-permute-start(bf16[192,512]{1,0:T(8,128)(2,1)S(1)} %collective-permute-done.refs_0_.refs_2_), channel_id=1, source_target_pairs={{0,2},{2,4},{4,6},{6,0},{1,3},{3,5},{5,7},{7,1},{8,10},{10,12},{12... | collective-permute-start | bytes 589832 | tf_op jit(solution)/shard_map/ppermute | solution.py:539
  17.9 2.7 %copy-start.5 = (bf16[192,512]{1,0:T(8,128)(2,1)}, bf16[192,512]{1,0:T(8,128)(2,1)S(1)}, u32[]{:S(2)}) copy-start(bf16[192,512]{1,0:T(8,128)(2,1)S(1)} %collective-permute-done.7.refs_4_.refs_6_) | copy-start | bytes 589828
  17.9 7.8 %collective-permute-start.3 = (bf16[192,512]{1,0:T(8,128)(2,1)S(1)}, bf16[192,512]{1,0:T(8,128)(2,1)S(1)}, u32[]{:S(2)}, u32[]{:S(2)}) collective-permute-start(bf16[192,512]{1,0:T(8,128)(2,1)S(1)} %collective-permute-done.2.refs_3_.refs_5_), channel_id=1, source_target_pairs={{0,6},{2,0},{4,2},{6,4},{1,7},{3,1},{5,3},{7,5},{8,14},{10,8},{12,... | collective-permute-start | bytes 589832 | tf_op jit(solution)/shard_map/ppermute | solution.py:539
  24.4 2.3 %copy-start.9 = (bf16[192,512]{1,0:T(8,128)(2,1)}, bf16[192,512]{1,0:T(8,128)(2,1)S(1)}, u32[]{:S(2)}) copy-start(bf16[192,512]{1,0:T(8,128)(2,1)S(1)} %collective-permute-done.1.refs_0_.refs_10_) | copy-start | bytes 589828
  25.8 1.7 %copy-start.20 = (f32[2]{0:T(128)S(1)}, f32[2]{0:T(128)}, u32[]{:S(2)}) copy-start(f32[2]{0:T(128)} %param.23) | copy-start | bytes 28
  25.8 1.4 %collective-permute-start.11 = (bf16[192,512]{1,0:T(8,128)(2,1)S(1)}, bf16[192,512]{1,0:T(8,128)(2,1)S(1)}, u32[]{:S(2)}, u32[]{:S(2)}) collective-permute-start(bf16[192,512]{1,0:T(8,128)(2,1)S(1)} %collective-permute-done.1.refs_0_.refs_10_), channel_id=1, source_target_pairs={{0,1},{1,0},{2,3},{3,2},{4,5},{5,4},{6,7},{7,6},{8,9},{9,8},{10,11... | collective-permute-start | bytes 589832 | tf_op jit(solution)/shard_map/ppermute | solution.py:539
  25.8 1.7 %collective-permute-start.12 = (bf16[192,512]{1,0:T(8,128)(2,1)S(1)}, bf16[192,512]{1,0:T(8,128)(2,1)S(1)}, u32[]{:S(2)}, u32[]{:S(2)}) collective-permute-start(bf16[192,512]{1,0:T(8,128)(2,1)S(1)} %collective-permute-done.3.refs_1_.refs_11_), channel_id=1, source_target_pairs={{0,1},{1,0},{2,3},{3,2},{4,5},{5,4},{6,7},{7,6},{8,9},{9,8},{10,11... | collective-permute-start | bytes 589832 | tf_op jit(solution)/shard_map/ppermute | solution.py:539
  27.2 5.9 %copy-start.11 = (bf16[192,512]{1,0:T(8,128)(2,1)}, bf16[192,512]{1,0:T(8,128)(2,1)S(1)}, u32[]{:S(2)}) copy-start(bf16[192,512]{1,0:T(8,128)(2,1)S(1)} %collective-permute-done.11.refs_0_.refs_12_) | copy-start | bytes 589828
  27.5 5.6 %copy-start.12 = (bf16[192,512]{1,0:T(8,128)(2,1)}, bf16[192,512]{1,0:T(8,128)(2,1)S(1)}, u32[]{:S(2)}) copy-start(bf16[192,512]{1,0:T(8,128)(2,1)S(1)} %collective-permute-done.12.refs_1_.refs_13_) | copy-start | bytes 589828
  33.1 12.9 %all-to-all-start = ((bf16[8,200,128]{2,1,0:T(8,128)(2,1)}), bf16[8,200,128]{2,1,0:T(8,128)(2,1)S(1)}, u32[]{:S(2)}, u32[]{:S(2)}) async-start(bf16[8,200,128]{2,1,0:T(8,128)(2,1)} %get-tuple-element.66), calls=%async_computation | async-start | bytes 819200 | tf_op jit(solution)/shard_map/all_to_all | solution.py:608
  37.2 22.2 %copy-start.14 = (f32[2,2]{1,0:T(2,128)S(1)}, f32[2,2]{1,0:T(2,128)}, u32[]{:S(2)}) copy-start(f32[2,2]{1,0:T(2,128)} %beta_ref.1) | copy-start | bytes 52
  37.2 22.2 %copy-start.15 = (f32[2,2]{1,0:T(2,128)S(1)}, f32[2,2]{1,0:T(2,128)}, u32[]{:S(2)}) copy-start(f32[2,2]{1,0:T(2,128)} %decay_ref.1) | copy-start | bytes 52
  37.2 22.2 %copy-start.16 = (bf16[2,2,128]{2,1,0:T(2,128)(2,1)S(1)}, bf16[2,2,128]{2,1,0:T(2,128)(2,1)}, u32[]{:S(2)}) copy-start(bf16[2,2,128]{2,1,0:T(2,128)(2,1)} %query_ref.1) | copy-start | bytes 3076
  37.3 22.2 %copy-start.17 = (bf16[2,2,128]{2,1,0:T(2,128)(2,1)S(1)}, bf16[2,2,128]{2,1,0:T(2,128)(2,1)}, u32[]{:S(2)}) copy-start(bf16[2,2,128]{2,1,0:T(2,128)(2,1)} %key_ref.1) | copy-start | bytes 3076
  37.3 22.2 %copy-start.18 = (bf16[2,2,128]{2,1,0:T(2,128)(2,1)S(1)}, bf16[2,2,128]{2,1,0:T(2,128)(2,1)}, u32[]{:S(2)}) copy-start(bf16[2,2,128]{2,1,0:T(2,128)(2,1)} %value_ref.1) | copy-start | bytes 3076
  43.4 27.1 %copy-start.13 = (f32[128]{0:T(128)S(1)}, f32[128]{0:T(128)}, u32[]{:S(2)}) copy-start(f32[128]{0:T(128)} %param.24) | copy-start | bytes 1540
  46.5 5.5 %collective-permute-start.13 = (bf16[200,128]{1,0:T(8,128)(2,1)S(1)}, bf16[200,128]{1,0:T(8,128)(2,1)S(1)}, u32[]{:S(2)}, u32[]{:S(2)}) collective-permute-start(bf16[200,128]{1,0:T(8,128)(2,1)S(1)} %shard_map.172._.own_ref), channel_id=1, source_target_pairs={{0,64},{64,0},{128,192},{192,128},{1,65},{65,1},{129,193},{193,129... | collective-permute-start | bytes 153608 | tf_op jit(solution)/shard_map/ppermute | solution.py:629
  52.1 7.4 %collective-permute-start.14 = (bf16[200,128]{1,0:T(8,128)(2,1)S(1)}, bf16[200,128]{1,0:T(8,128)(2,1)S(1)}, u32[]{:S(2)}, u32[]{:S(2)}) collective-permute-start(bf16[200,128]{1,0:T(8,128)(2,1)S(1)} %shard_map.174.pair_ref), channel_id=1, source_target_pairs={{0,192},{64,128},{128,64},{192,0},{1,193},{65,129},{129,65},{193,1... | collective-permute-start | bytes 153608 | tf_op jit(solution)/shard_map/ppermute | solution.py:629
  (5 other events, 7.2 us)

commit v12 on v11

--- a/solution.py
+++ b/solution.py
@@ -180,17 +180,12 @@
     causal_wide = (iota((wide, wide), 0) >= iota((wide, wide), 1)).astype(bf16)
     for seq in range(2):
         take = slice(seq * span, (seq + 1) * span)
-        padded = jnp.concatenate([decays[take], jnp.zeros((wide - span, head), f32)], axis=0)
-        cumulative = sum(dot(causal_wide, part) for part in thirds(padded))
+        cumulative = sum(dot(causal_wide, part) for part in thirds(decays[take]))
         table = jnp.where((lanes == 2) | (lanes == 3), cumulative, 0.0)
         for h in range(2):
             keys = key_rows[take, h * head : (h + 1) * head].astype(f32)
-            unit = jnp.concatenate(
-                [rms_scale(keys, unit_floor, False), jnp.zeros((wide - span, 1), f32)], axis=0
-            )
-            beta = jnp.concatenate(
-                [strength[take, h : h + 1], jnp.zeros((wide - span, 1), f32)], axis=0
-            )
+            unit = rms_scale(keys, unit_floor, False)
+            beta = strength[take, h : h + 1]
             table = jnp.where(lanes == h, beta, table)
             table = jnp.where(lanes == 4 + h, unit, table)
         cols_ref[seq] = table
@@ -546,7 +541,7 @@
     _, span, depth = tokens.shape
     head = out_gain.shape[0]
     half = head // 2
-    wide = 256
+    wide = span
     width = query_weight.shape[1]
     rows = head + half + PACK
     on, dma = pltpu.VMEM, pltpu.SemaphoreType.DMA

time: 71.8 us -> 71.7 us (level)
  no operation moved by 1% of the time
where the time goes in v12:
time: 71.7 us; the launch traced here: 71.4 us
  starting transfers between devices  20.7 us (29%)
  Pallas kernels  20.2 us (28%)
  waiting for transfers between devices  19 us (26%)
  blocking collectives  10.5 us (15%)
  between operations  0.93 us (1%)
    pallas_call x11, Pallas kernels, kernel(): pl.pallas_call(body, out_shape=tuple((out if kind == 'p' else plain(out)...  20.2 us
    ppermute x13, waiting for transfers between devices, shift(): lax.ppermute(value, axis, [(at, (at + by) % length) for at in range(lengt...  13.4 us
    all_to_all x1, blocking collectives, shards(): returned = lax.all_to_all(back, NEAR, 0, 0, tiled=True)  10.5 us
    ppermute x2, starting transfers between devices, shards(): lax.ppermute(value, 'zh', [(at, at ^ by) for at in range(4)])  8.58 us
    ppermute x13, starting transfers between devices, shift(): lax.ppermute(value, axis, [(at, (at + by) % length) for at in range(lengt...  8.05 us
    all_to_all x1, starting transfers between devices, shards(): arrived = lax.all_to_all(send, NEAR, 0, 0, tiled=True)  4.1 us
    ppermute x2, waiting for transfers between devices, shards(): lax.ppermute(value, 'zh', [(at, at ^ by) for at in range(4)])  3.01 us
    all_to_all x1, waiting for transfers between devices, shards(): arrived = lax.all_to_all(send, NEAR, 0, 0, tiled=True)  2.61 us
  transfers between devices with their start and end apart: 16, of which 10 were waited for; matrix products, arithmetic and copies ran while one was open for 0% of the time, Pallas kernels for 18%

profile of v12, /device:TPU:24, one launch (start us, length us, event | category | flops | bytes accessed | tf_op | source)
XLA Modules:
  0.0 71.4 jit_solution(13795285375896641910)
XLA Ops:
  0.6 0.1 collective-permute-start.4
  0.7 1.0 %shard_map.166 = (bf16[192,512]{1,0:T(8,128)(2,1)S(1)}, bf16[192,512]{1,0:T(8,128)(2,1)S(1)}) custom-call(bf16[2,192,512]{2,1,0:T(8,128)(2,1)} %refs_0_.1), custom_call_target="tpu_custom_call" | custom-call | tf_op jit(solution)/shard_map/pallas_call | solution.py:522
  1.8 2.0 %collective-permute-start = (bf16[192,512]{1,0:T(8,128)(2,1)S(1)}, bf16[192,512]{1,0:T(8,128)(2,1)S(1)}, u32[]{:S(2)}, u32[]{:S(2)}) collective-permute-start(bf16[192,512]{1,0:T(8,128)(2,1)S(1)} %get-tuple-element.49.own_first), channel_id=1, source_target_pairs={{0,2},{2,4},{4,6},{6,0},{1,3},{3,5},{5,7},{7,1},{8,10},{10,12},{12... | collective-permute-start | bytes 589832 | tf_op jit(solution)/shard_map/ppermute | solution.py:534
  3.8 0.1 collective-permute-start.2
  3.9 2.3 %shard_map.167 = (f32[384,512]{1,0:T(8,128)S(1)}, f32[384,128]{1,0:T(8,128)S(1)}, bf16[3072,512]{1,0:T(8,128)(2,1)S(1)}, bf16[16,4096]{1,0:T(8,128)(2,1)S(1)}) custom-call(bf16[192,512]{1,0:T(8,128)(2,1)S(1)} %get-tuple-element.49.own_first, bf16[192,512]{1,0:T(8,128)(2,1)S(1)} %get-tuple-element.48.own_second, ...), custom_call_target="tpu_custom_call" | custom-call | tf_op jit(solution)/shard_map/pallas_call | solution.py:522
  6.2 3.2 %collective-permute-start.5 = (bf16[192,512]{1,0:T(8,128)(2,1)S(1)}, bf16[192,512]{1,0:T(8,128)(2,1)S(1)}, u32[]{:S(2)}, u32[]{:S(2)}) collective-permute-start(bf16[192,512]{1,0:T(8,128)(2,1)S(1)} %get-tuple-element.48.own_second), channel_id=1, source_target_pairs={{0,2},{2,4},{4,6},{6,0},{1,3},{3,5},{5,7},{7,1},{8,10},{10,12},{12... | collective-permute-start | bytes 589832 | tf_op jit(solution)/shard_map/ppermute | solution.py:534
  9.6 2.5 %collective-permute-done.2.refs_3_.refs_5_ = bf16[192,512]{1,0:T(8,128)(2,1)S(1)} collective-permute-done((bf16[192,512]{1,0:T(8,128)(2,1)S(1)}, bf16[192,512]{1,0:T(8,128)(2,1)S(1)}, u32[]{:S(2)}, u32[]{:S(2)}) %collective-permute-start.2) | collective-permute-done | bytes 196640 | tf_op jit(solution)/shard_map/ppermute | solution.py:534
  12.0 1.7 %collective-permute-done.5.refs_1_.refs_3_ = bf16[192,512]{1,0:T(8,128)(2,1)S(1)} collective-permute-done((bf16[192,512]{1,0:T(8,128)(2,1)S(1)}, bf16[192,512]{1,0:T(8,128)(2,1)S(1)}, u32[]{:S(2)}, u32[]{:S(2)}) %collective-permute-start.5) | collective-permute-done | bytes 196640 | tf_op jit(solution)/shard_map/ppermute | solution.py:534
  13.7 3.4 %collective-permute-done.6.refs_2_.refs_4_ = bf16[192,512]{1,0:T(8,128)(2,1)S(1)} collective-permute-done((bf16[192,512]{1,0:T(8,128)(2,1)S(1)}, bf16[192,512]{1,0:T(8,128)(2,1)S(1)}, u32[]{:S(2)}, u32[]{:S(2)}) %collective-permute-start.6) | collective-permute-done | bytes 196640 | tf_op jit(solution)/shard_map/ppermute | solution.py:534
  17.1 0.8 %collective-permute-start.1 = (bf16[192,512]{1,0:T(8,128)(2,1)S(1)}, bf16[192,512]{1,0:T(8,128)(2,1)S(1)}, u32[]{:S(2)}, u32[]{:S(2)}) collective-permute-start(bf16[192,512]{1,0:T(8,128)(2,1)S(1)} %collective-permute-done.refs_0_.refs_2_), channel_id=1, source_target_pairs={{0,2},{2,4},{4,6},{6,0},{1,3},{3,5},{5,7},{7,1},{8,10},{10,12},{12... | collective-permute-start | bytes 589832 | tf_op jit(solution)/shard_map/ppermute | solution.py:534
  17.9 1.2 %collective-permute-start.3 = (bf16[192,512]{1,0:T(8,128)(2,1)S(1)}, bf16[192,512]{1,0:T(8,128)(2,1)S(1)}, u32[]{:S(2)}, u32[]{:S(2)}) collective-permute-start(bf16[192,512]{1,0:T(8,128)(2,1)S(1)} %collective-permute-done.2.refs_3_.refs_5_), channel_id=1, source_target_pairs={{0,6},{2,0},{4,2},{6,4},{1,7},{3,1},{5,3},{7,5},{8,14},{10,8},{12,... | collective-permute-start | bytes 589832 | tf_op jit(solution)/shard_map/ppermute | solution.py:534
  19.2 1.4 %shard_map.168 = (f32[384,512]{1,0:T(8,128)S(1)}, f32[384,128]{1,0:T(8,128)S(1)}) custom-call(bf16[192,512]{1,0:T(8,128)(2,1)S(1)} %collective-permute-done.refs_0_.refs_2_, bf16[192,512]{1,0:T(8,128)(2,1)S(1)} %collective-permute-done.5.refs_1_.refs_3_, bf16[192,512]{1,0:T(8,128)(2,1)S(1)} %collective-permute-done.6.refs_2_.refs_4_, ...), custom_call_target="tpu_custom_call" | custom-call | tf_op jit(solution)/shard_map/pallas_call | solution.py:522
  20.7 3.8 %collective-permute-done.1.refs_0_.refs_10_ = bf16[192,512]{1,0:T(8,128)(2,1)S(1)} collective-permute-done((bf16[192,512]{1,0:T(8,128)(2,1)S(1)}, bf16[192,512]{1,0:T(8,128)(2,1)S(1)}, u32[]{:S(2)}, u32[]{:S(2)}) %collective-permute-start.1) | collective-permute-done | bytes 196640 | tf_op jit(solution)/shard_map/ppermute | solution.py:534
  24.4 1.3 %collective-permute-done.3.refs_1_.refs_11_ = bf16[192,512]{1,0:T(8,128)(2,1)S(1)} collective-permute-done((bf16[192,512]{1,0:T(8,128)(2,1)S(1)}, bf16[192,512]{1,0:T(8,128)(2,1)S(1)}, u32[]{:S(2)}, u32[]{:S(2)}) %collective-permute-start.3) | collective-permute-done | bytes 196640 | tf_op jit(solution)/shard_map/ppermute | solution.py:534
  25.8 0.5 collective-permute-start.12
  26.3 0.5 shard_map.169
  26.8 0.4 collective-permute-done.11.refs_0_.refs_12_
  27.2 0.3 collective-permute-done.12.refs_1_.refs_13_
  27.5 5.5 %shard_map.170 = (bf16[8,200,128]{2,1,0:T(8,128)(2,1)}, bf16[384,256]{1,0:T(8,128)(2,1)}, bf16[4,192,128]{2,1,0:T(8,128)(2,1)}, bf16[4,192,128]{2,1,0:T(8,128)(2...) custom-call(f32[1,2]{1,0:T(1,128)S(1)} %bitcast.7, f32[1,2]{1,0:T(1,128)S(1)} %bitcast.8, ...), custom_call_target="tpu_custom_call" | custom-call | tf_op jit(solution)/shard_map/pallas_call | solution.py:522
  33.0 4.1 %all-to-all-start = ((bf16[8,200,128]{2,1,0:T(8,128)(2,1)}), bf16[8,200,128]{2,1,0:T(8,128)(2,1)S(1)}, u32[]{:S(2)}, u32[]{:S(2)}) async-start(bf16[8,200,128]{2,1,0:T(8,128)(2,1)} %get-tuple-element.66), calls=%async_computation | async-start | bytes 819200 | tf_op jit(solution)/shard_map/all_to_all | solution.py:603
  37.2 6.1 %shard_map.171 = (f32[4,192,128]{2,1,0:T(8,128)}, bf16[4,192,128]{2,1,0:T(8,128)(2,1)}, f32[4,192,128]{2,1,0:T(8,128)}) custom-call(bf16[2,192,512]{2,1,0:T(8,128)(2,1)} %refs_0_.1, bf16[2,192,512]{2,1,0:T(8,128)(2,1)} %copy-done, bf16[192,512]{1,0:T(8,128)(2,1)} %copy-done.1, bf16[192,512]{1,0:T(8,128)(2,1)} %copy-done.3, bf16[192,512]{1,0:T(8,128)(2,1)} %copy-done.4, ...), custom_call_target="tpu_custom_call" | custom-call | tf_op jit(solution)/shard_map/pallas_call | solution.py:522
  43.3 2.6 %all-to-all-done.in_ref = bf16[8,200,128]{2,1,0:T(8,128)(2,1)S(1)} async-done(((bf16[8,200,128]{2,1,0:T(8,128)(2,1)}), bf16[8,200,128]{2,1,0:T(8,128)(2,1)S(1)}, u32[]{:S(2)}, u32[]{:S(2)}) %all-to-all-start) | async-done | bytes 409632 | tf_op jit(solution)/shard_map/all_to_all | solution.py:603
  45.9 0.5 shard_map.172._.own_ref
  46.4 3.4 %collective-permute-start.13 = (bf16[200,128]{1,0:T(8,128)(2,1)S(1)}, bf16[200,128]{1,0:T(8,128)(2,1)S(1)}, u32[]{:S(2)}, u32[]{:S(2)}) collective-permute-start(bf16[200,128]{1,0:T(8,128)(2,1)S(1)} %shard_map.172._.own_ref), channel_id=1, source_target_pairs={{0,64},{64,0},{128,192},{192,128},{1,65},{65,1},{129,193},{193,129... | collective-permute-start | bytes 153608 | tf_op jit(solution)/shard_map/ppermute | solution.py:624
  49.7 1.2 %shard_map.173 = (bf16[7,128,128]{2,1,0:T(8,128)(2,1)S(1)}, f32[7,64,128]{2,1,0:T(8,128)S(1)}, f32[7,8,128]{2,1,0:T(8,128)S(1)}, f32[4,192,128]{2,1,0:T(8,128)S(...) custom-call(bf16[200,128]{1,0:T(8,128)(2,1)S(1)} %shard_map.172._.own_ref, ...), custom_call_target="tpu_custom_call" | custom-call | tf_op jit(solution)/shard_map/pallas_call | solution.py:522
  51.0 0.9 %collective-permute-done.13.near_ref = bf16[200,128]{1,0:T(8,128)(2,1)S(1)} collective-permute-done((bf16[200,128]{1,0:T(8,128)(2,1)S(1)}, bf16[200,128]{1,0:T(8,128)(2,1)S(1)}, u32[]{:S(2)}, u32[]{:S(2)}) %collective-permute-start.13) | collective-permute-done | bytes 51232 | tf_op jit(solution)/shard_map/ppermute | solution.py:624
  51.8 0.1 shard_map.174.pair_ref
  52.0 5.2 %collective-permute-start.14 = (bf16[200,128]{1,0:T(8,128)(2,1)S(1)}, bf16[200,128]{1,0:T(8,128)(2,1)S(1)}, u32[]{:S(2)}, u32[]{:S(2)}) collective-permute-start(bf16[200,128]{1,0:T(8,128)(2,1)S(1)} %shard_map.174.pair_ref), channel_id=1, source_target_pairs={{0,192},{64,128},{128,64},{192,0},{1,193},{65,129},{129,65},{193,1... | collective-permute-start | bytes 153608 | tf_op jit(solution)/shard_map/ppermute | solution.py:624
  57.2 2.1 %collective-permute-done.14.other_ref = bf16[200,128]{1,0:T(8,128)(2,1)S(1)} collective-permute-done((bf16[200,128]{1,0:T(8,128)(2,1)S(1)}, bf16[200,128]{1,0:T(8,128)(2,1)S(1)}, u32[]{:S(2)}, u32[]{:S(2)}) %collective-permute-start.14) | collective-permute-done | bytes 51232 | tf_op jit(solution)/shard_map/ppermute | solution.py:624
  59.4 0.5 shard_map.175
  59.9 10.5 %all_to_all.10.in_ref = bf16[8,72,128]{2,1,0:T(8,128)(2,1)S(1)} all-to-all(bf16[8,72,128]{2,1,0:T(8,128)(2,1)S(1)} %shard_map.175), channel_id=1, replica_groups=mesh['zh'=4,'zl'=2,'x'=4,'y'=4,'c'=2] {'zl','x'}, dimensions={0} | all-to-all | bytes 294912 | tf_op jit(solution)/shard_map/all_to_all | solution.py:651
  70.4 1.0 %shard_map.176 = (bf16[2,192,256]{2,1,0:T(8,128)(2,1)}, bf16[2,2,4,128]{3,2,1,0:T(4,128)(2,1)}, f32[2,256]{1,0:T(2,128)}) custom-call(bf16[8,72,128]{2,1,0:T(8,128)(2,1)S(1)} %all_to_all.10.in_ref, f32[4,192,128]{2,1,0:T(8,128)S(1)} %get-tuple-element.82.out_ref, bf16[4,192,128]{2,1,0:T(8,128)(2,1)S(1)} %get-tuple-element.83.reach_ref, ...), custom_call_target="tpu_custom_call" | custom-call | tf_op jit(solution)/shard_map/pallas_call | solution.py:522
  (54 shorter events, 0.2 us)
Async XLA Ops:
  0.6 3.3 %collective-permute-start.4 = (bf16[2,192,512]{2,1,0:T(8,128)(2,1)}, bf16[2,192,512]{2,1,0:T(8,128)(2,1)S(1)}, u32[]{:S(2)}, u32[]{:S(2)}) collective-permute-start(bf16[2,192,512]{2,1,0:T(8,128)(2,1)} %refs_0_.1), channel_id=1, source_target_pairs={{0,1},{1,0},{2,3},{3,2},{4,5},{5,4},{6,7},{7,6},{8,9},{9,8},{10,11... | collective-permute-start | bytes 1179656 | tf_op jit(solution)/shard_map/ppermute | solution.py:534
  1.8 7.7 %collective-permute-start = (bf16[192,512]{1,0:T(8,128)(2,1)S(1)}, bf16[192,512]{1,0:T(8,128)(2,1)S(1)}, u32[]{:S(2)}, u32[]{:S(2)}) collective-permute-start(bf16[192,512]{1,0:T(8,128)(2,1)S(1)} %get-tuple-element.49.own_first), channel_id=1, source_target_pairs={{0,2},{2,4},{4,6},{6,0},{1,3},{3,5},{5,7},{7,1},{8,10},{10,12},{12... | collective-permute-start | bytes 589832 | tf_op jit(solution)/shard_map/ppermute | solution.py:534
  3.8 8.2 %collective-permute-start.2 = (bf16[192,512]{1,0:T(8,128)(2,1)S(1)}, bf16[192,512]{1,0:T(8,128)(2,1)S(1)}, u32[]{:S(2)}, u32[]{:S(2)}) collective-permute-start(bf16[192,512]{1,0:T(8,128)(2,1)S(1)} %get-tuple-element.48.own_second), channel_id=1, source_target_pairs={{0,6},{2,0},{4,2},{6,4},{1,7},{3,1},{5,3},{7,5},{8,14},{10,8},{12,... | collective-permute-start | bytes 589832 | tf_op jit(solution)/shard_map/ppermute | solution.py:534
  3.9 2.3 %copy-start = (bf16[2,192,512]{2,1,0:T(8,128)(2,1)}, bf16[2,192,512]{2,1,0:T(8,128)(2,1)S(1)}, u32[]{:S(2)}) copy-start(bf16[2,192,512]{2,1,0:T(8,128)(2,1)S(1)} %collective-permute-done.4.own_c.refs_1_) | copy-start | bytes 1179652
  6.2 7.5 %collective-permute-start.5 = (bf16[192,512]{1,0:T(8,128)(2,1)S(1)}, bf16[192,512]{1,0:T(8,128)(2,1)S(1)}, u32[]{:S(2)}, u32[]{:S(2)}) collective-permute-start(bf16[192,512]{1,0:T(8,128)(2,1)S(1)} %get-tuple-element.48.own_second), channel_id=1, source_target_pairs={{0,2},{2,4},{4,6},{6,0},{1,3},{3,5},{5,7},{7,1},{8,10},{10,12},{12... | collective-permute-start | bytes 589832 | tf_op jit(solution)/shard_map/ppermute | solution.py:534
  9.4 7.7 %collective-permute-start.6 = (bf16[192,512]{1,0:T(8,128)(2,1)S(1)}, bf16[192,512]{1,0:T(8,128)(2,1)S(1)}, u32[]{:S(2)}, u32[]{:S(2)}) collective-permute-start(bf16[192,512]{1,0:T(8,128)(2,1)S(1)} %get-tuple-element.49.own_first), channel_id=1, source_target_pairs={{0,6},{2,0},{4,2},{6,4},{1,7},{3,1},{5,3},{7,5},{8,14},{10,8},{12,... | collective-permute-start | bytes 589832 | tf_op jit(solution)/shard_map/ppermute | solution.py:534
  9.4 11.1 %copy-start.1 = (bf16[192,512]{1,0:T(8,128)(2,1)}, bf16[192,512]{1,0:T(8,128)(2,1)S(1)}, u32[]{:S(2)}) copy-start(bf16[192,512]{1,0:T(8,128)(2,1)S(1)} %collective-permute-done.refs_0_.refs_2_) | copy-start | bytes 589828
  9.5 8.5 %collective-permute-start.7 = (bf16[192,512]{1,0:T(8,128)(2,1)S(1)}, bf16[192,512]{1,0:T(8,128)(2,1)S(1)}, u32[]{:S(2)}, u32[]{:S(2)}) collective-permute-start(bf16[192,512]{1,0:T(8,128)(2,1)S(1)} %collective-permute-done.refs_0_.refs_2_), channel_id=1, source_target_pairs={{0,1},{1,0},{2,3},{3,2},{4,5},{5,4},{6,7},{7,6},{8,9},{9,8},{10,11... | collective-permute-start | bytes 589832 | tf_op jit(solution)/shard_map/ppermute | solution.py:534
  12.0 8.6 %copy-start.2 = (bf16[192,512]{1,0:T(8,128)(2,1)}, bf16[192,512]{1,0:T(8,128)(2,1)S(1)}, u32[]{:S(2)}) copy-start(bf16[192,512]{1,0:T(8,128)(2,1)S(1)} %collective-permute-done.2.refs_3_.refs_5_) | copy-start | bytes 589828
  12.0 7.1 %collective-permute-start.10 = (bf16[192,512]{1,0:T(8,128)(2,1)S(1)}, bf16[192,512]{1,0:T(8,128)(2,1)S(1)}, u32[]{:S(2)}, u32[]{:S(2)}) collective-permute-start(bf16[192,512]{1,0:T(8,128)(2,1)S(1)} %collective-permute-done.2.refs_3_.refs_5_), channel_id=1, source_target_pairs={{0,1},{1,0},{2,3},{3,2},{4,5},{5,4},{6,7},{7,6},{8,9},{9,8},{10,11... | collective-permute-start | bytes 589832 | tf_op jit(solution)/shard_map/ppermute | solution.py:534
  13.7 6.9 %copy-start.3 = (bf16[192,512]{1,0:T(8,128)(2,1)}, bf16[192,512]{1,0:T(8,128)(2,1)S(1)}, u32[]{:S(2)}) copy-start(bf16[192,512]{1,0:T(8,128)(2,1)S(1)} %collective-permute-done.5.refs_1_.refs_3_) | copy-start | bytes 589828
  13.7 5.5 %collective-permute-start.8 = (bf16[192,512]{1,0:T(8,128)(2,1)S(1)}, bf16[192,512]{1,0:T(8,128)(2,1)S(1)}, u32[]{:S(2)}, u32[]{:S(2)}) collective-permute-start(bf16[192,512]{1,0:T(8,128)(2,1)S(1)} %collective-permute-done.5.refs_1_.refs_3_), channel_id=1, source_target_pairs={{0,1},{1,0},{2,3},{3,2},{4,5},{5,4},{6,7},{7,6},{8,9},{9,8},{10,11... | collective-permute-start | bytes 589832 | tf_op jit(solution)/shard_map/ppermute | solution.py:534
  17.1 3.5 %copy-start.4 = (bf16[192,512]{1,0:T(8,128)(2,1)}, bf16[192,512]{1,0:T(8,128)(2,1)S(1)}, u32[]{:S(2)}) copy-start(bf16[192,512]{1,0:T(8,128)(2,1)S(1)} %collective-permute-done.6.refs_2_.refs_4_) | copy-start | bytes 589828
  17.1 2.1 %collective-permute-start.9 = (bf16[192,512]{1,0:T(8,128)(2,1)S(1)}, bf16[192,512]{1,0:T(8,128)(2,1)S(1)}, u32[]{:S(2)}, u32[]{:S(2)}) collective-permute-start(bf16[192,512]{1,0:T(8,128)(2,1)S(1)} %collective-permute-done.6.refs_2_.refs_4_), channel_id=1, source_target_pairs={{0,1},{1,0},{2,3},{3,2},{4,5},{5,4},{6,7},{7,6},{8,9},{9,8},{10,11... | collective-permute-start | bytes 589832 | tf_op jit(solution)/shard_map/ppermute | solution.py:534
  17.1 7.3 %collective-permute-start.1 = (bf16[192,512]{1,0:T(8,128)(2,1)S(1)}, bf16[192,512]{1,0:T(8,128)(2,1)S(1)}, u32[]{:S(2)}, u32[]{:S(2)}) collective-permute-start(bf16[192,512]{1,0:T(8,128)(2,1)S(1)} %collective-permute-done.refs_0_.refs_2_), channel_id=1, source_target_pairs={{0,2},{2,4},{4,6},{6,0},{1,3},{3,5},{5,7},{7,1},{8,10},{10,12},{12... | collective-permute-start | bytes 589832 | tf_op jit(solution)/shard_map/ppermute | solution.py:534
  17.9 2.7 %copy-start.5 = (bf16[192,512]{1,0:T(8,128)(2,1)}, bf16[192,512]{1,0:T(8,128)(2,1)S(1)}, u32[]{:S(2)}) copy-start(bf16[192,512]{1,0:T(8,128)(2,1)S(1)} %collective-permute-done.7.refs_4_.refs_6_) | copy-start | bytes 589828
  17.9 7.8 %collective-permute-start.3 = (bf16[192,512]{1,0:T(8,128)(2,1)S(1)}, bf16[192,512]{1,0:T(8,128)(2,1)S(1)}, u32[]{:S(2)}, u32[]{:S(2)}) collective-permute-start(bf16[192,512]{1,0:T(8,128)(2,1)S(1)} %collective-permute-done.2.refs_3_.refs_5_), channel_id=1, source_target_pairs={{0,6},{2,0},{4,2},{6,4},{1,7},{3,1},{5,3},{7,5},{8,14},{10,8},{12,... | collective-permute-start | bytes 589832 | tf_op jit(solution)/shard_map/ppermute | solution.py:534
  24.4 2.3 %copy-start.9 = (bf16[192,512]{1,0:T(8,128)(2,1)}, bf16[192,512]{1,0:T(8,128)(2,1)S(1)}, u32[]{:S(2)}) copy-start(bf16[192,512]{1,0:T(8,128)(2,1)S(1)} %collective-permute-done.1.refs_0_.refs_10_) | copy-start | bytes 589828
  25.8 1.7 %copy-start.20 = (f32[2]{0:T(128)S(1)}, f32[2]{0:T(128)}, u32[]{:S(2)}) copy-start(f32[2]{0:T(128)} %param.23) | copy-start | bytes 28
  25.8 1.4 %collective-permute-start.11 = (bf16[192,512]{1,0:T(8,128)(2,1)S(1)}, bf16[192,512]{1,0:T(8,128)(2,1)S(1)}, u32[]{:S(2)}, u32[]{:S(2)}) collective-permute-start(bf16[192,512]{1,0:T(8,128)(2,1)S(1)} %collective-permute-done.1.refs_0_.refs_10_), channel_id=1, source_target_pairs={{0,1},{1,0},{2,3},{3,2},{4,5},{5,4},{6,7},{7,6},{8,9},{9,8},{10,11... | collective-permute-start | bytes 589832 | tf_op jit(solution)/shard_map/ppermute | solution.py:534
  25.8 1.7 %collective-permute-start.12 = (bf16[192,512]{1,0:T(8,128)(2,1)S(1)}, bf16[192,512]{1,0:T(8,128)(2,1)S(1)}, u32[]{:S(2)}, u32[]{:S(2)}) collective-permute-start(bf16[192,512]{1,0:T(8,128)(2,1)S(1)} %collective-permute-done.3.refs_1_.refs_11_), channel_id=1, source_target_pairs={{0,1},{1,0},{2,3},{3,2},{4,5},{5,4},{6,7},{7,6},{8,9},{9,8},{10,11... | collective-permute-start | bytes 589832 | tf_op jit(solution)/shard_map/ppermute | solution.py:534
  27.2 5.8 %copy-start.11 = (bf16[192,512]{1,0:T(8,128)(2,1)}, bf16[192,512]{1,0:T(8,128)(2,1)S(1)}, u32[]{:S(2)}) copy-start(bf16[192,512]{1,0:T(8,128)(2,1)S(1)} %collective-permute-done.11.refs_0_.refs_12_) | copy-start | bytes 589828
  27.5 5.5 %copy-start.12 = (bf16[192,512]{1,0:T(8,128)(2,1)}, bf16[192,512]{1,0:T(8,128)(2,1)S(1)}, u32[]{:S(2)}) copy-start(bf16[192,512]{1,0:T(8,128)(2,1)S(1)} %collective-permute-done.12.refs_1_.refs_13_) | copy-start | bytes 589828
  33.0 12.9 %all-to-all-start = ((bf16[8,200,128]{2,1,0:T(8,128)(2,1)}), bf16[8,200,128]{2,1,0:T(8,128)(2,1)S(1)}, u32[]{:S(2)}, u32[]{:S(2)}) async-start(bf16[8,200,128]{2,1,0:T(8,128)(2,1)} %get-tuple-element.66), calls=%async_computation | async-start | bytes 819200 | tf_op jit(solution)/shard_map/all_to_all | solution.py:603
  37.1 22.2 %copy-start.14 = (f32[2,2]{1,0:T(2,128)S(1)}, f32[2,2]{1,0:T(2,128)}, u32[]{:S(2)}) copy-start(f32[2,2]{1,0:T(2,128)} %beta_ref.1) | copy-start | bytes 52
  37.1 22.2 %copy-start.15 = (f32[2,2]{1,0:T(2,128)S(1)}, f32[2,2]{1,0:T(2,128)}, u32[]{:S(2)}) copy-start(f32[2,2]{1,0:T(2,128)} %decay_ref.1) | copy-start | bytes 52
  37.2 22.2 %copy-start.16 = (bf16[2,2,128]{2,1,0:T(2,128)(2,1)S(1)}, bf16[2,2,128]{2,1,0:T(2,128)(2,1)}, u32[]{:S(2)}) copy-start(bf16[2,2,128]{2,1,0:T(2,128)(2,1)} %query_ref.1) | copy-start | bytes 3076
  37.2 22.2 %copy-start.17 = (bf16[2,2,128]{2,1,0:T(2,128)(2,1)S(1)}, bf16[2,2,128]{2,1,0:T(2,128)(2,1)}, u32[]{:S(2)}) copy-start(bf16[2,2,128]{2,1,0:T(2,128)(2,1)} %key_ref.1) | copy-start | bytes 3076
  37.2 22.2 %copy-start.18 = (bf16[2,2,128]{2,1,0:T(2,128)(2,1)S(1)}, bf16[2,2,128]{2,1,0:T(2,128)(2,1)}, u32[]{:S(2)}) copy-start(bf16[2,2,128]{2,1,0:T(2,128)(2,1)} %value_ref.1) | copy-start | bytes 3076
  43.3 27.1 %copy-start.13 = (f32[128]{0:T(128)S(1)}, f32[128]{0:T(128)}, u32[]{:S(2)}) copy-start(f32[128]{0:T(128)} %param.24) | copy-start | bytes 1540
  46.4 5.5 %collective-permute-start.13 = (bf16[200,128]{1,0:T(8,128)(2,1)S(1)}, bf16[200,128]{1,0:T(8,128)(2,1)S(1)}, u32[]{:S(2)}, u32[]{:S(2)}) collective-permute-start(bf16[200,128]{1,0:T(8,128)(2,1)S(1)} %shard_map.172._.own_ref), channel_id=1, source_target_pairs={{0,64},{64,0},{128,192},{192,128},{1,65},{65,1},{129,193},{193,129... | collective-permute-start | bytes 153608 | tf_op jit(solution)/shard_map/ppermute | solution.py:624
  52.0 7.4 %collective-permute-start.14 = (bf16[200,128]{1,0:T(8,128)(2,1)S(1)}, bf16[200,128]{1,0:T(8,128)(2,1)S(1)}, u32[]{:S(2)}, u32[]{:S(2)}) collective-permute-start(bf16[200,128]{1,0:T(8,128)(2,1)S(1)} %shard_map.174.pair_ref), channel_id=1, source_target_pairs={{0,192},{64,128},{128,64},{192,0},{1,193},{65,129},{129,65},{193,1... | collective-permute-start | bytes 153608 | tf_op jit(solution)/shard_map/ppermute | solution.py:624
  (5 other events, 7.2 us)
